TPU v7x, 128 devices: a whole 4x4x4 slice. The times are simulated.
128 devices in a mesh: sp: 64 (over z, y, x), tp: 2 (over core).
Axes of the slice: x: 4, y: 4, z: 4, core: 2. Of those that a mesh axis runs over, the one named last changes fastest.
Arguments:
- residual: bfloat16 [16384, 2048], P(('sp', 'tp')), may hold values from -6 to 6
- query_nope: bfloat16 [16384, 1024], P('sp', 'tp'), may hold values from -24 to 24
- query_rope: bfloat16 [16384, 512], P('sp', 'tp'), may hold values from -400 to 400
- latent: bfloat16 [16384, 256], P(('sp', 'tp')), may hold values from -6 to 6
- key_rope: bfloat16 [16384, 64], P(('sp', 'tp')), may hold values from -6 to 6
- key_up: bfloat16 [256, 1024], P(None, 'tp'), may hold values from -0.375 to 0.375
- value_up: bfloat16 [256, 1024], P(None, 'tp'), may hold values from -0.375 to 0.375
- out_proj: bfloat16 [1024, 2048], replicated, may hold values from -0.375 to 0.375
- norm_gain: float32 [2048], replicated, may hold values from 0.1 to 1.9
- routes: int32 [16384, 2], P(('sp', 'tp')), may hold values from 0 to 63, all different within a row; in each aligned block of 128 rows (0 to 127, 128 to 255, ...) at most 8 rows name the same one
- route_weight: float32 [16384, 2], P(('sp', 'tp')), may hold values from 0.3 to 2.5
- w_gate: bfloat16 [64, 2048, 512], P('sp', None, 'tp'), may hold values from -0.125 to 0.125
- w_up: bfloat16 [64, 2048, 512], P('sp', None, 'tp'), may hold values from -0.125 to 0.125
- w_down: bfloat16 [64, 512, 2048], P('sp', 'tp'), may hold values from -0.25 to 0.25
Outputs:
- mixed: bfloat16 [16384, 2048], P(('sp', 'tp'))
Inputs may be any that keep to these rules, and one draw needn't show every extreme that they name: `routes`: each row names 2 different experts. Among the rows of one device no expert is named more than 8 times, a bound that some block reaches by the rows of some device.
All inputs are finite; a program needn't handle non-finite values.
Results may differ from a plain program's by a relative error of at most 0.015.
Values may be sent and summed in bfloat16 or wider, within the bound.
No kernel may reach another device: no remote copies, remote signals or barrier semaphores. Data moves between devices by JAX's collectives and lax.ppermute only.
A program may use at most 128 MiB of HBM per device.

v0:
```python
import jax
import jax.numpy as jnp
from jax import lax
from jax.sharding import PartitionSpec as P

QK_NOPE = 128
QK_ROPE = 64
V_DIM = 128
SEGMENT = 64


EPSILON = 1e-06
ROPE_BASE = 10000.0
NEG_LARGE = -1e30


def side_by_side(arrays, axis, dim, along):
    both = jnp.concatenate(arrays, axis=along)
    whole, at, finished = (lax.all_gather(both, axis, axis=dim, tiled=True), 0, [])
    for a in arrays:
        finished.append(lax.slice_in_dim(whole, at, at + a.shape[along], axis=along))
        at += a.shape[along]
    return tuple(finished)


def copy_for_each(value, axis):
    copies = jnp.broadcast_to(value, (lax.axis_size(axis), *value.shape))
    return lax.all_to_all(copies, axis, split_axis=0, concat_axis=0, tiled=True)


def laid_out(blocks, dim):
    dims = list(blocks.shape[1:])
    dims[dim] *= blocks.shape[0]
    return jnp.moveaxis(blocks, 0, dim).reshape(dims)


def collect(value, axis, dim):
    blocks = copy_for_each(value, axis)
    return laid_out(blocks, dim)


def split_up(value, dim, count):
    dims = value.shape
    blocks = value.reshape(*dims[:dim], count, dims[dim] // count, *dims[dim + 1 :])
    return jnp.moveaxis(blocks, dim, 0)


def sent_and_summed(value, axis, dim):
    blocks = split_up(value, dim, lax.axis_size(axis))
    arrived = lax.all_to_all(blocks, axis, split_axis=0, concat_axis=0, tiled=True)
    return arrived.astype(jnp.float32).sum(axis=0)


def rotary(values, positions):
    half_width = values.shape[-1] // 2
    inverse = ROPE_BASE ** (-2.0 * jnp.arange(half_width, dtype=jnp.float32) / values.shape[-1])
    angles = positions.astype(jnp.float32)[:, None] * inverse[None, :]
    cosine = jnp.cos(angles)
    sine_part = jnp.sin(angles)
    if values.ndim == 3:
        cosine = cosine[:, None, :]
        sine_part = sine_part[:, None, :]
    first_half = values[..., :half_width]
    second = values[..., half_width:]
    return jnp.concatenate(
        [first_half * cosine - second * sine_part, second * cosine + first_half * sine_part],
        axis=-1,
    )


def local(
    residual,
    query_nope,
    query_rope,
    latent,
    key_rope,
    key_up,
    value_up,
    out_proj,
    norm_gain,
    routes,
    route_weight,
    w_gate,
    w_up,
    w_down,
):
    tp_count = lax.axis_size("tp")
    tp_index = lax.axis_index("tp")
    sp_index = lax.axis_index("sp")
    row_count = residual.shape[0]
    tok_dev = query_nope.shape[0]
    heads_here = query_nope.shape[1] // QK_NOPE
    score_scale = (QK_NOPE + QK_ROPE) ** (-0.5)
    query_first = sp_index * tok_dev
    query_pos = query_first + jnp.arange(tok_dev, dtype=jnp.int32)
    query_rot = rotary(
        query_rope.astype(jnp.float32).reshape(tok_dev, heads_here, QK_ROPE), query_pos
    ).astype(jnp.bfloat16)
    query_heads = query_nope.reshape(tok_dev, heads_here, QK_NOPE)
    key_pos = query_first + tp_index * row_count + jnp.arange(row_count, dtype=jnp.int32)
    key_rot = rotary(key_rope.astype(jnp.float32), key_pos).astype(jnp.bfloat16)
    query_segment = query_pos // SEGMENT
    last_segment = (query_first + tok_dev - 1) // SEGMENT
    initial = (
        jnp.full((heads_here, tok_dev), NEG_LARGE, jnp.float32),
        jnp.zeros((heads_here, tok_dev), jnp.float32),
        jnp.zeros((tok_dev, heads_here, V_DIM), jnp.float32),
    )
    lat_rows, rot_rows = side_by_side((latent, key_rot), ("sp", "tp"), 0, 1)
    piece_rows = lat_rows.shape[0]
    key_block = piece_rows
    while key_block > 2048 and key_block % 2 == 0:
        key_block //= 2
    block_count = piece_rows // key_block

    def one_block(state_now, inputs):
        lat_block, rot_block, offset = inputs
        key_nope = jnp.dot(lat_block, key_up, preferred_element_type=jnp.float32).astype(
            jnp.bfloat16
        )
        key_nope = key_nope.reshape(key_block, heads_here, QK_NOPE)
        value_rows = jnp.dot(lat_block, value_up, preferred_element_type=jnp.float32).astype(
            jnp.bfloat16
        )
        value_rows = value_rows.reshape(key_block, heads_here, V_DIM)
        scores = jnp.einsum(
            "qhd,khd->hqk", query_heads, key_nope, preferred_element_type=jnp.float32
        )
        scores = (
            scores
            + jnp.einsum("qhr,kr->hqk", query_rot, rot_block, preferred_element_type=jnp.float32)
        ) * score_scale
        key_segment = (offset + jnp.arange(key_block, dtype=jnp.int32)) // SEGMENT
        allowed = (key_segment[None, :] <= query_segment[:, None])[None]
        scores = jnp.where(allowed, scores, NEG_LARGE)
        old_max, old_sum, old_acc = state_now
        new_max = jnp.maximum(old_max, jnp.max(scores, axis=-1))
        weights = jnp.where(allowed, jnp.exp(scores - new_max[:, :, None]), 0.0)
        shrink = jnp.exp(old_max - new_max)
        new_sum = old_sum * shrink + jnp.sum(weights, axis=-1)
        new_acc = old_acc * shrink.T[:, :, None] + jnp.einsum(
            "hqk,khv->qhv",
            weights.astype(jnp.bfloat16),
            value_rows,
            preferred_element_type=jnp.float32,
        )
        return ((new_max, new_sum, new_acc), None)

    def compute(state_now):
        result, unused = lax.scan(
            one_block,
            state_now,
            (
                lat_rows.reshape(block_count, key_block, lat_rows.shape[1]),
                rot_rows.reshape(block_count, key_block, rot_rows.shape[1]),
                jnp.arange(block_count, dtype=jnp.int32) * key_block,
            ),
        )
        return result

    def keep_state(state_now):
        return state_now

    row_max, weight_sum, weighted = lax.cond(
        jnp.int32(0) // SEGMENT <= last_segment, compute, keep_state, initial
    )
    attn_out = (
        (weighted / weight_sum.T[:, :, None])
        .astype(jnp.bfloat16)
        .reshape(tok_dev, heads_here * V_DIM)
    )
    all_heads = lax.all_to_all(attn_out, "tp", split_axis=0, concat_axis=1, tiled=True)
    projected = jnp.dot(all_heads, out_proj, preferred_element_type=jnp.float32)
    hidden_wide = residual.astype(jnp.float32) + projected
    hidden = hidden_wide.astype(jnp.bfloat16)
    hidden_wide = hidden.astype(jnp.float32)
    normed = hidden_wide * lax.rsqrt(
        jnp.mean(hidden_wide * hidden_wide, axis=-1, keepdims=True) + EPSILON
    )
    normed = (normed * norm_gain[None, :]).astype(jnp.bfloat16)
    expert_count = lax.axis_size("sp")
    capacity = max(2, 2 * (row_count * tp_count) // expert_count)
    top_count = routes.shape[1]
    width = normed.shape[1]
    flat_expert = routes.reshape(-1)
    onehot = (flat_expert[:, None] == jnp.arange(expert_count, dtype=jnp.int32)[None, :]).astype(
        jnp.int32
    )
    slot_rank = jnp.sum(jnp.cumsum(onehot, axis=0) * onehot, axis=1) - 1
    slot_index = flat_expert * capacity + slot_rank
    outgoing = (
        jnp.zeros((expert_count * capacity, width), jnp.bfloat16)
        .at[slot_index]
        .set(jnp.repeat(normed, top_count, axis=0))
    )
    gate_weight = w_gate[0]
    up_weight = w_up[0]
    down_weight = w_down[0]
    shard_piece = collect(
        lax.all_to_all(
            outgoing.reshape(expert_count, capacity, width),
            "sp",
            split_axis=0,
            concat_axis=0,
            tiled=True,
        ),
        "tp",
        0,
    )
    gate_part = jnp.dot(shard_piece, gate_weight, preferred_element_type=jnp.float32)
    up_part = jnp.dot(shard_piece, up_weight, preferred_element_type=jnp.float32)
    activated = (jax.nn.silu(gate_part) * up_part).astype(jnp.bfloat16)
    product = jnp.dot(activated, down_weight, preferred_element_type=jnp.float32)
    summed = sent_and_summed(
        lax.optimization_barrier(product.astype(jnp.bfloat16))
        .astype(jnp.float32)
        .astype(jnp.bfloat16),
        "tp",
        0,
    )
    returned = summed.astype(jnp.bfloat16)
    back_rows = lax.all_to_all(returned, "sp", split_axis=0, concat_axis=0, tiled=True)
    picked = back_rows.reshape(expert_count * capacity, width)[slot_index]
    combined = jnp.sum(
        picked.astype(jnp.float32).reshape(row_count, top_count, width) * route_weight[:, :, None],
        axis=1,
    )
    return (hidden_wide + combined).astype(jnp.bfloat16)


def solution(mesh):
    return jax.shard_map(
        local,
        mesh=mesh,
        in_specs=(
            P(("sp", "tp"), None),
            P("sp", "tp"),
            P("sp", "tp"),
            P(("sp", "tp"), None),
            P(("sp", "tp"), None),
            P(None, "tp"),
            P(None, "tp"),
            P(),
            P(),
            P(("sp", "tp"), None),
            P(("sp", "tp"), None),
            P("sp", None, "tp"),
            P("sp", None, "tp"),
            P("sp", "tp", None),
        ),
        out_specs=P(("sp", "tp"), None),
        check_vma=False,
    )
```

profile of v0, /device:TPU:1, one launch (start us, length us, event | category | flops | bytes accessed | tf_op | source)
XLA Modules:
  0.0 444.2 jit_solution(9489817846854970023)
XLA Ops:
  13.5 84.0 %all-gather.2.cloned.1.call-done = bf16[16384,320]{0,1:T(8,128)(2,1)} async-done(((bf16[128,320]{0,1:T(8,128)(2,1)}), bf16[16384,320]{0,1:T(8,128)(2,1)}) %all-gather.2.cloned.1.call-update) | async-done | bytes 10485776 | tf_op jit(solution)/shard_map/all_gather | solution.py:19
  97.4 201.9 %conditional.1 = (f32[4,256]{1,0:T(4,128)}, f32[256,4,128]{0,2,1:T(8,128)}) conditional(s32[]{:T(128)} %convert_element_type.82, () %tuple.28, (bf16[16384,320]{0,1:T(8,128)(2,1)}, bf16[256,512]{1,0:T(8,128)(2,1)}, s32[256]{0:T(256)S(1)}, s32[256]{0:T(256)S(1)}, s32[]{:T(128)}, /*index=5*/bf16[256,512]{1,0:T(8,128)(2,1)}, ...), branch_computations={%region_0.1_spmd, %region_1.6_spmd.clone} | conditional | flops 2439948032 | bytes 128145352 | solution.py:164
  97.4 7.7 %slice.34 = bf16[16384,256]{0,1:T(8,128)(2,1)} slice(bf16[16384,320]{0,1:T(8,128)(2,1)} %get-tuple-element.261), slice={[0:16384], [0:256]} | slice | bytes 16777216 | tf_op jit(solution)/shard_map/slice | solution.py:21
  105.1 11.9 %copy.78 = bf16[16384,256]{1,0:T(8,128)(2,1)} copy(bf16[16384,256]{0,1:T(8,128)(2,1)} %slice.34) | data formatting | bytes 16777216 | tf_op jit(solution)/shard_map/slice | solution.py:21
  120.7 178.7 %while.20 = (s32[]{:T(128)}, f32[4,256]{1,0:T(4,128)S(1)}, f32[4,256]{1,0:T(4,128)}, f32[256,4,128]{0,2,1:T(8,128)}, s32[8]{0:T(128)S(1)}, /*index=5*/s32[256]{0...) while((s32[]{:T(128)}, f32[4,256]{1,0:T(4,128)S(1)}, ...), condition=%wide.region_5.5_spmd.clone, body=%wide.region_2.4_spmd.clone.sunk | while | flops 2439944192 | bytes 82004680 | solution.py:150
  120.7 2.0 convolution_convert_fusion.5
  125.6 6.5 %fusion.96 = (f32[4,256]{1,0:T(4,128)S(1)}, f32[4,256,2048]{1,2,0:T(8,128)}) fusion(bf16[256,4,64]{0,2,1:T(8,128)(2,1)S(1)} %get-tuple-element.552, bf16[8,2048,64]{1,2,0:T(8,128)(2,1)} %get-tuple-element.551, s32[]{:T(128)} %get-tuple-element.528, f32[4,2048,256]{2,1,0:T(8,128)S(1)} %fusion.95, pred[256,2048]{0,1:T(8,128)(4,1)S(1)} %broadcast_compare_fusion.2), kind=kOutput, calls=%fused_computation.105.clone.1 | convolution fusion | flops 276823040 | bytes 17699328 | tf_op jit(solution)/shard_map/cond/branch_1_fun/while/body/eval_jaxpr/qhr,kr->hqk/dot_general | solution.py:131
  132.1 2.1 convolution_convert_fusion.6
  134.3 6.0 %fusion.100 = f32[256,4,128]{0,2,1:T(8,128)} fusion(bf16[2048,4,128]{0,2,1:T(8,128)(2,1)S(1)} %bitcast.116, f32[4,256,2048]{1,2,0:T(8,128)} %get-tuple-element.512, f32[4,256]{1,0:T(4,128)S(1)} %get-tuple-element.543, pred[256,2048]{0,1:T(8,128)(4,1)S(1)} %broadcast_compare_fusion.2, f32[256,4,128]{0,2,1:T(8,128)} %get-tuple-element.531, ...), kind=kOutput, calls=%fused_computation.15.clone.1 | convolution fusion | flops 543555584 | bytes 12066817 | tf_op jit(solution)/shard_map/cond/branch_1_fun/while/body/eval_jaxpr/hqk,khv->qhv/dot_general | solution.py:141
  142.4 2.0 convolution_convert_fusion.5
  147.3 6.5 %fusion.96 = (f32[4,256]{1,0:T(4,128)S(1)}, f32[4,256,2048]{1,2,0:T(8,128)}) fusion(bf16[256,4,64]{0,2,1:T(8,128)(2,1)S(1)} %get-tuple-element.552, bf16[8,2048,64]{1,2,0:T(8,128)(2,1)} %get-tuple-element.551, s32[]{:T(128)} %get-tuple-element.528, f32[4,2048,256]{2,1,0:T(8,128)S(1)} %fusion.95, pred[256,2048]{0,1:T(8,128)(4,1)S(1)} %broadcast_compare_fusion.2), kind=kOutput, calls=%fused_computation.105.clone.1 | convolution fusion | flops 276823040 | bytes 17699328 | tf_op jit(solution)/shard_map/cond/branch_1_fun/while/body/eval_jaxpr/qhr,kr->hqk/dot_general | solution.py:131
  153.8 2.1 convolution_convert_fusion.6
  156.0 6.1 %fusion.100 = f32[256,4,128]{0,2,1:T(8,128)} fusion(bf16[2048,4,128]{0,2,1:T(8,128)(2,1)S(1)} %bitcast.116, f32[4,256,2048]{1,2,0:T(8,128)} %get-tuple-element.512, f32[4,256]{1,0:T(4,128)S(1)} %get-tuple-element.543, pred[256,2048]{0,1:T(8,128)(4,1)S(1)} %broadcast_compare_fusion.2, f32[256,4,128]{0,2,1:T(8,128)} %get-tuple-element.531, ...), kind=kOutput, calls=%fused_computation.15.clone.1 | convolution fusion | flops 543555584 | bytes 12066817 | tf_op jit(solution)/shard_map/cond/branch_1_fun/while/body/eval_jaxpr/hqk,khv->qhv/dot_general | solution.py:141
  164.8 2.0 convolution_convert_fusion.5
  169.7 6.5 %fusion.96 = (f32[4,256]{1,0:T(4,128)S(1)}, f32[4,256,2048]{1,2,0:T(8,128)}) fusion(bf16[256,4,64]{0,2,1:T(8,128)(2,1)S(1)} %get-tuple-element.552, bf16[8,2048,64]{1,2,0:T(8,128)(2,1)} %get-tuple-element.551, s32[]{:T(128)} %get-tuple-element.528, f32[4,2048,256]{2,1,0:T(8,128)S(1)} %fusion.95, pred[256,2048]{0,1:T(8,128)(4,1)S(1)} %broadcast_compare_fusion.2), kind=kOutput, calls=%fused_computation.105.clone.1 | convolution fusion | flops 276823040 | bytes 17699328 | tf_op jit(solution)/shard_map/cond/branch_1_fun/while/body/eval_jaxpr/qhr,kr->hqk/dot_general | solution.py:131
  176.2 2.1 convolution_convert_fusion.6
  178.4 6.1 %fusion.100 = f32[256,4,128]{0,2,1:T(8,128)} fusion(bf16[2048,4,128]{0,2,1:T(8,128)(2,1)S(1)} %bitcast.116, f32[4,256,2048]{1,2,0:T(8,128)} %get-tuple-element.512, f32[4,256]{1,0:T(4,128)S(1)} %get-tuple-element.543, pred[256,2048]{0,1:T(8,128)(4,1)S(1)} %broadcast_compare_fusion.2, f32[256,4,128]{0,2,1:T(8,128)} %get-tuple-element.531, ...), kind=kOutput, calls=%fused_computation.15.clone.1 | convolution fusion | flops 543555584 | bytes 12066817 | tf_op jit(solution)/shard_map/cond/branch_1_fun/while/body/eval_jaxpr/hqk,khv->qhv/dot_general | solution.py:141
  192.1 6.5 %fusion.96 = (f32[4,256]{1,0:T(4,128)S(1)}, f32[4,256,2048]{1,2,0:T(8,128)}) fusion(bf16[256,4,64]{0,2,1:T(8,128)(2,1)S(1)} %get-tuple-element.552, bf16[8,2048,64]{1,2,0:T(8,128)(2,1)} %get-tuple-element.551, s32[]{:T(128)} %get-tuple-element.528, f32[4,2048,256]{2,1,0:T(8,128)S(1)} %fusion.95, pred[256,2048]{0,1:T(8,128)(4,1)S(1)} %broadcast_compare_fusion.2), kind=kOutput, calls=%fused_computation.105.clone.1 | convolution fusion | flops 276823040 | bytes 17699328 | tf_op jit(solution)/shard_map/cond/branch_1_fun/while/body/eval_jaxpr/qhr,kr->hqk/dot_general | solution.py:131
  198.7 2.1 convolution_convert_fusion.6
  200.8 6.1 %fusion.100 = f32[256,4,128]{0,2,1:T(8,128)} fusion(bf16[2048,4,128]{0,2,1:T(8,128)(2,1)S(1)} %bitcast.116, f32[4,256,2048]{1,2,0:T(8,128)} %get-tuple-element.512, f32[4,256]{1,0:T(4,128)S(1)} %get-tuple-element.543, pred[256,2048]{0,1:T(8,128)(4,1)S(1)} %broadcast_compare_fusion.2, f32[256,4,128]{0,2,1:T(8,128)} %get-tuple-element.531, ...), kind=kOutput, calls=%fused_computation.15.clone.1 | convolution fusion | flops 543555584 | bytes 12066817 | tf_op jit(solution)/shard_map/cond/branch_1_fun/while/body/eval_jaxpr/hqk,khv->qhv/dot_general | solution.py:141
  214.6 6.5 %fusion.96 = (f32[4,256]{1,0:T(4,128)S(1)}, f32[4,256,2048]{1,2,0:T(8,128)}) fusion(bf16[256,4,64]{0,2,1:T(8,128)(2,1)S(1)} %get-tuple-element.552, bf16[8,2048,64]{1,2,0:T(8,128)(2,1)} %get-tuple-element.551, s32[]{:T(128)} %get-tuple-element.528, f32[4,2048,256]{2,1,0:T(8,128)S(1)} %fusion.95, pred[256,2048]{0,1:T(8,128)(4,1)S(1)} %broadcast_compare_fusion.2), kind=kOutput, calls=%fused_computation.105.clone.1 | convolution fusion | flops 276823040 | bytes 17699328 | tf_op jit(solution)/shard_map/cond/branch_1_fun/while/body/eval_jaxpr/qhr,kr->hqk/dot_general | solution.py:131
  221.1 2.1 convolution_convert_fusion.6
  223.2 6.1 %fusion.100 = f32[256,4,128]{0,2,1:T(8,128)} fusion(bf16[2048,4,128]{0,2,1:T(8,128)(2,1)S(1)} %bitcast.116, f32[4,256,2048]{1,2,0:T(8,128)} %get-tuple-element.512, f32[4,256]{1,0:T(4,128)S(1)} %get-tuple-element.543, pred[256,2048]{0,1:T(8,128)(4,1)S(1)} %broadcast_compare_fusion.2, f32[256,4,128]{0,2,1:T(8,128)} %get-tuple-element.531, ...), kind=kOutput, calls=%fused_computation.15.clone.1 | convolution fusion | flops 543555584 | bytes 12066817 | tf_op jit(solution)/shard_map/cond/branch_1_fun/while/body/eval_jaxpr/hqk,khv->qhv/dot_general | solution.py:141
  237.0 6.5 %fusion.96 = (f32[4,256]{1,0:T(4,128)S(1)}, f32[4,256,2048]{1,2,0:T(8,128)}) fusion(bf16[256,4,64]{0,2,1:T(8,128)(2,1)S(1)} %get-tuple-element.552, bf16[8,2048,64]{1,2,0:T(8,128)(2,1)} %get-tuple-element.551, s32[]{:T(128)} %get-tuple-element.528, f32[4,2048,256]{2,1,0:T(8,128)S(1)} %fusion.95, pred[256,2048]{0,1:T(8,128)(4,1)S(1)} %broadcast_compare_fusion.2), kind=kOutput, calls=%fused_computation.105.clone.1 | convolution fusion | flops 276823040 | bytes 17699328 | tf_op jit(solution)/shard_map/cond/branch_1_fun/while/body/eval_jaxpr/qhr,kr->hqk/dot_general | solution.py:131
  243.5 2.1 convolution_convert_fusion.6
  245.7 6.1 %fusion.100 = f32[256,4,128]{0,2,1:T(8,128)} fusion(bf16[2048,4,128]{0,2,1:T(8,128)(2,1)S(1)} %bitcast.116, f32[4,256,2048]{1,2,0:T(8,128)} %get-tuple-element.512, f32[4,256]{1,0:T(4,128)S(1)} %get-tuple-element.543, pred[256,2048]{0,1:T(8,128)(4,1)S(1)} %broadcast_compare_fusion.2, f32[256,4,128]{0,2,1:T(8,128)} %get-tuple-element.531, ...), kind=kOutput, calls=%fused_computation.15.clone.1 | convolution fusion | flops 543555584 | bytes 12066817 | tf_op jit(solution)/shard_map/cond/branch_1_fun/while/body/eval_jaxpr/hqk,khv->qhv/dot_general | solution.py:141
  259.4 6.5 %fusion.96 = (f32[4,256]{1,0:T(4,128)S(1)}, f32[4,256,2048]{1,2,0:T(8,128)}) fusion(bf16[256,4,64]{0,2,1:T(8,128)(2,1)S(1)} %get-tuple-element.552, bf16[8,2048,64]{1,2,0:T(8,128)(2,1)} %get-tuple-element.551, s32[]{:T(128)} %get-tuple-element.528, f32[4,2048,256]{2,1,0:T(8,128)S(1)} %fusion.95, pred[256,2048]{0,1:T(8,128)(4,1)S(1)} %broadcast_compare_fusion.2), kind=kOutput, calls=%fused_computation.105.clone.1 | convolution fusion | flops 276823040 | bytes 17699328 | tf_op jit(solution)/shard_map/cond/branch_1_fun/while/body/eval_jaxpr/qhr,kr->hqk/dot_general | solution.py:131
  265.9 2.1 convolution_convert_fusion.6
  268.1 6.1 %fusion.100 = f32[256,4,128]{0,2,1:T(8,128)} fusion(bf16[2048,4,128]{0,2,1:T(8,128)(2,1)S(1)} %bitcast.116, f32[4,256,2048]{1,2,0:T(8,128)} %get-tuple-element.512, f32[4,256]{1,0:T(4,128)S(1)} %get-tuple-element.543, pred[256,2048]{0,1:T(8,128)(4,1)S(1)} %broadcast_compare_fusion.2, f32[256,4,128]{0,2,1:T(8,128)} %get-tuple-element.531, ...), kind=kOutput, calls=%fused_computation.15.clone.1 | convolution fusion | flops 543555584 | bytes 12066817 | tf_op jit(solution)/shard_map/cond/branch_1_fun/while/body/eval_jaxpr/hqk,khv->qhv/dot_general | solution.py:141
  277.0 2.0 convolution_convert_fusion.5
  281.8 6.5 %fusion.96 = (f32[4,256]{1,0:T(4,128)S(1)}, f32[4,256,2048]{1,2,0:T(8,128)}) fusion(bf16[256,4,64]{0,2,1:T(8,128)(2,1)S(1)} %get-tuple-element.552, bf16[8,2048,64]{1,2,0:T(8,128)(2,1)} %get-tuple-element.551, s32[]{:T(128)} %get-tuple-element.528, f32[4,2048,256]{2,1,0:T(8,128)S(1)} %fusion.95, pred[256,2048]{0,1:T(8,128)(4,1)S(1)} %broadcast_compare_fusion.2), kind=kOutput, calls=%fused_computation.105.clone.1 | convolution fusion | flops 276823040 | bytes 17699328 | tf_op jit(solution)/shard_map/cond/branch_1_fun/while/body/eval_jaxpr/qhr,kr->hqk/dot_general | solution.py:131
  288.4 2.1 convolution_convert_fusion.6
  290.5 6.1 %fusion.100 = f32[256,4,128]{0,2,1:T(8,128)} fusion(bf16[2048,4,128]{0,2,1:T(8,128)(2,1)S(1)} %bitcast.116, f32[4,256,2048]{1,2,0:T(8,128)} %get-tuple-element.512, f32[4,256]{1,0:T(4,128)S(1)} %get-tuple-element.543, pred[256,2048]{0,1:T(8,128)(4,1)S(1)} %broadcast_compare_fusion.2, f32[256,4,128]{0,2,1:T(8,128)} %get-tuple-element.531, ...), kind=kOutput, calls=%fused_computation.15.clone.1 | convolution fusion | flops 543555584 | bytes 12066817 | tf_op jit(solution)/shard_map/cond/branch_1_fun/while/body/eval_jaxpr/hqk,khv->qhv/dot_general | solution.py:141
  300.7 3.9 all_to_all.39
  304.8 3.0 multiply_reduce_fusion.1
  310.9 3.5 scatter_custom_fusion
  314.4 37.3 %all_to_all.40 = bf16[64,8,2048]{2,1,0:T(8,128)(2,1)S(1)} all-to-all(bf16[64,8,2048]{2,1,0:T(8,128)(2,1)S(1)} %bitcast.118), channel_id=1, replica_groups=mesh['sp'=64,'tp'=2] {'sp'}, dimensions={0} | all-to-all | bytes 4194304 | tf_op jit(solution)/shard_map/all_to_all | solution.py:200
  353.4 8.7 %all_to_all.41 = bf16[2,64,8,2048]{3,1,2,0:T(8,128)(2,1)S(1)} all-to-all(bf16[2,64,8,2048]{3,1,2,0:T(8,128)(2,1)S(1)} %broadcast_in_dim.75), channel_id=1, replica_groups=mesh['sp'=64,'tp'=2] {'tp'}, dimensions={0} | all-to-all | bytes 8388608 | tf_op jit(solution)/shard_map/all_to_all | solution.py:28
  365.9 8.5 %convolution_convert_fusion.2 = bf16[128,8,2048]{2,0,1:T(8,128)(2,1)} fusion(bf16[128,8,2048]{2,0,1:T(8,128)(2,1)} %bitcast.122, bf16[1,256,2048]{2,1,0:T(8,128)(2,1)S(1)} %copy-done, bf16[1,2048,256]{2,1,0:T(8,128)(2,1)S(1)} %copy-done.11, f32[128,8,256]{2,0,1:T(8,128)S(1)} %fusion.36), kind=kOutput, calls=%fused_computation.48 | convolution fusion | flops 2151153664 | bytes 11534336 | tf_op jit(solution)/shard_map/dot_general | solution.py:213
  374.4 2.5 copy.92
  376.9 8.3 %all_to_all.42 = bf16[2,64,8,2048]{3,1,2,0:T(8,128)(2,1)} all-to-all(bf16[2,64,8,2048]{3,1,2,0:T(8,128)(2,1)S(1)} %copy.92), channel_id=1, replica_groups=mesh['sp'=64,'tp'=2] {'tp'}, dimensions={0} | all-to-all | bytes 8388608 | tf_op jit(solution)/shard_map/all_to_all | solution.py:50
  385.2 3.5 reduce_sum.53
  388.7 2.5 copy.94
  391.2 5.4 %all-to-all-start.4 = ((bf16[64,8,2048]{2,1,0:T(8,128)(2,1)}), bf16[64,8,2048]{2,1,0:T(8,128)(2,1)S(1)}, u32[]{:S(2)}, u32[]{:S(2)}) async-start(bf16[64,8,2048]{2,1,0:T(8,128)(2,1)} %copy.94), calls=%async_computation.4 | async-start | bytes 4194304 | tf_op jit(solution)/shard_map/all_to_all | solution.py:222
  396.7 29.0 %all-to-all-done.4 = bf16[64,8,2048]{2,1,0:T(8,128)(2,1)S(1)} async-done(((bf16[64,8,2048]{2,1,0:T(8,128)(2,1)}), bf16[64,8,2048]{2,1,0:T(8,128)(2,1)S(1)}, u32[]{:S(2)}, u32[]{:S(2)}) %all-to-all-start.4) | async-done | bytes 2097184 | tf_op jit(solution)/shard_map/all_to_all | solution.py:222
  425.7 2.3 gather_fusion
  428.1 3.5 reshape.240
  431.5 4.8 %multiply_reduce_fusion = f32[128,2048]{1,0:T(8,128)S(1)} fusion(f32[128,2,2048]{2,1,0:T(2,128)} %reshape.240, f32[128,2]{1,0:T(8,128)S(1)} %copy.95), kind=kLoop, calls=%fused_computation.52 | loop fusion | flops 786432 | bytes 3146752 | tf_op jit(solution)/shard_map/reduce_sum | solution.py:224
  (184 shorter events, 74.2 us)
Async XLA Ops:
  6.5 359.4 %copy-start = (bf16[1,256,2048]{2,1,0:T(8,128)(2,1)S(1)}, bf16[1,256,2048]{2,1,0:T(8,128)(2,1)}, u32[]{:S(2)}) copy-start(bf16[1,256,2048]{2,1,0:T(8,128)(2,1)} %param.31) | copy-start | bytes 3145732
  6.5 90.9 %all-gather.2.cloned.1.call-start = ((), (), s32[]{:S(2)}) async-start(), calls=%async_computation.5 | async-start | bytes 10567680 | tf_op jit(solution)/shard_map/all_gather | solution.py:19
  97.4 207.4 %copy-start.6 = (bf16[128,2048]{1,0:T(8,128)(2,1)S(1)}, bf16[128,2048]{1,0:T(8,128)(2,1)}, u32[]{:S(2)}) copy-start(bf16[128,2048]{1,0:T(8,128)(2,1)} %param.18) | copy-start | bytes 1572868
  117.0 3.3 copy-start.7
  117.0 3.6 copy-start.3
  117.0 3.6 copy-start.4
  132.1 8.2 %slice-start = ((s8[8388608]{0:T(1024)(128)(4,1)}), s8[4194304]{0:T(1024)(128)(4,1)S(1)}, s32[]{:S(2)}) async-start(s8[8388608]{0:T(1024)(128)(4,1)} %bitcast.112), calls=%async_computation.6 | async-start | bytes 8388608 | tf_op jit(solution)/shard_map/cond/branch_1_fun/while
  134.3 6.0 %slice-start.1 = ((s8[8388608]{0:T(1024)(128)(4,1)}), s8[4194304]{0:T(1024)(128)(4,1)S(1)}, s32[]{:S(2)}) async-start(s8[8388608]{0:T(1024)(128)(4,1)} %bitcast.112), calls=%async_computation.7 | async-start | bytes 8388608 | tf_op jit(solution)/shard_map/cond/branch_1_fun/while
  153.8 8.2 %slice-start = ((s8[8388608]{0:T(1024)(128)(4,1)}), s8[4194304]{0:T(1024)(128)(4,1)S(1)}, s32[]{:S(2)}) async-start(s8[8388608]{0:T(1024)(128)(4,1)} %bitcast.112), calls=%async_computation.6 | async-start | bytes 8388608 | tf_op jit(solution)/shard_map/cond/branch_1_fun/while
  156.0 6.1 %slice-start.1 = ((s8[8388608]{0:T(1024)(128)(4,1)}), s8[4194304]{0:T(1024)(128)(4,1)S(1)}, s32[]{:S(2)}) async-start(s8[8388608]{0:T(1024)(128)(4,1)} %bitcast.112), calls=%async_computation.7 | async-start | bytes 8388608 | tf_op jit(solution)/shard_map/cond/branch_1_fun/while
  176.2 8.2 %slice-start = ((s8[8388608]{0:T(1024)(128)(4,1)}), s8[4194304]{0:T(1024)(128)(4,1)S(1)}, s32[]{:S(2)}) async-start(s8[8388608]{0:T(1024)(128)(4,1)} %bitcast.112), calls=%async_computation.6 | async-start | bytes 8388608 | tf_op jit(solution)/shard_map/cond/branch_1_fun/while
  178.4 6.1 %slice-start.1 = ((s8[8388608]{0:T(1024)(128)(4,1)}), s8[4194304]{0:T(1024)(128)(4,1)S(1)}, s32[]{:S(2)}) async-start(s8[8388608]{0:T(1024)(128)(4,1)} %bitcast.112), calls=%async_computation.7 | async-start | bytes 8388608 | tf_op jit(solution)/shard_map/cond/branch_1_fun/while
  198.7 8.2 %slice-start = ((s8[8388608]{0:T(1024)(128)(4,1)}), s8[4194304]{0:T(1024)(128)(4,1)S(1)}, s32[]{:S(2)}) async-start(s8[8388608]{0:T(1024)(128)(4,1)} %bitcast.112), calls=%async_computation.6 | async-start | bytes 8388608 | tf_op jit(solution)/shard_map/cond/branch_1_fun/while
  200.8 6.1 %slice-start.1 = ((s8[8388608]{0:T(1024)(128)(4,1)}), s8[4194304]{0:T(1024)(128)(4,1)S(1)}, s32[]{:S(2)}) async-start(s8[8388608]{0:T(1024)(128)(4,1)} %bitcast.112), calls=%async_computation.7 | async-start | bytes 8388608 | tf_op jit(solution)/shard_map/cond/branch_1_fun/while
  221.1 8.2 %slice-start = ((s8[8388608]{0:T(1024)(128)(4,1)}), s8[4194304]{0:T(1024)(128)(4,1)S(1)}, s32[]{:S(2)}) async-start(s8[8388608]{0:T(1024)(128)(4,1)} %bitcast.112), calls=%async_computation.6 | async-start | bytes 8388608 | tf_op jit(solution)/shard_map/cond/branch_1_fun/while
  223.2 6.1 %slice-start.1 = ((s8[8388608]{0:T(1024)(128)(4,1)}), s8[4194304]{0:T(1024)(128)(4,1)S(1)}, s32[]{:S(2)}) async-start(s8[8388608]{0:T(1024)(128)(4,1)} %bitcast.112), calls=%async_computation.7 | async-start | bytes 8388608 | tf_op jit(solution)/shard_map/cond/branch_1_fun/while
  243.5 8.2 %slice-start = ((s8[8388608]{0:T(1024)(128)(4,1)}), s8[4194304]{0:T(1024)(128)(4,1)S(1)}, s32[]{:S(2)}) async-start(s8[8388608]{0:T(1024)(128)(4,1)} %bitcast.112), calls=%async_computation.6 | async-start | bytes 8388608 | tf_op jit(solution)/shard_map/cond/branch_1_fun/while
  245.7 6.1 %slice-start.1 = ((s8[8388608]{0:T(1024)(128)(4,1)}), s8[4194304]{0:T(1024)(128)(4,1)S(1)}, s32[]{:S(2)}) async-start(s8[8388608]{0:T(1024)(128)(4,1)} %bitcast.112), calls=%async_computation.7 | async-start | bytes 8388608 | tf_op jit(solution)/shard_map/cond/branch_1_fun/while
  265.9 8.2 %slice-start = ((s8[8388608]{0:T(1024)(128)(4,1)}), s8[4194304]{0:T(1024)(128)(4,1)S(1)}, s32[]{:S(2)}) async-start(s8[8388608]{0:T(1024)(128)(4,1)} %bitcast.112), calls=%async_computation.6 | async-start | bytes 8388608 | tf_op jit(solution)/shard_map/cond/branch_1_fun/while
  268.1 6.1 %slice-start.1 = ((s8[8388608]{0:T(1024)(128)(4,1)}), s8[4194304]{0:T(1024)(128)(4,1)S(1)}, s32[]{:S(2)}) async-start(s8[8388608]{0:T(1024)(128)(4,1)} %bitcast.112), calls=%async_computation.7 | async-start | bytes 8388608 | tf_op jit(solution)/shard_map/cond/branch_1_fun/while
  288.4 8.2 %slice-start = ((s8[8388608]{0:T(1024)(128)(4,1)}), s8[4194304]{0:T(1024)(128)(4,1)S(1)}, s32[]{:S(2)}) async-start(s8[8388608]{0:T(1024)(128)(4,1)} %bitcast.112), calls=%async_computation.6 | async-start | bytes 8388608 | tf_op jit(solution)/shard_map/cond/branch_1_fun/while
  290.5 6.1 %slice-start.1 = ((s8[8388608]{0:T(1024)(128)(4,1)}), s8[4194304]{0:T(1024)(128)(4,1)S(1)}, s32[]{:S(2)}) async-start(s8[8388608]{0:T(1024)(128)(4,1)} %bitcast.112), calls=%async_computation.7 | async-start | bytes 8388608 | tf_op jit(solution)/shard_map/cond/branch_1_fun/while
  300.5 8.4 %copy-start.8 = (f32[2048]{0:T(1024)S(1)}, f32[2048]{0:T(1024)}, u32[]{:S(2)}) copy-start(f32[2048]{0:T(1024)} %param.26) | copy-start | bytes 24580
  307.8 1.1 copy-start.1
  362.1 2.5 copy-start.10
  362.7 1.9 copy-start.5
  364.7 1.3 copy-start.11
  388.7 7.9 %copy-start.9 = (f32[128,2]{0,1:T(2,128)S(1)}, f32[128,2]{0,1:T(2,128)}, u32[]{:S(2)}) copy-start(f32[128,2]{0,1:T(2,128)} %param.28) | copy-start | bytes 3076
  391.2 34.5 %all-to-all-start.4 = ((bf16[64,8,2048]{2,1,0:T(8,128)(2,1)}), bf16[64,8,2048]{2,1,0:T(8,128)(2,1)S(1)}, u32[]{:S(2)}, u32[]{:S(2)}) async-start(bf16[64,8,2048]{2,1,0:T(8,128)(2,1)} %copy.94), calls=%async_computation.4 | async-start | bytes 4194304 | tf_op jit(solution)/shard_map/all_to_all | solution.py:222
  428.1 8.3 %copy-start.2 = (f32[128,2048]{1,0:T(8,128)S(1)}, f32[128,2048]{1,0:T(8,128)}, u32[]{:S(2)}) copy-start(f32[128,2048]{1,0:T(8,128)} %copy-done.1) | copy-start | bytes 3145732
Sparse Core Ops, SparseCore 0:
  10.1 87.2 all-gather.1
where the time goes:
time: 447 us; the launch traced here: 444 us
  matrix products  157 us (35%)
  waiting for transfers between devices  113 us (25%)
  blocking collectives  58.2 us (13%)
  local copies, waits for them, and re-layouts  53.1 us (12%)
  other arithmetic  43.7 us (10%)
  between operations  13.7 us (3%)
  starting transfers between devices  5.4 us (1%)
    all_gather x1, waiting for transfers between devices, side_by_side(): lax.all_gather(both, axis, axis=dim, tiled=True)  84 us
    dot_general x8, matrix products, one_block(): jnp.einsum('qhr,kr->hqk', query_rot, rot_block, preferred_element_type=jn...  52.2 us
    dot_general x8, matrix products, one_block(): jnp.einsum('hqk,khv->qhv', weights.astype(jnp.bfloat16), value_rows, pref...  48.4 us
    all_to_all x1, blocking collectives, local(): lax.all_to_all(outgoing.reshape(expert_count, capacity, width), 'sp', spl...  37.3 us
    all_to_all x1, waiting for transfers between devices, local(): lax.all_to_all(returned, 'sp', split_axis=0, concat_axis=0, tiled=True)  29 us
    slice x3, local copies, waits for them, and re-layouts, side_by_side(): lax.slice_in_dim(whole, at, at + a.shape[along], axis=along)  21.4 us
    dot_general x8, matrix products, one_block(): jnp.dot(lat_block, value_up, preferred_element_type=jnp.float32)  17.1 us
    dot_general x8, matrix products, one_block(): jnp.dot(lat_block, key_up, preferred_element_type=jnp.float32)  15.8 us
  transfers between devices with their start and end apart: 2, of which 2 were waited for; matrix products, arithmetic and copies ran while one was open for 1% of the time, Pallas kernels for 0%

commit v1 on v0

v1 whole, which is shorter than its diff:
```python
import functools
import jax
import jax.numpy as jnp
import numpy as np
from jax import lax
from jax.experimental import pallas as pl
from jax.experimental.pallas import tpu as pltpu
from jax.sharding import PartitionSpec as P

QK_NOPE = 128
QK_ROPE = 64
V_DIM = 128
LATENT = 256
SEGMENT = 64
EPSILON = 1e-06
ROPE_BASE = 10000.0
NEG_LARGE = -1e30

N_SP = 64
N_TP = 2
HEADS_HERE = 4
ROWS = 128
SHARD = 160
UNIT = 4
KEYS = UNIT * ROWS
QROWS = HEADS_HERE * ROWS
CAP = 8
AXES = ("sp", "tp")
STEP = {"x": 1, "y": 4, "z": 16}
ORDER = (("z", "y", "x"), ("x", "z", "y"))
SHIFTS = (0, 1, -1, 2)
SCALE2 = float((QK_NOPE + QK_ROPE) ** (-0.5) * np.log2(np.e))


def moved(s, dim, by):
    step = STEP[dim]
    c = (s // step) % 4
    return s + step * ((c + by) % 4 - c)


def shift_pairs(phase, by):
    return [
        (s * N_TP + t, moved(s, ORDER[t][phase], by) * N_TP + t)
        for s in range(N_SP)
        for t in range(N_TP)
    ]


def shard_origin(s, t, k3, k2, k1):
    for phase, k in ((2, k3), (1, k2), (0, k1)):
        s = moved(s, ORDER[t][phase], -SHIFTS[k])
    return s


UNITS = 33
COLS = 12


@functools.lru_cache(None)
def work_table():
    table = np.zeros((N_SP * N_TP, UNITS + 1, COLS), np.int32)
    for s in range(N_SP):
        for t in range(N_TP):
            firsts = []
            for own in range(2):
                core = t if own == 0 else 1 - t
                for k3 in range(4):
                    for k2 in range(4):
                        for k1 in range(4):
                            firsts.append(4 * shard_origin(s, core, k3, k2, k1) + 2 * core)
            rows = []
            for group in range(2):
                base = 4 * s if group == 0 else 4 * (N_SP - 1 - s) + 2
                needed = [n for n in range(128) if firsts[n] <= base + 1]
                for at in range(0, len(needed), UNIT):
                    part = needed[at : at + UNIT]
                    segs = [firsts[n] for n in part]
                    masked = int(len(part) < UNIT or any(f + 1 > base for f in segs))
                    segs += [1 << 20] * (UNIT - len(part))
                    part = part + [part[-1]] * (UNIT - len(part))
                    rows.append([group, masked, base, t] + part + segs)
            assert len(rows) == UNITS
            rows.append(rows[-1])
            table[s * N_TP + t] = np.array(rows, np.int32)
    return table


def attention_body(
    units, qn_ref, q4_ref, key_up_ref, value_up_ref, *rest
):
    parts = rest[:8]
    out_ref = rest[8]
    keys, qabs, m_ref, l_ref, acc_ref, s0, s1, sems = rest[9:]
    part_rows = parts[0].shape[0]
    copies = []
    for n in range(8):
        copy = pltpu.make_async_copy(parts[n], keys.at[pl.ds(n * part_rows, part_rows)], sems.at[n])
        copy.start()
        copies.append(copy)
    nt = (((1,), (1,)), ((), ()))
    for g in range(2):
        for h in range(HEADS_HERE):
            cols = pl.ds(h * QK_NOPE, QK_NOPE)
            qabs[g, pl.ds(h * ROWS, ROWS), :] = lax.dot_general(
                qn_ref[g, :, cols], key_up_ref[:, cols], nt, preferred_element_type=jnp.float32
            ).astype(jnp.bfloat16)
    m_ref[...] = jnp.full(m_ref.shape, NEG_LARGE, jnp.float32)
    l_ref[...] = jnp.zeros(l_ref.shape, jnp.float32)
    acc_ref[...] = jnp.zeros(acc_ref.shape, jnp.float32)
    for copy in copies:
        copy.wait()

    def latent_tile(u, half):
        return jnp.concatenate(
            [keys[pl.ds(pl.multiple_of(units[u, 4 + j] * SHARD + half * SEGMENT, 32), SEGMENT), :] for j in range(UNIT)],
            axis=0,
        )

    def scores(u, s_ref):
        g = units[u, 0]
        rot = jnp.concatenate(
            [
                keys[pl.ds(pl.multiple_of(units[u, 4 + j] * SHARD + ROWS, 32), 32), pl.ds(h * 128, 128)]
                for j in range(UNIT)
                for h in range(2)
            ],
            axis=0,
        )
        q = qabs[g]
        for half in range(2):
            s_ref[:, pl.ds(half * 256, 256)] = lax.dot_general(
                q, latent_tile(u, half), nt, preferred_element_type=jnp.float32
            ) + lax.dot_general(q4_ref[g, half], rot, nt, preferred_element_type=jnp.float32)

    def fix(u, s_ref):
        @pl.when(units[u, 1] == 1)
        def _():
            lane = lax.broadcasted_iota(jnp.int32, (1, KEYS), 1)
            which = (lane % 256) // SEGMENT
            seg = jnp.full((1, KEYS), units[u, 8], jnp.int32)
            for j in range(1, UNIT):
                seg = jnp.where(which == j, units[u, 8 + j], seg)
            seg = seg + lane // 256
            row = lax.broadcasted_iota(jnp.int32, (QROWS, 1), 0)
            limit = units[u, 2] + (row % ROWS) // SEGMENT
            s_ref[...] = jnp.where(seg <= limit, s_ref[...], NEG_LARGE)

    def absorb(u, s_ref):
        g = units[u, 0]
        s = s_ref[...]
        before = m_ref[g][:, :1]
        after = jnp.maximum(before, jnp.max(s, axis=1, keepdims=True))
        p = jnp.exp2(s * SCALE2 - after * SCALE2)
        shrink = jnp.exp2((before - after) * SCALE2)
        partial = p[:, :128]
        for k in range(1, KEYS // 128):
            partial = partial + p[:, k * 128 : (k + 1) * 128]
        l_ref[g] = l_ref[g] * shrink + partial
        m_ref[g] = jnp.broadcast_to(after, (QROWS, 128))
        values = jnp.concatenate([latent_tile(u, 0), latent_tile(u, 1)], axis=0)
        acc_ref[g] = acc_ref[g] * shrink + jnp.dot(
            p.astype(jnp.bfloat16), values, preferred_element_type=jnp.float32
        )

    scores(0, s0)

    def pair(k, carry):
        u = k * 2
        fix(u, s0)
        scores(u + 1, s1)
        absorb(u, s0)
        fix(u + 1, s1)
        scores(u + 2, s0)
        absorb(u + 1, s1)
        return carry

    lax.fori_loop(0, UNITS // 2, pair, 0)
    fix(UNITS - 1, s0)
    absorb(UNITS - 1, s0)
    core = units[0, 3]
    for g in range(2):
        slot = 1 - core if g == 0 else core
        total = jnp.sum(l_ref[g], axis=1, keepdims=True)
        mean = (acc_ref[g] / total).astype(jnp.bfloat16)
        for h in range(HEADS_HERE):
            cols = pl.ds(h * V_DIM, V_DIM)
            out_ref[slot, :, cols] = jnp.dot(
                mean[h * ROWS : (h + 1) * ROWS], value_up_ref[:, cols], preferred_element_type=jnp.float32
            ).astype(jnp.bfloat16)


def attention(units, qn, q4, key_up, value_up, parts):
    vmem = pl.BlockSpec(memory_space=pltpu.VMEM)
    return pl.pallas_call(
        attention_body,
        out_shape=jax.ShapeDtypeStruct((2, ROWS, HEADS_HERE * V_DIM), jnp.bfloat16),
        in_specs=[pl.BlockSpec(memory_space=pltpu.SMEM)] + [vmem] * 4 + [pl.BlockSpec(memory_space=pl.ANY)] * 8,
        out_specs=vmem,
        scratch_shapes=[
            pltpu.VMEM((128 * SHARD, LATENT), jnp.bfloat16),
            pltpu.VMEM((2, QROWS, LATENT), jnp.bfloat16),
            pltpu.VMEM((2, QROWS, 128), jnp.float32),
            pltpu.VMEM((2, QROWS, 128), jnp.float32),
            pltpu.VMEM((2, QROWS, LATENT), jnp.float32),
            pltpu.VMEM((QROWS, KEYS), jnp.float32),
            pltpu.VMEM((QROWS, KEYS), jnp.float32),
            pltpu.SemaphoreType.DMA((8,)),
        ],
        compiler_params=pltpu.CompilerParams(vmem_limit_bytes=48 * 2**20),
        name="attention",
    )(units, qn, q4, key_up, value_up, *parts)


def project_body(first, second, out_proj, residual, gain, slots, hidden_ref, outgoing_ref):
    half = first.shape[1]
    projected = jnp.dot(first[...], out_proj[:half], preferred_element_type=jnp.float32) + jnp.dot(
        second[...], out_proj[half:], preferred_element_type=jnp.float32
    )
    hidden = (residual[...].astype(jnp.float32) + projected).astype(jnp.bfloat16)
    hidden_ref[...] = hidden
    wide = hidden.astype(jnp.float32)
    normed = wide * lax.rsqrt(jnp.mean(wide * wide, axis=-1, keepdims=True) + EPSILON)
    normed = (normed * gain[...]).astype(jnp.bfloat16)
    slot = lax.broadcasted_iota(jnp.int32, (outgoing_ref.shape[0], first.shape[0]), 0)
    pick = (slot == slots[0:1, :]) | (slot == slots[1:2, :])
    pick = jnp.where(pick, 1.0, 0.0).astype(jnp.bfloat16)
    outgoing_ref[...] = jnp.dot(pick, normed, preferred_element_type=jnp.float32).astype(jnp.bfloat16)


def project(first, second, out_proj, residual, gain, slots):
    width = residual.shape[1]
    vmem = pl.BlockSpec(memory_space=pltpu.VMEM)
    return pl.pallas_call(
        project_body,
        out_shape=(
            jax.ShapeDtypeStruct((ROWS, width), jnp.bfloat16),
            jax.ShapeDtypeStruct((N_SP * CAP, width), jnp.bfloat16),
        ),
        in_specs=[vmem] * 6,
        out_specs=(vmem, vmem),
        compiler_params=pltpu.CompilerParams(vmem_limit_bytes=40 * 2**20),
        name="project",
    )(first, second, out_proj, residual, gain, slots)


def experts_body(rows, gate_a, up_a, down_a, gate_b, up_b, down_b, out_ref):
    x = rows[...]
    halves = []
    for gate, up, down in ((gate_a, up_a, down_a), (gate_b, up_b, down_b)):
        gated = jnp.dot(x, gate[...], preferred_element_type=jnp.float32)
        raised = jnp.dot(x, up[...], preferred_element_type=jnp.float32)
        active = (gated / (1.0 + jnp.exp(-gated)) * raised).astype(jnp.bfloat16)
        halves.append(jnp.dot(active, down[...], preferred_element_type=jnp.float32).astype(jnp.bfloat16))
    out_ref[...] = (halves[0].astype(jnp.float32) + halves[1].astype(jnp.float32)).astype(jnp.bfloat16)


def experts(rows, own, other):
    count, width = rows.shape
    block = 256
    whole = lambda a: pl.BlockSpec(a.shape, lambda n: (0, 0))
    return pl.pallas_call(
        experts_body,
        grid=(count // block,),
        out_shape=jax.ShapeDtypeStruct((count, width), jnp.bfloat16),
        in_specs=[pl.BlockSpec((block, width), lambda n: (n, 0))] + [whole(a) for a in (*own, *other)],
        out_specs=pl.BlockSpec((block, width), lambda n: (n, 0)),
        compiler_params=pltpu.CompilerParams(
            dimension_semantics=("arbitrary",), vmem_limit_bytes=48 * 2**20
        ),
        name="experts",
    )(rows, *own, *other)


def combine_body(back, hidden, slots, weights, out_ref):
    slot = lax.broadcasted_iota(jnp.int32, (hidden.shape[0], back.shape[0]), 1)
    pick = jnp.where(slot == slots[:, 0:1], weights[:, 0:1], 0.0) + jnp.where(
        slot == slots[:, 1:2], weights[:, 1:2], 0.0
    )
    high = pick.astype(jnp.bfloat16)
    low = (pick - high.astype(jnp.float32)).astype(jnp.bfloat16)
    rows = back[...]
    mixed = jnp.dot(high, rows, preferred_element_type=jnp.float32) + jnp.dot(
        low, rows, preferred_element_type=jnp.float32
    )
    out_ref[...] = (hidden[...].astype(jnp.float32) + mixed).astype(jnp.bfloat16)


def combine(back, hidden, slots, weights):
    vmem = pl.BlockSpec(memory_space=pltpu.VMEM)
    return pl.pallas_call(
        combine_body,
        out_shape=jax.ShapeDtypeStruct(hidden.shape, jnp.bfloat16),
        in_specs=[vmem] * 4,
        out_specs=vmem,
        compiler_params=pltpu.CompilerParams(vmem_limit_bytes=32 * 2**20),
        name="combine",
    )(back, hidden, slots, weights)


def rotary(values, positions):
    half_width = values.shape[-1] // 2
    inverse = ROPE_BASE ** (-2.0 * jnp.arange(half_width, dtype=jnp.float32) / values.shape[-1])
    angles = positions.astype(jnp.float32)[:, None] * inverse[None, :]
    cosine = jnp.cos(angles)
    sine_part = jnp.sin(angles)
    if values.ndim == 3:
        cosine = cosine[:, None, :]
        sine_part = sine_part[:, None, :]
    first_half = values[..., :half_width]
    second = values[..., half_width:]
    return jnp.concatenate(
        [first_half * cosine - second * sine_part, second * cosine + first_half * sine_part],
        axis=-1,
    )


def gathered(shard):
    both = shard
    for phase in range(2):
        got = [both] + [lax.ppermute(both, AXES, shift_pairs(phase, by)) for by in SHIFTS[1:]]
        both = jnp.concatenate(got, axis=0)
    parts = [both] + [lax.ppermute(both, AXES, shift_pairs(2, by)) for by in SHIFTS[1:]]
    return parts


def local(
    residual,
    query_nope,
    query_rope,
    latent,
    key_rope,
    key_up,
    value_up,
    out_proj,
    norm_gain,
    routes,
    route_weight,
    w_gate,
    w_up,
    w_down,
):
    tp_index = lax.axis_index("tp")
    sp_index = lax.axis_index("sp")
    tok_dev = query_nope.shape[0]
    query_first = sp_index * tok_dev
    swap = [(0, 1), (1, 0)]

    key_pos = query_first + tp_index * ROWS + jnp.arange(ROWS, dtype=jnp.int32)
    key_rot = rotary(key_rope.astype(jnp.float32), key_pos).astype(jnp.bfloat16)
    packed = jnp.concatenate([key_rot[0:32], key_rot[64:96], key_rot[32:64], key_rot[96:128]], axis=1)
    shard = jnp.concatenate([latent, packed], axis=0)
    own_parts = gathered(shard)
    other_parts = [lax.ppermute(part, "tp", swap) for part in own_parts]

    query_pos = query_first + jnp.arange(tok_dev, dtype=jnp.int32)
    query_rot = rotary(
        query_rope.astype(jnp.float32).reshape(tok_dev, HEADS_HERE, QK_ROPE), query_pos
    ).astype(jnp.bfloat16)
    queries = jnp.concatenate([query_nope, query_rot.reshape(tok_dev, HEADS_HERE * QK_ROPE)], axis=1)
    mirror = [
        (s * N_TP + t, (N_SP - 1 - s) * N_TP + t) for s in range(N_SP) for t in range(N_TP)
    ]
    received = lax.ppermute(queries[ROWS:], AXES, mirror)
    sets = jnp.stack([queries[:ROWS], received])
    qn = sets[:, :, : HEADS_HERE * QK_NOPE]
    rot = sets[:, :, HEADS_HERE * QK_NOPE :].reshape(2, ROWS, HEADS_HERE, QK_ROPE)
    rot = jnp.swapaxes(rot, 1, 2).reshape(2, QROWS, QK_ROPE)
    none = jnp.zeros_like(rot)
    q4 = jnp.stack(
        [jnp.concatenate([rot, none], axis=-1), jnp.concatenate([none, rot], axis=-1)], axis=1
    )

    units = lax.dynamic_index_in_dim(
        jnp.asarray(work_table()), sp_index * N_TP + tp_index, 0, keepdims=False
    )
    attn = attention(units, qn, q4, key_up, value_up, own_parts + other_parts)
    cross = [(s * N_TP + 1, s * N_TP) for s in range(N_SP)] + [
        (s * N_TP, (N_SP - 1 - s) * N_TP + 1) for s in range(N_SP)
    ]
    straight = [(s * N_TP, s * N_TP) for s in range(N_SP)] + [
        (s * N_TP + 1, (N_SP - 1 - s) * N_TP + 1) for s in range(N_SP)
    ]
    crossed = lax.ppermute(attn[0], AXES, cross)
    kept = lax.ppermute(attn[1], AXES, straight)
    first = jnp.where(tp_index == 0, kept, crossed)
    second = jnp.where(tp_index == 0, crossed, kept)

    flat = routes.reshape(-1)
    order = jnp.arange(flat.shape[0], dtype=jnp.int32)
    earlier = (flat[:, None] == flat[None, :]) & (order[None, :] < order[:, None])
    rank = jnp.sum(earlier.astype(jnp.int32), axis=1)
    slots = (flat * CAP + rank).reshape(routes.shape)

    hidden, outgoing = project(first, second, out_proj, residual, norm_gain[None, :], slots.T)
    width = residual.shape[1]
    arrived = lax.all_to_all(
        outgoing.reshape(N_SP, CAP, width), "sp", split_axis=0, concat_axis=0, tiled=True
    ).reshape(N_SP * CAP, width)
    own = (w_gate[0], w_up[0], w_down[0])
    other = tuple(lax.ppermute(w, "tp", swap) for w in own)
    produced = experts(arrived, own, other)
    back = lax.all_to_all(
        produced.reshape(N_SP, CAP, width), "sp", split_axis=0, concat_axis=0, tiled=True
    ).reshape(N_SP * CAP, width)
    return combine(back, hidden, slots, route_weight)


def solution(mesh):
    return jax.shard_map(
        local,
        mesh=mesh,
        in_specs=(
            P(("sp", "tp"), None),
            P("sp", "tp"),
            P("sp", "tp"),
            P(("sp", "tp"), None),
            P(("sp", "tp"), None),
            P(None, "tp"),
            P(None, "tp"),
            P(),
            P(),
            P(("sp", "tp"), None),
            P(("sp", "tp"), None),
            P("sp", None, "tp"),
            P("sp", None, "tp"),
            P("sp", "tp", None),
        ),
        out_specs=P(("sp", "tp"), None),
        check_vma=False,
    )
```

time: 447 us -> 199 us (0.45)
  matrix products: 157 us -> 0 us
  blocking collectives: 58.2 us -> 0 us
  starting transfers between devices: 5.4 us -> 53.7 us
  Pallas kernels: 0 us -> 42 us
  other arithmetic: 43.7 us -> 2.05 us
  local copies, waits for them, and re-layouts: 53.1 us -> 12 us
  waiting for transfers between devices: 113 us -> 88.1 us
  between operations: 13.7 us -> 0.44 us
    dot_general x43 -> x0, matrix products: 157 us -> none  [the longest x8 52.2 us: one_block(): jnp.einsum('qhr,kr->hqk', query_rot, rot_block, preferred_element_type=jn...]
    all_gather x1 -> x0, waiting for transfers between devices: 84 us -> none  [side_by_side(): lax.all_gather(both, axis, axis=dim, tiled=True)]
    all_to_all x4 -> x0, blocking collectives: 58.2 us -> none  [the longest x1 37.3 us: local(): lax.all_to_all(outgoing.reshape(expert_count, capacity, width), 'sp', spl...]
    ppermute x0 -> x19, waiting for transfers between devices: none -> 43.1 us  [the longest x3 19.7 us: gathered(): lax.ppermute(both, AXES, shift_pairs(2, by))]
    pallas_call x0 -> x4, Pallas kernels: none -> 42 us  [the longest x1 30.9 us: attention(): pl.pallas_call(attention_body, out_shape=jax.ShapeDtypeStruct((2, ROWS, H...]
    ppermute x0 -> x19, starting transfers between devices: none -> 40.8 us  [the longest x4 12.8 us: local(): other_parts = [lax.ppermute(part, 'tp', swap) for part in own_parts]]
    slice x4 -> x1, local copies, waits for them, and re-layouts: 21.6 us -> 0.12 us  [local(): sets[:, :, HEADS_HERE * QK_NOPE:].reshape(2, ROWS, HEADS_HERE, QK_ROPE)]
    reduce_sum x11 -> x1, other arithmetic: 20.5 us -> 0.18 us  [local(): rank = jnp.sum(earlier.astype(jnp.int32), axis=1)]
  transfers between devices with their start and end apart: 2 -> 21, of which waited for: 2 -> 14; matrix products, arithmetic and copies ran while one was open for 1% -> 2% of each run, Pallas kernels for 0% -> 0%
where the time goes in v1:
time: 199 us; the launch traced here: 198 us
  waiting for transfers between devices  88.1 us (44%)
  starting transfers between devices  53.7 us (27%)
  Pallas kernels  42 us (21%)
  local copies, waits for them, and re-layouts  12 us (6%)
  other arithmetic  2.05 us (1%)
    pallas_call x1, Pallas kernels, attention(): pl.pallas_call(attention_body, out_shape=jax.ShapeDtypeStruct((2, ROWS, H...  30.9 us
    all_to_all x1, waiting for transfers between devices, local(): lax.all_to_all(produced.reshape(N_SP, CAP, width), 'sp', split_axis=0, co...  27 us
    ppermute x3, waiting for transfers between devices, gathered(): lax.ppermute(both, AXES, shift_pairs(2, by))  19.7 us
    all_to_all x1, waiting for transfers between devices, local(): lax.all_to_all(outgoing.reshape(N_SP, CAP, width), 'sp', split_axis=0, co...  18.1 us
    ppermute x4, starting transfers between devices, local(): other_parts = [lax.ppermute(part, 'tp', swap) for part in own_parts]  12.8 us
    ppermute x6, starting transfers between devices, gathered(): lax.ppermute(both, AXES, shift_pairs(phase, by))  10.5 us
    ppermute x6, waiting for transfers between devices, gathered(): lax.ppermute(both, AXES, shift_pairs(phase, by))  10.3 us
    unnamed x45, local copies, waits for them, and re-layouts  10.2 us
  transfers between devices with their start and end apart: 21, of which 14 were waited for; matrix products, arithmetic and copies ran while one was open for 2% of the time, Pallas kernels for 0%

profile of v1, /device:TPU:1, one launch (start us, length us, event | category | flops | bytes accessed | tf_op | source)
XLA Modules:
  0.0 198.4 jit_solution(4271893245283880869)
XLA Ops:
  0.0 0.8 copy.50
  1.3 0.9 maximum_maximum_fusion
  2.2 2.0 %collective-permute-start.1 = (bf16[160,256]{1,0:T(8,128)(2,1)S(1)}, bf16[160,256]{1,0:T(8,128)(2,1)S(1)}, u32[]{:S(2)}, u32[]{:S(2)}) collective-permute-start(bf16[160,256]{1,0:T(8,128)(2,1)S(1)} %maximum_maximum_fusion), channel_id=1, source_target_pairs={{0,32},{1,3},{2,34},{3,5},{4,36},{5,7},{6,38},{7,1},{8,40},{9,11},... | collective-permute-start | bytes 245768 | tf_op jit(solution)/shard_map/ppermute | solution.py:320
  4.3 1.4 collective-permute-start.2
  5.6 1.6 collective-permute-start.3
  7.3 0.8 constant_dynamic-update-slice_fusion.4
  8.3 2.1 %collective-permute-done.3 = bf16[160,256]{1,0:T(8,128)(2,1)S(1)} collective-permute-done((bf16[160,256]{1,0:T(8,128)(2,1)S(1)}, bf16[160,256]{1,0:T(8,128)(2,1)S(1)}, u32[]{:S(2)}, u32[]{:S(2)}) %collective-permute-start.3) | collective-permute-done | bytes 81952 | tf_op jit(solution)/shard_map/ppermute | solution.py:320
  10.4 1.8 collective-permute-start.4
  12.2 2.5 %collective-permute-start.5 = (bf16[640,256]{1,0:T(8,128)(2,1)S(1)}, bf16[640,256]{1,0:T(8,128)(2,1)S(1)}, u32[]{:S(2)}, u32[]{:S(2)}) collective-permute-start(bf16[640,256]{1,0:T(8,128)(2,1)S(1)} %get-tuple-element.19), channel_id=1, source_target_pairs={{0,24},{1,97},{2,26},{3,99},{4,28},{5,101},{6,30},{7,103},{8,0},{9... | collective-permute-start | bytes 983048 | tf_op jit(solution)/shard_map/ppermute | solution.py:320
  14.7 1.1 collective-permute-start.6
  15.8 3.6 %collective-permute-done.4 = bf16[640,256]{1,0:T(8,128)(2,1)S(1)} collective-permute-done((bf16[640,256]{1,0:T(8,128)(2,1)S(1)}, bf16[640,256]{1,0:T(8,128)(2,1)S(1)}, u32[]{:S(2)}, u32[]{:S(2)}) %collective-permute-start.4) | collective-permute-done | bytes 327712 | tf_op jit(solution)/shard_map/ppermute | solution.py:320
  19.4 2.8 %collective-permute-done.5 = bf16[640,256]{1,0:T(8,128)(2,1)S(1)} collective-permute-done((bf16[640,256]{1,0:T(8,128)(2,1)S(1)}, bf16[640,256]{1,0:T(8,128)(2,1)S(1)}, u32[]{:S(2)}, u32[]{:S(2)}) %collective-permute-start.5) | collective-permute-done | bytes 327712 | tf_op jit(solution)/shard_map/ppermute | solution.py:320
  22.3 1.8 collective-permute-done.6
  24.1 1.1 collective-permute-start.7
  25.2 1.8 collective-permute-start.8
  27.0 1.3 collective-permute-start.9
  28.4 3.8 %collective-permute-start.10 = (bf16[2560,256]{1,0:T(8,128)(2,1)S(1)}, bf16[2560,256]{1,0:T(8,128)(2,1)}, u32[]{:S(2)}, u32[]{:S(2)}) collective-permute-start(bf16[2560,256]{1,0:T(8,128)(2,1)S(1)} %constant_dynamic-update-slice_fusion.5.rest_0_), channel_id=1, source_target_pairs={{0,1},{1,0},{2,3},{3,2},{4,5},{5,4},{6,7},{7,6},{8,9},{9,8},{10,11... | collective-permute-start | bytes 3932168 | tf_op jit(solution)/shard_map/ppermute | solution.py:353
  32.3 9.9 %collective-permute-done.7.rest_1_ = bf16[2560,256]{1,0:T(8,128)(2,1)S(1)} collective-permute-done((bf16[2560,256]{1,0:T(8,128)(2,1)S(1)}, bf16[2560,256]{1,0:T(8,128)(2,1)S(1)}, u32[]{:S(2)}, u32[]{:S(2)}) %collective-permute-start.7) | collective-permute-done | bytes 1310752 | tf_op jit(solution)/shard_map/ppermute | solution.py:322
  42.2 3.6 %collective-permute-start.11 = (bf16[2560,256]{1,0:T(8,128)(2,1)S(1)}, bf16[2560,256]{1,0:T(8,128)(2,1)}, u32[]{:S(2)}, u32[]{:S(2)}) collective-permute-start(bf16[2560,256]{1,0:T(8,128)(2,1)S(1)} %collective-permute-done.7.rest_1_), channel_id=1, source_target_pairs={{0,1},{1,0},{2,3},{3,2},{4,5},{5,4},{6,7},{7,6},{8,9},{9,8},{10,11... | collective-permute-start | bytes 3932168 | tf_op jit(solution)/shard_map/ppermute | solution.py:353
  45.8 9.8 %collective-permute-done.8.rest_2_ = bf16[2560,256]{1,0:T(8,128)(2,1)} collective-permute-done((bf16[2560,256]{1,0:T(8,128)(2,1)S(1)}, bf16[2560,256]{1,0:T(8,128)(2,1)}, u32[]{:S(2)}, u32[]{:S(2)}) %collective-permute-start.8) | collective-permute-done | bytes 1310752 | tf_op jit(solution)/shard_map/ppermute | solution.py:322
  55.6 3.8 %collective-permute-start.12 = (bf16[2560,256]{1,0:T(8,128)(2,1)}, bf16[2560,256]{1,0:T(8,128)(2,1)}, u32[]{:S(2)}, u32[]{:S(2)}) collective-permute-start(bf16[2560,256]{1,0:T(8,128)(2,1)} %collective-permute-done.8.rest_2_), channel_id=1, source_target_pairs={{0,1},{1,0},{2,3},{3,2},{4,5},{5,4},{6,7},{7,6},{8,9},{9,8},{10,11... | collective-permute-start | bytes 3932168 | tf_op jit(solution)/shard_map/ppermute | solution.py:353
  59.4 1.5 collective-permute-start.13
  61.4 4.9 %collective-permute-start = (bf16[128,768]{1,0:T(8,128)(2,1)S(1)}, bf16[128,768]{1,0:T(8,128)(2,1)S(1)}, u32[]{:S(2)}, u32[]{:S(2)}) collective-permute-start(bf16[128,768]{1,0:T(8,128)(2,1)S(1)} %get-tuple-element.9), channel_id=1, source_target_pairs={{0,126},{1,127},{2,124},{3,125},{4,122},{5,123},{6,120},{7,121},{8... | collective-permute-start | bytes 589832 | tf_op jit(solution)/shard_map/ppermute | solution.py:363
  66.3 0.7 dynamic-slice_bitcast_fusion.units
  67.0 6.3 %collective-permute-done = bf16[128,768]{1,0:T(8,128)(2,1)S(1)} collective-permute-done((bf16[128,768]{1,0:T(8,128)(2,1)S(1)}, bf16[128,768]{1,0:T(8,128)(2,1)S(1)}, u32[]{:S(2)}, u32[]{:S(2)}) %collective-permute-start) | collective-permute-done | bytes 196640 | tf_op jit(solution)/shard_map/ppermute | solution.py:363
  74.0 0.6 copy-done.11
  74.7 30.9 %attention.1 = bf16[2,128,512]{2,1,0:T(8,128)(2,1)S(1)} custom-call(s32[34,12]{1,0:T(8,128)S(1)} %dynamic-slice_bitcast_fusion.units, bf16[2,128,512]{2,1,0:T(8,128)(2,1)S(1)} %fusion.qn_ref, bf16[2,2,512,128]{3,2,1,0:T(8,128)(2,1)S(1)} %pad_maximum_fusion.q4_ref, bf16[256,512]{1,0:T(8,128)(2,1)S(1)} %copy-done.11, bf16[256,512]{1,0:T(8,128)(2,1)S(1)} %copy-done.12, ...), custom_call_target="tpu_custom_call" | custom-call | tf_op jit(solution)/shard_map/attention/pallas_call | solution.py:194
  105.7 0.9 collective-permute-start.15
  106.6 6.9 %collective-permute-start.14 = (bf16[128,512]{1,0:T(8,128)(2,1)S(1)}, bf16[128,512]{1,0:T(8,128)(2,1)S(1)}, u32[]{:S(2)}, u32[]{:S(2)}) collective-permute-start(bf16[128,512]{1,0:T(8,128)(2,1)S(1)} %get-tuple-element.16), channel_id=1, source_target_pairs={{0,0},{2,2},{4,4},{6,6},{8,8},{10,10},{12,12},{14,14},{16,16},{18,... | collective-permute-start | bytes 393224 | tf_op jit(solution)/shard_map/ppermute | solution.py:384
  114.3 1.3 collective-permute-done.15
  115.6 2.2 %collective-permute-done.14 = bf16[128,512]{1,0:T(8,128)(2,1)S(1)} collective-permute-done((bf16[128,512]{1,0:T(8,128)(2,1)S(1)}, bf16[128,512]{1,0:T(8,128)(2,1)S(1)}, u32[]{:S(2)}, u32[]{:S(2)}) %collective-permute-start.14) | collective-permute-done | bytes 131104 | tf_op jit(solution)/shard_map/ppermute | solution.py:384
  117.8 2.2 %copy-done = bf16[1024,2048]{1,0:T(8,128)(2,1)S(1)} copy-done((bf16[1024,2048]{1,0:T(8,128)(2,1)S(1)}, bf16[1024,2048]{1,0:T(8,128)(2,1)}, u32[]{:S(2)}) %copy-start) | copy-done | bytes 4194328
  120.0 2.9 %project.1 = (bf16[128,2048]{1,0:T(8,128)(2,1)S(1)}, bf16[512,2048]{1,0:T(8,128)(2,1)}) custom-call(bf16[128,512]{1,0:T(8,128)(2,1)S(1)} %get-tuple-element.14.first, bf16[128,512]{1,0:T(8,128)(2,1)S(1)} %get-tuple-element.13.second, bf16[1024,2048]{1,0:T(8,128)(2,1)S(1)} %copy-done, bf16[128,2048]{1,0:T(8,128)(2,1)S(1)} %copy-done.10, ...), custom_call_target="tpu_custom_call" | custom-call | tf_op jit(solution)/shard_map/project/pallas_call | solution.py:233
  122.9 0.8 copy-done.8
  123.7 8.0 %all-to-all-start = ((bf16[64,8,2048]{2,1,0:T(8,128)(2,1)}), bf16[64,8,2048]{2,1,0:T(8,128)(2,1)}, u32[]{:S(2)}, u32[]{:S(2)}) async-start(bf16[64,8,2048]{2,1,0:T(8,128)(2,1)} %bitcast.16), calls=%async_computation | async-start | bytes 4194304 | tf_op jit(solution)/shard_map/all_to_all | solution.py:396
  131.8 0.5 collective-permute-start.17
  132.4 2.0 %collective-permute-done.16.gate_b = bf16[2048,256]{1,0:T(8,128)(2,1)S(1)} collective-permute-done((bf16[2048,256]{1,0:T(8,128)(2,1)S(1)}, bf16[2048,256]{1,0:T(8,128)(2,1)S(1)}, u32[]{:S(2)}, u32[]{:S(2)}) %collective-permute-start.16) | collective-permute-done | bytes 1048608 | tf_op jit(solution)/shard_map/ppermute | solution.py:400
  134.4 1.0 copy-done.4
  135.4 0.5 collective-permute-done.17.up_b
  135.9 1.0 copy-done.6
  136.9 0.7 collective-permute-done.18.down_b
  137.5 18.1 %all-to-all-done = bf16[64,8,2048]{2,1,0:T(8,128)(2,1)} async-done(((bf16[64,8,2048]{2,1,0:T(8,128)(2,1)}), bf16[64,8,2048]{2,1,0:T(8,128)(2,1)}, u32[]{:S(2)}, u32[]{:S(2)}) %all-to-all-start) | async-done | bytes 2097184 | tf_op jit(solution)/shard_map/all_to_all | solution.py:396
  155.6 1.2 copy-done.5
  156.8 1.2 copy-done.7
  158.1 6.6 %experts.1 = bf16[512,2048]{1,0:T(8,128)(2,1)} custom-call(bf16[512,2048]{1,0:T(8,128)(2,1)} %bitcast.17.rows, bf16[2048,256]{1,0:T(8,128)(2,1)S(1)} %bitcast.33, bf16[2048,256]{1,0:T(8,128)(2,1)S(1)} %bitcast.35, bf16[256,2048]{1,0:T(8,128)(2,1)S(1)} %bitcast.37, bf16[2048,256]{1,0:T(8,128)(2,1)S(1)} %copy-done.5, bf16[2048,256]{1,0:T(8,128)(2,1)S(1)} %copy-done.7, ...), custom_call_target="tpu_custom_call" | custom-call | tf_op jit(solution)/shard_map/experts/pallas_call | solution.py:261
  164.7 5.0 %all-to-all-start.1 = ((bf16[64,8,2048]{2,1,0:T(8,128)(2,1)}), bf16[64,8,2048]{2,1,0:T(8,128)(2,1)S(1)}, u32[]{:S(2)}, u32[]{:S(2)}) async-start(bf16[64,8,2048]{2,1,0:T(8,128)(2,1)} %bitcast.40), calls=%async_computation.1 | async-start | bytes 4194304 | tf_op jit(solution)/shard_map/all_to_all | solution.py:402
  169.8 27.0 %all-to-all-done.1 = bf16[64,8,2048]{2,1,0:T(8,128)(2,1)S(1)} async-done(((bf16[64,8,2048]{2,1,0:T(8,128)(2,1)}), bf16[64,8,2048]{2,1,0:T(8,128)(2,1)S(1)}, u32[]{:S(2)}, u32[]{:S(2)}) %all-to-all-start.1) | async-done | bytes 2097184 | tf_op jit(solution)/shard_map/all_to_all | solution.py:402
  196.8 1.6 combine.1
  (75 shorter events, 2.9 us)
Async XLA Ops:
  2.2 6.0 %collective-permute-start.1 = (bf16[160,256]{1,0:T(8,128)(2,1)S(1)}, bf16[160,256]{1,0:T(8,128)(2,1)S(1)}, u32[]{:S(2)}, u32[]{:S(2)}) collective-permute-start(bf16[160,256]{1,0:T(8,128)(2,1)S(1)} %maximum_maximum_fusion), channel_id=1, source_target_pairs={{0,32},{1,3},{2,34},{3,5},{4,36},{5,7},{6,38},{7,1},{8,40},{9,11},... | collective-permute-start | bytes 245768 | tf_op jit(solution)/shard_map/ppermute | solution.py:320
  4.3 4.0 %collective-permute-start.2 = (bf16[160,256]{1,0:T(8,128)(2,1)S(1)}, bf16[160,256]{1,0:T(8,128)(2,1)S(1)}, u32[]{:S(2)}, u32[]{:S(2)}) collective-permute-start(bf16[160,256]{1,0:T(8,128)(2,1)S(1)} %maximum_maximum_fusion), channel_id=1, source_target_pairs={{0,96},{1,7},{2,98},{3,1},{4,100},{5,3},{6,102},{7,5},{8,104},{9,1... | collective-permute-start | bytes 245768 | tf_op jit(solution)/shard_map/ppermute | solution.py:320
  5.6 4.8 %collective-permute-start.3 = (bf16[160,256]{1,0:T(8,128)(2,1)S(1)}, bf16[160,256]{1,0:T(8,128)(2,1)S(1)}, u32[]{:S(2)}, u32[]{:S(2)}) collective-permute-start(bf16[160,256]{1,0:T(8,128)(2,1)S(1)} %maximum_maximum_fusion), channel_id=1, source_target_pairs={{0,64},{1,5},{2,66},{3,7},{4,68},{5,1},{6,70},{7,3},{8,72},{9,13},... | collective-permute-start | bytes 245768 | tf_op jit(solution)/shard_map/ppermute | solution.py:320
  8.2 20.1 %copy-start.15 = (bf16[256,256]{1,0:T(8,128)(2,1)S(1)}, bf16[256,256]{1,0:T(8,128)(2,1)}, u32[]{:S(2)}) copy-start(bf16[256,256]{1,0:T(8,128)(2,1)} %param.17) | copy-start | bytes 393220
  10.4 9.0 %collective-permute-start.4 = (bf16[640,256]{1,0:T(8,128)(2,1)S(1)}, bf16[640,256]{1,0:T(8,128)(2,1)S(1)}, u32[]{:S(2)}, u32[]{:S(2)}) collective-permute-start(bf16[640,256]{1,0:T(8,128)(2,1)S(1)} %get-tuple-element.19), channel_id=1, source_target_pairs={{0,8},{1,33},{2,10},{3,35},{4,12},{5,37},{6,14},{7,39},{8,16},{9,4... | collective-permute-start | bytes 983048 | tf_op jit(solution)/shard_map/ppermute | solution.py:320
  12.2 10.0 %collective-permute-start.5 = (bf16[640,256]{1,0:T(8,128)(2,1)S(1)}, bf16[640,256]{1,0:T(8,128)(2,1)S(1)}, u32[]{:S(2)}, u32[]{:S(2)}) collective-permute-start(bf16[640,256]{1,0:T(8,128)(2,1)S(1)} %get-tuple-element.19), channel_id=1, source_target_pairs={{0,24},{1,97},{2,26},{3,99},{4,28},{5,101},{6,30},{7,103},{8,0},{9... | collective-permute-start | bytes 983048 | tf_op jit(solution)/shard_map/ppermute | solution.py:320
  14.7 9.4 %collective-permute-start.6 = (bf16[640,256]{1,0:T(8,128)(2,1)S(1)}, bf16[640,256]{1,0:T(8,128)(2,1)S(1)}, u32[]{:S(2)}, u32[]{:S(2)}) collective-permute-start(bf16[640,256]{1,0:T(8,128)(2,1)S(1)} %get-tuple-element.19), channel_id=1, source_target_pairs={{0,16},{1,65},{2,18},{3,67},{4,20},{5,69},{6,22},{7,71},{8,24},{9,... | collective-permute-start | bytes 983048 | tf_op jit(solution)/shard_map/ppermute | solution.py:320
  22.3 39.0 %copy-start.14 = (bf16[256,512]{1,0:T(8,128)(2,1)S(1)}, bf16[256,512]{1,0:T(8,128)(2,1)}, u32[]{:S(2)}) copy-start(bf16[256,512]{1,0:T(8,128)(2,1)} %param.16) | copy-start | bytes 786436
  24.1 18.1 %collective-permute-start.7 = (bf16[2560,256]{1,0:T(8,128)(2,1)S(1)}, bf16[2560,256]{1,0:T(8,128)(2,1)S(1)}, u32[]{:S(2)}, u32[]{:S(2)}) collective-permute-start(bf16[2560,256]{1,0:T(8,128)(2,1)S(1)} %constant_dynamic-update-slice_fusion.5.rest_0_), channel_id=1, source_target_pairs={{0,2},{1,9},{2,4},{3,11},{4,6},{5,13},{6,0},{7,15},{8,10},{9,17},{... | collective-permute-start | bytes 3932168 | tf_op jit(solution)/shard_map/ppermute | solution.py:322
  25.2 30.4 %collective-permute-start.8 = (bf16[2560,256]{1,0:T(8,128)(2,1)S(1)}, bf16[2560,256]{1,0:T(8,128)(2,1)}, u32[]{:S(2)}, u32[]{:S(2)}) collective-permute-start(bf16[2560,256]{1,0:T(8,128)(2,1)S(1)} %constant_dynamic-update-slice_fusion.5.rest_0_), channel_id=1, source_target_pairs={{0,6},{1,25},{2,0},{3,27},{4,2},{5,29},{6,4},{7,31},{8,14},{9,1},{... | collective-permute-start | bytes 3932168 | tf_op jit(solution)/shard_map/ppermute | solution.py:322
  27.0 32.4 %collective-permute-start.9 = (bf16[2560,256]{1,0:T(8,128)(2,1)S(1)}, bf16[2560,256]{1,0:T(8,128)(2,1)}, u32[]{:S(2)}, u32[]{:S(2)}) collective-permute-start(bf16[2560,256]{1,0:T(8,128)(2,1)S(1)} %constant_dynamic-update-slice_fusion.5.rest_0_), channel_id=1, source_target_pairs={{0,4},{1,17},{2,6},{3,19},{4,0},{5,21},{6,2},{7,23},{8,12},{9,25},... | collective-permute-start | bytes 3932168 | tf_op jit(solution)/shard_map/ppermute | solution.py:322
  28.4 45.5 %collective-permute-start.10 = (bf16[2560,256]{1,0:T(8,128)(2,1)S(1)}, bf16[2560,256]{1,0:T(8,128)(2,1)}, u32[]{:S(2)}, u32[]{:S(2)}) collective-permute-start(bf16[2560,256]{1,0:T(8,128)(2,1)S(1)} %constant_dynamic-update-slice_fusion.5.rest_0_), channel_id=1, source_target_pairs={{0,1},{1,0},{2,3},{3,2},{4,5},{5,4},{6,7},{7,6},{8,9},{9,8},{10,11... | collective-permute-start | bytes 3932168 | tf_op jit(solution)/shard_map/ppermute | solution.py:353
  42.2 31.8 %collective-permute-start.11 = (bf16[2560,256]{1,0:T(8,128)(2,1)S(1)}, bf16[2560,256]{1,0:T(8,128)(2,1)}, u32[]{:S(2)}, u32[]{:S(2)}) collective-permute-start(bf16[2560,256]{1,0:T(8,128)(2,1)S(1)} %collective-permute-done.7.rest_1_), channel_id=1, source_target_pairs={{0,1},{1,0},{2,3},{3,2},{4,5},{5,4},{6,7},{7,6},{8,9},{9,8},{10,11... | collective-permute-start | bytes 3932168 | tf_op jit(solution)/shard_map/ppermute | solution.py:353
  55.6 18.4 %collective-permute-start.12 = (bf16[2560,256]{1,0:T(8,128)(2,1)}, bf16[2560,256]{1,0:T(8,128)(2,1)}, u32[]{:S(2)}, u32[]{:S(2)}) collective-permute-start(bf16[2560,256]{1,0:T(8,128)(2,1)} %collective-permute-done.8.rest_2_), channel_id=1, source_target_pairs={{0,1},{1,0},{2,3},{3,2},{4,5},{5,4},{6,7},{7,6},{8,9},{9,8},{10,11... | collective-permute-start | bytes 3932168 | tf_op jit(solution)/shard_map/ppermute | solution.py:353
  59.4 14.6 %collective-permute-start.13 = (bf16[2560,256]{1,0:T(8,128)(2,1)}, bf16[2560,256]{1,0:T(8,128)(2,1)}, u32[]{:S(2)}, u32[]{:S(2)}) collective-permute-start(bf16[2560,256]{1,0:T(8,128)(2,1)} %collective-permute-done.9.rest_3_), channel_id=1, source_target_pairs={{0,1},{1,0},{2,3},{3,2},{4,5},{5,4},{6,7},{7,6},{8,9},{9,8},{10,11... | collective-permute-start | bytes 3932168 | tf_op jit(solution)/shard_map/ppermute | solution.py:353
  61.4 12.0 %collective-permute-start = (bf16[128,768]{1,0:T(8,128)(2,1)S(1)}, bf16[128,768]{1,0:T(8,128)(2,1)S(1)}, u32[]{:S(2)}, u32[]{:S(2)}) collective-permute-start(bf16[128,768]{1,0:T(8,128)(2,1)S(1)} %get-tuple-element.9), channel_id=1, source_target_pairs={{0,126},{1,127},{2,124},{3,125},{4,122},{5,123},{6,120},{7,121},{8... | collective-permute-start | bytes 589832 | tf_op jit(solution)/shard_map/ppermute | solution.py:363
  73.7 1.0 copy-start.11
  73.7 1.0 copy-start.12
  74.0 39.6 %copy-start.16 = (s32[128,2]{0,1:T(2,128)S(1)}, s32[128,2]{0,1:T(2,128)}, u32[]{:S(2)}) copy-start(s32[128,2]{0,1:T(2,128)} %param.24) | copy-start | bytes 3076
  105.7 12.1 %copy-start.10 = (bf16[128,2048]{1,0:T(8,128)(2,1)S(1)}, bf16[128,2048]{1,0:T(8,128)(2,1)}, u32[]{:S(2)}) copy-start(bf16[128,2048]{1,0:T(8,128)(2,1)} %residual.1) | copy-start | bytes 1572868
  105.7 12.1 %copy-start.13 = (f32[2048]{0:T(1024)S(1)}, f32[2048]{0:T(1024)}, u32[]{:S(2)}) copy-start(f32[2048]{0:T(1024)} %param.23) | copy-start | bytes 24580
  105.7 9.9 %collective-permute-start.15 = (bf16[128,512]{1,0:T(8,128)(2,1)S(1)}, bf16[128,512]{1,0:T(8,128)(2,1)S(1)}, u32[]{:S(2)}, u32[]{:S(2)}) collective-permute-start(bf16[128,512]{1,0:T(8,128)(2,1)S(1)} %get-tuple-element.15), channel_id=1, source_target_pairs={{1,0},{3,2},{5,4},{7,6},{9,8},{11,10},{13,12},{15,14},{17,16},{19,... | collective-permute-start | bytes 393224 | tf_op jit(solution)/shard_map/ppermute | solution.py:383
  106.6 11.1 %collective-permute-start.14 = (bf16[128,512]{1,0:T(8,128)(2,1)S(1)}, bf16[128,512]{1,0:T(8,128)(2,1)S(1)}, u32[]{:S(2)}, u32[]{:S(2)}) collective-permute-start(bf16[128,512]{1,0:T(8,128)(2,1)S(1)} %get-tuple-element.16), channel_id=1, source_target_pairs={{0,0},{2,2},{4,4},{6,6},{8,8},{10,10},{12,12},{14,14},{16,16},{18,... | collective-permute-start | bytes 393224 | tf_op jit(solution)/shard_map/ppermute | solution.py:384
  117.8 2.2 %copy-start = (bf16[1024,2048]{1,0:T(8,128)(2,1)S(1)}, bf16[1024,2048]{1,0:T(8,128)(2,1)}, u32[]{:S(2)}) copy-start(bf16[1024,2048]{1,0:T(8,128)(2,1)} %out_proj.1) | copy-start | bytes 12582916
  122.9 0.8 copy-start.8
  123.7 8.0 %copy-start.1 = (bf16[1,2048,256]{2,1,0:T(8,128)(2,1)S(1)}, bf16[1,2048,256]{2,1,0:T(8,128)(2,1)}, u32[]{:S(2)}) copy-start(bf16[1,2048,256]{2,1,0:T(8,128)(2,1)} %param.26) | copy-start | bytes 3145732
  123.7 8.1 %copy-start.2 = (bf16[1,2048,256]{2,1,0:T(8,128)(2,1)S(1)}, bf16[1,2048,256]{2,1,0:T(8,128)(2,1)}, u32[]{:S(2)}) copy-start(bf16[1,2048,256]{2,1,0:T(8,128)(2,1)} %param.27) | copy-start | bytes 3145732
  123.7 8.6 %copy-start.3 = (bf16[1,256,2048]{2,1,0:T(8,128)(2,1)S(1)}, bf16[1,256,2048]{2,1,0:T(8,128)(2,1)}, u32[]{:S(2)}) copy-start(bf16[1,256,2048]{2,1,0:T(8,128)(2,1)} %param.28) | copy-start | bytes 3145732
  123.7 31.9 %all-to-all-start = ((bf16[64,8,2048]{2,1,0:T(8,128)(2,1)}), bf16[64,8,2048]{2,1,0:T(8,128)(2,1)}, u32[]{:S(2)}, u32[]{:S(2)}) async-start(bf16[64,8,2048]{2,1,0:T(8,128)(2,1)} %bitcast.16), calls=%async_computation | async-start | bytes 4194304 | tf_op jit(solution)/shard_map/all_to_all | solution.py:396
  131.7 2.7 %collective-permute-start.16 = (bf16[2048,256]{1,0:T(8,128)(2,1)S(1)}, bf16[2048,256]{1,0:T(8,128)(2,1)S(1)}, u32[]{:S(2)}, u32[]{:S(2)}) collective-permute-start(bf16[2048,256]{1,0:T(8,128)(2,1)S(1)} %bitcast.32), channel_id=1, source_target_pairs={{0,1},{1,0},{2,3},{3,2},{4,5},{5,4},{6,7},{7,6},{8,9},{9,8},{10,11... | collective-permute-start | bytes 3145736 | tf_op jit(solution)/shard_map/ppermute | solution.py:400
  131.8 4.1 %collective-permute-start.17 = (bf16[2048,256]{1,0:T(8,128)(2,1)S(1)}, bf16[2048,256]{1,0:T(8,128)(2,1)S(1)}, u32[]{:S(2)}, u32[]{:S(2)}) collective-permute-start(bf16[2048,256]{1,0:T(8,128)(2,1)S(1)} %bitcast.34), channel_id=1, source_target_pairs={{0,1},{1,0},{2,3},{3,2},{4,5},{5,4},{6,7},{7,6},{8,9},{9,8},{10,11... | collective-permute-start | bytes 3145736 | tf_op jit(solution)/shard_map/ppermute | solution.py:400
  132.3 5.3 %collective-permute-start.18 = (bf16[256,2048]{1,0:T(8,128)(2,1)S(1)}, bf16[256,2048]{1,0:T(8,128)(2,1)}, u32[]{:S(2)}, u32[]{:S(2)}) collective-permute-start(bf16[256,2048]{1,0:T(8,128)(2,1)S(1)} %bitcast.36), channel_id=1, source_target_pairs={{0,1},{1,0},{2,3},{3,2},{4,5},{5,4},{6,7},{7,6},{8,9},{9,8},{10,11... | collective-permute-start | bytes 3145736 | tf_op jit(solution)/shard_map/ppermute | solution.py:400
  134.4 1.0 copy-start.4
  135.9 1.0 copy-start.6
  155.6 1.2 copy-start.5
  156.8 1.2 copy-start.7
  164.7 5.0 %copy-start.17 = (f32[128,2]{0,1:T(2,128)S(1)}, f32[128,2]{0,1:T(2,128)}, u32[]{:S(2)}) copy-start(f32[128,2]{0,1:T(2,128)} %param.25) | copy-start | bytes 3076
  164.7 32.1 %copy-start.9 = (bf16[128,2048]{1,0:T(8,128)(2,1)S(1)}, bf16[128,2048]{1,0:T(8,128)(2,1)}, u32[]{:S(2)}) copy-start(bf16[128,2048]{1,0:T(8,128)(2,1)} %copy-done.8) | copy-start | bytes 1572868
  164.7 32.1 %all-to-all-start.1 = ((bf16[64,8,2048]{2,1,0:T(8,128)(2,1)}), bf16[64,8,2048]{2,1,0:T(8,128)(2,1)S(1)}, u32[]{:S(2)}, u32[]{:S(2)}) async-start(bf16[64,8,2048]{2,1,0:T(8,128)(2,1)} %bitcast.40), calls=%async_computation.1 | async-start | bytes 4194304 | tf_op jit(solution)/shard_map/all_to_all | solution.py:402

commit v2 on v1

v2 whole, which is shorter than its diff:
```python
import functools
import jax
import jax.numpy as jnp
import numpy as np
from jax import lax
from jax.experimental import pallas as pl
from jax.experimental.pallas import tpu as pltpu
from jax.sharding import PartitionSpec as P

QK_NOPE = 128
QK_ROPE = 64
V_DIM = 128
LATENT = 256
SEGMENT = 64
EPSILON = 1e-06
ROPE_BASE = 10000.0
NEG_LARGE = -1e30

N_SP = 64
N_TP = 2
HEADS_HERE = 4
ROWS = 128
SHARD = 160
UNIT = 4
KEYS = UNIT * ROWS
QROWS = HEADS_HERE * ROWS
CAP = 8
AXES = ("sp", "tp")
STEP = {"x": 1, "y": 4, "z": 16}
Z_FIRST = {(0, 0): (3, 0), (1, 0): (2, 0), (0, 1): (1, 0), (1, 1): (0, 0), (2, 1): (1, 1), (3, 1): (0, 1), (2, 0): (3, 1), (3, 0): (2, 1)}
Z_SECOND = {(0, 1): (2, 0), (1, 1): (3, 0), (2, 0): (0, 1), (3, 0): (1, 1)}
ORDER = (("y", "x"), ("x", "y"))
SHIFTS = (0, 1, -1, 2)
SCALE2 = float((QK_NOPE + QK_ROPE) ** (-0.5) * np.log2(np.e))
PLANE = 16
COLS = 12
GROUPS = 4
CHUNK = 64
MESSAGE = HEADS_HERE * V_DIM + 128


def moved(s, dim, by):
    step = STEP[dim]
    c = (s // step) % 4
    return s + step * ((c + by) % 4 - c)


def shift_pairs(phase, by):
    return [
        (s * N_TP + t, moved(s, ORDER[t][phase], by) * N_TP + t)
        for s in range(N_SP)
        for t in range(N_TP)
    ]


def plane_pairs(table):
    return [
        ((from_z * PLANE + r) * N_TP + from_core, (z * PLANE + r) * N_TP + core)
        for (z, core), (from_z, from_core) in table.items()
        for r in range(PLANE)
    ]


def shard_first(s, t, k3, k2, kz):
    s = moved(s, ORDER[t][1], -SHIFTS[k3])
    s = moved(s, ORDER[t][0], -SHIFTS[k2])
    z, r = divmod(s, PLANE)
    source = (z, t)
    if kz == 1:
        source = Z_FIRST[source]
    elif source in Z_SECOND:
        source = Z_SECOND[source]
    return 4 * (source[0] * PLANE + r) + 2 * source[1]


@functools.lru_cache(None)
def work_table():
    lists = []
    for s in range(N_SP):
        for t in range(N_TP):
            firsts = [
                shard_first(s, core, k3, k2, kz)
                for core in (t, 1 - t)
                for k3 in range(4)
                for k2 in range(4)
                for kz in range(2)
            ]
            rows = []
            for group in range(GROUPS):
                block = s if group < 2 else N_SP - 1 - s
                base = 4 * block + 2 * (group % 2)
                needed = [n for n in range(len(firsts)) if firsts[n] <= base + 1]
                for at in range(0, len(needed), UNIT):
                    part = needed[at : at + UNIT]
                    segs = [firsts[n] for n in part]
                    masked = int(len(part) < UNIT or any(f + 1 > base for f in segs))
                    segs += [1 << 20] * (UNIT - len(part))
                    part = part + [part[-1]] * (UNIT - len(part))
                    rows.append([group, masked, base, t] + part + segs)
            lists.append(rows)
    count = max(len(rows) for rows in lists)
    count += 1 - count % 2
    table = []
    for rows in lists:
        idle = [rows[-1][:1] + [1] + rows[-1][2:8] + [1 << 20] * UNIT]
        table.append(rows + idle * (count + 1 - len(rows)))
    return count, np.array(table, np.int32).reshape(len(lists), -1)


def attention_body(steps, table, qn_ref, q4_ref, key_up_ref, value_up_ref, *rest):
    parts = rest[:8]
    out_ref = rest[8]
    keys, qabs, m_ref, l_ref, acc_ref, s0, s1, p_ref, shrink_ref, sems = rest[9:]
    part_rows = parts[0].shape[0]
    copies = []
    for n in range(8):
        copy = pltpu.make_async_copy(parts[n], keys.at[pl.ds(n * part_rows, part_rows)], sems.at[n])
        copy.start()
        copies.append(copy)
    nt = (((1,), (1,)), ((), ()))
    for g in range(GROUPS):
        for h in range(HEADS_HERE):
            cols = pl.ds(h * QK_NOPE, QK_NOPE)
            qabs[g, pl.ds(h * ROWS, ROWS), :] = lax.dot_general(
                qn_ref[g, :, cols], key_up_ref[:, cols], nt, preferred_element_type=jnp.float32
            ).astype(jnp.bfloat16)
    m_ref[...] = jnp.full(m_ref.shape, NEG_LARGE, jnp.float32)
    l_ref[...] = jnp.zeros(l_ref.shape, jnp.float32)
    acc_ref[...] = jnp.zeros(acc_ref.shape, jnp.float32)
    for copy in copies:
        copy.wait()

    def field(u, n):
        return table[u * COLS + n]

    def latent_tile(u, half):
        return jnp.concatenate(
            [
                keys[pl.ds(pl.multiple_of(field(u, 4 + j) * SHARD + half * SEGMENT, 32), SEGMENT), :]
                for j in range(UNIT)
            ],
            axis=0,
        )

    def scores(u, s_ref):
        g = field(u, 0)
        rot = jnp.concatenate(
            [
                keys[pl.ds(pl.multiple_of(field(u, 4 + j) * SHARD + ROWS, 32), 32), pl.ds(h * 128, 128)]
                for j in range(UNIT)
                for h in range(2)
            ],
            axis=0,
        )
        q = qabs[g]
        for half in range(2):
            s_ref[:, pl.ds(half * 256, 256)] = lax.dot_general(
                q, latent_tile(u, half), nt, preferred_element_type=jnp.float32
            ) + lax.dot_general(q4_ref[g, half], rot, nt, preferred_element_type=jnp.float32)

    def fix(u, s_ref):
        @pl.when(field(u, 1) == 1)
        def _():
            lane = lax.broadcasted_iota(jnp.int32, (1, KEYS), 1)
            which = (lane % 256) // SEGMENT
            seg = jnp.full((1, KEYS), field(u, 8), jnp.int32)
            for j in range(1, UNIT):
                seg = jnp.where(which == j, field(u, 8 + j), seg)
            seg = seg + lane // 256
            base = field(u, 2)
            for at in range(0, QROWS, SEGMENT):
                rows = pl.ds(at, SEGMENT)
                limit = base + (at % ROWS) // SEGMENT
                s_ref[rows, :] = jnp.where(seg <= limit, s_ref[rows, :], NEG_LARGE)

    def absorb(u, s_ref):
        g = field(u, 0)
        for at in range(0, QROWS, CHUNK):
            rows = pl.ds(at, CHUNK)
            s = s_ref[rows, :]
            before = m_ref[g, rows, :]
            top = s[:, :128]
            for k in range(1, KEYS // 128):
                top = jnp.maximum(top, s[:, k * 128 : (k + 1) * 128])
            after = jnp.maximum(before, jnp.max(top, axis=1, keepdims=True))
            m_ref[g, rows, :] = after
            shrink = jnp.exp2((before - after) * SCALE2)
            shrink_ref[rows, :] = shrink
            after = after * SCALE2
            partial = l_ref[g, rows, :] * shrink
            for k in range(KEYS // 128):
                p = jnp.exp2(s[:, k * 128 : (k + 1) * 128] * SCALE2 - after)
                partial = partial + p
                p_ref[rows, pl.ds(k * 128, 128)] = p.astype(jnp.bfloat16)
            l_ref[g, rows, :] = partial
        values = jnp.concatenate([latent_tile(u, 0), latent_tile(u, 1)], axis=0)
        product = jnp.dot(p_ref[...], values, preferred_element_type=jnp.float32)
        for k in range(LATENT // 128):
            cols = pl.ds(k * 128, 128)
            acc_ref[g, :, cols] = acc_ref[g, :, cols] * shrink_ref[...] + product[:, k * 128 : (k + 1) * 128]

    scores(0, s0)

    def pair(k, carry):
        u = k * 2
        fix(u, s0)
        scores(u + 1, s1)
        absorb(u, s0)
        fix(u + 1, s1)
        scores(u + 2, s0)
        absorb(u + 1, s1)
        return carry

    lax.fori_loop(0, steps // 2, pair, 0)
    fix(steps - 1, s0)
    absorb(steps - 1, s0)
    core = field(0, 3)
    lane = lax.broadcasted_iota(jnp.int32, (ROWS, 128), 1)
    for g in range(GROUPS):
        place = 2 * (g // 2) + jnp.where(core == g % 2, 0, 1)
        total = jnp.sum(l_ref[g], axis=1, keepdims=True)
        total = jnp.where(total > 0.0, total, 1.0)
        mean = (acc_ref[g] / total).astype(jnp.bfloat16)
        size = m_ref[g] * SCALE2 + jnp.log2(total)
        notes = jnp.zeros((ROWS, 128), jnp.bfloat16)
        for h in range(HEADS_HERE):
            cols = pl.ds(h * V_DIM, V_DIM)
            rows = slice(h * ROWS, (h + 1) * ROWS)
            out_ref[place, :, cols] = jnp.dot(
                mean[rows], value_up_ref[:, cols], preferred_element_type=jnp.float32
            ).astype(jnp.bfloat16)
            left = size[rows]
            for n in range(3):
                term = left.astype(jnp.bfloat16)
                notes = jnp.where(lane == n * HEADS_HERE + h, term, notes)
                left = left - term.astype(jnp.float32)
        out_ref[place, :, pl.ds(HEADS_HERE * V_DIM, 128)] = notes


def attention(table, qn, q4, key_up, value_up, parts):
    vmem = pl.BlockSpec(memory_space=pltpu.VMEM)
    steps = work_table()[0]
    return pl.pallas_call(
        functools.partial(attention_body, steps),
        out_shape=jax.ShapeDtypeStruct((4, ROWS, MESSAGE), jnp.bfloat16),
        in_specs=[pl.BlockSpec(memory_space=pltpu.SMEM)] + [vmem] * 4 + [pl.BlockSpec(memory_space=pl.ANY)] * 8,
        out_specs=vmem,
        scratch_shapes=[
            pltpu.VMEM((64 * SHARD, LATENT), jnp.bfloat16),
            pltpu.VMEM((GROUPS, QROWS, LATENT), jnp.bfloat16),
            pltpu.VMEM((GROUPS, QROWS, 128), jnp.float32),
            pltpu.VMEM((GROUPS, QROWS, 128), jnp.float32),
            pltpu.VMEM((GROUPS, QROWS, LATENT), jnp.float32),
            pltpu.VMEM((QROWS, KEYS), jnp.float32),
            pltpu.VMEM((QROWS, KEYS), jnp.float32),
            pltpu.VMEM((QROWS, KEYS), jnp.bfloat16),
            pltpu.VMEM((QROWS, 128), jnp.float32),
            pltpu.SemaphoreType.DMA((8,)),
        ],
        compiler_params=pltpu.CompilerParams(vmem_limit_bytes=24 * 2**20),
        name="attention",
    )(table, qn, q4, key_up, value_up, *parts)


def merged(one, two):
    width = HEADS_HERE * V_DIM
    outs = []
    for h in range(HEADS_HERE):
        sizes = []
        for part in (one, two):
            notes = part[:, width : width + 128].astype(jnp.float32)
            sizes.append(
                notes[:, h : h + 1] + notes[:, HEADS_HERE + h : HEADS_HERE + h + 1]
                + notes[:, 2 * HEADS_HERE + h : 2 * HEADS_HERE + h + 1]
            )
        most = jnp.maximum(sizes[0], sizes[1])
        first, second = (jnp.exp2(size - most) for size in sizes)
        cols = slice(h * V_DIM, (h + 1) * V_DIM)
        value = first * one[:, cols].astype(jnp.float32) + second * two[:, cols].astype(jnp.float32)
        outs.append((value / (first + second)).astype(jnp.bfloat16))
    return jnp.concatenate(outs, axis=1)


def project_body(core, local_part, mirror_same, swapped, mirror_cross, out_proj, residual, gain, slots, hidden_ref, outgoing_ref):
    half = HEADS_HERE * V_DIM
    mine = merged(local_part[...], mirror_same[...])
    theirs = merged(swapped[...], mirror_cross[...])
    at = pl.multiple_of(core[0] * half, half)
    other = pl.multiple_of((1 - core[0]) * half, half)
    projected = jnp.dot(mine, out_proj[pl.ds(at, half), :], preferred_element_type=jnp.float32) + jnp.dot(
        theirs, out_proj[pl.ds(other, half), :], preferred_element_type=jnp.float32
    )
    hidden = (residual[...].astype(jnp.float32) + projected).astype(jnp.bfloat16)
    hidden_ref[...] = hidden
    wide = hidden.astype(jnp.float32)
    normed = wide * lax.rsqrt(jnp.mean(wide * wide, axis=-1, keepdims=True) + EPSILON)
    normed = (normed * gain[...]).astype(jnp.bfloat16)
    slot = lax.broadcasted_iota(jnp.int32, (outgoing_ref.shape[0], hidden.shape[0]), 0)
    pick = (slot == slots[0:1, :]) | (slot == slots[1:2, :])
    pick = jnp.where(pick, 1.0, 0.0).astype(jnp.bfloat16)
    outgoing_ref[...] = jnp.dot(pick, normed, preferred_element_type=jnp.float32).astype(jnp.bfloat16)


def project(core, messages, out_proj, residual, gain, slots):
    width = residual.shape[1]
    vmem = pl.BlockSpec(memory_space=pltpu.VMEM)
    return pl.pallas_call(
        project_body,
        out_shape=(
            jax.ShapeDtypeStruct((ROWS, width), jnp.bfloat16),
            jax.ShapeDtypeStruct((N_SP * CAP, width), jnp.bfloat16),
        ),
        in_specs=[pl.BlockSpec(memory_space=pltpu.SMEM)] + [vmem] * 8,
        out_specs=(vmem, vmem),
        compiler_params=pltpu.CompilerParams(vmem_limit_bytes=20 * 2**20),
        name="project",
    )(core, *messages, out_proj, residual, gain, slots)


def experts_body(rows, gate_a, up_a, down_a, gate_b, up_b, down_b, out_ref):
    x = rows[...]
    halves = []
    for gate, up, down in ((gate_a, up_a, down_a), (gate_b, up_b, down_b)):
        gated = jnp.dot(x, gate[...], preferred_element_type=jnp.float32)
        raised = jnp.dot(x, up[...], preferred_element_type=jnp.float32)
        active = (gated / (1.0 + jnp.exp(-gated)) * raised).astype(jnp.bfloat16)
        halves.append(jnp.dot(active, down[...], preferred_element_type=jnp.float32).astype(jnp.bfloat16))
    out_ref[...] = (halves[0].astype(jnp.float32) + halves[1].astype(jnp.float32)).astype(jnp.bfloat16)


def experts(rows, own, other):
    count, width = rows.shape
    block = 256
    whole = lambda a: pl.BlockSpec(a.shape, lambda n: (0, 0))
    return pl.pallas_call(
        experts_body,
        grid=(count // block,),
        out_shape=jax.ShapeDtypeStruct((count, width), jnp.bfloat16),
        in_specs=[pl.BlockSpec((block, width), lambda n: (n, 0))] + [whole(a) for a in (*own, *other)],
        out_specs=pl.BlockSpec((block, width), lambda n: (n, 0)),
        compiler_params=pltpu.CompilerParams(
            dimension_semantics=("arbitrary",), vmem_limit_bytes=24 * 2**20
        ),
        name="experts",
    )(rows, *own, *other)


def combine_body(back, hidden, slots, weights, out_ref):
    slot = lax.broadcasted_iota(jnp.int32, (hidden.shape[0], back.shape[0]), 1)
    pick = jnp.where(slot == slots[:, 0:1], weights[:, 0:1], 0.0) + jnp.where(
        slot == slots[:, 1:2], weights[:, 1:2], 0.0
    )
    high = pick.astype(jnp.bfloat16)
    low = (pick - high.astype(jnp.float32)).astype(jnp.bfloat16)
    rows = back[...]
    mixed = jnp.dot(high, rows, preferred_element_type=jnp.float32) + jnp.dot(
        low, rows, preferred_element_type=jnp.float32
    )
    out_ref[...] = (hidden[...].astype(jnp.float32) + mixed).astype(jnp.bfloat16)


def combine(back, hidden, slots, weights):
    vmem = pl.BlockSpec(memory_space=pltpu.VMEM)
    return pl.pallas_call(
        combine_body,
        out_shape=jax.ShapeDtypeStruct(hidden.shape, jnp.bfloat16),
        in_specs=[vmem] * 4,
        out_specs=vmem,
        compiler_params=pltpu.CompilerParams(vmem_limit_bytes=16 * 2**20),
        name="combine",
    )(back, hidden, slots, weights)


def rotary(values, positions):
    half_width = values.shape[-1] // 2
    inverse = ROPE_BASE ** (-2.0 * jnp.arange(half_width, dtype=jnp.float32) / values.shape[-1])
    angles = positions.astype(jnp.float32)[:, None] * inverse[None, :]
    cosine = jnp.cos(angles)
    sine_part = jnp.sin(angles)
    if values.ndim == 3:
        cosine = cosine[:, None, :]
        sine_part = sine_part[:, None, :]
    first_half = values[..., :half_width]
    second = values[..., half_width:]
    return jnp.concatenate(
        [first_half * cosine - second * sine_part, second * cosine + first_half * sine_part],
        axis=-1,
    )


def local(
    residual,
    query_nope,
    query_rope,
    latent,
    key_rope,
    key_up,
    value_up,
    out_proj,
    norm_gain,
    routes,
    route_weight,
    w_gate,
    w_up,
    w_down,
):
    tp_index = lax.axis_index("tp")
    sp_index = lax.axis_index("sp")
    tok_dev = query_nope.shape[0]
    query_first = sp_index * tok_dev
    swap = [(0, 1), (1, 0)]

    key_pos = query_first + tp_index * ROWS + jnp.arange(ROWS, dtype=jnp.int32)
    key_rot = rotary(key_rope.astype(jnp.float32), key_pos).astype(jnp.bfloat16)
    packed = jnp.concatenate([key_rot[0:32], key_rot[64:96], key_rot[32:64], key_rot[96:128]], axis=1)
    shard = jnp.concatenate([latent, packed], axis=0)
    near = lax.ppermute(shard, AXES, plane_pairs(Z_FIRST))
    far = lax.ppermute(shard, AXES, plane_pairs(Z_SECOND))
    main = (tp_index == 0) == (sp_index < 2 * PLANE)
    both = jnp.concatenate([jnp.where(main, shard, far), near], axis=0)

    query_pos = query_first + jnp.arange(tok_dev, dtype=jnp.int32)
    query_rot = rotary(
        query_rope.astype(jnp.float32).reshape(tok_dev, HEADS_HERE, QK_ROPE), query_pos
    ).astype(jnp.bfloat16)
    queries = jnp.concatenate([query_nope, query_rot.reshape(tok_dev, HEADS_HERE * QK_ROPE)], axis=1)
    mirror = [
        (s * N_TP + t, (N_SP - 1 - s) * N_TP + t) for s in range(N_SP) for t in range(N_TP)
    ]
    crossing = [
        (s * N_TP + t, (N_SP - 1 - s) * N_TP + 1 - t) for s in range(N_SP) for t in range(N_TP)
    ]
    received = lax.ppermute(queries, AXES, mirror)

    got = [both] + [lax.ppermute(both, AXES, shift_pairs(0, by)) for by in SHIFTS[1:]]
    both = jnp.concatenate(got, axis=0)
    both, received = lax.optimization_barrier((both, received))
    own_parts = [both] + [lax.ppermute(both, AXES, shift_pairs(1, by)) for by in SHIFTS[1:]]
    other_parts = [lax.ppermute(part, "tp", swap) for part in own_parts]

    sets = jnp.concatenate([queries, received], axis=0).reshape(GROUPS, ROWS, -1)
    qn = sets[:, :, : HEADS_HERE * QK_NOPE]
    rot = sets[:, :, HEADS_HERE * QK_NOPE :].reshape(GROUPS, ROWS, HEADS_HERE, QK_ROPE)
    rot = jnp.swapaxes(rot, 1, 2).reshape(GROUPS, QROWS, QK_ROPE)
    none = jnp.zeros_like(rot)
    q4 = jnp.stack(
        [jnp.concatenate([rot, none], axis=-1), jnp.concatenate([none, rot], axis=-1)], axis=1
    )
    table = lax.dynamic_index_in_dim(
        jnp.asarray(work_table()[1]), sp_index * N_TP + tp_index, 0, keepdims=False
    )
    attn = attention(table, qn, q4, key_up, value_up, own_parts + other_parts)
    mirror_same = lax.ppermute(attn[2], AXES, mirror)
    mirror_cross = lax.ppermute(attn[3], AXES, crossing)
    swapped = lax.ppermute(attn[1], "tp", swap)
    messages = (attn[0], mirror_same, swapped, mirror_cross)

    flat = routes.reshape(-1)
    order = jnp.arange(flat.shape[0], dtype=jnp.int32)
    earlier = (flat[:, None] == flat[None, :]) & (order[None, :] < order[:, None])
    rank = jnp.sum(earlier.astype(jnp.int32), axis=1)
    slots = (flat * CAP + rank).reshape(routes.shape)

    hidden, outgoing = project(
        tp_index.reshape(1).astype(jnp.int32), messages, out_proj, residual, norm_gain[None, :], slots.T
    )
    width = residual.shape[1]
    arrived = lax.all_to_all(
        outgoing.reshape(N_SP, CAP, width), "sp", split_axis=0, concat_axis=0, tiled=True
    ).reshape(N_SP * CAP, width)
    own = (w_gate[0], w_up[0], w_down[0])
    other = tuple(lax.ppermute(w, "tp", swap) for w in own)
    produced = experts(arrived, own, other)
    back = lax.all_to_all(
        produced.reshape(N_SP, CAP, width), "sp", split_axis=0, concat_axis=0, tiled=True
    ).reshape(N_SP * CAP, width)
    return combine(back, hidden, slots, route_weight)


def solution(mesh):
    return jax.shard_map(
        local,
        mesh=mesh,
        in_specs=(
            P(("sp", "tp"), None),
            P("sp", "tp"),
            P("sp", "tp"),
            P(("sp", "tp"), None),
            P(("sp", "tp"), None),
            P(None, "tp"),
            P(None, "tp"),
            P(),
            P(),
            P(("sp", "tp"), None),
            P(("sp", "tp"), None),
            P("sp", None, "tp"),
            P("sp", None, "tp"),
            P("sp", "tp", None),
        ),
        out_specs=P(("sp", "tp"), None),
        check_vma=False,
    )
```

time: 199 us -> 202 us (1.015)
  starting transfers between devices: 53.7 us -> 41.9 us
  local copies, waits for them, and re-layouts: 12 us -> 23.7 us
  waiting for transfers between devices: 88.1 us -> 91.2 us
  Pallas kernels: 42 us -> 39.8 us
    ppermute x4, starting transfers between devices: 12.8 us -> 3.82 us  [local(): other_parts = [lax.ppermute(part, 'tp', swap) for part in own_parts]]
    unnamed x45 -> x49, local copies, waits for them, and re-layouts: 10.2 us -> 17.9 us
    all_to_all x1, waiting for transfers between devices: 18.1 us -> 23.3 us  [local(): lax.all_to_all(outgoing.reshape(N_SP, CAP, width), 'sp', split_axis=0, co...]
    ppermute x12, waiting for transfers between devices: 39.8 us -> 36.4 us  [the longest x3 13.3 us: local(): lax.ppermute(both, AXES, shift_pairs(1, by))]
    all_to_all x1, starting transfers between devices: 7.96 us -> 5.23 us  [local(): lax.all_to_all(outgoing.reshape(N_SP, CAP, width), 'sp', split_axis=0, co...]
    pallas_call x1, Pallas kernels: 6.61 us -> 4.08 us  [experts(): pl.pallas_call(experts_body, grid=(count // block,), out_shape=jax.ShapeD...]
  transfers between devices with their start and end apart: 21 -> 21, of which waited for: 14 -> 12; matrix products, arithmetic and copies ran while one was open for 2% -> 4% of each run, Pallas kernels for 0% -> 0%
where the time goes in v2:
time: 202 us; the launch traced here: 200 us
  waiting for transfers between devices  91.2 us (45%)
  starting transfers between devices  41.9 us (21%)
  Pallas kernels  39.8 us (20%)
  local copies, waits for them, and re-layouts  23.7 us (12%)
  other arithmetic  3.03 us (2%)
    pallas_call x1, Pallas kernels, attention(): pl.pallas_call(functools.partial(attention_body, steps), out_shape=jax.Sh...  32 us
    all_to_all x1, waiting for transfers between devices, local(): lax.all_to_all(produced.reshape(N_SP, CAP, width), 'sp', split_axis=0, co...  28.3 us
    all_to_all x1, waiting for transfers between devices, local(): lax.all_to_all(outgoing.reshape(N_SP, CAP, width), 'sp', split_axis=0, co...  23.3 us
    unnamed x49, local copies, waits for them, and re-layouts  17.9 us
    ppermute x3, waiting for transfers between devices, local(): lax.ppermute(both, AXES, shift_pairs(1, by))  13.3 us
    ppermute x3, waiting for transfers between devices, local(): lax.ppermute(both, AXES, shift_pairs(0, by))  10 us
    ppermute x1, starting transfers between devices, local(): far = lax.ppermute(shard, AXES, plane_pairs(Z_SECOND))  6.87 us
    ppermute x1, waiting for transfers between devices, local(): mirror_cross = lax.ppermute(attn[3], AXES, crossing)  5.79 us
  transfers between devices with their start and end apart: 21, of which 12 were waited for; matrix products, arithmetic and copies ran while one was open for 4% of the time, Pallas kernels for 0%

profile of v2, /device:TPU:1, one launch (start us, length us, event | category | flops | bytes accessed | tf_op | source)
XLA Modules:
  0.0 200.0 jit_solution(9664694935852173615)
XLA Ops:
  0.0 0.9 copy.47
  1.3 0.9 fusion.12
  2.3 6.9 %collective-permute-start = (bf16[160,256]{1,0:T(8,128)(2,1)S(1)}, bf16[160,256]{1,0:T(8,128)(2,1)S(1)}, u32[]{:S(2)}, u32[]{:S(2)}) collective-permute-start(bf16[160,256]{1,0:T(8,128)(2,1)S(1)} %fusion.12), channel_id=1, source_target_pairs={{64,1},{66,3},{68,5},{70,7},{72,9},{74,11},{76,13},{78,15},{80,17}... | collective-permute-start | bytes 245768 | tf_op jit(solution)/shard_map/ppermute | solution.py:418
  9.5 1.0 copy.45
  11.3 1.7 collective-permute-done.1
  13.1 1.3 collective-permute-start.2
  14.4 5.2 %collective-permute-start.5 = (bf16[256,768]{1,0:T(8,128)(2,1)S(1)}, bf16[256,768]{1,0:T(8,128)(2,1)}, u32[]{:S(2)}, u32[]{:S(2)}) collective-permute-start(bf16[256,768]{1,0:T(8,128)(2,1)S(1)} %pad_maximum_fusion.2), channel_id=1, source_target_pairs={{0,126},{1,127},{2,124},{3,125},{4,122},{5,123},{6,120},{7,121},{8... | collective-permute-start | bytes 1179656 | tf_op jit(solution)/shard_map/ppermute | solution.py:433
  19.6 1.2 collective-permute-start.3
  20.8 1.2 collective-permute-start.4
  22.1 10.0 %collective-permute-done.3 = bf16[320,256]{1,0:T(8,128)(2,1)S(1)} collective-permute-done((bf16[320,256]{1,0:T(8,128)(2,1)S(1)}, bf16[320,256]{1,0:T(8,128)(2,1)S(1)}, u32[]{:S(2)}, u32[]{:S(2)}) %collective-permute-start.3) | collective-permute-done | bytes 163872 | tf_op jit(solution)/shard_map/ppermute | solution.py:435
  32.2 1.2 collective-permute-done.5
  33.7 2.4 %collective-permute-start.7 = (bf16[1280,256]{1,0:T(8,128)(2,1)S(1)}, bf16[1280,256]{1,0:T(8,128)(2,1)S(1)}, u32[]{:S(2)}, u32[]{:S(2)}) collective-permute-start(bf16[1280,256]{1,0:T(8,128)(2,1)S(1)} %constant_dynamic-update-slice_fusion.rest_0_), channel_id=1, source_target_pairs={{0,6},{1,25},{2,0},{3,27},{4,2},{5,29},{6,4},{7,31},{8,14},{9,1},{... | collective-permute-start | bytes 1966088 | tf_op jit(solution)/shard_map/ppermute | solution.py:438
  36.6 1.5 collective-permute-start.9
  38.1 13.3 %collective-permute-done.6.rest_1_ = bf16[1280,256]{1,0:T(8,128)(2,1)S(1)} collective-permute-done((bf16[1280,256]{1,0:T(8,128)(2,1)S(1)}, bf16[1280,256]{1,0:T(8,128)(2,1)S(1)}, u32[]{:S(2)}, u32[]{:S(2)}) %collective-permute-start.6) | collective-permute-done | bytes 655392 | tf_op jit(solution)/shard_map/ppermute | solution.py:438
  51.4 1.4 collective-permute-start.11
  52.8 0.9 collective-permute-start.12
  54.3 0.7 constant_dynamic-slice_fusion
  55.0 1.0 pad_maximum_fusion.1
  56.1 0.8 copy.49
  57.0 2.0 copy.50
  59.0 1.5 pad_bitcast_fusion.1
  60.7 32.0 %attention.1 = bf16[4,128,640]{2,1,0:T(8,128)(2,1)S(1)} custom-call(s32[432]{0:T(512)S(1)} %bitcast.45, bf16[4,128,512]{2,1,0:T(8,128)(2,1)S(1)} %slice.66.qn_ref, bf16[4,2,512,128]{3,2,1,0:T(8,128)(2,1)S(1)} %pad_maximum_fusion.q4_ref, bf16[256,512]{1,0:T(8,128)(2,1)S(1)} %copy-done.15, bf16[256,512]{1,0:T(8,128)(2,1)S(1)} %copy-done.16, ...), custom_call_target="tpu_custom_call" | custom-call | tf_op jit(solution)/shard_map/attention/pallas_call | solution.py:243
  92.7 5.0 %collective-permute-start.13 = (bf16[128,640]{1,0:T(8,128)(2,1)S(1)}, bf16[128,640]{1,0:T(8,128)(2,1)S(1)}, u32[]{:S(2)}, u32[]{:S(2)}) collective-permute-start(bf16[128,640]{1,0:T(8,128)(2,1)S(1)} %get-tuple-element.17), channel_id=1, source_target_pairs={{0,126},{1,127},{2,124},{3,125},{4,122},{5,123},{6,120},{7,121},{8... | collective-permute-start | bytes 491528 | tf_op jit(solution)/shard_map/ppermute | solution.py:453
  97.8 0.8 collective-permute-start.14
  98.6 1.5 collective-permute-start.15
  100.3 3.7 %collective-permute-done.13.mirror_same = bf16[128,640]{1,0:T(8,128)(2,1)S(1)} collective-permute-done((bf16[128,640]{1,0:T(8,128)(2,1)S(1)}, bf16[128,640]{1,0:T(8,128)(2,1)S(1)}, u32[]{:S(2)}, u32[]{:S(2)}) %collective-permute-start.13) | collective-permute-done | bytes 163872 | tf_op jit(solution)/shard_map/ppermute | solution.py:453
  104.0 5.8 %collective-permute-done.15.mirror_cross = bf16[128,640]{1,0:T(8,128)(2,1)S(1)} collective-permute-done((bf16[128,640]{1,0:T(8,128)(2,1)S(1)}, bf16[128,640]{1,0:T(8,128)(2,1)S(1)}, u32[]{:S(2)}, u32[]{:S(2)}) %collective-permute-start.15) | collective-permute-done | bytes 163872 | tf_op jit(solution)/shard_map/ppermute | solution.py:454
  109.8 2.2 %copy-done.1 = bf16[1024,2048]{1,0:T(8,128)(2,1)S(1)} copy-done((bf16[1024,2048]{1,0:T(8,128)(2,1)S(1)}, bf16[1024,2048]{1,0:T(8,128)(2,1)}, u32[]{:S(2)}) %copy-start.1) | copy-done | bytes 4194328
  112.0 1.0 copy-done.12
  113.0 2.1 %project.1 = (bf16[128,2048]{1,0:T(8,128)(2,1)S(1)}, bf16[512,2048]{1,0:T(8,128)(2,1)S(1)}) custom-call(s32[1]{0:T(128)} %bitcast.core, bf16[128,640]{1,0:T(8,128)(2,1)S(1)} %get-tuple-element.18.local_part, bf16[128,640]{1,0:T(8,128)(2,1)S(1)} %collective-permute-done.13.mirror_same, bf16[128,640]{1,0:T(8,128)(2,1)S(1)} %collective-permute-done.14.swapped, ...), custom_call_target="tpu_custom_call" | custom-call | tf_op jit(solution)/shard_map/project/pallas_call | solution.py:307
  115.1 1.3 copy-done.2
  116.5 0.8 copy-done.13
  117.2 5.2 %all-to-all-start = ((bf16[64,8,2048]{2,1,0:T(8,128)(2,1)}), bf16[64,8,2048]{2,1,0:T(8,128)(2,1)S(1)}, u32[]{:S(2)}, u32[]{:S(2)}) async-start(bf16[64,8,2048]{2,1,0:T(8,128)(2,1)} %bitcast.36), calls=%async_computation | async-start | bytes 4194304 | tf_op jit(solution)/shard_map/all_to_all | solution.py:468
  123.2 2.1 %collective-permute-done.16.gate_b = bf16[2048,256]{1,0:T(8,128)(2,1)S(1)} collective-permute-done((bf16[2048,256]{1,0:T(8,128)(2,1)S(1)}, bf16[2048,256]{1,0:T(8,128)(2,1)S(1)}, u32[]{:S(2)}, u32[]{:S(2)}) %collective-permute-start.16) | collective-permute-done | bytes 1048608 | tf_op jit(solution)/shard_map/ppermute | solution.py:472
  125.2 1.0 copy-done.6
  126.7 1.0 copy-done.8
  128.2 1.0 copy-done.10
  129.2 23.3 %all-to-all-done = bf16[64,8,2048]{2,1,0:T(8,128)(2,1)S(1)} async-done(((bf16[64,8,2048]{2,1,0:T(8,128)(2,1)}), bf16[64,8,2048]{2,1,0:T(8,128)(2,1)S(1)}, u32[]{:S(2)}, u32[]{:S(2)}) %all-to-all-start) | async-done | bytes 2097184 | tf_op jit(solution)/shard_map/all_to_all | solution.py:468
  152.6 1.2 copy-done.4
  153.8 1.2 copy-done.5
  155.0 1.2 copy-done.7
  156.3 1.2 copy-done.9
  157.5 1.2 copy-done.11
  158.7 4.1 %experts.1 = bf16[512,2048]{1,0:T(8,128)(2,1)S(1)} custom-call(bf16[512,2048]{1,0:T(8,128)(2,1)S(1)} %bitcast.33, bf16[2048,256]{1,0:T(8,128)(2,1)S(1)} %bitcast.38, bf16[2048,256]{1,0:T(8,128)(2,1)S(1)} %bitcast.40, bf16[256,2048]{1,0:T(8,128)(2,1)S(1)} %bitcast.42, bf16[2048,256]{1,0:T(8,128)(2,1)S(1)} %copy-done.7, bf16[2048,256]{1,0:T(8,128)(2,1)S(1)} %copy-done.9, ...), custom_call_target="tpu_custom_call" | custom-call | tf_op jit(solution)/shard_map/experts/pallas_call | solution.py:335
  162.8 1.3 copy-done
  164.1 5.7 %all-to-all-start.1 = ((bf16[64,8,2048]{2,1,0:T(8,128)(2,1)}), bf16[64,8,2048]{2,1,0:T(8,128)(2,1)S(1)}, u32[]{:S(2)}, u32[]{:S(2)}) async-start(bf16[64,8,2048]{2,1,0:T(8,128)(2,1)} %bitcast.34), calls=%async_computation.1 | async-start | bytes 4194304 | tf_op jit(solution)/shard_map/all_to_all | solution.py:474
  170.0 28.3 %all-to-all-done.1 = bf16[64,8,2048]{2,1,0:T(8,128)(2,1)S(1)} async-done(((bf16[64,8,2048]{2,1,0:T(8,128)(2,1)}), bf16[64,8,2048]{2,1,0:T(8,128)(2,1)S(1)}, u32[]{:S(2)}, u32[]{:S(2)}) %all-to-all-start.1) | async-done | bytes 2097184 | tf_op jit(solution)/shard_map/all_to_all | solution.py:474
  198.3 1.6 combine.1
  (79 shorter events, 5.3 us)
Async XLA Ops:
  0.0 14.4 %copy-start.18 = (bf16[256,512]{1,0:T(8,128)(2,1)S(1)}, bf16[256,512]{1,0:T(8,128)(2,1)}, u32[]{:S(2)}) copy-start(bf16[256,512]{1,0:T(8,128)(2,1)} %param.16) | copy-start | bytes 786436
  2.3 9.1 %collective-permute-start = (bf16[160,256]{1,0:T(8,128)(2,1)S(1)}, bf16[160,256]{1,0:T(8,128)(2,1)S(1)}, u32[]{:S(2)}, u32[]{:S(2)}) collective-permute-start(bf16[160,256]{1,0:T(8,128)(2,1)S(1)} %fusion.12), channel_id=1, source_target_pairs={{64,1},{66,3},{68,5},{70,7},{72,9},{74,11},{76,13},{78,15},{80,17}... | collective-permute-start | bytes 245768 | tf_op jit(solution)/shard_map/ppermute | solution.py:418
  9.1 3.9 %collective-permute-start.1 = (bf16[160,256]{1,0:T(8,128)(2,1)S(1)}, bf16[160,256]{1,0:T(8,128)(2,1)S(1)}, u32[]{:S(2)}, u32[]{:S(2)}) collective-permute-start(bf16[160,256]{1,0:T(8,128)(2,1)S(1)} %fusion.12), channel_id=1, source_target_pairs={{96,0},{98,2},{100,4},{102,6},{104,8},{106,10},{108,12},{110,14},{... | collective-permute-start | bytes 245768 | tf_op jit(solution)/shard_map/ppermute | solution.py:417
  9.5 44.2 %copy-start.19 = (s32[128,2]{0,1:T(2,128)S(1)}, s32[128,2]{0,1:T(2,128)}, u32[]{:S(2)}) copy-start(s32[128,2]{0,1:T(2,128)} %param.24) | copy-start | bytes 3076
  13.1 9.0 %collective-permute-start.2 = (bf16[320,256]{1,0:T(8,128)(2,1)S(1)}, bf16[320,256]{1,0:T(8,128)(2,1)S(1)}, u32[]{:S(2)}, u32[]{:S(2)}) collective-permute-start(bf16[320,256]{1,0:T(8,128)(2,1)S(1)} %pad_maximum_fusion.3), channel_id=1, source_target_pairs={{0,8},{1,3},{2,10},{3,5},{4,12},{5,7},{6,14},{7,1},{8,16},{9,11},{... | collective-permute-start | bytes 491528 | tf_op jit(solution)/shard_map/ppermute | solution.py:435
  14.4 19.0 %collective-permute-start.5 = (bf16[256,768]{1,0:T(8,128)(2,1)S(1)}, bf16[256,768]{1,0:T(8,128)(2,1)}, u32[]{:S(2)}, u32[]{:S(2)}) collective-permute-start(bf16[256,768]{1,0:T(8,128)(2,1)S(1)} %pad_maximum_fusion.2), channel_id=1, source_target_pairs={{0,126},{1,127},{2,124},{3,125},{4,122},{5,123},{6,120},{7,121},{8... | collective-permute-start | bytes 1179656 | tf_op jit(solution)/shard_map/ppermute | solution.py:433
  19.6 12.5 %collective-permute-start.3 = (bf16[320,256]{1,0:T(8,128)(2,1)S(1)}, bf16[320,256]{1,0:T(8,128)(2,1)S(1)}, u32[]{:S(2)}, u32[]{:S(2)}) collective-permute-start(bf16[320,256]{1,0:T(8,128)(2,1)S(1)} %pad_maximum_fusion.3), channel_id=1, source_target_pairs={{0,24},{1,7},{2,26},{3,1},{4,28},{5,3},{6,30},{7,5},{8,0},{9,15},{... | collective-permute-start | bytes 491528 | tf_op jit(solution)/shard_map/ppermute | solution.py:435
  20.8 11.3 %collective-permute-start.4 = (bf16[320,256]{1,0:T(8,128)(2,1)S(1)}, bf16[320,256]{1,0:T(8,128)(2,1)S(1)}, u32[]{:S(2)}, u32[]{:S(2)}) collective-permute-start(bf16[320,256]{1,0:T(8,128)(2,1)S(1)} %pad_maximum_fusion.3), channel_id=1, source_target_pairs={{0,16},{1,5},{2,18},{3,7},{4,20},{5,1},{6,22},{7,3},{8,24},{9,13},... | collective-permute-start | bytes 491528 | tf_op jit(solution)/shard_map/ppermute | solution.py:435
  33.4 18.0 %collective-permute-start.6 = (bf16[1280,256]{1,0:T(8,128)(2,1)S(1)}, bf16[1280,256]{1,0:T(8,128)(2,1)S(1)}, u32[]{:S(2)}, u32[]{:S(2)}) collective-permute-start(bf16[1280,256]{1,0:T(8,128)(2,1)S(1)} %constant_dynamic-update-slice_fusion.rest_0_), channel_id=1, source_target_pairs={{0,2},{1,9},{2,4},{3,11},{4,6},{5,13},{6,0},{7,15},{8,10},{9,17},{... | collective-permute-start | bytes 1966088 | tf_op jit(solution)/shard_map/ppermute | solution.py:438
  33.7 17.7 %collective-permute-start.7 = (bf16[1280,256]{1,0:T(8,128)(2,1)S(1)}, bf16[1280,256]{1,0:T(8,128)(2,1)S(1)}, u32[]{:S(2)}, u32[]{:S(2)}) collective-permute-start(bf16[1280,256]{1,0:T(8,128)(2,1)S(1)} %constant_dynamic-update-slice_fusion.rest_0_), channel_id=1, source_target_pairs={{0,6},{1,25},{2,0},{3,27},{4,2},{5,29},{6,4},{7,31},{8,14},{9,1},{... | collective-permute-start | bytes 1966088 | tf_op jit(solution)/shard_map/ppermute | solution.py:438
  36.1 16.7 %collective-permute-start.8 = (bf16[1280,256]{1,0:T(8,128)(2,1)S(1)}, bf16[1280,256]{1,0:T(8,128)(2,1)S(1)}, u32[]{:S(2)}, u32[]{:S(2)}) collective-permute-start(bf16[1280,256]{1,0:T(8,128)(2,1)S(1)} %constant_dynamic-update-slice_fusion.rest_0_), channel_id=1, source_target_pairs={{0,4},{1,17},{2,6},{3,19},{4,0},{5,21},{6,2},{7,23},{8,12},{9,25},... | collective-permute-start | bytes 1966088 | tf_op jit(solution)/shard_map/ppermute | solution.py:438
  36.6 24.0 %collective-permute-start.9 = (bf16[1280,256]{1,0:T(8,128)(2,1)S(1)}, bf16[1280,256]{1,0:T(8,128)(2,1)}, u32[]{:S(2)}, u32[]{:S(2)}) collective-permute-start(bf16[1280,256]{1,0:T(8,128)(2,1)S(1)} %constant_dynamic-update-slice_fusion.rest_0_), channel_id=1, source_target_pairs={{0,1},{1,0},{2,3},{3,2},{4,5},{5,4},{6,7},{7,6},{8,9},{9,8},{10,11... | collective-permute-start | bytes 1966088 | tf_op jit(solution)/shard_map/ppermute | solution.py:439
  51.4 9.2 %collective-permute-start.10 = (bf16[1280,256]{1,0:T(8,128)(2,1)S(1)}, bf16[1280,256]{1,0:T(8,128)(2,1)}, u32[]{:S(2)}, u32[]{:S(2)}) collective-permute-start(bf16[1280,256]{1,0:T(8,128)(2,1)S(1)} %collective-permute-done.6.rest_1_), channel_id=1, source_target_pairs={{0,1},{1,0},{2,3},{3,2},{4,5},{5,4},{6,7},{7,6},{8,9},{9,8},{10,11... | collective-permute-start | bytes 1966088 | tf_op jit(solution)/shard_map/ppermute | solution.py:439
  51.4 9.2 %collective-permute-start.11 = (bf16[1280,256]{1,0:T(8,128)(2,1)S(1)}, bf16[1280,256]{1,0:T(8,128)(2,1)}, u32[]{:S(2)}, u32[]{:S(2)}) collective-permute-start(bf16[1280,256]{1,0:T(8,128)(2,1)S(1)} %collective-permute-done.7.rest_2_), channel_id=1, source_target_pairs={{0,1},{1,0},{2,3},{3,2},{4,5},{5,4},{6,7},{7,6},{8,9},{9,8},{10,11... | collective-permute-start | bytes 1966088 | tf_op jit(solution)/shard_map/ppermute | solution.py:439
  52.8 7.8 %collective-permute-start.12 = (bf16[1280,256]{1,0:T(8,128)(2,1)S(1)}, bf16[1280,256]{1,0:T(8,128)(2,1)}, u32[]{:S(2)}, u32[]{:S(2)}) collective-permute-start(bf16[1280,256]{1,0:T(8,128)(2,1)S(1)} %collective-permute-done.8.rest_3_), channel_id=1, source_target_pairs={{0,1},{1,0},{2,3},{3,2},{4,5},{5,4},{6,7},{7,6},{8,9},{9,8},{10,11... | collective-permute-start | bytes 1966088 | tf_op jit(solution)/shard_map/ppermute | solution.py:439
  57.0 3.7 %copy-start.15 = (bf16[256,512]{1,0:T(8,128)(2,1)S(1)}, bf16[256,512]{1,0:T(8,128)(2,1)}, u32[]{:S(2)}) copy-start(bf16[256,512]{1,0:T(8,128)(2,1)} %key_up_ref.1) | copy-start | bytes 786436
  59.0 1.7 copy-start.16
  60.7 49.2 %copy-start.17 = (f32[2048]{0:T(1024)S(1)}, f32[2048]{0:T(1024)}, u32[]{:S(2)}) copy-start(f32[2048]{0:T(1024)} %param.23) | copy-start | bytes 24580
  92.7 11.3 %collective-permute-start.13 = (bf16[128,640]{1,0:T(8,128)(2,1)S(1)}, bf16[128,640]{1,0:T(8,128)(2,1)S(1)}, u32[]{:S(2)}, u32[]{:S(2)}) collective-permute-start(bf16[128,640]{1,0:T(8,128)(2,1)S(1)} %get-tuple-element.17), channel_id=1, source_target_pairs={{0,126},{1,127},{2,124},{3,125},{4,122},{5,123},{6,120},{7,121},{8... | collective-permute-start | bytes 491528 | tf_op jit(solution)/shard_map/ppermute | solution.py:453
  97.8 6.3 %collective-permute-start.14 = (bf16[128,640]{1,0:T(8,128)(2,1)S(1)}, bf16[128,640]{1,0:T(8,128)(2,1)S(1)}, u32[]{:S(2)}, u32[]{:S(2)}) collective-permute-start(bf16[128,640]{1,0:T(8,128)(2,1)S(1)} %get-tuple-element.16), channel_id=1, source_target_pairs={{0,1},{1,0},{2,3},{3,2},{4,5},{5,4},{6,7},{7,6},{8,9},{9,8},{10,11... | collective-permute-start | bytes 491528 | tf_op jit(solution)/shard_map/ppermute | solution.py:455
  98.6 11.2 %collective-permute-start.15 = (bf16[128,640]{1,0:T(8,128)(2,1)S(1)}, bf16[128,640]{1,0:T(8,128)(2,1)S(1)}, u32[]{:S(2)}, u32[]{:S(2)}) collective-permute-start(bf16[128,640]{1,0:T(8,128)(2,1)S(1)} %get-tuple-element.15), channel_id=1, source_target_pairs={{0,127},{1,126},{2,125},{3,124},{4,123},{5,122},{6,121},{7,120},{8... | collective-permute-start | bytes 491528 | tf_op jit(solution)/shard_map/ppermute | solution.py:454
  109.8 2.2 %copy-start.1 = (bf16[1024,2048]{1,0:T(8,128)(2,1)S(1)}, bf16[1024,2048]{1,0:T(8,128)(2,1)}, u32[]{:S(2)}) copy-start(bf16[1024,2048]{1,0:T(8,128)(2,1)} %out_proj.1) | copy-start | bytes 12582916
  112.0 1.0 copy-start.12
  115.1 1.3 copy-start.2
  116.5 0.8 copy-start.13
  117.2 5.2 %copy-start.3 = (bf16[1,2048,256]{2,1,0:T(8,128)(2,1)S(1)}, bf16[1,2048,256]{2,1,0:T(8,128)(2,1)}, u32[]{:S(2)}) copy-start(bf16[1,2048,256]{2,1,0:T(8,128)(2,1)} %param.26) | copy-start | bytes 3145732
  117.2 35.3 %all-to-all-start = ((bf16[64,8,2048]{2,1,0:T(8,128)(2,1)}), bf16[64,8,2048]{2,1,0:T(8,128)(2,1)S(1)}, u32[]{:S(2)}, u32[]{:S(2)}) async-start(bf16[64,8,2048]{2,1,0:T(8,128)(2,1)} %bitcast.36), calls=%async_computation | async-start | bytes 4194304 | tf_op jit(solution)/shard_map/all_to_all | solution.py:468
  122.5 2.7 %collective-permute-start.16 = (bf16[2048,256]{1,0:T(8,128)(2,1)S(1)}, bf16[2048,256]{1,0:T(8,128)(2,1)S(1)}, u32[]{:S(2)}, u32[]{:S(2)}) collective-permute-start(bf16[2048,256]{1,0:T(8,128)(2,1)S(1)} %bitcast.37), channel_id=1, source_target_pairs={{0,1},{1,0},{2,3},{3,2},{4,5},{5,4},{6,7},{7,6},{8,9},{9,8},{10,11... | collective-permute-start | bytes 3145736 | tf_op jit(solution)/shard_map/ppermute | solution.py:472
  122.6 4.1 %collective-permute-start.17 = (bf16[2048,256]{1,0:T(8,128)(2,1)}, bf16[2048,256]{1,0:T(8,128)(2,1)S(1)}, u32[]{:S(2)}, u32[]{:S(2)}) collective-permute-start(bf16[2048,256]{1,0:T(8,128)(2,1)} %bitcast.39), channel_id=1, source_target_pairs={{0,1},{1,0},{2,3},{3,2},{4,5},{5,4},{6,7},{7,6},{8,9},{9,8},{10,11... | collective-permute-start | bytes 3145736 | tf_op jit(solution)/shard_map/ppermute | solution.py:472
  123.1 5.1 %collective-permute-start.18 = (bf16[256,2048]{1,0:T(8,128)(2,1)}, bf16[256,2048]{1,0:T(8,128)(2,1)S(1)}, u32[]{:S(2)}, u32[]{:S(2)}) collective-permute-start(bf16[256,2048]{1,0:T(8,128)(2,1)} %bitcast.41), channel_id=1, source_target_pairs={{0,1},{1,0},{2,3},{3,2},{4,5},{5,4},{6,7},{7,6},{8,9},{9,8},{10,11... | collective-permute-start | bytes 3145736 | tf_op jit(solution)/shard_map/ppermute | solution.py:472
  125.2 1.0 copy-start.6
  126.7 1.0 copy-start.8
  128.2 1.0 copy-start.10
  152.6 1.2 copy-start.4
  153.8 1.2 copy-start.5
  155.0 1.2 copy-start.7
  156.3 1.2 copy-start.9
  157.5 1.2 copy-start.11
  162.8 1.3 copy-start
  164.1 5.8 %copy-start.20 = (f32[128,2]{0,1:T(2,128)S(1)}, f32[128,2]{0,1:T(2,128)}, u32[]{:S(2)}) copy-start(f32[128,2]{0,1:T(2,128)} %param.25) | copy-start | bytes 3076
  164.1 34.2 %copy-start.14 = (bf16[128,2048]{1,0:T(8,128)(2,1)S(1)}, bf16[128,2048]{1,0:T(8,128)(2,1)}, u32[]{:S(2)}) copy-start(bf16[128,2048]{1,0:T(8,128)(2,1)} %copy-done.13) | copy-start | bytes 1572868
  164.1 34.2 %all-to-all-start.1 = ((bf16[64,8,2048]{2,1,0:T(8,128)(2,1)}), bf16[64,8,2048]{2,1,0:T(8,128)(2,1)S(1)}, u32[]{:S(2)}, u32[]{:S(2)}) async-start(bf16[64,8,2048]{2,1,0:T(8,128)(2,1)} %bitcast.34), calls=%async_computation.1 | async-start | bytes 4194304 | tf_op jit(solution)/shard_map/all_to_all | solution.py:474

commit v3 on v2

v3 whole, which is shorter than its diff:
```python
import functools
import jax
import jax.numpy as jnp
import numpy as np
from jax import lax
from jax.experimental import pallas as pl
from jax.experimental.pallas import tpu as pltpu
from jax.sharding import PartitionSpec as P

QK_NOPE = 128
QK_ROPE = 64
V_DIM = 128
LATENT = 256
SEGMENT = 64
EPSILON = 1e-06
ROPE_BASE = 10000.0
NEG_LARGE = -1e30

N_SP = 64
N_TP = 2
HEADS_HERE = 4
ROWS = 128
SHARD = 160
UNIT = 4
KEYS = UNIT * ROWS
QROWS = HEADS_HERE * ROWS
CAP = 8
AXES = ("sp", "tp")
STEP = {"x": 1, "y": 4, "z": 16}
Z_FIRST = {(0, 0): (3, 0), (1, 0): (2, 0), (0, 1): (1, 0), (1, 1): (0, 0), (2, 1): (1, 1), (3, 1): (0, 1), (2, 0): (3, 1), (3, 0): (2, 1)}
Z_SECOND = {(0, 1): (2, 0), (1, 1): (3, 0), (2, 0): (0, 1), (3, 0): (1, 1)}
ORDER = (("y", "x"), ("x", "y"))
SHIFTS = (0, 1, -1, 2)
SCALE2 = float((QK_NOPE + QK_ROPE) ** (-0.5) * np.log2(np.e))
PLANE = 16
GROUPS = 4
CHUNK = 64
MESSAGE = HEADS_HERE * V_DIM + 128


def moved(s, dim, by):
    step = STEP[dim]
    c = (s // step) % 4
    return s + step * ((c + by) % 4 - c)


def shift_pairs(phase, by):
    return [
        (s * N_TP + t, moved(s, ORDER[t][phase], by) * N_TP + t)
        for s in range(N_SP)
        for t in range(N_TP)
    ]


def plane_pairs(table):
    return [
        ((from_z * PLANE + r) * N_TP + from_core, (z * PLANE + r) * N_TP + core)
        for (z, core), (from_z, from_core) in table.items()
        for r in range(PLANE)
    ]


def shard_first(s, t, k3, k2, kz):
    s = moved(s, ORDER[t][1], -SHIFTS[k3])
    s = moved(s, ORDER[t][0], -SHIFTS[k2])
    z, r = divmod(s, PLANE)
    source = (z, t)
    if kz == 1:
        source = Z_FIRST[source]
    elif source in Z_SECOND:
        source = Z_SECOND[source]
    return 4 * (source[0] * PLANE + r) + 2 * source[1]


CALLS = (((0, 0), (1, 0)), ((0, 1), (0, 2), (0, 3)), ((1, 1), (1, 2), (1, 3)))
PART_SHARDS = 8


@functools.lru_cache(None)
def work_table(call):
    lists = []
    for s in range(N_SP):
        for t in range(N_TP):
            firsts = [
                shard_first(s, t if own == 0 else 1 - t, k3, k2, kz)
                for own, k3 in CALLS[call]
                for k2 in range(4)
                for kz in range(2)
            ]
            rows = []
            for group in range(GROUPS):
                block = s if group < 2 else N_SP - 1 - s
                base = 4 * block + 2 * (group % 2)
                needed = [n for n in range(len(firsts)) if firsts[n] <= base + 1]
                for at in range(0, len(needed), UNIT):
                    part = needed[at : at + UNIT]
                    segs = [firsts[n] for n in part] + [1 << 20] * (UNIT - len(part))
                    part = part + [part[-1]] * (UNIT - len(part))
                    bits = 0
                    for half in range(2):
                        for j in range(UNIT):
                            for late in range(2):
                                if segs[j] + half > base + late:
                                    bits |= 1 << ((half * UNIT + j) * 2 + late)
                    rows.append([group, bits, t] + part)
            lists.append(rows)
    count = max(len(rows) for rows in lists)
    count += 1 - count % 2
    everything = (1 << (4 * UNIT)) - 1
    idle = lambda rows, t: rows[-1][:1] + [everything] + rows[-1][2:] if rows else [0, everything, t] + [0] * UNIT
    table = []
    for n, rows in enumerate(lists):
        table.append(rows + [idle(rows, n % N_TP)] * (count + 1 - len(rows)))
    return count, np.array(table, np.int32).reshape(len(lists), -1)


NT = (((1,), (1,)), ((), ()))


def attention_body(call, steps, part_count, table, *rest):
    first, last = call == 0, call == len(CALLS) - 1
    if first:
        qn_ref, key_up_ref, q4_ref = rest[:3]
        taken = 3
    else:
        q4_ref, qabs, m_in, l_in, acc_in = rest[:5]
        taken = 5
    if last:
        value_up_ref = rest[taken]
        taken += 1
    parts = rest[taken : taken + part_count]
    taken += part_count
    if first:
        qabs, m_ref, l_ref, acc_ref = rest[taken : taken + 4]
        taken += 4
    elif last:
        out_ref, m_ref, l_ref, acc_ref = rest[taken : taken + 4]
        taken += 4
    else:
        m_ref, l_ref, acc_ref = rest[taken : taken + 3]
        taken += 3
    keys, s0, s1, p0, p1, shrink0, shrink1, sems = rest[taken:]
    part_rows = parts[0].shape[0]
    copies = []
    for n in range(part_count):
        copy = pltpu.make_async_copy(parts[n], keys.at[pl.ds(n * part_rows, part_rows)], sems.at[n])
        copy.start()
        copies.append(copy)
    if first:
        for g in range(GROUPS):
            for h in range(HEADS_HERE):
                cols = pl.ds(h * QK_NOPE, QK_NOPE)
                qabs[g, pl.ds(h * ROWS, ROWS), :] = lax.dot_general(
                    qn_ref[g, :, cols], key_up_ref[:, cols], NT, preferred_element_type=jnp.float32
                ).astype(jnp.bfloat16)
        m_ref[...] = jnp.full(m_ref.shape, NEG_LARGE, jnp.float32)
        l_ref[...] = jnp.zeros(l_ref.shape, jnp.float32)
        acc_ref[...] = jnp.zeros(acc_ref.shape, jnp.float32)
    else:
        m_ref[...] = m_in[...]
        l_ref[...] = l_in[...]
        acc_ref[...] = acc_in[...]
    for copy in copies:
        copy.wait()

    cols_per_step = 3 + UNIT

    def field(u, n):
        return table[u * cols_per_step + n]

    def latent_tile(u, half):
        return jnp.concatenate(
            [
                keys[pl.ds(pl.multiple_of(field(u, 3 + j) * SHARD + half * SEGMENT, 32), SEGMENT), :]
                for j in range(UNIT)
            ],
            axis=0,
        )

    note_lane = lax.broadcasted_iota(jnp.int32, (16, 128), 1)

    def scores(u, s_ref):
        g = field(u, 0)
        bits = field(u, 1)
        rot = jnp.concatenate(
            [
                keys[pl.ds(pl.multiple_of(field(u, 3 + j) * SHARD + ROWS, 32), 32), pl.ds(h * 128, 128)]
                for j in range(UNIT)
                for h in range(2)
            ],
            axis=0,
        )
        q = qabs[g]
        for half in range(2):
            notes = []
            for j in range(UNIT):
                at = (half * UNIT + j) * 2
                early, late = (
                    jnp.where((bits >> (at + n)) & 1 == 1, jnp.float32(NEG_LARGE), jnp.float32(0.0)) for n in range(2)
                )
                note = jnp.where(note_lane == 0, early, jnp.where(note_lane == 1, late, 0.0)).astype(jnp.bfloat16)
                notes += [note] * (SEGMENT // 16)
            extra = jnp.concatenate([rot, jnp.concatenate(notes, axis=0)], axis=1)
            s_ref[:, pl.ds(half * 256, 256)] = lax.dot_general(
                q, latent_tile(u, half), NT, preferred_element_type=jnp.float32
            ) + lax.dot_general(q4_ref[g, half], extra, NT, preferred_element_type=jnp.float32)

    def absorb(u, s_ref, p_ref, shrink_ref):
        g = field(u, 0)
        for at in range(0, QROWS, CHUNK):
            rows = pl.ds(at, CHUNK)
            s = s_ref[rows, :]
            before = m_ref[g, rows, :]
            top = s[:, :128]
            for k in range(1, KEYS // 128):
                top = jnp.maximum(top, s[:, k * 128 : (k + 1) * 128])
            after = jnp.maximum(before, jnp.max(top, axis=1, keepdims=True))
            m_ref[g, rows, :] = after
            shrink = jnp.exp2((before - after) * SCALE2)
            shrink_ref[rows, :] = shrink
            after = after * SCALE2
            partial = l_ref[g, rows, :] * shrink
            for k in range(KEYS // 128):
                p = jnp.exp2(s[:, k * 128 : (k + 1) * 128] * SCALE2 - after)
                partial = partial + p
                p_ref[rows, pl.ds(k * 128, 128)] = p.astype(jnp.bfloat16)
            l_ref[g, rows, :] = partial
        values = jnp.concatenate([latent_tile(u, 0), latent_tile(u, 1)], axis=0)
        for at in range(0, QROWS, QROWS // 2):
            rows = pl.ds(at, QROWS // 2)
            product = jnp.dot(p_ref[rows, :], values, preferred_element_type=jnp.float32)
            for k in range(LATENT // 128):
                cols = pl.ds(k * 128, 128)
                acc_ref[g, rows, cols] = (
                    acc_ref[g, rows, cols] * shrink_ref[rows, :] + product[:, k * 128 : (k + 1) * 128]
                )

    scores(0, s0)

    def pair(k, carry):
        u = k * 2
        scores(u + 1, s1)
        absorb(u, s0, p0, shrink0)
        scores(u + 2, s0)
        absorb(u + 1, s1, p1, shrink1)
        return carry

    lax.fori_loop(0, steps // 2, pair, 0)
    absorb(steps - 1, s0, p0, shrink0)
    if not last:
        return
    core = field(0, 2)
    lane = lax.broadcasted_iota(jnp.int32, (ROWS, 128), 1)
    for g in range(GROUPS):
        place = 2 * (g // 2) + jnp.where(core == g % 2, 0, 1)
        total = jnp.sum(l_ref[g], axis=1, keepdims=True)
        total = jnp.where(total > 0.0, total, 1.0)
        mean = (acc_ref[g] / total).astype(jnp.bfloat16)
        size = m_ref[g] * SCALE2 + jnp.log2(total)
        notes = jnp.zeros((ROWS, 128), jnp.bfloat16)
        for h in range(HEADS_HERE):
            cols = pl.ds(h * V_DIM, V_DIM)
            rows = slice(h * ROWS, (h + 1) * ROWS)
            out_ref[place, :, cols] = jnp.dot(
                mean[rows], value_up_ref[:, cols], preferred_element_type=jnp.float32
            ).astype(jnp.bfloat16)
            left = size[rows]
            for n in range(3):
                term = left.astype(jnp.bfloat16)
                notes = jnp.where(lane == n * HEADS_HERE + h, term, notes)
                left = left - term.astype(jnp.float32)
        out_ref[place, :, pl.ds(HEADS_HERE * V_DIM, 128)] = notes


def attention(call, table, operands, parts):
    vmem = pl.BlockSpec(memory_space=pltpu.VMEM)
    steps = work_table(call)[0]
    first, last = call == 0, call == len(CALLS) - 1
    f32 = lambda width: jax.ShapeDtypeStruct((GROUPS, QROWS, width), jnp.float32)
    state = [f32(128), f32(128), f32(LATENT)]
    scratch = []
    if first:
        outs = [jax.ShapeDtypeStruct((GROUPS, QROWS, LATENT), jnp.bfloat16)] + state
    elif last:
        outs = [jax.ShapeDtypeStruct((4, ROWS, MESSAGE), jnp.bfloat16)]
        scratch = [pltpu.VMEM(s.shape, s.dtype) for s in state]
    else:
        outs = state
    work = steps * QROWS * KEYS * 3 * LATENT * 2
    return pl.pallas_call(
        functools.partial(attention_body, call, steps, len(parts)),
        out_shape=outs,
        in_specs=[pl.BlockSpec(memory_space=pltpu.SMEM)]
        + [vmem] * len(operands)
        + [pl.BlockSpec(memory_space=pl.ANY)] * len(parts),
        out_specs=[vmem] * len(outs),
        scratch_shapes=scratch
        + [
            pltpu.VMEM((len(parts) * PART_SHARDS * SHARD, LATENT), jnp.bfloat16),
            pltpu.VMEM((QROWS, KEYS), jnp.float32),
            pltpu.VMEM((QROWS, KEYS), jnp.float32),
            pltpu.VMEM((QROWS, KEYS), jnp.bfloat16),
            pltpu.VMEM((QROWS, KEYS), jnp.bfloat16),
            pltpu.VMEM((QROWS, 128), jnp.float32),
            pltpu.VMEM((QROWS, 128), jnp.float32),
            pltpu.SemaphoreType.DMA((len(parts),)),
        ],
        cost_estimate=pl.CostEstimate(
            flops=work, bytes_accessed=2**20, transcendentals=steps * QROWS * KEYS
        ),
        compiler_params=pltpu.CompilerParams(vmem_limit_bytes=24 * 2**20),
    )(table, *operands, *parts)


def in_hbm(x):
    return pltpu.with_memory_space_constraint(x, pltpu.HBM)


def merged(one, two):
    width = HEADS_HERE * V_DIM
    outs = []
    for h in range(HEADS_HERE):
        sizes = []
        for part in (one, two):
            notes = part[:, width : width + 128].astype(jnp.float32)
            sizes.append(
                notes[:, h : h + 1] + notes[:, HEADS_HERE + h : HEADS_HERE + h + 1]
                + notes[:, 2 * HEADS_HERE + h : 2 * HEADS_HERE + h + 1]
            )
        most = jnp.maximum(sizes[0], sizes[1])
        first, second = (jnp.exp2(size - most) for size in sizes)
        cols = slice(h * V_DIM, (h + 1) * V_DIM)
        value = first * one[:, cols].astype(jnp.float32) + second * two[:, cols].astype(jnp.float32)
        outs.append((value / (first + second)).astype(jnp.bfloat16))
    return jnp.concatenate(outs, axis=1)


PIECES = 4


def project_body(
    core, local_part, mirror_same, swapped, mirror_cross, gain, slots, residual_hbm, out_proj_hbm,
    hidden_hbm, outgoing_hbm, residual, out_proj, projected, hidden, outgoing, sems, out_sems,
):
    width = residual.shape[1]
    piece = width // PIECES
    loads = [pltpu.make_async_copy(residual_hbm, residual, sems.at[PIECES])]
    for n in range(PIECES):
        cols = pl.ds(n * piece, piece)
        loads.append(pltpu.make_async_copy(out_proj_hbm.at[:, cols], out_proj.at[:, cols], sems.at[n]))
    for load in loads[1:] + loads[:1]:
        load.start()
    half = HEADS_HERE * V_DIM
    mine = merged(local_part[...], mirror_same[...])
    theirs = merged(swapped[...], mirror_cross[...])
    at = pl.multiple_of(core[0] * half, half)
    other = pl.multiple_of((1 - core[0]) * half, half)
    for n in range(PIECES):
        cols = pl.ds(n * piece, piece)
        loads[1 + n].wait()
        projected[:, cols] = jnp.dot(
            mine, out_proj[pl.ds(at, half), cols], preferred_element_type=jnp.float32
        ) + jnp.dot(theirs, out_proj[pl.ds(other, half), cols], preferred_element_type=jnp.float32)
    loads[0].wait()
    result = (residual[...].astype(jnp.float32) + projected[...]).astype(jnp.bfloat16)
    hidden[...] = result
    store = pltpu.make_async_copy(hidden, hidden_hbm, out_sems.at[PIECES])
    store.start()
    wide = result.astype(jnp.float32)
    normed = wide * lax.rsqrt(jnp.mean(wide * wide, axis=-1, keepdims=True) + EPSILON)
    normed = (normed * gain[...]).astype(jnp.bfloat16)
    count = outgoing.shape[0] // PIECES
    stores = [store]
    for n in range(PIECES):
        slot = lax.broadcasted_iota(jnp.int32, (count, normed.shape[0]), 0) + n * count
        pick = (slot == slots[0:1, :]) | (slot == slots[1:2, :])
        pick = jnp.where(pick, 1.0, 0.0).astype(jnp.bfloat16)
        rows = pl.ds(n * count, count)
        outgoing[rows, :] = jnp.dot(pick, normed, preferred_element_type=jnp.float32).astype(jnp.bfloat16)
        store = pltpu.make_async_copy(outgoing.at[rows], outgoing_hbm.at[rows], out_sems.at[n])
        store.start()
        stores.append(store)
    for store in stores:
        store.wait()


def project(core, messages, out_proj, residual, gain, slots):
    width = residual.shape[1]
    vmem = pl.BlockSpec(memory_space=pltpu.VMEM)
    hbm = pl.BlockSpec(memory_space=pltpu.HBM)
    return pl.pallas_call(
        project_body,
        out_shape=(
            pltpu.HBM((ROWS, width), jnp.bfloat16),
            pltpu.HBM((N_SP * CAP, width), jnp.bfloat16),
        ),
        in_specs=[pl.BlockSpec(memory_space=pltpu.SMEM)] + [vmem] * 6 + [hbm] * 2,
        out_specs=(hbm, hbm),
        scratch_shapes=[
            pltpu.VMEM((ROWS, width), jnp.bfloat16),
            pltpu.VMEM(out_proj.shape, jnp.bfloat16),
            pltpu.VMEM((ROWS, width), jnp.float32),
            pltpu.VMEM((ROWS, width), jnp.bfloat16),
            pltpu.VMEM((N_SP * CAP, width), jnp.bfloat16),
            pltpu.SemaphoreType.DMA((PIECES + 1,)),
            pltpu.SemaphoreType.DMA((PIECES + 1,)),
        ],
        compiler_params=pltpu.CompilerParams(vmem_limit_bytes=20 * 2**20),
        name="project",
    )(core, *messages, gain, slots, in_hbm(residual), in_hbm(out_proj))


def experts_body(rows, *rest):
    sources = rest[:6]
    out_hbm = rest[6]
    weights = rest[7:13]
    first, out, sems, out_sems = rest[13:]
    loads = []
    for n in range(6):
        load = pltpu.make_async_copy(sources[n], weights[n], sems.at[n])
        load.start()
        loads.append(load)
    count = rows.shape[0]
    block = count // 2
    stores = []
    for n in range(2):
        gate, up, down = weights[3 * n : 3 * n + 3]
        for k in range(2):
            at = pl.ds(k * block, block)
            x = rows[at, :]
            if k == 0:
                loads[3 * n].wait()
            gated = jnp.dot(x, gate[...], preferred_element_type=jnp.float32)
            if k == 0:
                loads[3 * n + 1].wait()
            raised = jnp.dot(x, up[...], preferred_element_type=jnp.float32)
            active = (gated / (1.0 + jnp.exp(-gated)) * raised).astype(jnp.bfloat16)
            if k == 0:
                loads[3 * n + 2].wait()
            product = jnp.dot(active, down[...], preferred_element_type=jnp.float32).astype(jnp.bfloat16)
            if n == 0:
                first[at, :] = product
            else:
                out[at, :] = (first[at, :].astype(jnp.float32) + product.astype(jnp.float32)).astype(jnp.bfloat16)
                store = pltpu.make_async_copy(out.at[at], out_hbm.at[at], out_sems.at[k])
                store.start()
                stores.append(store)
    for store in stores:
        store.wait()


def experts(rows, own, other):
    count, width = rows.shape
    hbm = pl.BlockSpec(memory_space=pltpu.HBM)
    return pl.pallas_call(
        experts_body,
        out_shape=pltpu.HBM((count, width), jnp.bfloat16),
        in_specs=[pl.BlockSpec(memory_space=pltpu.VMEM)] + [hbm] * 6,
        out_specs=hbm,
        scratch_shapes=[pltpu.VMEM(w.shape, w.dtype) for w in (*own, *other)]
        + [
            pltpu.VMEM((count, width), jnp.bfloat16),
            pltpu.VMEM((count, width), jnp.bfloat16),
            pltpu.SemaphoreType.DMA((6,)),
            pltpu.SemaphoreType.DMA((2,)),
        ],
        compiler_params=pltpu.CompilerParams(vmem_limit_bytes=28 * 2**20),
        name="experts",
    )(rows, *[in_hbm(w) for w in (*own, *other)])


def combine_body(back, hidden, slots, weights, out_ref):
    slot = lax.broadcasted_iota(jnp.int32, (hidden.shape[0], back.shape[0]), 1)
    pick = jnp.where(slot == slots[:, 0:1], weights[:, 0:1], 0.0) + jnp.where(
        slot == slots[:, 1:2], weights[:, 1:2], 0.0
    )
    high = pick.astype(jnp.bfloat16)
    low = (pick - high.astype(jnp.float32)).astype(jnp.bfloat16)
    rows = back[...]
    mixed = jnp.dot(high, rows, preferred_element_type=jnp.float32) + jnp.dot(
        low, rows, preferred_element_type=jnp.float32
    )
    out_ref[...] = (hidden[...].astype(jnp.float32) + mixed).astype(jnp.bfloat16)


def combine(back, hidden, slots, weights):
    vmem = pl.BlockSpec(memory_space=pltpu.VMEM)
    return pl.pallas_call(
        combine_body,
        out_shape=jax.ShapeDtypeStruct(hidden.shape, jnp.bfloat16),
        in_specs=[vmem] * 4,
        out_specs=vmem,
        compiler_params=pltpu.CompilerParams(vmem_limit_bytes=16 * 2**20),
        name="combine",
    )(back, hidden, slots, weights)


def rotary(values, positions):
    half_width = values.shape[-1] // 2
    inverse = ROPE_BASE ** (-2.0 * jnp.arange(half_width, dtype=jnp.float32) / values.shape[-1])
    angles = positions.astype(jnp.float32)[:, None] * inverse[None, :]
    cosine = jnp.cos(angles)
    sine_part = jnp.sin(angles)
    if values.ndim == 3:
        cosine = cosine[:, None, :]
        sine_part = sine_part[:, None, :]
    first_half = values[..., :half_width]
    second = values[..., half_width:]
    return jnp.concatenate(
        [first_half * cosine - second * sine_part, second * cosine + first_half * sine_part],
        axis=-1,
    )


def local(
    residual,
    query_nope,
    query_rope,
    latent,
    key_rope,
    key_up,
    value_up,
    out_proj,
    norm_gain,
    routes,
    route_weight,
    w_gate,
    w_up,
    w_down,
):
    tp_index = lax.axis_index("tp")
    sp_index = lax.axis_index("sp")
    tok_dev = query_nope.shape[0]
    query_first = sp_index * tok_dev
    swap = [(0, 1), (1, 0)]

    key_pos = query_first + tp_index * ROWS + jnp.arange(ROWS, dtype=jnp.int32)
    key_rot = rotary(key_rope.astype(jnp.float32), key_pos).astype(jnp.bfloat16)
    packed = jnp.concatenate([key_rot[0:32], key_rot[64:96], key_rot[32:64], key_rot[96:128]], axis=1)
    shard = jnp.concatenate([latent, packed], axis=0)
    mirror = [
        (s * N_TP + t, (N_SP - 1 - s) * N_TP + t) for s in range(N_SP) for t in range(N_TP)
    ]
    crossing = [
        (s * N_TP + t, (N_SP - 1 - s) * N_TP + 1 - t) for s in range(N_SP) for t in range(N_TP)
    ]
    received_nope = lax.ppermute(query_nope, AXES, mirror)
    received_rope = lax.ppermute(query_rope, AXES, mirror)

    near = lax.ppermute(shard, AXES, plane_pairs(Z_FIRST))
    far = lax.ppermute(shard, AXES, plane_pairs(Z_SECOND))
    main = (tp_index == 0) == (sp_index < 2 * PLANE)
    both = jnp.concatenate([jnp.where(main, shard, far), near], axis=0)
    got = [both] + [lax.ppermute(both, AXES, shift_pairs(0, by)) for by in SHIFTS[1:]]
    both = jnp.concatenate(got, axis=0)

    tokens = jnp.arange(tok_dev, dtype=jnp.int32)
    query_pos = jnp.concatenate([query_first + tokens, (N_SP - 1 - sp_index) * tok_dev + tokens])
    query_rot = rotary(
        jnp.concatenate([query_rope, received_rope], axis=0)
        .astype(jnp.float32)
        .reshape(2 * tok_dev, HEADS_HERE, QK_ROPE),
        query_pos,
    ).astype(jnp.bfloat16)
    rot = jnp.swapaxes(query_rot.reshape(GROUPS, ROWS, HEADS_HERE, QK_ROPE), 1, 2)
    rot = rot.reshape(GROUPS, QROWS, QK_ROPE)
    none = jnp.zeros_like(rot)
    late = (jnp.arange(QROWS) % ROWS) // SEGMENT
    marks = (late[:, None] == jnp.arange(128)[None, :]).astype(jnp.bfloat16)
    marks = jnp.broadcast_to(marks[None], (GROUPS, QROWS, 128))
    q4 = jnp.stack(
        [jnp.concatenate([rot, none, marks], axis=-1), jnp.concatenate([none, rot, marks], axis=-1)], axis=1
    )
    qn = jnp.concatenate([query_nope, received_nope], axis=0).reshape(GROUPS, ROWS, -1)

    both, qn, q4 = lax.optimization_barrier((both, qn, q4))
    own_parts = [both]
    for by in SHIFTS[1:]:
        own_parts.append(lax.ppermute(both, AXES, shift_pairs(1, by)))
    pieces = (own_parts, [lax.ppermute(part, "tp", swap) for part in own_parts])

    state = ()
    for call in range(len(CALLS)):
        table = lax.dynamic_index_in_dim(
            jnp.asarray(work_table(call)[1]), sp_index * N_TP + tp_index, 0, keepdims=False
        )
        operands = (qn, key_up, q4) if call == 0 else (q4, qabs, *state)
        if call == len(CALLS) - 1:
            operands = (*operands, value_up)
        state = attention(call, table, operands, [pieces[own][k3] for own, k3 in CALLS[call]])
        if call == 0:
            qabs, *state = state
    attn = state[0]
    mirror_same = lax.ppermute(attn[2], AXES, mirror)
    mirror_cross = lax.ppermute(attn[3], AXES, crossing)
    swapped = lax.ppermute(attn[1], "tp", swap)
    messages = (attn[0], mirror_same, swapped, mirror_cross)

    flat = routes.reshape(-1)
    order = jnp.arange(flat.shape[0], dtype=jnp.int32)
    earlier = (flat[:, None] == flat[None, :]) & (order[None, :] < order[:, None])
    rank = jnp.sum(earlier.astype(jnp.int32), axis=1)
    slots = (flat * CAP + rank).reshape(routes.shape)

    hidden, outgoing = project(
        tp_index.reshape(1).astype(jnp.int32), messages, out_proj, residual, norm_gain[None, :], slots.T
    )
    width = residual.shape[1]
    arrived = lax.all_to_all(
        outgoing.reshape(N_SP, CAP, width), "sp", split_axis=0, concat_axis=0, tiled=True
    ).reshape(N_SP * CAP, width)
    own = (w_gate[0], w_up[0], w_down[0])
    other = tuple(lax.ppermute(w, "tp", swap) for w in own)
    produced = experts(arrived, own, other)
    back = lax.all_to_all(
        produced.reshape(N_SP, CAP, width), "sp", split_axis=0, concat_axis=0, tiled=True
    ).reshape(N_SP * CAP, width)
    return combine(back, hidden, slots, route_weight)


def solution(mesh):
    return jax.shard_map(
        local,
        mesh=mesh,
        in_specs=(
            P(("sp", "tp"), None),
            P("sp", "tp"),
            P("sp", "tp"),
            P(("sp", "tp"), None),
            P(("sp", "tp"), None),
            P(None, "tp"),
            P(None, "tp"),
            P(),
            P(),
            P(("sp", "tp"), None),
            P(("sp", "tp"), None),
            P("sp", None, "tp"),
            P("sp", None, "tp"),
            P("sp", "tp", None),
        ),
        out_specs=P(("sp", "tp"), None),
        check_vma=False,
    )
```

time: 202 us -> 191 us (0.946)
  waiting for transfers between devices: 91.2 us -> 70.6 us
  local copies, waits for them, and re-layouts: 23.7 us -> 9.29 us
  starting transfers between devices: 41.9 us -> 55.6 us
  Pallas kernels: 39.8 us -> 48.4 us
    ppermute x8 -> x9, waiting for transfers between devices: 14.5 us -> 0.27 us  [the longest x3 0.25 us: local(): own_parts.append(lax.ppermute(both, AXES, shift_pairs(1, by)))]
    unnamed x49 -> x29, local copies, waits for them, and re-layouts: 17.9 us -> 4.68 us
    ppermute x8 -> x9, starting transfers between devices: 12.2 us -> 24.3 us  [the longest x4 13.6 us: local(): pieces = (own_parts, [lax.ppermute(part, 'tp', swap) for part in own_parts])]
    pallas_call x3 -> x5, Pallas kernels: 38.2 us -> 46.8 us  [the longest x3 34.1 us: attention(): pl.pallas_call(functools.partial(attention_body, call, steps, len(parts))...]
    ppermute x3, waiting for transfers between devices: 10 us -> 6.69 us  [local(): lax.ppermute(both, AXES, shift_pairs(0, by))]
    squeeze x0 -> x3, local copies, waits for them, and re-layouts: none -> 2.07 us  [local(): lax.dynamic_index_in_dim(jnp.asarray(work_table(call)[1]), sp_index * N_T...]
  transfers between devices with their start and end apart: 21 -> 22, of which waited for: 12 -> 9; matrix products, arithmetic and copies ran while one was open for 4% -> 5% of each run, Pallas kernels for 0% -> 12%
where the time goes in v3:
time: 191 us; the launch traced here: 189 us
  waiting for transfers between devices  70.6 us (37%)
  starting transfers between devices  55.6 us (29%)
  Pallas kernels  48.4 us (25%)
  local copies, waits for them, and re-layouts  9.29 us (5%)
  other arithmetic  4.48 us (2%)
    pallas_call x3, Pallas kernels, attention(): pl.pallas_call(functools.partial(attention_body, call, steps, len(parts))...  34.1 us
    all_to_all x1, waiting for transfers between devices, local(): lax.all_to_all(produced.reshape(N_SP, CAP, width), 'sp', split_axis=0, co...  28.3 us
    all_to_all x1, waiting for transfers between devices, local(): lax.all_to_all(outgoing.reshape(N_SP, CAP, width), 'sp', split_axis=0, co...  23.5 us
    ppermute x4, starting transfers between devices, local(): pieces = (own_parts, [lax.ppermute(part, 'tp', swap) for part in own_parts])  13.6 us
    pallas_call x1, Pallas kernels, experts(): pl.pallas_call(experts_body, out_shape=pltpu.HBM((count, width), jnp.bflo...  7.84 us
    ppermute x1, starting transfers between devices, local(): far = lax.ppermute(shard, AXES, plane_pairs(Z_SECOND))  6.87 us
    ppermute x3, waiting for transfers between devices, local(): lax.ppermute(both, AXES, shift_pairs(0, by))  6.69 us
    all_to_all x1, starting transfers between devices, local(): lax.all_to_all(produced.reshape(N_SP, CAP, width), 'sp', split_axis=0, co...  6.08 us
  transfers between devices with their start and end apart: 22, of which 9 were waited for; matrix products, arithmetic and copies ran while one was open for 5% of the time, Pallas kernels for 12%

profile of v3, /device:TPU:1, one launch (start us, length us, event | category | flops | bytes accessed | tf_op | source)
XLA Modules:
  0.0 188.8 jit_solution(7859888240354928875)
XLA Ops:
  0.0 0.8 copy.44
  0.9 0.3 fusion.17
  1.3 0.9 fusion.15
  2.2 6.9 %collective-permute-start = (bf16[160,256]{1,0:T(8,128)(2,1)S(1)}, bf16[160,256]{1,0:T(8,128)(2,1)S(1)}, u32[]{:S(2)}, u32[]{:S(2)}) collective-permute-start(bf16[160,256]{1,0:T(8,128)(2,1)S(1)} %fusion.15), channel_id=1, source_target_pairs={{64,1},{66,3},{68,5},{70,7},{72,9},{74,11},{76,13},{78,15},{80,17}... | collective-permute-start | bytes 245768 | tf_op jit(solution)/shard_map/ppermute | solution.py:551
  9.2 1.0 copy.46
  10.2 5.0 %collective-permute-start.6 = (bf16[256,256]{0,1:T(8,128)(2,1)S(1)}, bf16[256,256]{0,1:T(8,128)(2,1)S(1)}, u32[]{:S(2)}, u32[]{:S(2)}) collective-permute-start(bf16[256,256]{0,1:T(8,128)(2,1)S(1)} %copy.46), channel_id=1, source_target_pairs={{0,126},{1,127},{2,124},{3,125},{4,122},{5,123},{6,120},{7,121},{8... | collective-permute-start | bytes 393224 | tf_op jit(solution)/shard_map/ppermute | solution.py:548
  15.2 2.0 %collective-permute-start.5 = (bf16[256,512]{1,0:T(8,128)(2,1)}, bf16[256,512]{1,0:T(8,128)(2,1)}, u32[]{:S(2)}, u32[]{:S(2)}) collective-permute-start(bf16[256,512]{1,0:T(8,128)(2,1)} %param.18), channel_id=1, source_target_pairs={{0,126},{1,127},{2,124},{3,125},{4,122},{5,123},{6,120},{7,121},{8... | collective-permute-start | bytes 786440 | tf_op jit(solution)/shard_map/ppermute | solution.py:547
  17.2 0.3 multiply_cosine_fusion
  17.8 2.7 %collective-permute-start.3 = (bf16[320,256]{1,0:T(8,128)(2,1)S(1)}, bf16[320,256]{1,0:T(8,128)(2,1)S(1)}, u32[]{:S(2)}, u32[]{:S(2)}) collective-permute-start(bf16[320,256]{1,0:T(8,128)(2,1)S(1)} %pad_maximum_fusion.4), channel_id=1, source_target_pairs={{0,24},{1,7},{2,26},{3,1},{4,28},{5,3},{6,30},{7,5},{8,0},{9,15},{... | collective-permute-start | bytes 491528 | tf_op jit(solution)/shard_map/ppermute | solution.py:554
  20.5 1.0 collective-permute-start.4
  21.9 0.3 copy.48
  22.4 0.9 fusion
  23.6 6.7 %collective-permute-done.2 = bf16[320,256]{1,0:T(8,128)(2,1)} collective-permute-done((bf16[320,256]{1,0:T(8,128)(2,1)S(1)}, bf16[320,256]{1,0:T(8,128)(2,1)}, u32[]{:S(2)}, u32[]{:S(2)}) %collective-permute-start.2) | collective-permute-done | bytes 163872 | tf_op jit(solution)/shard_map/ppermute | solution.py:554
  30.2 0.9 constant_dynamic-update-slice_fusion.2
  31.2 1.0 pad_maximum_fusion.3
  32.4 2.6 %collective-permute-start.9 = (bf16[1280,256]{1,0:T(8,128)(2,1)S(1)}, bf16[1280,256]{1,0:T(8,128)(2,1)}, u32[]{:S(2)}, u32[]{:S(2)}) collective-permute-start(bf16[1280,256]{1,0:T(8,128)(2,1)S(1)} %constant_dynamic-update-slice_fusion.rest_3_), channel_id=1, source_target_pairs={{0,6},{1,25},{2,0},{3,27},{4,2},{5,29},{6,4},{7,31},{8,14},{9,1},{... | collective-permute-start | bytes 1966088 | tf_op jit(solution)/shard_map/ppermute | solution.py:579
  35.0 1.0 collective-permute-start.10
  36.0 2.4 %collective-permute-start.7 = (bf16[1280,256]{1,0:T(8,128)(2,1)S(1)}, bf16[1280,256]{1,0:T(8,128)(2,1)}, u32[]{:S(2)}, u32[]{:S(2)}) collective-permute-start(bf16[1280,256]{1,0:T(8,128)(2,1)S(1)} %constant_dynamic-update-slice_fusion.rest_3_), channel_id=1, source_target_pairs={{0,1},{1,0},{2,3},{3,2},{4,5},{5,4},{6,7},{7,6},{8,9},{9,8},{10,11... | collective-permute-start | bytes 1966088 | tf_op jit(solution)/shard_map/ppermute | solution.py:580
  38.4 0.7 copy.50
  39.1 1.0 eq.51
  40.3 0.8 reduce_sum.12
  41.0 0.7 fusion.30.table
  41.7 0.7 fusion.31.table
  42.4 0.7 fusion.29.table
  43.1 0.2 collective-permute-done.8.rest_5_
  43.4 10.7 %collective-permute-start.11 = (bf16[1280,256]{1,0:T(8,128)(2,1)}, bf16[1280,256]{1,0:T(8,128)(2,1)S(1)}, u32[]{:S(2)}, u32[]{:S(2)}) collective-permute-start(bf16[1280,256]{1,0:T(8,128)(2,1)} %collective-permute-done.8.rest_5_), channel_id=1, source_target_pairs={{0,1},{1,0},{2,3},{3,2},{4,5},{5,4},{6,7},{7,6},{8,9},{9,8},{10,11... | collective-permute-start | bytes 1966088 | tf_op jit(solution)/shard_map/ppermute | solution.py:580
  54.0 0.5 collective-permute-start.13
  54.6 9.7 %shard_map.163 = (bf16[4,512,256]{2,1,0:T(8,128)(2,1)S(1)}, f32[4,512,128]{2,1,0:T(8,128)S(1)}, f32[4,512,128]{2,1,0:T(8,128)S(1)}, f32[4,512,256]{2,1,0:T(8,128)S(1)}) custom-call(s32[84]{0:T(128)S(1)} %fusion.30.table, bf16[4,128,512]{2,1,0:T(8,128)(2,1)S(1)} %bitcast.43, bf16[256,512]{1,0:T(8,128)(2,1)S(1)} %copy-done.2, ...), custom_call_target="tpu_custom_call" | custom-call | flops 4429185024 | bytes 1048576 | tf_op jit(solution)/shard_map/pallas_call | solution.py:290
  64.3 12.3 %shard_map.164 = (f32[4,512,128]{2,1,0:T(8,128)S(1)}, f32[4,512,128]{2,1,0:T(8,128)S(1)}, f32[4,512,256]{2,1,0:T(8,128)S(1)}) custom-call(s32[112]{0:T(128)S(1)} %fusion.31.table, bf16[4,2,512,256]{3,2,1,0:T(8,128)(2,1)S(1)} %pad_maximum_fusion.rest_2_.rest_0_, bf16[4,512,256]{2,1,0:T(8,128)(2,1)S(1)} %get-tuple-element.20.rest_1_, ...), custom_call_target="tpu_custom_call" | custom-call | flops 6039797760 | bytes 1048576 | tf_op jit(solution)/shard_map/pallas_call | solution.py:290
  76.7 12.1 %shard_map.165 = bf16[4,128,640]{2,1,0:T(8,128)(2,1)S(1)} custom-call(s32[112]{0:T(128)S(1)} %fusion.29.table, bf16[4,2,512,256]{3,2,1,0:T(8,128)(2,1)S(1)} %pad_maximum_fusion.rest_2_.rest_0_, bf16[4,512,256]{2,1,0:T(8,128)(2,1)S(1)} %get-tuple-element.20.rest_1_, f32[4,512,128]{2,1,0:T(8,128)S(1)} %get-tuple-element.24.rest_2_, ...), custom_call_target="tpu_custom_call" | custom-call | flops 6039797760 | bytes 1048576 | tf_op jit(solution)/shard_map/pallas_call | solution.py:290
  88.8 3.4 %collective-permute-start.14 = (bf16[128,640]{1,0:T(8,128)(2,1)S(1)}, bf16[128,640]{1,0:T(8,128)(2,1)S(1)}, u32[]{:S(2)}, u32[]{:S(2)}) collective-permute-start(bf16[128,640]{1,0:T(8,128)(2,1)S(1)} %get-tuple-element.35), channel_id=1, source_target_pairs={{0,126},{1,127},{2,124},{3,125},{4,122},{5,123},{6,120},{7,121},{8... | collective-permute-start | bytes 491528 | tf_op jit(solution)/shard_map/ppermute | solution.py:594
  92.3 0.8 collective-permute-start.15
  93.0 3.2 %collective-permute-start.16 = (bf16[128,640]{1,0:T(8,128)(2,1)S(1)}, bf16[128,640]{1,0:T(8,128)(2,1)S(1)}, u32[]{:S(2)}, u32[]{:S(2)}) collective-permute-start(bf16[128,640]{1,0:T(8,128)(2,1)S(1)} %get-tuple-element.33), channel_id=1, source_target_pairs={{0,127},{1,126},{2,125},{3,124},{4,123},{5,122},{6,121},{7,120},{8... | collective-permute-start | bytes 491528 | tf_op jit(solution)/shard_map/ppermute | solution.py:595
  96.4 3.4 %collective-permute-done.14.mirror_same = bf16[128,640]{1,0:T(8,128)(2,1)S(1)} collective-permute-done((bf16[128,640]{1,0:T(8,128)(2,1)S(1)}, bf16[128,640]{1,0:T(8,128)(2,1)S(1)}, u32[]{:S(2)}, u32[]{:S(2)}) %collective-permute-start.14) | collective-permute-done | bytes 163872 | tf_op jit(solution)/shard_map/ppermute | solution.py:594
  99.8 4.4 %collective-permute-done.16.mirror_cross = bf16[128,640]{1,0:T(8,128)(2,1)S(1)} collective-permute-done((bf16[128,640]{1,0:T(8,128)(2,1)S(1)}, bf16[128,640]{1,0:T(8,128)(2,1)S(1)}, u32[]{:S(2)}, u32[]{:S(2)}) %collective-permute-start.16) | collective-permute-done | bytes 163872 | tf_op jit(solution)/shard_map/ppermute | solution.py:595
  104.3 4.9 %project.1 = (bf16[128,2048]{1,0:T(8,128)(2,1)}, bf16[512,2048]{1,0:T(8,128)(2,1)}) custom-call(s32[1]{0:T(128)} %bitcast.core, bf16[128,640]{1,0:T(8,128)(2,1)S(1)} %get-tuple-element.36.local_part, bf16[128,640]{1,0:T(8,128)(2,1)S(1)} %collective-permute-done.14.mirror_same, bf16[128,640]{1,0:T(8,128)(2,1)S(1)} %collective-permute-done.15.swapped, ...), custom_call_target="tpu_custom_call" | custom-call | tf_op jit(solution)/shard_map/project/pallas_call | solution.py:391
  109.2 6.0 %all-to-all-start = ((bf16[64,8,2048]{2,1,0:T(8,128)(2,1)}), bf16[64,8,2048]{2,1,0:T(8,128)(2,1)S(1)}, u32[]{:S(2)}, u32[]{:S(2)}) async-start(bf16[64,8,2048]{2,1,0:T(8,128)(2,1)} %bitcast.47), calls=%async_computation | async-start | bytes 4194304 | tf_op jit(solution)/shard_map/all_to_all | solution.py:609
  115.2 0.6 collective-permute-start.17
  116.0 0.3 collective-permute-start.19
  116.3 1.9 collective-permute-done.17.rest_3_
  118.2 1.5 collective-permute-done.18.rest_4_
  119.7 1.0 copy-done.6
  120.7 0.6 collective-permute-done.19.rest_5_
  121.3 23.5 %all-to-all-done = bf16[64,8,2048]{2,1,0:T(8,128)(2,1)S(1)} async-done(((bf16[64,8,2048]{2,1,0:T(8,128)(2,1)}), bf16[64,8,2048]{2,1,0:T(8,128)(2,1)S(1)}, u32[]{:S(2)}, u32[]{:S(2)}) %all-to-all-start) | async-done | bytes 2097184 | tf_op jit(solution)/shard_map/all_to_all | solution.py:609
  144.8 7.8 %experts.1 = bf16[512,2048]{1,0:T(8,128)(2,1)} custom-call(bf16[512,2048]{1,0:T(8,128)(2,1)S(1)} %bitcast.40, bf16[2048,256]{1,0:T(8,128)(2,1)} %bitcast.48, bf16[2048,256]{1,0:T(8,128)(2,1)} %bitcast.51, bf16[256,2048]{1,0:T(8,128)(2,1)} %bitcast.53, bf16[2048,256]{1,0:T(8,128)(2,1)} %copy-done.5, bf16[2048,256]{1,0:T(8,128)(2,1)} %copy-done.6, ...), custom_call_target="tpu_custom_call" | custom-call | tf_op jit(solution)/shard_map/experts/pallas_call | solution.py:455
  152.7 6.1 %all-to-all-start.1 = ((bf16[64,8,2048]{2,1,0:T(8,128)(2,1)}), bf16[64,8,2048]{2,1,0:T(8,128)(2,1)S(1)}, u32[]{:S(2)}, u32[]{:S(2)}) async-start(bf16[64,8,2048]{2,1,0:T(8,128)(2,1)} %bitcast.45), calls=%async_computation.1 | async-start | bytes 4194304 | tf_op jit(solution)/shard_map/all_to_all | solution.py:615
  158.9 28.3 %all-to-all-done.1 = bf16[64,8,2048]{2,1,0:T(8,128)(2,1)S(1)} async-done(((bf16[64,8,2048]{2,1,0:T(8,128)(2,1)}), bf16[64,8,2048]{2,1,0:T(8,128)(2,1)S(1)}, u32[]{:S(2)}, u32[]{:S(2)}) %all-to-all-start.1) | async-done | bytes 2097184 | tf_op jit(solution)/shard_map/all_to_all | solution.py:615
  187.2 1.6 combine.1
  (67 shorter events, 2.2 us)
Async XLA Ops:
  2.2 15.5 %collective-permute-start = (bf16[160,256]{1,0:T(8,128)(2,1)S(1)}, bf16[160,256]{1,0:T(8,128)(2,1)S(1)}, u32[]{:S(2)}, u32[]{:S(2)}) collective-permute-start(bf16[160,256]{1,0:T(8,128)(2,1)S(1)} %fusion.15), channel_id=1, source_target_pairs={{64,1},{66,3},{68,5},{70,7},{72,9},{74,11},{76,13},{78,15},{80,17}... | collective-permute-start | bytes 245768 | tf_op jit(solution)/shard_map/ppermute | solution.py:551
  9.1 8.6 %collective-permute-start.1 = (bf16[160,256]{1,0:T(8,128)(2,1)S(1)}, bf16[160,256]{1,0:T(8,128)(2,1)S(1)}, u32[]{:S(2)}, u32[]{:S(2)}) collective-permute-start(bf16[160,256]{1,0:T(8,128)(2,1)S(1)} %fusion.15), channel_id=1, source_target_pairs={{96,0},{98,2},{100,4},{102,6},{104,8},{106,10},{108,12},{110,14},{... | collective-permute-start | bytes 245768 | tf_op jit(solution)/shard_map/ppermute | solution.py:550
  10.2 11.3 %collective-permute-start.6 = (bf16[256,256]{0,1:T(8,128)(2,1)S(1)}, bf16[256,256]{0,1:T(8,128)(2,1)S(1)}, u32[]{:S(2)}, u32[]{:S(2)}) collective-permute-start(bf16[256,256]{0,1:T(8,128)(2,1)S(1)} %copy.46), channel_id=1, source_target_pairs={{0,126},{1,127},{2,124},{3,125},{4,122},{5,123},{6,120},{7,121},{8... | collective-permute-start | bytes 393224 | tf_op jit(solution)/shard_map/ppermute | solution.py:548
  15.2 16.0 %collective-permute-start.5 = (bf16[256,512]{1,0:T(8,128)(2,1)}, bf16[256,512]{1,0:T(8,128)(2,1)}, u32[]{:S(2)}, u32[]{:S(2)}) collective-permute-start(bf16[256,512]{1,0:T(8,128)(2,1)} %param.18), channel_id=1, source_target_pairs={{0,126},{1,127},{2,124},{3,125},{4,122},{5,123},{6,120},{7,121},{8... | collective-permute-start | bytes 786440 | tf_op jit(solution)/shard_map/ppermute | solution.py:547
  17.7 12.5 %collective-permute-start.2 = (bf16[320,256]{1,0:T(8,128)(2,1)S(1)}, bf16[320,256]{1,0:T(8,128)(2,1)}, u32[]{:S(2)}, u32[]{:S(2)}) collective-permute-start(bf16[320,256]{1,0:T(8,128)(2,1)S(1)} %pad_maximum_fusion.4), channel_id=1, source_target_pairs={{0,8},{1,3},{2,10},{3,5},{4,12},{5,7},{6,14},{7,1},{8,16},{9,11},{... | collective-permute-start | bytes 491528 | tf_op jit(solution)/shard_map/ppermute | solution.py:554
  17.8 13.3 %collective-permute-start.3 = (bf16[320,256]{1,0:T(8,128)(2,1)S(1)}, bf16[320,256]{1,0:T(8,128)(2,1)S(1)}, u32[]{:S(2)}, u32[]{:S(2)}) collective-permute-start(bf16[320,256]{1,0:T(8,128)(2,1)S(1)} %pad_maximum_fusion.4), channel_id=1, source_target_pairs={{0,24},{1,7},{2,26},{3,1},{4,28},{5,3},{6,30},{7,5},{8,0},{9,15},{... | collective-permute-start | bytes 491528 | tf_op jit(solution)/shard_map/ppermute | solution.py:554
  20.5 10.7 %collective-permute-start.4 = (bf16[320,256]{1,0:T(8,128)(2,1)S(1)}, bf16[320,256]{1,0:T(8,128)(2,1)S(1)}, u32[]{:S(2)}, u32[]{:S(2)}) collective-permute-start(bf16[320,256]{1,0:T(8,128)(2,1)S(1)} %pad_maximum_fusion.4), channel_id=1, source_target_pairs={{0,16},{1,5},{2,18},{3,7},{4,20},{5,1},{6,22},{7,3},{8,24},{9,13},... | collective-permute-start | bytes 491528 | tf_op jit(solution)/shard_map/ppermute | solution.py:554
  23.3 7.9 %copy-start.8 = (bf16[256,512]{1,0:T(8,128)(2,1)S(1)}, bf16[256,512]{1,0:T(8,128)(2,1)}, u32[]{:S(2)}) copy-start(bf16[256,512]{1,0:T(8,128)(2,1)} %param.18) | copy-start | bytes 786436
  23.3 15.0 %copy-start.9 = (s32[128,2]{0,1:T(2,128)S(1)}, s32[128,2]{0,1:T(2,128)}, u32[]{:S(2)}) copy-start(s32[128,2]{0,1:T(2,128)} %param.26) | copy-start | bytes 3076
  23.5 31.0 %copy-start.2 = (bf16[256,512]{1,0:T(8,128)(2,1)S(1)}, bf16[256,512]{1,0:T(8,128)(2,1)}, u32[]{:S(2)}) copy-start(bf16[256,512]{1,0:T(8,128)(2,1)} %rest_1_.1) | copy-start | bytes 786436
  32.2 11.1 %collective-permute-start.8 = (bf16[1280,256]{1,0:T(8,128)(2,1)S(1)}, bf16[1280,256]{1,0:T(8,128)(2,1)}, u32[]{:S(2)}, u32[]{:S(2)}) collective-permute-start(bf16[1280,256]{1,0:T(8,128)(2,1)S(1)} %constant_dynamic-update-slice_fusion.rest_3_), channel_id=1, source_target_pairs={{0,2},{1,9},{2,4},{3,11},{4,6},{5,13},{6,0},{7,15},{8,10},{9,17},{... | collective-permute-start | bytes 1966088 | tf_op jit(solution)/shard_map/ppermute | solution.py:579
  32.4 21.6 %collective-permute-start.9 = (bf16[1280,256]{1,0:T(8,128)(2,1)S(1)}, bf16[1280,256]{1,0:T(8,128)(2,1)}, u32[]{:S(2)}, u32[]{:S(2)}) collective-permute-start(bf16[1280,256]{1,0:T(8,128)(2,1)S(1)} %constant_dynamic-update-slice_fusion.rest_3_), channel_id=1, source_target_pairs={{0,6},{1,25},{2,0},{3,27},{4,2},{5,29},{6,4},{7,31},{8,14},{9,1},{... | collective-permute-start | bytes 1966088 | tf_op jit(solution)/shard_map/ppermute | solution.py:579
  35.0 19.1 %collective-permute-start.10 = (bf16[1280,256]{1,0:T(8,128)(2,1)S(1)}, bf16[1280,256]{1,0:T(8,128)(2,1)}, u32[]{:S(2)}, u32[]{:S(2)}) collective-permute-start(bf16[1280,256]{1,0:T(8,128)(2,1)S(1)} %constant_dynamic-update-slice_fusion.rest_3_), channel_id=1, source_target_pairs={{0,4},{1,17},{2,6},{3,19},{4,0},{5,21},{6,2},{7,23},{8,12},{9,25},... | collective-permute-start | bytes 1966088 | tf_op jit(solution)/shard_map/ppermute | solution.py:579
  36.0 18.6 %collective-permute-start.7 = (bf16[1280,256]{1,0:T(8,128)(2,1)S(1)}, bf16[1280,256]{1,0:T(8,128)(2,1)}, u32[]{:S(2)}, u32[]{:S(2)}) collective-permute-start(bf16[1280,256]{1,0:T(8,128)(2,1)S(1)} %constant_dynamic-update-slice_fusion.rest_3_), channel_id=1, source_target_pairs={{0,1},{1,0},{2,3},{3,2},{4,5},{5,4},{6,7},{7,6},{8,9},{9,8},{10,11... | collective-permute-start | bytes 1966088 | tf_op jit(solution)/shard_map/ppermute | solution.py:580
  43.4 33.3 %collective-permute-start.11 = (bf16[1280,256]{1,0:T(8,128)(2,1)}, bf16[1280,256]{1,0:T(8,128)(2,1)S(1)}, u32[]{:S(2)}, u32[]{:S(2)}) collective-permute-start(bf16[1280,256]{1,0:T(8,128)(2,1)} %collective-permute-done.8.rest_5_), channel_id=1, source_target_pairs={{0,1},{1,0},{2,3},{3,2},{4,5},{5,4},{6,7},{7,6},{8,9},{9,8},{10,11... | collective-permute-start | bytes 1966088 | tf_op jit(solution)/shard_map/ppermute | solution.py:580
  54.0 22.6 %collective-permute-start.12 = (bf16[1280,256]{1,0:T(8,128)(2,1)}, bf16[1280,256]{1,0:T(8,128)(2,1)S(1)}, u32[]{:S(2)}, u32[]{:S(2)}) collective-permute-start(bf16[1280,256]{1,0:T(8,128)(2,1)} %collective-permute-done.9.rest_6_), channel_id=1, source_target_pairs={{0,1},{1,0},{2,3},{3,2},{4,5},{5,4},{6,7},{7,6},{8,9},{9,8},{10,11... | collective-permute-start | bytes 1966088 | tf_op jit(solution)/shard_map/ppermute | solution.py:580
  54.0 22.6 %collective-permute-start.13 = (bf16[1280,256]{1,0:T(8,128)(2,1)}, bf16[1280,256]{1,0:T(8,128)(2,1)S(1)}, u32[]{:S(2)}, u32[]{:S(2)}) collective-permute-start(bf16[1280,256]{1,0:T(8,128)(2,1)} %collective-permute-done.10.rest_7_), channel_id=1, source_target_pairs={{0,1},{1,0},{2,3},{3,2},{4,5},{5,4},{6,7},{7,6},{8,9},{9,8},{10,11... | collective-permute-start | bytes 1966088 | tf_op jit(solution)/shard_map/ppermute | solution.py:580
  64.2 12.4 %copy-start.3 = (bf16[256,512]{1,0:T(8,128)(2,1)S(1)}, bf16[256,512]{1,0:T(8,128)(2,1)}, u32[]{:S(2)}) copy-start(bf16[256,512]{1,0:T(8,128)(2,1)} %rest_5_.1) | copy-start | bytes 786436
  76.7 19.7 %copy-start.7 = (s32[128,2]{1,0:T(8,128)S(1)}, s32[128,2]{1,0:T(8,128)}, u32[]{:S(2)}) copy-start(s32[128,2]{1,0:T(8,128)} %reduce_sum.12) | copy-start | bytes 3076
  76.7 27.6 %copy-start.1 = (f32[2048]{0:T(1024)S(1)}, f32[2048]{0:T(1024)}, u32[]{:S(2)}) copy-start(f32[2048]{0:T(1024)} %param.25) | copy-start | bytes 24580
  88.8 11.0 %collective-permute-start.14 = (bf16[128,640]{1,0:T(8,128)(2,1)S(1)}, bf16[128,640]{1,0:T(8,128)(2,1)S(1)}, u32[]{:S(2)}, u32[]{:S(2)}) collective-permute-start(bf16[128,640]{1,0:T(8,128)(2,1)S(1)} %get-tuple-element.35), channel_id=1, source_target_pairs={{0,126},{1,127},{2,124},{3,125},{4,122},{5,123},{6,120},{7,121},{8... | collective-permute-start | bytes 491528 | tf_op jit(solution)/shard_map/ppermute | solution.py:594
  92.3 7.6 %collective-permute-start.15 = (bf16[128,640]{1,0:T(8,128)(2,1)S(1)}, bf16[128,640]{1,0:T(8,128)(2,1)S(1)}, u32[]{:S(2)}, u32[]{:S(2)}) collective-permute-start(bf16[128,640]{1,0:T(8,128)(2,1)S(1)} %get-tuple-element.34), channel_id=1, source_target_pairs={{0,1},{1,0},{2,3},{3,2},{4,5},{5,4},{6,7},{7,6},{8,9},{9,8},{10,11... | collective-permute-start | bytes 491528 | tf_op jit(solution)/shard_map/ppermute | solution.py:596
  93.0 11.2 %collective-permute-start.16 = (bf16[128,640]{1,0:T(8,128)(2,1)S(1)}, bf16[128,640]{1,0:T(8,128)(2,1)S(1)}, u32[]{:S(2)}, u32[]{:S(2)}) collective-permute-start(bf16[128,640]{1,0:T(8,128)(2,1)S(1)} %get-tuple-element.33), channel_id=1, source_target_pairs={{0,127},{1,126},{2,125},{3,124},{4,123},{5,122},{6,121},{7,120},{8... | collective-permute-start | bytes 491528 | tf_op jit(solution)/shard_map/ppermute | solution.py:595
  109.1 6.0 %copy-start.4 = (bf16[1,2048,256]{2,1,0:T(8,128)(2,1)S(1)}, bf16[1,2048,256]{2,1,0:T(8,128)(2,1)}, u32[]{:S(2)}) copy-start(bf16[1,2048,256]{2,1,0:T(8,128)(2,1)} %param.28) | copy-start | bytes 3145732
  109.2 35.7 %all-to-all-start = ((bf16[64,8,2048]{2,1,0:T(8,128)(2,1)}), bf16[64,8,2048]{2,1,0:T(8,128)(2,1)S(1)}, u32[]{:S(2)}, u32[]{:S(2)}) async-start(bf16[64,8,2048]{2,1,0:T(8,128)(2,1)} %bitcast.47), calls=%async_computation | async-start | bytes 4194304 | tf_op jit(solution)/shard_map/all_to_all | solution.py:609
  115.2 3.0 %collective-permute-start.17 = (bf16[2048,256]{1,0:T(8,128)(2,1)S(1)}, bf16[2048,256]{1,0:T(8,128)(2,1)S(1)}, u32[]{:S(2)}, u32[]{:S(2)}) collective-permute-start(bf16[2048,256]{1,0:T(8,128)(2,1)S(1)} %bitcast.49), channel_id=1, source_target_pairs={{0,1},{1,0},{2,3},{3,2},{4,5},{5,4},{6,7},{7,6},{8,9},{9,8},{10,11... | collective-permute-start | bytes 3145736 | tf_op jit(solution)/shard_map/ppermute | solution.py:613
  115.8 3.9 %collective-permute-start.18 = (bf16[2048,256]{1,0:T(8,128)(2,1)}, bf16[2048,256]{1,0:T(8,128)(2,1)S(1)}, u32[]{:S(2)}, u32[]{:S(2)}) collective-permute-start(bf16[2048,256]{1,0:T(8,128)(2,1)} %bitcast.50), channel_id=1, source_target_pairs={{0,1},{1,0},{2,3},{3,2},{4,5},{5,4},{6,7},{7,6},{8,9},{9,8},{10,11... | collective-permute-start | bytes 3145736 | tf_op jit(solution)/shard_map/ppermute | solution.py:613
  116.0 5.3 %collective-permute-start.19 = (bf16[256,2048]{1,0:T(8,128)(2,1)}, bf16[256,2048]{1,0:T(8,128)(2,1)}, u32[]{:S(2)}, u32[]{:S(2)}) collective-permute-start(bf16[256,2048]{1,0:T(8,128)(2,1)} %bitcast.52), channel_id=1, source_target_pairs={{0,1},{1,0},{2,3},{3,2},{4,5},{5,4},{6,7},{7,6},{8,9},{9,8},{10,11... | collective-permute-start | bytes 3145736 | tf_op jit(solution)/shard_map/ppermute | solution.py:613
  118.2 1.5 copy-start.5
  119.7 1.0 copy-start.6
  152.7 6.1 %copy-start.10 = (f32[128,2]{0,1:T(2,128)S(1)}, f32[128,2]{0,1:T(2,128)}, u32[]{:S(2)}) copy-start(f32[128,2]{0,1:T(2,128)} %param.27) | copy-start | bytes 3076
  152.7 34.5 %copy-start = (bf16[128,2048]{1,0:T(8,128)(2,1)S(1)}, bf16[128,2048]{1,0:T(8,128)(2,1)}, u32[]{:S(2)}) copy-start(bf16[128,2048]{1,0:T(8,128)(2,1)} %get-tuple-element.28.hidden) | copy-start | bytes 1572868
  152.7 34.5 %all-to-all-start.1 = ((bf16[64,8,2048]{2,1,0:T(8,128)(2,1)}), bf16[64,8,2048]{2,1,0:T(8,128)(2,1)S(1)}, u32[]{:S(2)}, u32[]{:S(2)}) async-start(bf16[64,8,2048]{2,1,0:T(8,128)(2,1)} %bitcast.45), calls=%async_computation.1 | async-start | bytes 4194304 | tf_op jit(solution)/shard_map/all_to_all | solution.py:615

commit v4 on v3

--- a/solution.py
+++ b/solution.py
@@ -36,6 +36,7 @@
 GROUPS = 4
 CHUNK = 64
 MESSAGE = HEADS_HERE * V_DIM + 128
+EARLY = 1024
 
 
 def moved(s, dim, by):
@@ -105,7 +106,6 @@
                     rows.append([group, bits, t] + part)
             lists.append(rows)
     count = max(len(rows) for rows in lists)
-    count += 1 - count % 2
     everything = (1 << (4 * UNIT)) - 1
     idle = lambda rows, t: rows[-1][:1] + [everything] + rows[-1][2:] if rows else [0, everything, t] + [0] * UNIT
     table = []
@@ -117,80 +117,99 @@
 NT = (((1,), (1,)), ((), ()))
 
 
-def attention_body(call, steps, part_count, table, *rest):
+def attention_body(call, steps, offset, part_count, table, *rest):
     first, last = call == 0, call == len(CALLS) - 1
+    rest = list(rest)
+    take = lambda n: [rest.pop(0) for _ in range(n)]
     if first:
-        qn_ref, key_up_ref, q4_ref = rest[:3]
-        taken = 3
+        own_ref, own_rope_ref, received_ref, key_up_ref, cosine_ref, sine_ref = take(6)
     else:
-        q4_ref, qabs, m_in, l_in, acc_in = rest[:5]
-        taken = 5
+        q4_ref, qabs, _, _, _ = take(5)
     if last:
-        value_up_ref = rest[taken]
-        taken += 1
-    parts = rest[taken : taken + part_count]
-    taken += part_count
+        value_up_ref, out_proj_hbm, residual_hbm = take(3)
+    parts = take(part_count)
+    if last:
+        out_ref, out_proj_ref, residual_ref = take(3)
     if first:
-        qabs, m_ref, l_ref, acc_ref = rest[taken : taken + 4]
-        taken += 4
-    elif last:
-        out_ref, m_ref, l_ref, acc_ref = rest[taken : taken + 4]
-        taken += 4
-    else:
-        m_ref, l_ref, acc_ref = rest[taken : taken + 3]
-        taken += 3
-    keys, s0, s1, p0, p1, shrink0, shrink1, sems = rest[taken:]
+        qabs, q4_ref = take(2)
+    m_ref, l_ref, acc_ref, keys, s0, s1, p0, p1, shrink0, shrink1 = take(10)
+    fetches = []
+    if last:
+        (sems,) = rest
+        early = pl.ds(0, out_proj_ref.shape[1])
+        for n, (source, target) in enumerate(((out_proj_hbm.at[:, early], out_proj_ref), (residual_hbm, residual_ref))):
+            fetch = pltpu.make_async_copy(source, target, sems.at[n])
+            fetch.start()
+            fetches.append(fetch)
     part_rows = parts[0].shape[0]
-    copies = []
     for n in range(part_count):
-        copy = pltpu.make_async_copy(parts[n], keys.at[pl.ds(n * part_rows, part_rows)], sems.at[n])
-        copy.start()
-        copies.append(copy)
+        for k in range(2):
+            keys[k, pl.ds(n * part_rows, part_rows), :] = parts[n][:, pl.ds(k * 128, 128)]
     if first:
         for g in range(GROUPS):
+            source = own_ref if g < 2 else received_ref
             for h in range(HEADS_HERE):
                 cols = pl.ds(h * QK_NOPE, QK_NOPE)
-                qabs[g, pl.ds(h * ROWS, ROWS), :] = lax.dot_general(
-                    qn_ref[g, :, cols], key_up_ref[:, cols], NT, preferred_element_type=jnp.float32
+                latent_query = lax.dot_general(
+                    source[pl.ds((g % 2) * ROWS, ROWS), cols],
+                    key_up_ref[:, cols],
+                    NT,
+                    preferred_element_type=jnp.float32,
                 ).astype(jnp.bfloat16)
+                for k in range(2):
+                    qabs[g, k, pl.ds(h * ROWS, ROWS), :] = latent_query[:, k * 128 : (k + 1) * 128]
+        lane = lax.broadcasted_iota(jnp.int32, (ROWS, 128), 1)
+        for g in range(GROUPS):
+            tokens = pl.ds((g % 2) * ROWS, ROWS)
+            for k in range(2):
+                cols = pl.ds(k * 128, 128)
+                if g < 2:
+                    x = own_rope_ref[tokens, cols]
+                else:
+                    x = received_ref[tokens, pl.ds(HEADS_HERE * QK_NOPE + k * 128, 128)]
+                x = x.astype(jnp.float32)
+                opposite = jnp.where(lane % QK_ROPE < QK_ROPE // 2, pltpu.roll(x, 96, 1), pltpu.roll(x, 32, 1))
+                at = pl.ds(g * ROWS, ROWS)
+                turned = (x * cosine_ref[at, cols] + opposite * sine_ref[at, cols]).astype(jnp.bfloat16).astype(jnp.float32)
+                flipped = pltpu.roll(turned, QK_ROPE, 1)
+                for odd in range(2):
+                    rows = pl.ds((2 * k + odd) * ROWS, ROWS)
+                    for half in range(2):
+                        source = turned if odd == half else flipped
+                        keep = lane < QK_ROPE if half == 0 else lane >= QK_ROPE
+                        q4_ref[g, half, rows, :] = jnp.where(keep, source, 0.0).astype(jnp.bfloat16)
         m_ref[...] = jnp.full(m_ref.shape, NEG_LARGE, jnp.float32)
         l_ref[...] = jnp.zeros(l_ref.shape, jnp.float32)
         acc_ref[...] = jnp.zeros(acc_ref.shape, jnp.float32)
-    else:
-        m_ref[...] = m_in[...]
-        l_ref[...] = l_in[...]
-        acc_ref[...] = acc_in[...]
-    for copy in copies:
-        copy.wait()
 
     cols_per_step = 3 + UNIT
 
     def field(u, n):
-        return table[u * cols_per_step + n]
+        return table[offset + u * cols_per_step + n]
+
+    def wide(at, count):
+        rows = pl.ds(pl.multiple_of(at, 32), count)
+        return jnp.concatenate([keys[k, rows, :] for k in range(2)], axis=1)
 
     def latent_tile(u, half):
-        return jnp.concatenate(
-            [
-                keys[pl.ds(pl.multiple_of(field(u, 3 + j) * SHARD + half * SEGMENT, 32), SEGMENT), :]
-                for j in range(UNIT)
-            ],
-            axis=0,
-        )
+        return jnp.concatenate([wide(field(u, 3 + j) * SHARD + half * SEGMENT, SEGMENT) for j in range(UNIT)], axis=0)
 
     note_lane = lax.broadcasted_iota(jnp.int32, (16, 128), 1)
+    mark = [jnp.where(note_lane == n, 1.0, 0.0).astype(jnp.bfloat16) for n in range(2)]
+    marks = jnp.concatenate(([mark[0]] * (SEGMENT // 16) + [mark[1]] * (SEGMENT // 16)) * HEADS_HERE, axis=0)
 
     def scores(u, s_ref):
         g = field(u, 0)
         bits = field(u, 1)
         rot = jnp.concatenate(
             [
-                keys[pl.ds(pl.multiple_of(field(u, 3 + j) * SHARD + ROWS, 32), 32), pl.ds(h * 128, 128)]
+                keys[h, pl.ds(pl.multiple_of(field(u, 3 + j) * SHARD + ROWS, 32), 32), :]
                 for j in range(UNIT)
                 for h in range(2)
             ],
             axis=0,
         )
-        q = qabs[g]
+        q = jnp.concatenate([qabs[g, k] for k in range(2)], axis=1)
         for half in range(2):
             notes = []
             for j in range(UNIT):
@@ -201,19 +220,21 @@
                 note = jnp.where(note_lane == 0, early, jnp.where(note_lane == 1, late, 0.0)).astype(jnp.bfloat16)
                 notes += [note] * (SEGMENT // 16)
             extra = jnp.concatenate([rot, jnp.concatenate(notes, axis=0)], axis=1)
-            s_ref[:, pl.ds(half * 256, 256)] = lax.dot_general(
+            total = lax.dot_general(
                 q, latent_tile(u, half), NT, preferred_element_type=jnp.float32
-            ) + lax.dot_general(q4_ref[g, half], extra, NT, preferred_element_type=jnp.float32)
+            ) + lax.dot_general(
+                jnp.concatenate([q4_ref[g, half], marks], axis=1), extra, NT, preferred_element_type=jnp.float32
+            )
+            for k in range(2):
+                s_ref[half * 2 + k, pl.ds(0, QROWS), :] = total[:, k * 128 : (k + 1) * 128]
 
     def absorb(u, s_ref, p_ref, shrink_ref):
         g = field(u, 0)
         for at in range(0, QROWS, CHUNK):
             rows = pl.ds(at, CHUNK)
-            s = s_ref[rows, :]
+            s = [s_ref[k, rows, :] for k in range(KEYS // 128)]
             before = m_ref[g, rows, :]
-            top = s[:, :128]
-            for k in range(1, KEYS // 128):
-                top = jnp.maximum(top, s[:, k * 128 : (k + 1) * 128])
+            top = jnp.maximum(jnp.maximum(s[0], s[1]), jnp.maximum(s[2], s[3]))
             after = jnp.maximum(before, jnp.max(top, axis=1, keepdims=True))
             m_ref[g, rows, :] = after
             shrink = jnp.exp2((before - after) * SCALE2)
@@ -221,18 +242,18 @@
             after = after * SCALE2
             partial = l_ref[g, rows, :] * shrink
             for k in range(KEYS // 128):
-                p = jnp.exp2(s[:, k * 128 : (k + 1) * 128] * SCALE2 - after)
+                p = jnp.exp2(s[k] * SCALE2 - after)
                 partial = partial + p
-                p_ref[rows, pl.ds(k * 128, 128)] = p.astype(jnp.bfloat16)
+                p_ref[k, rows, :] = p.astype(jnp.bfloat16)
             l_ref[g, rows, :] = partial
         values = jnp.concatenate([latent_tile(u, 0), latent_tile(u, 1)], axis=0)
         for at in range(0, QROWS, QROWS // 2):
             rows = pl.ds(at, QROWS // 2)
-            product = jnp.dot(p_ref[rows, :], values, preferred_element_type=jnp.float32)
+            weights = jnp.concatenate([p_ref[k, rows, :] for k in range(KEYS // 128)], axis=1)
+            product = jnp.dot(weights, values, preferred_element_type=jnp.float32)
             for k in range(LATENT // 128):
-                cols = pl.ds(k * 128, 128)
-                acc_ref[g, rows, cols] = (
-                    acc_ref[g, rows, cols] * shrink_ref[rows, :] + product[:, k * 128 : (k + 1) * 128]
+                acc_ref[g, k, rows, :] = (
+                    acc_ref[g, k, rows, :] * shrink_ref[rows, :] + product[:, k * 128 : (k + 1) * 128]
                 )
 
     scores(0, s0)
@@ -245,8 +266,13 @@
         absorb(u + 1, s1, p1, shrink1)
         return carry
 
-    lax.fori_loop(0, steps // 2, pair, 0)
-    absorb(steps - 1, s0, p0, shrink0)
+    lax.fori_loop(0, (steps - 1) // 2, pair, 0)
+    if steps % 2 == 0:
+        scores(steps - 1, s1)
+        absorb(steps - 2, s0, p0, shrink0)
+        absorb(steps - 1, s1, p1, shrink1)
+    else:
+        absorb(steps - 1, s0, p0, shrink0)
     if not last:
         return
     core = field(0, 2)
@@ -255,7 +281,7 @@
         place = 2 * (g // 2) + jnp.where(core == g % 2, 0, 1)
         total = jnp.sum(l_ref[g], axis=1, keepdims=True)
         total = jnp.where(total > 0.0, total, 1.0)
-        mean = (acc_ref[g] / total).astype(jnp.bfloat16)
+        mean = jnp.concatenate([acc_ref[g, k] / total for k in range(2)], axis=1).astype(jnp.bfloat16)
         size = m_ref[g] * SCALE2 + jnp.log2(total)
         notes = jnp.zeros((ROWS, 128), jnp.bfloat16)
         for h in range(HEADS_HERE):
@@ -270,46 +296,65 @@
                 notes = jnp.where(lane == n * HEADS_HERE + h, term, notes)
                 left = left - term.astype(jnp.float32)
         out_ref[place, :, pl.ds(HEADS_HERE * V_DIM, 128)] = notes
+    for fetch in fetches:
+        fetch.wait()
 
 
 def attention(call, table, operands, parts):
     vmem = pl.BlockSpec(memory_space=pltpu.VMEM)
+    hbm = pl.BlockSpec(memory_space=pltpu.HBM)
     steps = work_table(call)[0]
+    offset = sum(work_table(n)[1].shape[1] for n in range(call))
     first, last = call == 0, call == len(CALLS) - 1
-    f32 = lambda width: jax.ShapeDtypeStruct((GROUPS, QROWS, width), jnp.float32)
-    state = [f32(128), f32(128), f32(LATENT)]
+    outs = [
+        pltpu.VMEM((GROUPS, QROWS, 128), jnp.float32),
+        pltpu.VMEM((GROUPS, QROWS, 128), jnp.float32),
+        pltpu.VMEM((GROUPS, 2, QROWS, 128), jnp.float32),
+    ]
+    specs = [vmem] * len(operands)
     scratch = []
+    aliases = {}
     if first:
-        outs = [jax.ShapeDtypeStruct((GROUPS, QROWS, LATENT), jnp.bfloat16)] + state
+        outs = [pltpu.VMEM((GROUPS, 2, QROWS, 128), jnp.bfloat16)] * 2 + outs
     elif last:
-        outs = [jax.ShapeDtypeStruct((4, ROWS, MESSAGE), jnp.bfloat16)]
-        scratch = [pltpu.VMEM(s.shape, s.dtype) for s in state]
-    else:
-        outs = state
+        fetched = operands[-2:]
+        outs = [
+            pltpu.VMEM((4, ROWS, MESSAGE), jnp.bfloat16),
+            pltpu.VMEM((fetched[0].shape[0], EARLY), jnp.bfloat16),
+            pltpu.VMEM(fetched[1].shape, jnp.bfloat16),
+        ] + outs
+        specs = specs[:-2] + [hbm] * 2
+        operands = (*operands[:-2], *[in_hbm(f) for f in fetched])
+        scratch = [pltpu.SemaphoreType.DMA((2,))]
+    if not first:
+        aliases = {3 + n: len(outs) - 3 + n for n in range(3)}
+        operands = tuple(in_vmem(x) if 1 <= n < 5 else x for n, x in enumerate(operands))
     work = steps * QROWS * KEYS * 3 * LATENT * 2
     return pl.pallas_call(
-        functools.partial(attention_body, call, steps, len(parts)),
+        functools.partial(attention_body, call, steps, offset, len(parts)),
         out_shape=outs,
-        in_specs=[pl.BlockSpec(memory_space=pltpu.SMEM)]
-        + [vmem] * len(operands)
-        + [pl.BlockSpec(memory_space=pl.ANY)] * len(parts),
+        in_specs=[pl.BlockSpec(memory_space=pltpu.SMEM)] + specs + [vmem] * len(parts),
         out_specs=[vmem] * len(outs),
-        scratch_shapes=scratch
-        + [
-            pltpu.VMEM((len(parts) * PART_SHARDS * SHARD, LATENT), jnp.bfloat16),
-            pltpu.VMEM((QROWS, KEYS), jnp.float32),
-            pltpu.VMEM((QROWS, KEYS), jnp.float32),
-            pltpu.VMEM((QROWS, KEYS), jnp.bfloat16),
-            pltpu.VMEM((QROWS, KEYS), jnp.bfloat16),
+        input_output_aliases=aliases,
+        scratch_shapes=[
+            pltpu.VMEM((2, len(parts) * PART_SHARDS * SHARD, 128), jnp.bfloat16),
+            pltpu.VMEM((KEYS // 128, QROWS, 128), jnp.float32),
+            pltpu.VMEM((KEYS // 128, QROWS, 128), jnp.float32),
+            pltpu.VMEM((KEYS // 128, QROWS, 128), jnp.bfloat16),
+            pltpu.VMEM((KEYS // 128, QROWS, 128), jnp.bfloat16),
             pltpu.VMEM((QROWS, 128), jnp.float32),
             pltpu.VMEM((QROWS, 128), jnp.float32),
-            pltpu.SemaphoreType.DMA((len(parts),)),
-        ],
+        ]
+        + scratch,
         cost_estimate=pl.CostEstimate(
             flops=work, bytes_accessed=2**20, transcendentals=steps * QROWS * KEYS
         ),
         compiler_params=pltpu.CompilerParams(vmem_limit_bytes=24 * 2**20),
-    )(table, *operands, *parts)
+    )(table, *operands, *[in_vmem(part) for part in parts])
+
+
+def in_vmem(x):
+    return pltpu.with_memory_space_constraint(x, pltpu.VMEM)
 
 
 def in_hbm(x):
@@ -339,30 +384,26 @@
 
 
 def project_body(
-    core, local_part, mirror_same, swapped, mirror_cross, gain, slots, residual_hbm, out_proj_hbm,
-    hidden_hbm, outgoing_hbm, residual, out_proj, projected, hidden, outgoing, sems, out_sems,
+    core, local_part, mirror_same, swapped, mirror_cross, gain, slots, residual, out_early, out_proj_hbm,
+    hidden_hbm, outgoing_hbm, hidden, outgoing, out_late, out_sems, late_sem,
 ):
-    width = residual.shape[1]
-    piece = width // PIECES
-    loads = [pltpu.make_async_copy(residual_hbm, residual, sems.at[PIECES])]
-    for n in range(PIECES):
-        cols = pl.ds(n * piece, piece)
-        loads.append(pltpu.make_async_copy(out_proj_hbm.at[:, cols], out_proj.at[:, cols], sems.at[n]))
-    for load in loads[1:] + loads[:1]:
-        load.start()
+    fetch = pltpu.make_async_copy(out_proj_hbm.at[:, pl.ds(EARLY, out_late.shape[1])], out_late, late_sem)
+    fetch.start()
     half = HEADS_HERE * V_DIM
     mine = merged(local_part[...], mirror_same[...])
     theirs = merged(swapped[...], mirror_cross[...])
     at = pl.multiple_of(core[0] * half, half)
     other = pl.multiple_of((1 - core[0]) * half, half)
-    for n in range(PIECES):
-        cols = pl.ds(n * piece, piece)
-        loads[1 + n].wait()
-        projected[:, cols] = jnp.dot(
-            mine, out_proj[pl.ds(at, half), cols], preferred_element_type=jnp.float32
-        ) + jnp.dot(theirs, out_proj[pl.ds(other, half), cols], preferred_element_type=jnp.float32)
-    loads[0].wait()
-    result = (residual[...].astype(jnp.float32) + projected[...]).astype(jnp.bfloat16)
+    projected = []
+    for weights in (out_early, out_late):
+        if weights is out_late:
+            fetch.wait()
+        projected.append(
+            jnp.dot(mine, weights[pl.ds(at, half), :], preferred_element_type=jnp.float32)
+            + jnp.dot(theirs, weights[pl.ds(other, half), :], preferred_element_type=jnp.float32)
+        )
+    projected = jnp.concatenate(projected, axis=1)
+    result = (residual[...].astype(jnp.float32) + projected).astype(jnp.bfloat16)
     hidden[...] = result
     store = pltpu.make_async_copy(hidden, hidden_hbm, out_sems.at[PIECES])
     store.start()
@@ -384,7 +425,7 @@
         store.wait()
 
 
-def project(core, messages, out_proj, residual, gain, slots):
+def project(core, messages, out_early, out_proj, residual, gain, slots):
     width = residual.shape[1]
     vmem = pl.BlockSpec(memory_space=pltpu.VMEM)
     hbm = pl.BlockSpec(memory_space=pltpu.HBM)
@@ -394,20 +435,18 @@
             pltpu.HBM((ROWS, width), jnp.bfloat16),
             pltpu.HBM((N_SP * CAP, width), jnp.bfloat16),
         ),
-        in_specs=[pl.BlockSpec(memory_space=pltpu.SMEM)] + [vmem] * 6 + [hbm] * 2,
+        in_specs=[pl.BlockSpec(memory_space=pltpu.SMEM)] + [vmem] * 8 + [hbm],
         out_specs=(hbm, hbm),
         scratch_shapes=[
             pltpu.VMEM((ROWS, width), jnp.bfloat16),
-            pltpu.VMEM(out_proj.shape, jnp.bfloat16),
-            pltpu.VMEM((ROWS, width), jnp.float32),
-            pltpu.VMEM((ROWS, width), jnp.bfloat16),
             pltpu.VMEM((N_SP * CAP, width), jnp.bfloat16),
+            pltpu.VMEM((out_proj.shape[0], width - EARLY), jnp.bfloat16),
             pltpu.SemaphoreType.DMA((PIECES + 1,)),
-            pltpu.SemaphoreType.DMA((PIECES + 1,)),
+            pltpu.SemaphoreType.DMA,
         ],
-        compiler_params=pltpu.CompilerParams(vmem_limit_bytes=20 * 2**20),
+        compiler_params=pltpu.CompilerParams(vmem_limit_bytes=16 * 2**20),
         name="project",
-    )(core, *messages, gain, slots, in_hbm(residual), in_hbm(out_proj))
+    )(core, *messages, gain, slots, in_vmem(residual), in_vmem(out_early), in_hbm(out_proj))
 
 
 def experts_body(rows, *rest):
@@ -425,19 +464,18 @@
     stores = []
     for n in range(2):
         gate, up, down = weights[3 * n : 3 * n + 3]
+        loads[3 * n].wait()
+        loads[3 * n + 1].wait()
+        actives = []
+        for k in range(2):
+            x = rows[pl.ds(k * block, block), :]
+            gated = jnp.dot(x, gate[...], preferred_element_type=jnp.float32)
+            raised = jnp.dot(x, up[...], preferred_element_type=jnp.float32)
+            actives.append((gated / (1.0 + jnp.exp(-gated)) * raised).astype(jnp.bfloat16))
+        loads[3 * n + 2].wait()
         for k in range(2):
             at = pl.ds(k * block, block)
-            x = rows[at, :]
-            if k == 0:
-                loads[3 * n].wait()
-            gated = jnp.dot(x, gate[...], preferred_element_type=jnp.float32)
-            if k == 0:
-                loads[3 * n + 1].wait()
-            raised = jnp.dot(x, up[...], preferred_element_type=jnp.float32)
-            active = (gated / (1.0 + jnp.exp(-gated)) * raised).astype(jnp.bfloat16)
-            if k == 0:
-                loads[3 * n + 2].wait()
-            product = jnp.dot(active, down[...], preferred_element_type=jnp.float32).astype(jnp.bfloat16)
+            product = jnp.dot(actives[k], down[...], preferred_element_type=jnp.float32).astype(jnp.bfloat16)
             if n == 0:
                 first[at, :] = product
             else:
@@ -544,74 +582,72 @@
     crossing = [
         (s * N_TP + t, (N_SP - 1 - s) * N_TP + 1 - t) for s in range(N_SP) for t in range(N_TP)
     ]
-    received_nope = lax.ppermute(query_nope, AXES, mirror)
-    received_rope = lax.ppermute(query_rope, AXES, mirror)
+    queries = jnp.concatenate([query_nope, query_rope], axis=1)
+    received = lax.ppermute(queries, AXES, mirror)
 
     near = lax.ppermute(shard, AXES, plane_pairs(Z_FIRST))
     far = lax.ppermute(shard, AXES, plane_pairs(Z_SECOND))
     main = (tp_index == 0) == (sp_index < 2 * PLANE)
     both = jnp.concatenate([jnp.where(main, shard, far), near], axis=0)
-    got = [both] + [lax.ppermute(both, AXES, shift_pairs(0, by)) for by in SHIFTS[1:]]
-    both = jnp.concatenate(got, axis=0)
-
-    tokens = jnp.arange(tok_dev, dtype=jnp.int32)
-    query_pos = jnp.concatenate([query_first + tokens, (N_SP - 1 - sp_index) * tok_dev + tokens])
-    query_rot = rotary(
-        jnp.concatenate([query_rope, received_rope], axis=0)
-        .astype(jnp.float32)
-        .reshape(2 * tok_dev, HEADS_HERE, QK_ROPE),
-        query_pos,
-    ).astype(jnp.bfloat16)
-    rot = jnp.swapaxes(query_rot.reshape(GROUPS, ROWS, HEADS_HERE, QK_ROPE), 1, 2)
-    rot = rot.reshape(GROUPS, QROWS, QK_ROPE)
-    none = jnp.zeros_like(rot)
-    late = (jnp.arange(QROWS) % ROWS) // SEGMENT
-    marks = (late[:, None] == jnp.arange(128)[None, :]).astype(jnp.bfloat16)
-    marks = jnp.broadcast_to(marks[None], (GROUPS, QROWS, 128))
-    q4 = jnp.stack(
-        [jnp.concatenate([rot, none, marks], axis=-1), jnp.concatenate([none, rot, marks], axis=-1)], axis=1
-    )
-    qn = jnp.concatenate([query_nope, received_nope], axis=0).reshape(GROUPS, ROWS, -1)
-
-    both, qn, q4 = lax.optimization_barrier((both, qn, q4))
-    own_parts = [both]
-    for by in SHIFTS[1:]:
-        own_parts.append(lax.ppermute(both, AXES, shift_pairs(1, by)))
-    pieces = (own_parts, [lax.ppermute(part, "tp", swap) for part in own_parts])
-
-    state = ()
-    for call in range(len(CALLS)):
-        table = lax.dynamic_index_in_dim(
-            jnp.asarray(work_table(call)[1]), sp_index * N_TP + tp_index, 0, keepdims=False
-        )
-        operands = (qn, key_up, q4) if call == 0 else (q4, qabs, *state)
-        if call == len(CALLS) - 1:
-            operands = (*operands, value_up)
-        state = attention(call, table, operands, [pieces[own][k3] for own, k3 in CALLS[call]])
-        if call == 0:
-            qabs, *state = state
-    attn = state[0]
-    mirror_same = lax.ppermute(attn[2], AXES, mirror)
-    mirror_cross = lax.ppermute(attn[3], AXES, crossing)
-    swapped = lax.ppermute(attn[1], "tp", swap)
-    messages = (attn[0], mirror_same, swapped, mirror_cross)
 
     flat = routes.reshape(-1)
     order = jnp.arange(flat.shape[0], dtype=jnp.int32)
     earlier = (flat[:, None] == flat[None, :]) & (order[None, :] < order[:, None])
     rank = jnp.sum(earlier.astype(jnp.int32), axis=1)
     slots = (flat * CAP + rank).reshape(routes.shape)
+    slots_across = slots.T
+    tables = np.concatenate([work_table(call)[1] for call in range(len(CALLS))], axis=1)
+    table = lax.dynamic_index_in_dim(jnp.asarray(tables), sp_index * N_TP + tp_index, 0, keepdims=False)
+    tokens = jnp.arange(tok_dev, dtype=jnp.int32)
+    query_pos = jnp.concatenate([query_first + tokens, (N_SP - 1 - sp_index) * tok_dev + tokens])
+    half_width = QK_ROPE // 2
+    pair = jnp.arange(HEADS_HERE * QK_ROPE, dtype=jnp.int32) % half_width
+    inverse = ROPE_BASE ** (-2.0 * pair.astype(jnp.float32) / QK_ROPE)
+    angles = query_pos.astype(jnp.float32)[:, None] * inverse[None, :]
+    behind = jnp.arange(HEADS_HERE * QK_ROPE, dtype=jnp.int32) % QK_ROPE >= half_width
+    cosine = jnp.cos(angles)
+    sine = jnp.where(behind[None, :], jnp.sin(angles), -jnp.sin(angles))
+    both, table, slots, slots_across, cosine, sine = lax.optimization_barrier(
+        (both, table, slots, slots_across, cosine, sine)
+    )
+    got = [both]
+    for by in SHIFTS[1:]:
+        got.append(lax.ppermute(both, AXES, shift_pairs(0, by)))
+    both = jnp.concatenate(got, axis=0)
+
+    own_parts = [both]
+    for by in SHIFTS[1:]:
+        own_parts.append(lax.ppermute(both, AXES, shift_pairs(1, by)))
+    pieces = (own_parts, [lax.ppermute(part, "tp", swap) for part in own_parts])
+    own_weights = (w_gate[0], w_up[0], w_down[0])
+    other_weights = []
+    for w in own_weights:
+        other_weights.append(lax.ppermute(w, "tp", swap))
+
+    state = ()
+    for call in range(len(CALLS)):
+        operands = (
+            (query_nope, query_rope, received, key_up, cosine, sine) if call == 0 else (q4, qabs, *state)
+        )
+        if call == len(CALLS) - 1:
+            operands = (*operands, value_up, out_proj, residual)
+        state = attention(call, table, operands, [pieces[own][k3] for own, k3 in CALLS[call]])
+        if call == 0:
+            qabs, q4, *state = state
+    attn, out_early, residual = state[:3]
+    mirror_same = lax.ppermute(attn[2], AXES, mirror)
+    mirror_cross = lax.ppermute(attn[3], AXES, crossing)
+    swapped = lax.ppermute(attn[1], "tp", swap)
+    messages = (attn[0], mirror_same, swapped, mirror_cross)
 
     hidden, outgoing = project(
-        tp_index.reshape(1).astype(jnp.int32), messages, out_proj, residual, norm_gain[None, :], slots.T
+        tp_index.reshape(1).astype(jnp.int32), messages, out_early, out_proj, residual, norm_gain[None, :], slots_across
     )
     width = residual.shape[1]
     arrived = lax.all_to_all(
         outgoing.reshape(N_SP, CAP, width), "sp", split_axis=0, concat_axis=0, tiled=True
     ).reshape(N_SP * CAP, width)
-    own = (w_gate[0], w_up[0], w_down[0])
-    other = tuple(lax.ppermute(w, "tp", swap) for w in own)
-    produced = experts(arrived, own, other)
+    produced = experts(arrived, own_weights, other_weights)
     back = lax.all_to_all(
         produced.reshape(N_SP, CAP, width), "sp", split_axis=0, concat_axis=0, tiled=True
     ).reshape(N_SP * CAP, width)

time: 191 us -> 184 us (0.963)
  waiting for transfers between devices: 70.6 us -> 79.1 us
  Pallas kernels: 48.4 us -> 41 us
  local copies, waits for them, and re-layouts: 9.29 us -> 4.85 us
  starting transfers between devices: 55.6 us -> 53.4 us
    ppermute x8 -> x7, starting transfers between devices: 11.8 us -> 6.6 us  [the longest x3 4.36 us: local(): got.append(lax.ppermute(both, AXES, shift_pairs(0, by)))]
    pallas_call x3, Pallas kernels: 34.1 us -> 28.9 us  [attention(): pl.pallas_call(functools.partial(attention_body, call, steps, offset, len...]
    ppermute x8 -> x7, waiting for transfers between devices: 10.7 us -> 14.8 us  [the longest x1 6.26 us: local(): received = lax.ppermute(queries, AXES, mirror)]
    ppermute x1, starting transfers between devices: 0.77 us -> 4.42 us  [local(): swapped = lax.ppermute(attn[1], 'tp', swap)]
    ppermute x4, starting transfers between devices: 13.6 us -> 17.1 us  [local(): pieces = (own_parts, [lax.ppermute(part, 'tp', swap) for part in own_parts])]
    ppermute x1, waiting for transfers between devices: 4.45 us -> 6.79 us  [local(): mirror_cross = lax.ppermute(attn[3], AXES, crossing)]
    squeeze x3 -> x0, local copies, waits for them, and re-layouts: 2.07 us -> none  [local(): lax.dynamic_index_in_dim(jnp.asarray(work_table(call)[1]), sp_index * N_T...]
    ppermute x1, starting transfers between devices: 3.19 us -> 1.2 us  [local(): mirror_cross = lax.ppermute(attn[3], AXES, crossing)]
  transfers between devices with their start and end apart: 22 -> 21, of which waited for: 9 -> 11; matrix products, arithmetic and copies ran while one was open for 5% -> 3% of each run, Pallas kernels for 12% -> 10%
where the time goes in v4:
time: 184 us; the launch traced here: 183 us
  waiting for transfers between devices  79.1 us (43%)
  starting transfers between devices  53.4 us (29%)
  Pallas kernels  41 us (22%)
  local copies, waits for them, and re-layouts  4.85 us (3%)
  other arithmetic  4.24 us (2%)
    pallas_call x3, Pallas kernels, attention(): pl.pallas_call(functools.partial(attention_body, call, steps, offset, len...  28.9 us
    all_to_all x1, waiting for transfers between devices, local(): lax.all_to_all(produced.reshape(N_SP, CAP, width), 'sp', split_axis=0, co...  28.3 us
    all_to_all x1, waiting for transfers between devices, local(): lax.all_to_all(outgoing.reshape(N_SP, CAP, width), 'sp', split_axis=0, co...  23.9 us
    ppermute x4, starting transfers between devices, local(): pieces = (own_parts, [lax.ppermute(part, 'tp', swap) for part in own_parts])  17.1 us
    ppermute x1, starting transfers between devices, local(): far = lax.ppermute(shard, AXES, plane_pairs(Z_SECOND))  6.87 us
    ppermute x1, waiting for transfers between devices, local(): mirror_cross = lax.ppermute(attn[3], AXES, crossing)  6.79 us
    pallas_call x1, Pallas kernels, experts(): pl.pallas_call(experts_body, out_shape=pltpu.HBM((count, width), jnp.bflo...  6.69 us
    ppermute x1, waiting for transfers between devices, local(): received = lax.ppermute(queries, AXES, mirror)  6.26 us
  transfers between devices with their start and end apart: 21, of which 11 were waited for; matrix products, arithmetic and copies ran while one was open for 3% of the time, Pallas kernels for 10%

profile of v4, /device:TPU:1, one launch (start us, length us, event | category | flops | bytes accessed | tf_op | source)
XLA Modules:
  0.0 182.9 jit_solution(8372647406818790961)
XLA Ops:
  0.0 0.9 copy.39
  0.9 0.3 fusion.14
  1.3 0.9 fusion.12
  2.3 6.9 %collective-permute-start = (bf16[160,256]{1,0:T(8,128)(2,1)S(1)}, bf16[160,256]{1,0:T(8,128)(2,1)S(1)}, u32[]{:S(2)}, u32[]{:S(2)}) collective-permute-start(bf16[160,256]{1,0:T(8,128)(2,1)S(1)} %fusion.12), channel_id=1, source_target_pairs={{64,1},{66,3},{68,5},{70,7},{72,9},{74,11},{76,13},{78,15},{80,17}... | collective-permute-start | bytes 245768 | tf_op jit(solution)/shard_map/ppermute | solution.py:589
  9.3 0.8 copy.41
  10.1 0.7 broadcast_multiply_fusion
  10.8 0.1 eq.26
  10.9 1.9 %negate_select_fusion = (f32[512,256]{1,0:T(8,128)S(1)}, f32[512,256]{1,0:T(8,128)S(1)}) fusion(f32[256]{0:T(256)S(1)} %fusion.22, f32[512]{0:T(512)S(1)} %add_convert_fusion, pred[256]{0:T(512)(128)(4,1)S(1)} %fusion.23), kind=kLoop, calls=%fused_computation | loop fusion | flops 393216 | bytes 1051904 | tf_op jit(solution)/shard_map/jit(_where)/select_n | solution.py:609
  12.9 0.2 convert_reduce_fusion
  13.1 0.1 reduce_sum.12
  13.2 0.1 copy.42
  13.3 0.7 dynamic-slice_reduce_fusion.table
  14.1 1.3 collective-permute-start.3
  15.4 1.5 collective-permute-start.4
  16.9 1.6 collective-permute-start.5
  18.5 1.4 collective-permute-done.3
  19.9 2.7 %collective-permute-done.5 = bf16[320,256]{1,0:T(8,128)(2,1)S(1)} collective-permute-done((bf16[320,256]{1,0:T(8,128)(2,1)S(1)}, bf16[320,256]{1,0:T(8,128)(2,1)S(1)}, u32[]{:S(2)}, u32[]{:S(2)}) %collective-permute-start.5) | collective-permute-done | bytes 163872 | tf_op jit(solution)/shard_map/ppermute | solution.py:615
  22.7 1.4 collective-permute-start.7
  24.0 1.8 collective-permute-start.8
  25.9 1.3 collective-permute-start.9
  27.1 3.5 %collective-permute-start.6 = (bf16[1280,256]{1,0:T(8,128)(2,1)S(1)}, bf16[1280,256]{1,0:T(8,128)(2,1)S(1)}, u32[]{:S(2)}, u32[]{:S(2)}) collective-permute-start(bf16[1280,256]{1,0:T(8,128)(2,1)S(1)} %constant_dynamic-update-slice_fusion.rest_6_), channel_id=1, source_target_pairs={{0,1},{1,0},{2,3},{3,2},{4,5},{5,4},{6,7},{7,6},{8,9},{9,8},{10,11... | collective-permute-start | bytes 1966088 | tf_op jit(solution)/shard_map/ppermute | solution.py:621
  30.6 1.6 collective-permute-start.2
  32.2 1.8 %collective-permute-done.7.rest_5_ = bf16[1280,256]{1,0:T(8,128)(2,1)S(1)} collective-permute-done((bf16[1280,256]{1,0:T(8,128)(2,1)S(1)}, bf16[1280,256]{1,0:T(8,128)(2,1)S(1)}, u32[]{:S(2)}, u32[]{:S(2)}) %collective-permute-start.7) | collective-permute-done | bytes 655392 | tf_op jit(solution)/shard_map/ppermute | solution.py:620
  34.0 12.0 %collective-permute-start.10 = (bf16[1280,256]{1,0:T(8,128)(2,1)S(1)}, bf16[1280,256]{1,0:T(8,128)(2,1)S(1)}, u32[]{:S(2)}, u32[]{:S(2)}) collective-permute-start(bf16[1280,256]{1,0:T(8,128)(2,1)S(1)} %collective-permute-done.7.rest_5_), channel_id=1, source_target_pairs={{0,1},{1,0},{2,3},{3,2},{4,5},{5,4},{6,7},{7,6},{8,9},{9,8},{10,11... | collective-permute-start | bytes 1966088 | tf_op jit(solution)/shard_map/ppermute | solution.py:621
  46.1 1.6 collective-permute-start.11
  47.7 6.3 %collective-permute-done.2.rest_2_ = bf16[256,768]{1,0:T(8,128)(2,1)S(1)} collective-permute-done((bf16[256,768]{1,0:T(8,128)(2,1)S(1)}, bf16[256,768]{1,0:T(8,128)(2,1)S(1)}, u32[]{:S(2)}, u32[]{:S(2)}) %collective-permute-start.2) | collective-permute-done | bytes 393248 | tf_op jit(solution)/shard_map/ppermute | solution.py:586
  54.0 8.0 %shard_map.145 = (bf16[4,2,512,128]{3,2,1,0:T(8,128)(2,1)S(1)}, bf16[4,2,512,128]{3,2,1,0:T(8,128)(2,1)S(1)}, f32[4,512,128]{2,1,0:T(8,128)S(1)}, f32[4,512,128]{2,1,0:T(8,128)S(1)}, f32[4,2,512,128]{3,2,1,0:T(8,128)S(1)}) custom-call(s32[287]{0:T(512)S(1)} %dynamic-slice_reduce_fusion.table, bf16[256,512]{1,0:T(8,128)(2,1)S(1)} %copy-done.1, ...), custom_call_target="tpu_custom_call" | custom-call | flops 4026531840 | bytes 1048576 | tf_op jit(solution)/shard_map/pallas_call | solution.py:333
  62.0 9.9 %shard_map.146 = (f32[4,512,128]{2,1,0:T(8,128)S(1)}, f32[4,512,128]{2,1,0:T(8,128)S(1)}, f32[4,2,512,128]{3,2,1,0:T(8,128)S(1)}) custom-call(s32[287]{0:T(512)S(1)} %dynamic-slice_reduce_fusion.table, bf16[4,2,512,128]{3,2,1,0:T(8,128)(2,1)S(1)} %get-tuple-element.28.rest_0_, ...), custom_call_target="tpu_custom_call", output_to_operand_aliasing={{0}: (3, {}), {1}: (4, {}), {2}: (5, {})} | custom-call | flops 5637144576 | bytes 1048576 | tf_op jit(solution)/shard_map/pallas_call | solution.py:333
  72.0 10.9 %shard_map.147 = (bf16[4,128,640]{2,1,0:T(8,128)(2,1)S(1)}, bf16[1024,1024]{1,0:T(8,128)(2,1)S(1)}, bf16[128,2048]{1,0:T(8,128)(2,1)S(1)}, f32[4,512,128]{2,1,0:...) custom-call(s32[287]{0:T(512)S(1)} %dynamic-slice_reduce_fusion.tabl, ...), custom_call_target="tpu_custom_call", output_to_operand_aliasing={{3}: (3, {}), {4}: (4, {}), {5}: (5, {})} | custom-call | flops 5637144576 | bytes 1048576 | tf_op jit(solution)/shard_map/pallas_call | solution.py:333
  83.0 0.8 slice_bitcast_fusion
  83.8 1.9 %collective-permute-start.13 = (bf16[128,640]{1,0:T(8,128)(2,1)}, bf16[128,640]{1,0:T(8,128)(2,1)S(1)}, u32[]{:S(2)}, u32[]{:S(2)}) collective-permute-start(bf16[128,640]{1,0:T(8,128)(2,1)} %get-tuple-element.45), channel_id=1, source_target_pairs={{0,126},{1,127},{2,124},{3,125},{4,122},{5,123},{6,120},{7,121},{8... | collective-permute-start | bytes 491528 | tf_op jit(solution)/shard_map/ppermute | solution.py:638
  85.6 4.4 %collective-permute-start.14 = (bf16[128,640]{1,0:T(8,128)(2,1)}, bf16[128,640]{1,0:T(8,128)(2,1)S(1)}, u32[]{:S(2)}, u32[]{:S(2)}) collective-permute-start(bf16[128,640]{1,0:T(8,128)(2,1)} %get-tuple-element.44), channel_id=1, source_target_pairs={{0,1},{1,0},{2,3},{3,2},{4,5},{5,4},{6,7},{7,6},{8,9},{9,8},{10,11... | collective-permute-start | bytes 491528 | tf_op jit(solution)/shard_map/ppermute | solution.py:640
  90.1 1.2 collective-permute-start.15
  91.3 3.4 %collective-permute-done.13.mirror_same = bf16[128,640]{1,0:T(8,128)(2,1)S(1)} collective-permute-done((bf16[128,640]{1,0:T(8,128)(2,1)}, bf16[128,640]{1,0:T(8,128)(2,1)S(1)}, u32[]{:S(2)}, u32[]{:S(2)}) %collective-permute-start.13) | collective-permute-done | bytes 163872 | tf_op jit(solution)/shard_map/ppermute | solution.py:638
  94.7 6.8 %collective-permute-done.15.mirror_cross = bf16[128,640]{1,0:T(8,128)(2,1)S(1)} collective-permute-done((bf16[128,640]{1,0:T(8,128)(2,1)}, bf16[128,640]{1,0:T(8,128)(2,1)S(1)}, u32[]{:S(2)}, u32[]{:S(2)}) %collective-permute-start.15) | collective-permute-done | bytes 163872 | tf_op jit(solution)/shard_map/ppermute | solution.py:639
  101.5 3.8 %project.1 = (bf16[128,2048]{1,0:T(8,128)(2,1)}, bf16[512,2048]{1,0:T(8,128)(2,1)}) custom-call(s32[1]{0:T(128)} %bitcast.core, bf16[128,640]{1,0:T(8,128)(2,1)S(1)} %get-tuple-element.46.local_part, bf16[128,640]{1,0:T(8,128)(2,1)S(1)} %collective-permute-done.13.mirror_same, bf16[128,640]{1,0:T(8,128)(2,1)S(1)} %collective-permute-done.14.swapped, ...), custom_call_target="tpu_custom_call" | custom-call | tf_op jit(solution)/shard_map/project/pallas_call | solution.py:432
  105.3 4.9 %all-to-all-start = ((bf16[64,8,2048]{2,1,0:T(8,128)(2,1)}), bf16[64,8,2048]{2,1,0:T(8,128)(2,1)S(1)}, u32[]{:S(2)}, u32[]{:S(2)}) async-start(bf16[64,8,2048]{2,1,0:T(8,128)(2,1)} %bitcast.23), calls=%async_computation | async-start | bytes 4194304 | tf_op jit(solution)/shard_map/all_to_all | solution.py:647
  110.4 0.5 collective-permute-start.17
  111.0 2.3 %collective-permute-done.16.rest_3_ = bf16[2048,256]{1,0:T(8,128)(2,1)S(1)} collective-permute-done((bf16[2048,256]{1,0:T(8,128)(2,1)}, bf16[2048,256]{1,0:T(8,128)(2,1)S(1)}, u32[]{:S(2)}, u32[]{:S(2)}) %collective-permute-start.16) | collective-permute-done | bytes 1048608 | tf_op jit(solution)/shard_map/ppermute | solution.py:625
  113.2 1.5 collective-permute-done.17.rest_4_
  114.7 1.0 copy-done.7
  115.7 0.7 collective-permute-done.18.rest_5_
  116.4 23.9 %all-to-all-done = bf16[64,8,2048]{2,1,0:T(8,128)(2,1)S(1)} async-done(((bf16[64,8,2048]{2,1,0:T(8,128)(2,1)}), bf16[64,8,2048]{2,1,0:T(8,128)(2,1)S(1)}, u32[]{:S(2)}, u32[]{:S(2)}) %all-to-all-start) | async-done | bytes 2097184 | tf_op jit(solution)/shard_map/all_to_all | solution.py:647
  140.3 6.7 %experts.1 = bf16[512,2048]{1,0:T(8,128)(2,1)} custom-call(bf16[512,2048]{1,0:T(8,128)(2,1)S(1)} %bitcast.18, bf16[2048,256]{1,0:T(8,128)(2,1)} %bitcast.25, bf16[2048,256]{1,0:T(8,128)(2,1)} %bitcast.27, bf16[256,2048]{1,0:T(8,128)(2,1)} %bitcast.29, bf16[2048,256]{1,0:T(8,128)(2,1)} %copy-done.6, bf16[2048,256]{1,0:T(8,128)(2,1)} %copy-done.7, ...), custom_call_target="tpu_custom_call" | custom-call | tf_op jit(solution)/shard_map/experts/pallas_call | solution.py:493
  147.0 5.8 %all-to-all-start.1 = ((bf16[64,8,2048]{2,1,0:T(8,128)(2,1)}), bf16[64,8,2048]{2,1,0:T(8,128)(2,1)S(1)}, u32[]{:S(2)}, u32[]{:S(2)}) async-start(bf16[64,8,2048]{2,1,0:T(8,128)(2,1)} %bitcast.22), calls=%async_computation.1 | async-start | bytes 4194304 | tf_op jit(solution)/shard_map/all_to_all | solution.py:651
  152.8 0.1 copy.44.weights
  153.0 28.3 %all-to-all-done.1 = bf16[64,8,2048]{2,1,0:T(8,128)(2,1)S(1)} async-done(((bf16[64,8,2048]{2,1,0:T(8,128)(2,1)}), bf16[64,8,2048]{2,1,0:T(8,128)(2,1)S(1)}, u32[]{:S(2)}, u32[]{:S(2)}) %all-to-all-start.1) | async-done | bytes 2097184 | tf_op jit(solution)/shard_map/all_to_all | solution.py:651
  181.3 1.6 combine.1
  (48 shorter events, 0.6 us)
Async XLA Ops:
  0.0 30.6 %copy-start.1 = (bf16[256,512]{1,0:T(8,128)(2,1)S(1)}, bf16[256,512]{1,0:T(8,128)(2,1)}, u32[]{:S(2)}) copy-start(bf16[256,512]{1,0:T(8,128)(2,1)} %rest_0_.1) | copy-start | bytes 786436
  0.0 30.6 %copy-start.2 = (bf16[256,256]{1,0:T(8,128)(2,1)S(1)}, bf16[256,256]{1,0:T(8,128)(2,1)}, u32[]{:S(2)}) copy-start(bf16[256,256]{1,0:T(8,128)(2,1)} %rest_1_.1) | copy-start | bytes 393220
  2.3 11.8 %collective-permute-start = (bf16[160,256]{1,0:T(8,128)(2,1)S(1)}, bf16[160,256]{1,0:T(8,128)(2,1)S(1)}, u32[]{:S(2)}, u32[]{:S(2)}) collective-permute-start(bf16[160,256]{1,0:T(8,128)(2,1)S(1)} %fusion.12), channel_id=1, source_target_pairs={{64,1},{66,3},{68,5},{70,7},{72,9},{74,11},{76,13},{78,15},{80,17}... | collective-permute-start | bytes 245768 | tf_op jit(solution)/shard_map/ppermute | solution.py:589
  9.1 5.0 %collective-permute-start.1 = (bf16[160,256]{1,0:T(8,128)(2,1)S(1)}, bf16[160,256]{1,0:T(8,128)(2,1)S(1)}, u32[]{:S(2)}, u32[]{:S(2)}) collective-permute-start(bf16[160,256]{1,0:T(8,128)(2,1)S(1)} %fusion.12), channel_id=1, source_target_pairs={{96,0},{98,2},{100,4},{102,6},{104,8},{106,10},{108,12},{110,14},{... | collective-permute-start | bytes 245768 | tf_op jit(solution)/shard_map/ppermute | solution.py:588
  9.3 44.7 %copy-start.4 = (bf16[256,512]{1,0:T(8,128)(2,1)S(1)}, bf16[256,512]{1,0:T(8,128)(2,1)}, u32[]{:S(2)}) copy-start(bf16[256,512]{1,0:T(8,128)(2,1)} %rest_3_.1) | copy-start | bytes 786436
  14.1 5.7 %collective-permute-start.3 = (bf16[320,256]{1,0:T(8,128)(2,1)S(1)}, bf16[320,256]{1,0:T(8,128)(2,1)S(1)}, u32[]{:S(2)}, u32[]{:S(2)}) collective-permute-start(bf16[320,256]{1,0:T(8,128)(2,1)S(1)} %pad_maximum_fusion.1), channel_id=1, source_target_pairs={{0,8},{1,3},{2,10},{3,5},{4,12},{5,7},{6,14},{7,1},{8,16},{9,11},{... | collective-permute-start | bytes 491528 | tf_op jit(solution)/shard_map/ppermute | solution.py:615
  15.4 4.5 %collective-permute-start.4 = (bf16[320,256]{1,0:T(8,128)(2,1)S(1)}, bf16[320,256]{1,0:T(8,128)(2,1)S(1)}, u32[]{:S(2)}, u32[]{:S(2)}) collective-permute-start(bf16[320,256]{1,0:T(8,128)(2,1)S(1)} %pad_maximum_fusion.1), channel_id=1, source_target_pairs={{0,24},{1,7},{2,26},{3,1},{4,28},{5,3},{6,30},{7,5},{8,0},{9,15},{... | collective-permute-start | bytes 491528 | tf_op jit(solution)/shard_map/ppermute | solution.py:615
  16.9 5.8 %collective-permute-start.5 = (bf16[320,256]{1,0:T(8,128)(2,1)S(1)}, bf16[320,256]{1,0:T(8,128)(2,1)S(1)}, u32[]{:S(2)}, u32[]{:S(2)}) collective-permute-start(bf16[320,256]{1,0:T(8,128)(2,1)S(1)} %pad_maximum_fusion.1), channel_id=1, source_target_pairs={{0,16},{1,5},{2,18},{3,7},{4,20},{5,1},{6,22},{7,3},{8,24},{9,13},... | collective-permute-start | bytes 491528 | tf_op jit(solution)/shard_map/ppermute | solution.py:615
  22.7 11.4 %collective-permute-start.7 = (bf16[1280,256]{1,0:T(8,128)(2,1)S(1)}, bf16[1280,256]{1,0:T(8,128)(2,1)S(1)}, u32[]{:S(2)}, u32[]{:S(2)}) collective-permute-start(bf16[1280,256]{1,0:T(8,128)(2,1)S(1)} %constant_dynamic-update-slice_fusion.rest_6_), channel_id=1, source_target_pairs={{0,2},{1,9},{2,4},{3,11},{4,6},{5,13},{6,0},{7,15},{8,10},{9,17},{... | collective-permute-start | bytes 1966088 | tf_op jit(solution)/shard_map/ppermute | solution.py:620
  24.0 22.0 %collective-permute-start.8 = (bf16[1280,256]{1,0:T(8,128)(2,1)S(1)}, bf16[1280,256]{1,0:T(8,128)(2,1)S(1)}, u32[]{:S(2)}, u32[]{:S(2)}) collective-permute-start(bf16[1280,256]{1,0:T(8,128)(2,1)S(1)} %constant_dynamic-update-slice_fusion.rest_6_), channel_id=1, source_target_pairs={{0,6},{1,25},{2,0},{3,27},{4,2},{5,29},{6,4},{7,31},{8,14},{9,1},{... | collective-permute-start | bytes 1966088 | tf_op jit(solution)/shard_map/ppermute | solution.py:620
  25.9 21.8 %collective-permute-start.9 = (bf16[1280,256]{1,0:T(8,128)(2,1)S(1)}, bf16[1280,256]{1,0:T(8,128)(2,1)S(1)}, u32[]{:S(2)}, u32[]{:S(2)}) collective-permute-start(bf16[1280,256]{1,0:T(8,128)(2,1)S(1)} %constant_dynamic-update-slice_fusion.rest_6_), channel_id=1, source_target_pairs={{0,4},{1,17},{2,6},{3,19},{4,0},{5,21},{6,2},{7,23},{8,12},{9,25},... | collective-permute-start | bytes 1966088 | tf_op jit(solution)/shard_map/ppermute | solution.py:620
  27.1 26.8 %collective-permute-start.6 = (bf16[1280,256]{1,0:T(8,128)(2,1)S(1)}, bf16[1280,256]{1,0:T(8,128)(2,1)S(1)}, u32[]{:S(2)}, u32[]{:S(2)}) collective-permute-start(bf16[1280,256]{1,0:T(8,128)(2,1)S(1)} %constant_dynamic-update-slice_fusion.rest_6_), channel_id=1, source_target_pairs={{0,1},{1,0},{2,3},{3,2},{4,5},{5,4},{6,7},{7,6},{8,9},{9,8},{10,11... | collective-permute-start | bytes 1966088 | tf_op jit(solution)/shard_map/ppermute | solution.py:621
  30.6 23.3 %collective-permute-start.2 = (bf16[256,768]{1,0:T(8,128)(2,1)S(1)}, bf16[256,768]{1,0:T(8,128)(2,1)S(1)}, u32[]{:S(2)}, u32[]{:S(2)}) collective-permute-start(bf16[256,768]{1,0:T(8,128)(2,1)S(1)} %pad_maximum_fusion), channel_id=1, source_target_pairs={{0,126},{1,127},{2,124},{3,125},{4,122},{5,123},{6,120},{7,121},{8... | collective-permute-start | bytes 1179656 | tf_op jit(solution)/shard_map/ppermute | solution.py:586
  34.0 37.9 %collective-permute-start.10 = (bf16[1280,256]{1,0:T(8,128)(2,1)S(1)}, bf16[1280,256]{1,0:T(8,128)(2,1)S(1)}, u32[]{:S(2)}, u32[]{:S(2)}) collective-permute-start(bf16[1280,256]{1,0:T(8,128)(2,1)S(1)} %collective-permute-done.7.rest_5_), channel_id=1, source_target_pairs={{0,1},{1,0},{2,3},{3,2},{4,5},{5,4},{6,7},{7,6},{8,9},{9,8},{10,11... | collective-permute-start | bytes 1966088 | tf_op jit(solution)/shard_map/ppermute | solution.py:621
  46.1 25.9 %collective-permute-start.11 = (bf16[1280,256]{1,0:T(8,128)(2,1)S(1)}, bf16[1280,256]{1,0:T(8,128)(2,1)S(1)}, u32[]{:S(2)}, u32[]{:S(2)}) collective-permute-start(bf16[1280,256]{1,0:T(8,128)(2,1)S(1)} %collective-permute-done.8.rest_6_), channel_id=1, source_target_pairs={{0,1},{1,0},{2,3},{3,2},{4,5},{5,4},{6,7},{7,6},{8,9},{9,8},{10,11... | collective-permute-start | bytes 1966088 | tf_op jit(solution)/shard_map/ppermute | solution.py:621
  47.7 24.3 %collective-permute-start.12 = (bf16[1280,256]{1,0:T(8,128)(2,1)S(1)}, bf16[1280,256]{1,0:T(8,128)(2,1)S(1)}, u32[]{:S(2)}, u32[]{:S(2)}) collective-permute-start(bf16[1280,256]{1,0:T(8,128)(2,1)S(1)} %collective-permute-done.9.rest_7_), channel_id=1, source_target_pairs={{0,1},{1,0},{2,3},{3,2},{4,5},{5,4},{6,7},{7,6},{8,9},{9,8},{10,11... | collective-permute-start | bytes 1966088 | tf_op jit(solution)/shard_map/ppermute | solution.py:621
  62.0 10.0 %copy-start.5 = (bf16[256,512]{1,0:T(8,128)(2,1)S(1)}, bf16[256,512]{1,0:T(8,128)(2,1)}, u32[]{:S(2)}) copy-start(bf16[256,512]{1,0:T(8,128)(2,1)} %rest_5_.1) | copy-start | bytes 786436
  72.0 29.5 %copy-start.3 = (f32[2048]{0:T(1024)S(1)}, f32[2048]{0:T(1024)}, u32[]{:S(2)}) copy-start(f32[2048]{0:T(1024)} %param.23) | copy-start | bytes 24580
  83.8 11.0 %collective-permute-start.13 = (bf16[128,640]{1,0:T(8,128)(2,1)}, bf16[128,640]{1,0:T(8,128)(2,1)S(1)}, u32[]{:S(2)}, u32[]{:S(2)}) collective-permute-start(bf16[128,640]{1,0:T(8,128)(2,1)} %get-tuple-element.45), channel_id=1, source_target_pairs={{0,126},{1,127},{2,124},{3,125},{4,122},{5,123},{6,120},{7,121},{8... | collective-permute-start | bytes 491528 | tf_op jit(solution)/shard_map/ppermute | solution.py:638
  85.6 9.1 %collective-permute-start.14 = (bf16[128,640]{1,0:T(8,128)(2,1)}, bf16[128,640]{1,0:T(8,128)(2,1)S(1)}, u32[]{:S(2)}, u32[]{:S(2)}) collective-permute-start(bf16[128,640]{1,0:T(8,128)(2,1)} %get-tuple-element.44), channel_id=1, source_target_pairs={{0,1},{1,0},{2,3},{3,2},{4,5},{5,4},{6,7},{7,6},{8,9},{9,8},{10,11... | collective-permute-start | bytes 491528 | tf_op jit(solution)/shard_map/ppermute | solution.py:640
  90.1 11.5 %collective-permute-start.15 = (bf16[128,640]{1,0:T(8,128)(2,1)}, bf16[128,640]{1,0:T(8,128)(2,1)S(1)}, u32[]{:S(2)}, u32[]{:S(2)}) collective-permute-start(bf16[128,640]{1,0:T(8,128)(2,1)} %get-tuple-element.43), channel_id=1, source_target_pairs={{0,127},{1,126},{2,125},{3,124},{4,123},{5,122},{6,121},{7,120},{8... | collective-permute-start | bytes 491528 | tf_op jit(solution)/shard_map/ppermute | solution.py:639
  105.3 35.0 %all-to-all-start = ((bf16[64,8,2048]{2,1,0:T(8,128)(2,1)}), bf16[64,8,2048]{2,1,0:T(8,128)(2,1)S(1)}, u32[]{:S(2)}, u32[]{:S(2)}) async-start(bf16[64,8,2048]{2,1,0:T(8,128)(2,1)} %bitcast.23), calls=%async_computation | async-start | bytes 4194304 | tf_op jit(solution)/shard_map/all_to_all | solution.py:647
  110.3 3.0 %collective-permute-start.16 = (bf16[2048,256]{1,0:T(8,128)(2,1)}, bf16[2048,256]{1,0:T(8,128)(2,1)S(1)}, u32[]{:S(2)}, u32[]{:S(2)}) collective-permute-start(bf16[2048,256]{1,0:T(8,128)(2,1)} %bitcast.24), channel_id=1, source_target_pairs={{0,1},{1,0},{2,3},{3,2},{4,5},{5,4},{6,7},{7,6},{8,9},{9,8},{10,11... | collective-permute-start | bytes 3145736 | tf_op jit(solution)/shard_map/ppermute | solution.py:625
  110.4 4.4 %collective-permute-start.17 = (bf16[2048,256]{1,0:T(8,128)(2,1)}, bf16[2048,256]{1,0:T(8,128)(2,1)S(1)}, u32[]{:S(2)}, u32[]{:S(2)}) collective-permute-start(bf16[2048,256]{1,0:T(8,128)(2,1)} %bitcast.26), channel_id=1, source_target_pairs={{0,1},{1,0},{2,3},{3,2},{4,5},{5,4},{6,7},{7,6},{8,9},{9,8},{10,11... | collective-permute-start | bytes 3145736 | tf_op jit(solution)/shard_map/ppermute | solution.py:625
  110.9 5.5 %collective-permute-start.18 = (bf16[256,2048]{1,0:T(8,128)(2,1)}, bf16[256,2048]{1,0:T(8,128)(2,1)}, u32[]{:S(2)}, u32[]{:S(2)}) collective-permute-start(bf16[256,2048]{1,0:T(8,128)(2,1)} %bitcast.28), channel_id=1, source_target_pairs={{0,1},{1,0},{2,3},{3,2},{4,5},{5,4},{6,7},{7,6},{8,9},{9,8},{10,11... | collective-permute-start | bytes 3145736 | tf_op jit(solution)/shard_map/ppermute | solution.py:625
  113.2 1.5 copy-start.6
  114.7 1.0 copy-start.7
  147.0 5.8 %copy-start.8 = (f32[128,2]{0,1:T(2,128)S(1)}, f32[128,2]{0,1:T(2,128)}, u32[]{:S(2)}) copy-start(f32[128,2]{0,1:T(2,128)} %param.25) | copy-start | bytes 3076
  147.0 34.2 %copy-start = (bf16[128,2048]{1,0:T(8,128)(2,1)S(1)}, bf16[128,2048]{1,0:T(8,128)(2,1)}, u32[]{:S(2)}) copy-start(bf16[128,2048]{1,0:T(8,128)(2,1)} %get-tuple-element.41.hidden) | copy-start | bytes 1572868
  147.0 34.2 %all-to-all-start.1 = ((bf16[64,8,2048]{2,1,0:T(8,128)(2,1)}), bf16[64,8,2048]{2,1,0:T(8,128)(2,1)S(1)}, u32[]{:S(2)}, u32[]{:S(2)}) async-start(bf16[64,8,2048]{2,1,0:T(8,128)(2,1)} %bitcast.22), calls=%async_computation.1 | async-start | bytes 4194304 | tf_op jit(solution)/shard_map/all_to_all | solution.py:651

commit v5 on v4

--- a/solution.py
+++ b/solution.py
@@ -73,8 +73,7 @@
     return 4 * (source[0] * PLANE + r) + 2 * source[1]
 
 
-CALLS = (((0, 0), (1, 0)), ((0, 1), (0, 2), (0, 3)), ((1, 1), (1, 2), (1, 3)))
-PART_SHARDS = 8
+CALLS = (((0, 0), (1, 0)), ((0, 1), (0, 2)), ((1, 1), (1, 2)), ((0, 3), (1, 3)))
 
 
 @functools.lru_cache(None)
@@ -141,10 +140,11 @@
             fetch = pltpu.make_async_copy(source, target, sems.at[n])
             fetch.start()
             fetches.append(fetch)
-    part_rows = parts[0].shape[0]
-    for n in range(part_count):
+    at = 0
+    for part in parts:
         for k in range(2):
-            keys[k, pl.ds(n * part_rows, part_rows), :] = parts[n][:, pl.ds(k * 128, 128)]
+            keys[k, pl.ds(at, part.shape[0]), :] = part[:, pl.ds(k * 128, 128)]
+        at += part.shape[0]
     if first:
         for g in range(GROUPS):
             source = own_ref if g < 2 else received_ref
@@ -337,7 +337,7 @@
         out_specs=[vmem] * len(outs),
         input_output_aliases=aliases,
         scratch_shapes=[
-            pltpu.VMEM((2, len(parts) * PART_SHARDS * SHARD, 128), jnp.bfloat16),
+            pltpu.VMEM((2, sum(part.shape[0] for part in parts), 128), jnp.bfloat16),
             pltpu.VMEM((KEYS // 128, QROWS, 128), jnp.float32),
             pltpu.VMEM((KEYS // 128, QROWS, 128), jnp.float32),
             pltpu.VMEM((KEYS // 128, QROWS, 128), jnp.bfloat16),
@@ -607,18 +607,27 @@
     behind = jnp.arange(HEADS_HERE * QK_ROPE, dtype=jnp.int32) % QK_ROPE >= half_width
     cosine = jnp.cos(angles)
     sine = jnp.where(behind[None, :], jnp.sin(angles), -jnp.sin(angles))
-    both, table, slots, slots_across, cosine, sine = lax.optimization_barrier(
-        (both, table, slots, slots_across, cosine, sine)
-    )
     got = [both]
     for by in SHIFTS[1:]:
         got.append(lax.ppermute(both, AXES, shift_pairs(0, by)))
     both = jnp.concatenate(got, axis=0)
 
-    own_parts = [both]
-    for by in SHIFTS[1:]:
-        own_parts.append(lax.ppermute(both, AXES, shift_pairs(1, by)))
-    pieces = (own_parts, [lax.ppermute(part, "tp", swap) for part in own_parts])
+    both, table, slots, slots_across, cosine, sine = lax.optimization_barrier(
+        (both, table, slots, slots_across, cosine, sine)
+    )
+    around = []
+    for by in (1, -1):
+        around.append(lax.ppermute(both, AXES, shift_pairs(1, by)))
+    half = both.shape[0] // 2
+    beyond = []
+    for n, by in enumerate((1, -1)):
+        passed = around[n][n * half : (n + 1) * half]
+        beyond.append(lax.ppermute(passed, AXES, shift_pairs(1, by)))
+    own_parts = [[both], [around[0]], [around[1]], beyond]
+    other_parts = []
+    for group in own_parts:
+        other_parts.append([lax.ppermute(part, "tp", swap) for part in group])
+    pieces = (own_parts, other_parts)
     own_weights = (w_gate[0], w_up[0], w_down[0])
     other_weights = []
     for w in own_weights:
@@ -631,7 +640,7 @@
         )
         if call == len(CALLS) - 1:
             operands = (*operands, value_up, out_proj, residual)
-        state = attention(call, table, operands, [pieces[own][k3] for own, k3 in CALLS[call]])
+        state = attention(call, table, operands, [part for own, k3 in CALLS[call] for part in pieces[own][k3]])
         if call == 0:
             qabs, q4, *state = state
     attn, out_early, residual = state[:3]

time: 184 us -> 182 us (0.989)
  waiting for transfers between devices: 79.1 us -> 73.1 us
  Pallas kernels: 41 us -> 43.2 us
    ppermute x1, waiting for transfers between devices: 6.26 us -> 0.87 us  [local(): received = lax.ppermute(queries, AXES, mirror)]
    ppermute x1, starting transfers between devices: 4.42 us -> 0.4 us  [local(): swapped = lax.ppermute(attn[1], 'tp', swap)]
    ppermute x1, starting transfers between devices: 1.88 us -> 5.35 us  [local(): mirror_same = lax.ppermute(attn[2], AXES, mirror)]
    ppermute x7 -> x9, starting transfers between devices: 21.6 us -> 19.1 us  [the longest x5 13.1 us: local(): other_parts.append([lax.ppermute(part, 'tp', swap) for part in group])]
    pallas_call x3 -> x4, Pallas kernels: 28.9 us -> 31 us  [attention(): pl.pallas_call(functools.partial(attention_body, call, steps, offset, len...]
  transfers between devices with their start and end apart: 21 -> 23, of which waited for: 11 -> 13; matrix products, arithmetic and copies ran while one was open for 3% -> 3% of each run, Pallas kernels for 10% -> 13%
where the time goes in v5:
time: 182 us; the launch traced here: 180 us
  waiting for transfers between devices  73.1 us (40%)
  starting transfers between devices  53.6 us (29%)
  Pallas kernels  43.2 us (24%)
  local copies, waits for them, and re-layouts  5.8 us (3%)
  other arithmetic  4.24 us (2%)
    pallas_call x4, Pallas kernels, attention(): pl.pallas_call(functools.partial(attention_body, call, steps, offset, len...  31 us
    all_to_all x1, waiting for transfers between devices, local(): lax.all_to_all(produced.reshape(N_SP, CAP, width), 'sp', split_axis=0, co...  28.3 us
    all_to_all x1, waiting for transfers between devices, local(): lax.all_to_all(outgoing.reshape(N_SP, CAP, width), 'sp', split_axis=0, co...  23.3 us
    ppermute x5, starting transfers between devices, local(): other_parts.append([lax.ppermute(part, 'tp', swap) for part in group])  13.1 us
    ppermute x1, starting transfers between devices, local(): far = lax.ppermute(shard, AXES, plane_pairs(Z_SECOND))  6.87 us
    pallas_call x1, Pallas kernels, experts(): pl.pallas_call(experts_body, out_shape=pltpu.HBM((count, width), jnp.bflo...  6.71 us
    all_to_all x1, starting transfers between devices, local(): lax.all_to_all(produced.reshape(N_SP, CAP, width), 'sp', split_axis=0, co...  6.29 us
    ppermute x1, waiting for transfers between devices, local(): mirror_cross = lax.ppermute(attn[3], AXES, crossing)  6.01 us
  transfers between devices with their start and end apart: 23, of which 13 were waited for; matrix products, arithmetic and copies ran while one was open for 3% of the time, Pallas kernels for 13%

profile of v5, /device:TPU:1, one launch (start us, length us, event | category | flops | bytes accessed | tf_op | source)
XLA Modules:
  0.0 180.2 jit_solution(9638525864170043299)
XLA Ops:
  0.0 0.9 copy.42
  0.9 0.3 fusion.14
  1.3 0.9 fusion.12
  2.3 6.9 %collective-permute-start = (bf16[160,256]{1,0:T(8,128)(2,1)S(1)}, bf16[160,256]{1,0:T(8,128)(2,1)S(1)}, u32[]{:S(2)}, u32[]{:S(2)}) collective-permute-start(bf16[160,256]{1,0:T(8,128)(2,1)S(1)} %fusion.12), channel_id=1, source_target_pairs={{64,1},{66,3},{68,5},{70,7},{72,9},{74,11},{76,13},{78,15},{80,17}... | collective-permute-start | bytes 245768 | tf_op jit(solution)/shard_map/ppermute | solution.py:589
  9.3 1.9 %negate_select_fusion = (f32[512,256]{1,0:T(8,128)S(1)}, f32[512,256]{1,0:T(8,128)S(1)}) fusion(f32[256]{0:T(256)S(1)} %fusion.22, f32[512]{0:T(512)S(1)} %add_convert_fusion, pred[256]{0:T(512)(128)(4,1)S(1)} %fusion.23), kind=kLoop, calls=%fused_computation | loop fusion | flops 393216 | bytes 1051904 | tf_op jit(solution)/shard_map/jit(_where)/select_n | solution.py:609
  11.2 0.7 broadcast_multiply_fusion
  11.9 0.8 copy.44
  12.9 0.2 collective-permute-done.1
  13.1 1.3 collective-permute-start.2
  14.8 0.7 dynamic-slice_reduce_fusion.table
  15.6 1.5 collective-permute-start.3
  17.1 1.5 collective-permute-start.4
  18.9 1.2 collective-permute-done.3
  20.1 2.7 %collective-permute-done.4 = bf16[320,256]{1,0:T(8,128)(2,1)S(1)} collective-permute-done((bf16[320,256]{1,0:T(8,128)(2,1)S(1)}, bf16[320,256]{1,0:T(8,128)(2,1)S(1)}, u32[]{:S(2)}, u32[]{:S(2)}) %collective-permute-start.4) | collective-permute-done | bytes 163872 | tf_op jit(solution)/shard_map/ppermute | solution.py:612
  22.8 1.4 collective-permute-start.7
  24.2 1.8 %collective-permute-start.8 = (bf16[1280,256]{1,0:T(8,128)(2,1)S(1)}, bf16[1280,256]{1,0:T(8,128)(2,1)S(1)}, u32[]{:S(2)}, u32[]{:S(2)}) collective-permute-start(bf16[1280,256]{1,0:T(8,128)(2,1)S(1)} %constant_dynamic-update-slice_fusion.rest_6_), channel_id=1, source_target_pairs={{0,6},{1,25},{2,0},{3,27},{4,2},{5,29},{6,4},{7,31},{8,14},{9,1},{... | collective-permute-start | bytes 1966088 | tf_op jit(solution)/shard_map/ppermute | solution.py:620
  26.0 2.8 %collective-permute-start.6 = (bf16[1280,256]{1,0:T(8,128)(2,1)S(1)}, bf16[1280,256]{1,0:T(8,128)(2,1)S(1)}, u32[]{:S(2)}, u32[]{:S(2)}) collective-permute-start(bf16[1280,256]{1,0:T(8,128)(2,1)S(1)} %constant_dynamic-update-slice_fusion.rest_6_), channel_id=1, source_target_pairs={{0,1},{1,0},{2,3},{3,2},{4,5},{5,4},{6,7},{7,6},{8,9},{9,8},{10,11... | collective-permute-start | bytes 1966088 | tf_op jit(solution)/shard_map/ppermute | solution.py:629
  28.8 3.2 %collective-permute-start.5 = (bf16[256,768]{1,0:T(8,128)(2,1)S(1)}, bf16[256,768]{1,0:T(8,128)(2,1)S(1)}, u32[]{:S(2)}, u32[]{:S(2)}) collective-permute-start(bf16[256,768]{1,0:T(8,128)(2,1)S(1)} %pad_maximum_fusion), channel_id=1, source_target_pairs={{0,126},{1,127},{2,124},{3,125},{4,122},{5,123},{6,120},{7,121},{8... | collective-permute-start | bytes 1179656 | tf_op jit(solution)/shard_map/ppermute | solution.py:586
  32.0 2.2 %collective-permute-done.7.rest_5_ = bf16[1280,256]{1,0:T(8,128)(2,1)S(1)} collective-permute-done((bf16[1280,256]{1,0:T(8,128)(2,1)S(1)}, bf16[1280,256]{1,0:T(8,128)(2,1)S(1)}, u32[]{:S(2)}, u32[]{:S(2)}) %collective-permute-start.7) | collective-permute-done | bytes 655392 | tf_op jit(solution)/shard_map/ppermute | solution.py:620
  34.3 2.7 %collective-permute-start.12 = (bf16[640,256]{1,0:T(8,128)(2,1)S(1)}, bf16[640,256]{1,0:T(8,128)(2,1)S(1)}, u32[]{:S(2)}, u32[]{:S(2)}) collective-permute-start(bf16[640,256]{1,0:T(8,128)(2,1)S(1)} %slice.57), channel_id=1, source_target_pairs={{0,6},{1,25},{2,0},{3,27},{4,2},{5,29},{6,4},{7,31},{8,14},{9,1},{... | collective-permute-start | bytes 983048 | tf_op jit(solution)/shard_map/ppermute | solution.py:625
  37.0 7.5 %collective-permute-start.10 = (bf16[1280,256]{1,0:T(8,128)(2,1)S(1)}, bf16[1280,256]{1,0:T(8,128)(2,1)S(1)}, u32[]{:S(2)}, u32[]{:S(2)}) collective-permute-start(bf16[1280,256]{1,0:T(8,128)(2,1)S(1)} %collective-permute-done.8.rest_6_), channel_id=1, source_target_pairs={{0,1},{1,0},{2,3},{3,2},{4,5},{5,4},{6,7},{7,6},{8,9},{9,8},{10,11... | collective-permute-start | bytes 1966088 | tf_op jit(solution)/shard_map/ppermute | solution.py:629
  44.6 0.9 collective-permute-done.5.rest_2_
  45.5 2.2 %collective-permute-start.9 = (bf16[1280,256]{1,0:T(8,128)(2,1)S(1)}, bf16[1280,256]{1,0:T(8,128)(2,1)S(1)}, u32[]{:S(2)}, u32[]{:S(2)}) collective-permute-start(bf16[1280,256]{1,0:T(8,128)(2,1)S(1)} %collective-permute-done.7.rest_5_), channel_id=1, source_target_pairs={{0,1},{1,0},{2,3},{3,2},{4,5},{5,4},{6,7},{7,6},{8,9},{9,8},{10,11... | collective-permute-start | bytes 1966088 | tf_op jit(solution)/shard_map/ppermute | solution.py:629
  47.7 0.9 copy-done.4
  48.6 8.1 %shard_map.145 = (bf16[4,2,512,128]{3,2,1,0:T(8,128)(2,1)S(1)}, bf16[4,2,512,128]{3,2,1,0:T(8,128)(2,1)S(1)}, f32[4,512,128]{2,1,0:T(8,128)S(1)}, f32[4,512,128]{2,1,0:T(8,128)S(1)}, f32[4,2,512,128]{3,2,1,0:T(8,128)S(1)}) custom-call(s32[308]{0:T(512)S(1)} %dynamic-slice_reduce_fusion.table, bf16[256,512]{1,0:T(8,128)(2,1)S(1)} %copy-done.1, ...), custom_call_target="tpu_custom_call" | custom-call | flops 4026531840 | bytes 1048576 | tf_op jit(solution)/shard_map/pallas_call | solution.py:333
  56.7 7.3 %shard_map.146 = (f32[4,512,128]{2,1,0:T(8,128)S(1)}, f32[4,512,128]{2,1,0:T(8,128)S(1)}, f32[4,2,512,128]{3,2,1,0:T(8,128)S(1)}) custom-call(s32[308]{0:T(512)S(1)} %dynamic-slice_reduce_fusion.table, bf16[4,2,512,128]{3,2,1,0:T(8,128)(2,1)S(1)} %get-tuple-element.31.rest_0_, ...), custom_call_target="tpu_custom_call", output_to_operand_aliasing={{0}: (3, {}), {1}: (4, {}), {2}: (5, {})} | custom-call | flops 4026531840 | bytes 1048576 | tf_op jit(solution)/shard_map/pallas_call | solution.py:333
  64.1 0.5 collective-permute-start.14
  64.6 7.3 %shard_map.147 = (f32[4,512,128]{2,1,0:T(8,128)S(1)}, f32[4,512,128]{2,1,0:T(8,128)S(1)}, f32[4,2,512,128]{3,2,1,0:T(8,128)S(1)}) custom-call(s32[308]{0:T(512)S(1)} %dynamic-slice_reduce_fusion.table, bf16[4,2,512,128]{3,2,1,0:T(8,128)(2,1)S(1)} %get-tuple-element.31.rest_0_, ...), custom_call_target="tpu_custom_call", output_to_operand_aliasing={{0}: (3, {}), {1}: (4, {}), {2}: (5, {})} | custom-call | flops 4026531840 | bytes 1048576 | tf_op jit(solution)/shard_map/pallas_call | solution.py:333
  72.0 8.3 %shard_map.148 = (bf16[4,128,640]{2,1,0:T(8,128)(2,1)S(1)}, bf16[1024,1024]{1,0:T(8,128)(2,1)S(1)}, bf16[128,2048]{1,0:T(8,128)(2,1)S(1)}, f32[4,512,128]{2,1,0:...) custom-call(s32[308]{0:T(512)S(1)} %dynamic-slice_reduce_fusion.tabl, ...), custom_call_target="tpu_custom_call", output_to_operand_aliasing={{3}: (3, {}), {4}: (4, {}), {5}: (5, {})} | custom-call | flops 4026531840 | bytes 1048576 | tf_op jit(solution)/shard_map/pallas_call | solution.py:333
  80.3 0.8 slice_bitcast_fusion
  81.1 5.3 %collective-permute-start.15 = (bf16[128,640]{1,0:T(8,128)(2,1)}, bf16[128,640]{1,0:T(8,128)(2,1)S(1)}, u32[]{:S(2)}, u32[]{:S(2)}) collective-permute-start(bf16[128,640]{1,0:T(8,128)(2,1)} %get-tuple-element.53), channel_id=1, source_target_pairs={{0,126},{1,127},{2,124},{3,125},{4,122},{5,123},{6,120},{7,121},{8... | collective-permute-start | bytes 491528 | tf_op jit(solution)/shard_map/ppermute | solution.py:647
  86.4 0.4 collective-permute-start.16
  86.8 1.5 collective-permute-start.17
  88.5 3.9 %collective-permute-done.15.mirror_same = bf16[128,640]{1,0:T(8,128)(2,1)S(1)} collective-permute-done((bf16[128,640]{1,0:T(8,128)(2,1)}, bf16[128,640]{1,0:T(8,128)(2,1)S(1)}, u32[]{:S(2)}, u32[]{:S(2)}) %collective-permute-start.15) | collective-permute-done | bytes 163872 | tf_op jit(solution)/shard_map/ppermute | solution.py:647
  92.4 6.0 %collective-permute-done.17.mirror_cross = bf16[128,640]{1,0:T(8,128)(2,1)S(1)} collective-permute-done((bf16[128,640]{1,0:T(8,128)(2,1)}, bf16[128,640]{1,0:T(8,128)(2,1)S(1)}, u32[]{:S(2)}, u32[]{:S(2)}) %collective-permute-start.17) | collective-permute-done | bytes 163872 | tf_op jit(solution)/shard_map/ppermute | solution.py:648
  98.4 3.8 %project.1 = (bf16[128,2048]{1,0:T(8,128)(2,1)}, bf16[512,2048]{1,0:T(8,128)(2,1)}) custom-call(s32[1]{0:T(128)} %bitcast.core, bf16[128,640]{1,0:T(8,128)(2,1)S(1)} %get-tuple-element.54.local_part, bf16[128,640]{1,0:T(8,128)(2,1)S(1)} %collective-permute-done.15.mirror_same, bf16[128,640]{1,0:T(8,128)(2,1)S(1)} %collective-permute-done.16.swapped, ...), custom_call_target="tpu_custom_call" | custom-call | tf_op jit(solution)/shard_map/project/pallas_call | solution.py:432
  102.2 5.4 %all-to-all-start = ((bf16[64,8,2048]{2,1,0:T(8,128)(2,1)}), bf16[64,8,2048]{2,1,0:T(8,128)(2,1)S(1)}, u32[]{:S(2)}, u32[]{:S(2)}) async-start(bf16[64,8,2048]{2,1,0:T(8,128)(2,1)} %bitcast.23), calls=%async_computation | async-start | bytes 4194304 | tf_op jit(solution)/shard_map/all_to_all | solution.py:656
  107.7 0.5 collective-permute-start.18
  108.3 0.4 collective-permute-start.20
  108.6 2.0 %collective-permute-done.18.rest_3_ = bf16[2048,256]{1,0:T(8,128)(2,1)S(1)} collective-permute-done((bf16[2048,256]{1,0:T(8,128)(2,1)}, bf16[2048,256]{1,0:T(8,128)(2,1)S(1)}, u32[]{:S(2)}, u32[]{:S(2)}) %collective-permute-start.18) | collective-permute-done | bytes 1048608 | tf_op jit(solution)/shard_map/ppermute | solution.py:634
  110.6 1.5 collective-permute-done.19.rest_4_
  112.1 1.0 copy-done.7
  113.1 0.6 collective-permute-done.20.rest_5_
  113.8 23.3 %all-to-all-done = bf16[64,8,2048]{2,1,0:T(8,128)(2,1)S(1)} async-done(((bf16[64,8,2048]{2,1,0:T(8,128)(2,1)}), bf16[64,8,2048]{2,1,0:T(8,128)(2,1)S(1)}, u32[]{:S(2)}, u32[]{:S(2)}) %all-to-all-start) | async-done | bytes 2097184 | tf_op jit(solution)/shard_map/all_to_all | solution.py:656
  137.1 6.7 %experts.1 = bf16[512,2048]{1,0:T(8,128)(2,1)} custom-call(bf16[512,2048]{1,0:T(8,128)(2,1)S(1)} %bitcast.18, bf16[2048,256]{1,0:T(8,128)(2,1)} %bitcast.25, bf16[2048,256]{1,0:T(8,128)(2,1)} %bitcast.27, bf16[256,2048]{1,0:T(8,128)(2,1)} %bitcast.29, bf16[2048,256]{1,0:T(8,128)(2,1)} %copy-done.6, bf16[2048,256]{1,0:T(8,128)(2,1)} %copy-done.7, ...), custom_call_target="tpu_custom_call" | custom-call | tf_op jit(solution)/shard_map/experts/pallas_call | solution.py:493
  143.8 6.3 %all-to-all-start.1 = ((bf16[64,8,2048]{2,1,0:T(8,128)(2,1)}), bf16[64,8,2048]{2,1,0:T(8,128)(2,1)S(1)}, u32[]{:S(2)}, u32[]{:S(2)}) async-start(bf16[64,8,2048]{2,1,0:T(8,128)(2,1)} %bitcast.22), calls=%async_computation.1 | async-start | bytes 4194304 | tf_op jit(solution)/shard_map/all_to_all | solution.py:660
  150.2 28.3 %all-to-all-done.1 = bf16[64,8,2048]{2,1,0:T(8,128)(2,1)S(1)} async-done(((bf16[64,8,2048]{2,1,0:T(8,128)(2,1)}), bf16[64,8,2048]{2,1,0:T(8,128)(2,1)S(1)}, u32[]{:S(2)}, u32[]{:S(2)}) %all-to-all-start.1) | async-done | bytes 2097184 | tf_op jit(solution)/shard_map/all_to_all | solution.py:660
  178.5 1.6 combine.1
  (55 shorter events, 1.7 us)
Async XLA Ops:
  0.0 28.7 %copy-start.1 = (bf16[256,512]{1,0:T(8,128)(2,1)S(1)}, bf16[256,512]{1,0:T(8,128)(2,1)}, u32[]{:S(2)}) copy-start(bf16[256,512]{1,0:T(8,128)(2,1)} %rest_0_.1) | copy-start | bytes 786436
  0.0 28.7 %copy-start.2 = (bf16[256,256]{1,0:T(8,128)(2,1)S(1)}, bf16[256,256]{1,0:T(8,128)(2,1)}, u32[]{:S(2)}) copy-start(bf16[256,256]{1,0:T(8,128)(2,1)} %rest_1_.1) | copy-start | bytes 393220
  2.3 10.6 %collective-permute-start = (bf16[160,256]{1,0:T(8,128)(2,1)S(1)}, bf16[160,256]{1,0:T(8,128)(2,1)S(1)}, u32[]{:S(2)}, u32[]{:S(2)}) collective-permute-start(bf16[160,256]{1,0:T(8,128)(2,1)S(1)} %fusion.12), channel_id=1, source_target_pairs={{64,1},{66,3},{68,5},{70,7},{72,9},{74,11},{76,13},{78,15},{80,17}... | collective-permute-start | bytes 245768 | tf_op jit(solution)/shard_map/ppermute | solution.py:589
  9.1 3.9 %collective-permute-start.1 = (bf16[160,256]{1,0:T(8,128)(2,1)S(1)}, bf16[160,256]{1,0:T(8,128)(2,1)S(1)}, u32[]{:S(2)}, u32[]{:S(2)}) collective-permute-start(bf16[160,256]{1,0:T(8,128)(2,1)S(1)} %fusion.12), channel_id=1, source_target_pairs={{96,0},{98,2},{100,4},{102,6},{104,8},{106,10},{108,12},{110,14},{... | collective-permute-start | bytes 245768 | tf_op jit(solution)/shard_map/ppermute | solution.py:588
  13.1 5.7 %collective-permute-start.2 = (bf16[320,256]{1,0:T(8,128)(2,1)S(1)}, bf16[320,256]{1,0:T(8,128)(2,1)S(1)}, u32[]{:S(2)}, u32[]{:S(2)}) collective-permute-start(bf16[320,256]{1,0:T(8,128)(2,1)S(1)} %pad_maximum_fusion.1), channel_id=1, source_target_pairs={{0,8},{1,3},{2,10},{3,5},{4,12},{5,7},{6,14},{7,1},{8,16},{9,11},{... | collective-permute-start | bytes 491528 | tf_op jit(solution)/shard_map/ppermute | solution.py:612
  15.6 4.5 %collective-permute-start.3 = (bf16[320,256]{1,0:T(8,128)(2,1)S(1)}, bf16[320,256]{1,0:T(8,128)(2,1)S(1)}, u32[]{:S(2)}, u32[]{:S(2)}) collective-permute-start(bf16[320,256]{1,0:T(8,128)(2,1)S(1)} %pad_maximum_fusion.1), channel_id=1, source_target_pairs={{0,24},{1,7},{2,26},{3,1},{4,28},{5,3},{6,30},{7,5},{8,0},{9,15},{... | collective-permute-start | bytes 491528 | tf_op jit(solution)/shard_map/ppermute | solution.py:612
  17.1 5.7 %collective-permute-start.4 = (bf16[320,256]{1,0:T(8,128)(2,1)S(1)}, bf16[320,256]{1,0:T(8,128)(2,1)S(1)}, u32[]{:S(2)}, u32[]{:S(2)}) collective-permute-start(bf16[320,256]{1,0:T(8,128)(2,1)S(1)} %pad_maximum_fusion.1), channel_id=1, source_target_pairs={{0,16},{1,5},{2,18},{3,7},{4,20},{5,1},{6,22},{7,3},{8,24},{9,13},... | collective-permute-start | bytes 491528 | tf_op jit(solution)/shard_map/ppermute | solution.py:612
  22.8 11.4 %collective-permute-start.7 = (bf16[1280,256]{1,0:T(8,128)(2,1)S(1)}, bf16[1280,256]{1,0:T(8,128)(2,1)S(1)}, u32[]{:S(2)}, u32[]{:S(2)}) collective-permute-start(bf16[1280,256]{1,0:T(8,128)(2,1)S(1)} %constant_dynamic-update-slice_fusion.rest_6_), channel_id=1, source_target_pairs={{0,2},{1,9},{2,4},{3,11},{4,6},{5,13},{6,0},{7,15},{8,10},{9,17},{... | collective-permute-start | bytes 1966088 | tf_op jit(solution)/shard_map/ppermute | solution.py:620
  24.2 10.1 %collective-permute-start.8 = (bf16[1280,256]{1,0:T(8,128)(2,1)S(1)}, bf16[1280,256]{1,0:T(8,128)(2,1)S(1)}, u32[]{:S(2)}, u32[]{:S(2)}) collective-permute-start(bf16[1280,256]{1,0:T(8,128)(2,1)S(1)} %constant_dynamic-update-slice_fusion.rest_6_), channel_id=1, source_target_pairs={{0,6},{1,25},{2,0},{3,27},{4,2},{5,29},{6,4},{7,31},{8,14},{9,1},{... | collective-permute-start | bytes 1966088 | tf_op jit(solution)/shard_map/ppermute | solution.py:620
  26.0 21.7 %collective-permute-start.6 = (bf16[1280,256]{1,0:T(8,128)(2,1)S(1)}, bf16[1280,256]{1,0:T(8,128)(2,1)S(1)}, u32[]{:S(2)}, u32[]{:S(2)}) collective-permute-start(bf16[1280,256]{1,0:T(8,128)(2,1)S(1)} %constant_dynamic-update-slice_fusion.rest_6_), channel_id=1, source_target_pairs={{0,1},{1,0},{2,3},{3,2},{4,5},{5,4},{6,7},{7,6},{8,9},{9,8},{10,11... | collective-permute-start | bytes 1966088 | tf_op jit(solution)/shard_map/ppermute | solution.py:629
  28.8 16.7 %collective-permute-start.5 = (bf16[256,768]{1,0:T(8,128)(2,1)S(1)}, bf16[256,768]{1,0:T(8,128)(2,1)S(1)}, u32[]{:S(2)}, u32[]{:S(2)}) collective-permute-start(bf16[256,768]{1,0:T(8,128)(2,1)S(1)} %pad_maximum_fusion), channel_id=1, source_target_pairs={{0,126},{1,127},{2,124},{3,125},{4,122},{5,123},{6,120},{7,121},{8... | collective-permute-start | bytes 1179656 | tf_op jit(solution)/shard_map/ppermute | solution.py:586
  34.2 29.8 %collective-permute-start.11 = (bf16[640,256]{1,0:T(8,128)(2,1)S(1)}, bf16[640,256]{1,0:T(8,128)(2,1)S(1)}, u32[]{:S(2)}, u32[]{:S(2)}) collective-permute-start(bf16[640,256]{1,0:T(8,128)(2,1)S(1)} %slice.56), channel_id=1, source_target_pairs={{0,2},{1,9},{2,4},{3,11},{4,6},{5,13},{6,0},{7,15},{8,10},{9,17},{... | collective-permute-start | bytes 983048 | tf_op jit(solution)/shard_map/ppermute | solution.py:625
  34.3 29.8 %collective-permute-start.12 = (bf16[640,256]{1,0:T(8,128)(2,1)S(1)}, bf16[640,256]{1,0:T(8,128)(2,1)S(1)}, u32[]{:S(2)}, u32[]{:S(2)}) collective-permute-start(bf16[640,256]{1,0:T(8,128)(2,1)S(1)} %slice.57), channel_id=1, source_target_pairs={{0,6},{1,25},{2,0},{3,27},{4,2},{5,29},{6,4},{7,31},{8,14},{9,1},{... | collective-permute-start | bytes 983048 | tf_op jit(solution)/shard_map/ppermute | solution.py:625
  37.0 27.6 %collective-permute-start.10 = (bf16[1280,256]{1,0:T(8,128)(2,1)S(1)}, bf16[1280,256]{1,0:T(8,128)(2,1)S(1)}, u32[]{:S(2)}, u32[]{:S(2)}) collective-permute-start(bf16[1280,256]{1,0:T(8,128)(2,1)S(1)} %collective-permute-done.8.rest_6_), channel_id=1, source_target_pairs={{0,1},{1,0},{2,3},{3,2},{4,5},{5,4},{6,7},{7,6},{8,9},{9,8},{10,11... | collective-permute-start | bytes 1966088 | tf_op jit(solution)/shard_map/ppermute | solution.py:629
  45.5 19.2 %collective-permute-start.9 = (bf16[1280,256]{1,0:T(8,128)(2,1)S(1)}, bf16[1280,256]{1,0:T(8,128)(2,1)S(1)}, u32[]{:S(2)}, u32[]{:S(2)}) collective-permute-start(bf16[1280,256]{1,0:T(8,128)(2,1)S(1)} %collective-permute-done.7.rest_5_), channel_id=1, source_target_pairs={{0,1},{1,0},{2,3},{3,2},{4,5},{5,4},{6,7},{7,6},{8,9},{9,8},{10,11... | collective-permute-start | bytes 1966088 | tf_op jit(solution)/shard_map/ppermute | solution.py:629
  47.7 1.0 copy-start.4
  64.0 8.0 %collective-permute-start.13 = (bf16[640,256]{1,0:T(8,128)(2,1)S(1)}, bf16[640,256]{1,0:T(8,128)(2,1)S(1)}, u32[]{:S(2)}, u32[]{:S(2)}) collective-permute-start(bf16[640,256]{1,0:T(8,128)(2,1)S(1)} %collective-permute-done.11.rest_8_), channel_id=1, source_target_pairs={{0,1},{1,0},{2,3},{3,2},{4,5},{5,4},{6,7},{7,6},{8,9},{9,8},{10,11... | collective-permute-start | bytes 983048 | tf_op jit(solution)/shard_map/ppermute | solution.py:629
  64.1 7.9 %collective-permute-start.14 = (bf16[640,256]{1,0:T(8,128)(2,1)S(1)}, bf16[640,256]{1,0:T(8,128)(2,1)S(1)}, u32[]{:S(2)}, u32[]{:S(2)}) collective-permute-start(bf16[640,256]{1,0:T(8,128)(2,1)S(1)} %collective-permute-done.12.rest_9_), channel_id=1, source_target_pairs={{0,1},{1,0},{2,3},{3,2},{4,5},{5,4},{6,7},{7,6},{8,9},{9,8},{10,11... | collective-permute-start | bytes 983048 | tf_op jit(solution)/shard_map/ppermute | solution.py:629
  64.6 7.4 %copy-start.5 = (bf16[256,512]{1,0:T(8,128)(2,1)S(1)}, bf16[256,512]{1,0:T(8,128)(2,1)}, u32[]{:S(2)}) copy-start(bf16[256,512]{1,0:T(8,128)(2,1)} %rest_5_.1) | copy-start | bytes 786436
  72.0 26.4 %copy-start.3 = (f32[2048]{0:T(1024)S(1)}, f32[2048]{0:T(1024)}, u32[]{:S(2)}) copy-start(f32[2048]{0:T(1024)} %param.23) | copy-start | bytes 24580
  81.1 11.3 %collective-permute-start.15 = (bf16[128,640]{1,0:T(8,128)(2,1)}, bf16[128,640]{1,0:T(8,128)(2,1)S(1)}, u32[]{:S(2)}, u32[]{:S(2)}) collective-permute-start(bf16[128,640]{1,0:T(8,128)(2,1)} %get-tuple-element.53), channel_id=1, source_target_pairs={{0,126},{1,127},{2,124},{3,125},{4,122},{5,123},{6,120},{7,121},{8... | collective-permute-start | bytes 491528 | tf_op jit(solution)/shard_map/ppermute | solution.py:647
  86.4 6.0 %collective-permute-start.16 = (bf16[128,640]{1,0:T(8,128)(2,1)}, bf16[128,640]{1,0:T(8,128)(2,1)S(1)}, u32[]{:S(2)}, u32[]{:S(2)}) collective-permute-start(bf16[128,640]{1,0:T(8,128)(2,1)} %get-tuple-element.52), channel_id=1, source_target_pairs={{0,1},{1,0},{2,3},{3,2},{4,5},{5,4},{6,7},{7,6},{8,9},{9,8},{10,11... | collective-permute-start | bytes 491528 | tf_op jit(solution)/shard_map/ppermute | solution.py:649
  86.8 11.6 %collective-permute-start.17 = (bf16[128,640]{1,0:T(8,128)(2,1)}, bf16[128,640]{1,0:T(8,128)(2,1)S(1)}, u32[]{:S(2)}, u32[]{:S(2)}) collective-permute-start(bf16[128,640]{1,0:T(8,128)(2,1)} %get-tuple-element.51), channel_id=1, source_target_pairs={{0,127},{1,126},{2,125},{3,124},{4,123},{5,122},{6,121},{7,120},{8... | collective-permute-start | bytes 491528 | tf_op jit(solution)/shard_map/ppermute | solution.py:648
  102.2 34.8 %all-to-all-start = ((bf16[64,8,2048]{2,1,0:T(8,128)(2,1)}), bf16[64,8,2048]{2,1,0:T(8,128)(2,1)S(1)}, u32[]{:S(2)}, u32[]{:S(2)}) async-start(bf16[64,8,2048]{2,1,0:T(8,128)(2,1)} %bitcast.23), calls=%async_computation | async-start | bytes 4194304 | tf_op jit(solution)/shard_map/all_to_all | solution.py:656
  107.7 3.0 %collective-permute-start.18 = (bf16[2048,256]{1,0:T(8,128)(2,1)}, bf16[2048,256]{1,0:T(8,128)(2,1)S(1)}, u32[]{:S(2)}, u32[]{:S(2)}) collective-permute-start(bf16[2048,256]{1,0:T(8,128)(2,1)} %bitcast.24), channel_id=1, source_target_pairs={{0,1},{1,0},{2,3},{3,2},{4,5},{5,4},{6,7},{7,6},{8,9},{9,8},{10,11... | collective-permute-start | bytes 3145736 | tf_op jit(solution)/shard_map/ppermute | solution.py:634
  108.1 4.0 %collective-permute-start.19 = (bf16[2048,256]{1,0:T(8,128)(2,1)}, bf16[2048,256]{1,0:T(8,128)(2,1)S(1)}, u32[]{:S(2)}, u32[]{:S(2)}) collective-permute-start(bf16[2048,256]{1,0:T(8,128)(2,1)} %bitcast.26), channel_id=1, source_target_pairs={{0,1},{1,0},{2,3},{3,2},{4,5},{5,4},{6,7},{7,6},{8,9},{9,8},{10,11... | collective-permute-start | bytes 3145736 | tf_op jit(solution)/shard_map/ppermute | solution.py:634
  108.3 5.5 %collective-permute-start.20 = (bf16[256,2048]{1,0:T(8,128)(2,1)}, bf16[256,2048]{1,0:T(8,128)(2,1)}, u32[]{:S(2)}, u32[]{:S(2)}) collective-permute-start(bf16[256,2048]{1,0:T(8,128)(2,1)} %bitcast.28), channel_id=1, source_target_pairs={{0,1},{1,0},{2,3},{3,2},{4,5},{5,4},{6,7},{7,6},{8,9},{9,8},{10,11... | collective-permute-start | bytes 3145736 | tf_op jit(solution)/shard_map/ppermute | solution.py:634
  110.6 1.5 copy-start.6
  112.1 1.0 copy-start.7
  143.8 6.3 %copy-start.8 = (f32[128,2]{0,1:T(2,128)S(1)}, f32[128,2]{0,1:T(2,128)}, u32[]{:S(2)}) copy-start(f32[128,2]{0,1:T(2,128)} %param.25) | copy-start | bytes 3076
  143.8 34.7 %copy-start = (bf16[128,2048]{1,0:T(8,128)(2,1)S(1)}, bf16[128,2048]{1,0:T(8,128)(2,1)}, u32[]{:S(2)}) copy-start(bf16[128,2048]{1,0:T(8,128)(2,1)} %get-tuple-element.47.hidden) | copy-start | bytes 1572868
  143.8 34.7 %all-to-all-start.1 = ((bf16[64,8,2048]{2,1,0:T(8,128)(2,1)}), bf16[64,8,2048]{2,1,0:T(8,128)(2,1)S(1)}, u32[]{:S(2)}, u32[]{:S(2)}) async-start(bf16[64,8,2048]{2,1,0:T(8,128)(2,1)} %bitcast.22), calls=%async_computation.1 | async-start | bytes 4194304 | tf_op jit(solution)/shard_map/all_to_all | solution.py:660

commit v6 on v5

--- a/solution.py
+++ b/solution.py
@@ -53,16 +53,12 @@
     ]
 
 
-def plane_pairs(table):
-    return [
-        ((from_z * PLANE + r) * N_TP + from_core, (z * PLANE + r) * N_TP + core)
-        for (z, core), (from_z, from_core) in table.items()
-        for r in range(PLANE)
-    ]
-
-
-def shard_first(s, t, k3, k2, kz):
-    s = moved(s, ORDER[t][1], -SHIFTS[k3])
+def partner(s):
+    z, y, x = s // 16, (s // 4) % 4, s % 4
+    return (3 - z) * 16 + (3 - y) * 4 + x
+
+
+def shard_source(s, t, k2, kz):
     s = moved(s, ORDER[t][0], -SHIFTS[k2])
     z, r = divmod(s, PLANE)
     source = (z, t)
@@ -70,7 +66,22 @@
         source = Z_FIRST[source]
     elif source in Z_SECOND:
         source = Z_SECOND[source]
-    return 4 * (source[0] * PLANE + r) + 2 * source[1]
+    return source[0] * PLANE + r, source[1]
+
+
+def line_pairs(k2, kz):
+    pairs = []
+    for s in range(N_SP):
+        for t in range(N_TP):
+            chip, core = shard_source(s, t, k2, kz)
+            if (chip, core) != (s, t):
+                pairs.append((chip * N_TP + core, s * N_TP + t))
+    return pairs
+
+
+def shard_first(s, t, k3, k2, kz):
+    chip, core = shard_source(moved(s, ORDER[t][1], -SHIFTS[k3]), t, k2, kz)
+    return 4 * chip + 2 * core
 
 
 CALLS = (((0, 0), (1, 0)), ((0, 1), (0, 2)), ((1, 1), (1, 2)), ((0, 3), (1, 3)))
@@ -89,7 +100,7 @@
             ]
             rows = []
             for group in range(GROUPS):
-                block = s if group < 2 else N_SP - 1 - s
+                block = s if group < 2 else partner(s)
                 base = 4 * block + 2 * (group % 2)
                 needed = [n for n in range(len(firsts)) if firsts[n] <= base + 1]
                 for at in range(0, len(needed), UNIT):
@@ -128,7 +139,7 @@
         value_up_ref, out_proj_hbm, residual_hbm = take(3)
     parts = take(part_count)
     if last:
-        out_ref, out_proj_ref, residual_ref = take(3)
+        home_same, home_cross, away_same, away_cross, out_proj_ref, residual_ref = take(6)
     if first:
         qabs, q4_ref = take(2)
     m_ref, l_ref, acc_ref, keys, s0, s1, p0, p1, shrink0, shrink1 = take(10)
@@ -278,24 +289,34 @@
     core = field(0, 2)
     lane = lax.broadcasted_iota(jnp.int32, (ROWS, 128), 1)
     for g in range(GROUPS):
-        place = 2 * (g // 2) + jnp.where(core == g % 2, 0, 1)
         total = jnp.sum(l_ref[g], axis=1, keepdims=True)
         total = jnp.where(total > 0.0, total, 1.0)
         mean = jnp.concatenate([acc_ref[g, k] / total for k in range(2)], axis=1).astype(jnp.bfloat16)
         size = m_ref[g] * SCALE2 + jnp.log2(total)
         notes = jnp.zeros((ROWS, 128), jnp.bfloat16)
+        message = []
         for h in range(HEADS_HERE):
             cols = pl.ds(h * V_DIM, V_DIM)
             rows = slice(h * ROWS, (h + 1) * ROWS)
-            out_ref[place, :, cols] = jnp.dot(
-                mean[rows], value_up_ref[:, cols], preferred_element_type=jnp.float32
-            ).astype(jnp.bfloat16)
+            message.append(
+                jnp.dot(mean[rows], value_up_ref[:, cols], preferred_element_type=jnp.float32).astype(jnp.bfloat16)
+            )
             left = size[rows]
             for n in range(3):
                 term = left.astype(jnp.bfloat16)
                 notes = jnp.where(lane == n * HEADS_HERE + h, term, notes)
                 left = left - term.astype(jnp.float32)
-        out_ref[place, :, pl.ds(HEADS_HERE * V_DIM, 128)] = notes
+        message = jnp.concatenate(message + [notes], axis=1)
+        same, cross = (home_same, home_cross) if g < 2 else (away_same, away_cross)
+
+        @pl.when(core == g % 2)
+        def _(same=same, message=message):
+            same[...] = message
+
+        @pl.when(core != g % 2)
+        def _(cross=cross, message=message):
+            cross[...] = message
+
     for fetch in fetches:
         fetch.wait()
 
@@ -319,7 +340,7 @@
     elif last:
         fetched = operands[-2:]
         outs = [
-            pltpu.VMEM((4, ROWS, MESSAGE), jnp.bfloat16),
+            *[pltpu.VMEM((ROWS, MESSAGE), jnp.bfloat16)] * 4,
             pltpu.VMEM((fetched[0].shape[0], EARLY), jnp.bfloat16),
             pltpu.VMEM(fetched[1].shape, jnp.bfloat16),
         ] + outs
@@ -577,18 +598,13 @@
     packed = jnp.concatenate([key_rot[0:32], key_rot[64:96], key_rot[32:64], key_rot[96:128]], axis=1)
     shard = jnp.concatenate([latent, packed], axis=0)
     mirror = [
-        (s * N_TP + t, (N_SP - 1 - s) * N_TP + t) for s in range(N_SP) for t in range(N_TP)
+        (s * N_TP + t, partner(s) * N_TP + t) for s in range(N_SP) for t in range(N_TP)
     ]
     crossing = [
-        (s * N_TP + t, (N_SP - 1 - s) * N_TP + 1 - t) for s in range(N_SP) for t in range(N_TP)
+        (s * N_TP + t, partner(s) * N_TP + 1 - t) for s in range(N_SP) for t in range(N_TP)
     ]
     queries = jnp.concatenate([query_nope, query_rope], axis=1)
     received = lax.ppermute(queries, AXES, mirror)
-
-    near = lax.ppermute(shard, AXES, plane_pairs(Z_FIRST))
-    far = lax.ppermute(shard, AXES, plane_pairs(Z_SECOND))
-    main = (tp_index == 0) == (sp_index < 2 * PLANE)
-    both = jnp.concatenate([jnp.where(main, shard, far), near], axis=0)
 
     flat = routes.reshape(-1)
     order = jnp.arange(flat.shape[0], dtype=jnp.int32)
@@ -599,7 +615,7 @@
     tables = np.concatenate([work_table(call)[1] for call in range(len(CALLS))], axis=1)
     table = lax.dynamic_index_in_dim(jnp.asarray(tables), sp_index * N_TP + tp_index, 0, keepdims=False)
     tokens = jnp.arange(tok_dev, dtype=jnp.int32)
-    query_pos = jnp.concatenate([query_first + tokens, (N_SP - 1 - sp_index) * tok_dev + tokens])
+    query_pos = jnp.concatenate([query_first + tokens, partner(sp_index) * tok_dev + tokens])
     half_width = QK_ROPE // 2
     pair = jnp.arange(HEADS_HERE * QK_ROPE, dtype=jnp.int32) % half_width
     inverse = ROPE_BASE ** (-2.0 * pair.astype(jnp.float32) / QK_ROPE)
@@ -607,11 +623,13 @@
     behind = jnp.arange(HEADS_HERE * QK_ROPE, dtype=jnp.int32) % QK_ROPE >= half_width
     cosine = jnp.cos(angles)
     sine = jnp.where(behind[None, :], jnp.sin(angles), -jnp.sin(angles))
-    got = [both]
-    for by in SHIFTS[1:]:
-        got.append(lax.ppermute(both, AXES, shift_pairs(0, by)))
+    main = (tp_index == 0) == (sp_index < 2 * PLANE)
+    got = []
+    for n in range(8):
+        k2, kz = divmod(n, 2)
+        piece = lax.ppermute(shard, AXES, line_pairs(k2, kz))
+        got.append(jnp.where(main, shard, piece) if n == 0 else piece)
     both = jnp.concatenate(got, axis=0)
-
     both, table, slots, slots_across, cosine, sine = lax.optimization_barrier(
         (both, table, slots, slots_across, cosine, sine)
     )
@@ -643,11 +661,11 @@
         state = attention(call, table, operands, [part for own, k3 in CALLS[call] for part in pieces[own][k3]])
         if call == 0:
             qabs, q4, *state = state
-    attn, out_early, residual = state[:3]
-    mirror_same = lax.ppermute(attn[2], AXES, mirror)
-    mirror_cross = lax.ppermute(attn[3], AXES, crossing)
-    swapped = lax.ppermute(attn[1], "tp", swap)
-    messages = (attn[0], mirror_same, swapped, mirror_cross)
+    home_same, home_cross, away_same, away_cross, out_early, residual = state[:6]
+    mirror_same = lax.ppermute(away_same, AXES, mirror)
+    mirror_cross = lax.ppermute(away_cross, AXES, crossing)
+    swapped = lax.ppermute(home_cross, "tp", swap)
+    messages = (home_same, mirror_same, swapped, mirror_cross)
 
     hidden, outgoing = project(
         tp_index.reshape(1).astype(jnp.int32), messages, out_early, out_proj, residual, norm_gain[None, :], slots_across

time: 182 us -> 183 us (level)
  waiting for transfers between devices: 73.1 us -> 75.5 us
    ppermute x8 -> x11, starting transfers between devices: 18.6 us -> 24.7 us  [the longest x8 19.5 us: local(): piece = lax.ppermute(shard, AXES, line_pairs(k2, kz))]
    ppermute x5, starting transfers between devices: 13.1 us -> 9.62 us  [local(): other_parts.append([lax.ppermute(part, 'tp', swap) for part in group])]
    ppermute x1, starting transfers between devices: 3.2 us -> 0.09 us  [local(): received = lax.ppermute(queries, AXES, mirror)]
    ppermute x2, waiting for transfers between devices: 2.19 us -> 5.03 us  [local(): around.append(lax.ppermute(both, AXES, shift_pairs(1, by)))]
    ppermute x8 -> x11, waiting for transfers between devices: 14.3 us -> 12 us  [the longest x8 4.29 us: local(): piece = lax.ppermute(shard, AXES, line_pairs(k2, kz))]
    unnamed x24 -> x29, local copies, waits for them, and re-layouts: 3.77 us -> 2.86 us
  transfers between devices with their start and end apart: 23 -> 26, of which waited for: 13 -> 12; matrix products, arithmetic and copies ran while one was open for 3% -> 3% of each run, Pallas kernels for 13% -> 13%
where the time goes in v6:
time: 183 us; the launch traced here: 181 us
  waiting for transfers between devices  75.5 us (41%)
  starting transfers between devices  52.6 us (29%)
  Pallas kernels  44.6 us (24%)
  other arithmetic  4.23 us (2%)
  local copies, waits for them, and re-layouts  4.1 us (2%)
    pallas_call x4, Pallas kernels, attention(): pl.pallas_call(functools.partial(attention_body, call, steps, offset, len...  32.4 us
    all_to_all x1, waiting for transfers between devices, local(): lax.all_to_all(produced.reshape(N_SP, CAP, width), 'sp', split_axis=0, co...  28.3 us
    all_to_all x1, waiting for transfers between devices, local(): lax.all_to_all(outgoing.reshape(N_SP, CAP, width), 'sp', split_axis=0, co...  23.9 us
    ppermute x8, starting transfers between devices, local(): piece = lax.ppermute(shard, AXES, line_pairs(k2, kz))  19.5 us
    ppermute x5, starting transfers between devices, local(): other_parts.append([lax.ppermute(part, 'tp', swap) for part in group])  9.62 us
    pallas_call x1, Pallas kernels, experts(): pl.pallas_call(experts_body, out_shape=pltpu.HBM((count, width), jnp.bflo...  6.7 us
    all_to_all x1, starting transfers between devices, local(): lax.all_to_all(produced.reshape(N_SP, CAP, width), 'sp', split_axis=0, co...  6.04 us
    all_to_all x1, starting transfers between devices, local(): lax.all_to_all(outgoing.reshape(N_SP, CAP, width), 'sp', split_axis=0, co...  5.25 us
  transfers between devices with their start and end apart: 26, of which 12 were waited for; matrix products, arithmetic and copies ran while one was open for 3% of the time, Pallas kernels for 13%

profile of v6, /device:TPU:1, one launch (start us, length us, event | category | flops | bytes accessed | tf_op | source)
XLA Modules:
  0.0 181.4 jit_solution(12621338207671066842)
XLA Ops:
  0.0 0.9 copy.42
  0.9 0.3 fusion.14
  1.3 0.9 fusion.12
  2.3 6.9 %collective-permute-start = (bf16[160,256]{1,0:T(8,128)(2,1)S(1)}, bf16[160,256]{1,0:T(8,128)(2,1)S(1)}, u32[]{:S(2)}, u32[]{:S(2)}) collective-permute-start(bf16[160,256]{1,0:T(8,128)(2,1)S(1)} %fusion.12), channel_id=1, source_target_pairs={{64,1},{66,3},{68,5},{70,7},{72,9},{74,11},{76,13},{78,15},{80,17}... | collective-permute-start | bytes 245768 | tf_op jit(solution)/shard_map/ppermute | solution.py:630
  9.2 1.1 collective-permute-start.2
  10.3 1.3 collective-permute-start.3
  11.7 5.1 %collective-permute-start.4 = (bf16[160,256]{1,0:T(8,128)(2,1)S(1)}, bf16[160,256]{1,0:T(8,128)(2,1)S(1)}, u32[]{:S(2)}, u32[]{:S(2)}) collective-permute-start(bf16[160,256]{1,0:T(8,128)(2,1)S(1)} %fusion.12), channel_id=1, source_target_pairs={{8,0},{66,1},{10,2},{68,3},{12,4},{70,5},{14,6},{64,7},{16,8},{74,... | collective-permute-start | bytes 245768 | tf_op jit(solution)/shard_map/ppermute | solution.py:630
  16.7 0.8 copy.44
  17.5 0.7 broadcast_multiply_fusion
  18.4 1.9 %negate_select_fusion = (f32[512,256]{1,0:T(8,128)S(1)}, f32[512,256]{1,0:T(8,128)S(1)}) fusion(f32[256]{0:T(256)S(1)} %fusion.22, f32[512]{0:T(512)S(1)} %add_convert_fusion, pred[256]{0:T(512)(128)(4,1)S(1)} %fusion.23), kind=kLoop, calls=%fused_computation | loop fusion | flops 393216 | bytes 1051904 | tf_op jit(solution)/shard_map/jit(_where)/select_n | solution.py:625
  20.3 0.2 convert_reduce_fusion
  20.8 0.7 dynamic-slice_reduce_fusion.table
  21.5 0.6 collective-permute-start.5
  22.1 1.6 collective-permute-start.6
  23.7 2.8 %collective-permute-start.7 = (bf16[160,256]{1,0:T(8,128)(2,1)S(1)}, bf16[160,256]{1,0:T(8,128)(2,1)S(1)}, u32[]{:S(2)}, u32[]{:S(2)}) collective-permute-start(bf16[160,256]{1,0:T(8,128)(2,1)S(1)} %fusion.12), channel_id=1, source_target_pairs={{112,0},{36,1},{114,2},{38,3},{116,4},{32,5},{118,6},{34,7},{120,8... | collective-permute-start | bytes 245768 | tf_op jit(solution)/shard_map/ppermute | solution.py:630
  26.7 3.6 %collective-permute-done.6 = bf16[160,256]{1,0:T(8,128)(2,1)S(1)} collective-permute-done((bf16[160,256]{1,0:T(8,128)(2,1)S(1)}, bf16[160,256]{1,0:T(8,128)(2,1)S(1)}, u32[]{:S(2)}, u32[]{:S(2)}) %collective-permute-start.6) | collective-permute-done | bytes 81952 | tf_op jit(solution)/shard_map/ppermute | solution.py:630
  30.3 0.7 collective-permute-done.7
  30.9 0.4 collective-permute-start.10
  31.4 2.2 %collective-permute-start.11 = (bf16[1280,256]{1,0:T(8,128)(2,1)S(1)}, bf16[1280,256]{1,0:T(8,128)(2,1)S(1)}, u32[]{:S(2)}, u32[]{:S(2)}) collective-permute-start(bf16[1280,256]{1,0:T(8,128)(2,1)S(1)} %constant_dynamic-update-slice_fusion.rest_6_), channel_id=1, source_target_pairs={{0,6},{1,25},{2,0},{3,27},{4,2},{5,29},{6,4},{7,31},{8,14},{9,1},{... | collective-permute-start | bytes 1966088 | tf_op jit(solution)/shard_map/ppermute | solution.py:638
  33.6 4.5 %collective-permute-start.9 = (bf16[1280,256]{1,0:T(8,128)(2,1)S(1)}, bf16[1280,256]{1,0:T(8,128)(2,1)S(1)}, u32[]{:S(2)}, u32[]{:S(2)}) collective-permute-start(bf16[1280,256]{1,0:T(8,128)(2,1)S(1)} %constant_dynamic-update-slice_fusion.rest_6_), channel_id=1, source_target_pairs={{0,1},{1,0},{2,3},{3,2},{4,5},{5,4},{6,7},{7,6},{8,9},{9,8},{10,11... | collective-permute-start | bytes 1966088 | tf_op jit(solution)/shard_map/ppermute | solution.py:647
  38.2 4.0 %collective-permute-done.10.rest_5_ = bf16[1280,256]{1,0:T(8,128)(2,1)S(1)} collective-permute-done((bf16[1280,256]{1,0:T(8,128)(2,1)S(1)}, bf16[1280,256]{1,0:T(8,128)(2,1)S(1)}, u32[]{:S(2)}, u32[]{:S(2)}) %collective-permute-start.10) | collective-permute-done | bytes 655392 | tf_op jit(solution)/shard_map/ppermute | solution.py:638
  42.3 1.0 collective-permute-done.11.rest_6_
  43.4 3.5 %collective-permute-start.15 = (bf16[640,256]{1,0:T(8,128)(2,1)S(1)}, bf16[640,256]{1,0:T(8,128)(2,1)S(1)}, u32[]{:S(2)}, u32[]{:S(2)}) collective-permute-start(bf16[640,256]{1,0:T(8,128)(2,1)S(1)} %slice.41), channel_id=1, source_target_pairs={{0,6},{1,25},{2,0},{3,27},{4,2},{5,29},{6,4},{7,31},{8,14},{9,1},{... | collective-permute-start | bytes 983048 | tf_op jit(solution)/shard_map/ppermute | solution.py:643
  46.9 3.2 %collective-permute-start.12 = (bf16[1280,256]{1,0:T(8,128)(2,1)S(1)}, bf16[1280,256]{1,0:T(8,128)(2,1)S(1)}, u32[]{:S(2)}, u32[]{:S(2)}) collective-permute-start(bf16[1280,256]{1,0:T(8,128)(2,1)S(1)} %collective-permute-done.10.rest_5_), channel_id=1, source_target_pairs={{0,1},{1,0},{2,3},{3,2},{4,5},{5,4},{6,7},{7,6},{8,9},{9,8},{10,11... | collective-permute-start | bytes 1966088 | tf_op jit(solution)/shard_map/ppermute | solution.py:647
  50.1 2.1 %collective-permute-done.8.rest_2_ = bf16[256,768]{1,0:T(8,128)(2,1)S(1)} collective-permute-done((bf16[256,768]{1,0:T(8,128)(2,1)S(1)}, bf16[256,768]{1,0:T(8,128)(2,1)S(1)}, u32[]{:S(2)}, u32[]{:S(2)}) %collective-permute-start.8) | collective-permute-done | bytes 393248 | tf_op jit(solution)/shard_map/ppermute | solution.py:607
  52.2 1.3 collective-permute-start.13
  53.5 8.1 %shard_map.145 = (bf16[4,2,512,128]{3,2,1,0:T(8,128)(2,1)S(1)}, bf16[4,2,512,128]{3,2,1,0:T(8,128)(2,1)S(1)}, f32[4,512,128]{2,1,0:T(8,128)S(1)}, f32[4,512,128]{2,1,0:T(8,128)S(1)}, f32[4,2,512,128]{3,2,1,0:T(8,128)S(1)}) custom-call(s32[308]{0:T(512)S(1)} %dynamic-slice_reduce_fusion.table, bf16[256,512]{1,0:T(8,128)(2,1)S(1)} %copy-done.1, ...), custom_call_target="tpu_custom_call" | custom-call | flops 4026531840 | bytes 1048576 | tf_op jit(solution)/shard_map/pallas_call | solution.py:354
  61.6 7.3 %shard_map.146 = (f32[4,512,128]{2,1,0:T(8,128)S(1)}, f32[4,512,128]{2,1,0:T(8,128)S(1)}, f32[4,2,512,128]{3,2,1,0:T(8,128)S(1)}) custom-call(s32[308]{0:T(512)S(1)} %dynamic-slice_reduce_fusion.table, bf16[4,2,512,128]{3,2,1,0:T(8,128)(2,1)S(1)} %get-tuple-element.34.rest_0_, ...), custom_call_target="tpu_custom_call", output_to_operand_aliasing={{0}: (3, {}), {1}: (4, {}), {2}: (5, {})} | custom-call | flops 4026531840 | bytes 1048576 | tf_op jit(solution)/shard_map/pallas_call | solution.py:354
  69.1 0.5 collective-permute-start.17
  69.6 7.4 %shard_map.147 = (f32[4,512,128]{2,1,0:T(8,128)S(1)}, f32[4,512,128]{2,1,0:T(8,128)S(1)}, f32[4,2,512,128]{3,2,1,0:T(8,128)S(1)}) custom-call(s32[308]{0:T(512)S(1)} %dynamic-slice_reduce_fusion.table, bf16[4,2,512,128]{3,2,1,0:T(8,128)(2,1)S(1)} %get-tuple-element.34.rest_0_, ...), custom_call_target="tpu_custom_call", output_to_operand_aliasing={{0}: (3, {}), {1}: (4, {}), {2}: (5, {})} | custom-call | flops 4026531840 | bytes 1048576 | tf_op jit(solution)/shard_map/pallas_call | solution.py:354
  77.0 9.6 %shard_map.148 = (bf16[128,640]{1,0:T(8,128)(2,1)S(1)}, bf16[128,640]{1,0:T(8,128)(2,1)}, bf16[128,640]{1,0:T(8,128)(2,1)}, bf16[128,640]{1,0:T(8,128)(2,1)S(1)}...) custom-call(s32[308]{0:T(512)S(1)} %dynamic-slice_reduce_fusion.tabl, ...), custom_call_target="tpu_custom_call", output_to_operand_aliasing={{6}: (3, {}), {7}: (4, {}), {8}: (5, {})} | custom-call | flops 4026531840 | bytes 1048576 | tf_op jit(solution)/shard_map/pallas_call | solution.py:354
  86.6 1.4 collective-permute-start.18
  88.1 0.7 collective-permute-start.19
  88.8 3.1 %collective-permute-start.20 = (bf16[128,640]{1,0:T(8,128)(2,1)S(1)}, bf16[128,640]{1,0:T(8,128)(2,1)S(1)}, u32[]{:S(2)}, u32[]{:S(2)}) collective-permute-start(bf16[128,640]{1,0:T(8,128)(2,1)S(1)} %get-tuple-element.48), channel_id=1, source_target_pairs={{0,121},{1,120},{2,123},{3,122},{4,125},{5,124},{6,127},{7,126},{8... | collective-permute-start | bytes 491528 | tf_op jit(solution)/shard_map/ppermute | solution.py:666
  92.0 4.0 %collective-permute-done.18.mirror_same = bf16[128,640]{1,0:T(8,128)(2,1)S(1)} collective-permute-done((bf16[128,640]{1,0:T(8,128)(2,1)}, bf16[128,640]{1,0:T(8,128)(2,1)S(1)}, u32[]{:S(2)}, u32[]{:S(2)}) %collective-permute-start.18) | collective-permute-done | bytes 163872 | tf_op jit(solution)/shard_map/ppermute | solution.py:665
  95.9 3.7 %collective-permute-done.20.mirror_cross = bf16[128,640]{1,0:T(8,128)(2,1)S(1)} collective-permute-done((bf16[128,640]{1,0:T(8,128)(2,1)S(1)}, bf16[128,640]{1,0:T(8,128)(2,1)S(1)}, u32[]{:S(2)}, u32[]{:S(2)}) %collective-permute-start.20) | collective-permute-done | bytes 163872 | tf_op jit(solution)/shard_map/ppermute | solution.py:666
  99.7 3.8 %project.1 = (bf16[128,2048]{1,0:T(8,128)(2,1)}, bf16[512,2048]{1,0:T(8,128)(2,1)}) custom-call(s32[1]{0:T(128)} %bitcast.core, bf16[128,640]{1,0:T(8,128)(2,1)S(1)} %get-tuple-element.45.local_part, bf16[128,640]{1,0:T(8,128)(2,1)S(1)} %collective-permute-done.18.mirror_same, bf16[128,640]{1,0:T(8,128)(2,1)S(1)} %collective-permute-done.19.swapped, ...), custom_call_target="tpu_custom_call" | custom-call | tf_op jit(solution)/shard_map/project/pallas_call | solution.py:453
  103.5 5.2 %all-to-all-start = ((bf16[64,8,2048]{2,1,0:T(8,128)(2,1)}), bf16[64,8,2048]{2,1,0:T(8,128)(2,1)S(1)}, u32[]{:S(2)}, u32[]{:S(2)}) async-start(bf16[64,8,2048]{2,1,0:T(8,128)(2,1)} %bitcast.15), calls=%async_computation | async-start | bytes 4194304 | tf_op jit(solution)/shard_map/all_to_all | solution.py:674
  109.0 0.4 collective-permute-start.22
  109.5 2.1 %collective-permute-done.21.rest_3_ = bf16[2048,256]{1,0:T(8,128)(2,1)S(1)} collective-permute-done((bf16[2048,256]{1,0:T(8,128)(2,1)S(1)}, bf16[2048,256]{1,0:T(8,128)(2,1)S(1)}, u32[]{:S(2)}, u32[]{:S(2)}) %collective-permute-start.21) | collective-permute-done | bytes 1048608 | tf_op jit(solution)/shard_map/ppermute | solution.py:652
  111.5 1.5 collective-permute-done.22.rest_4_
  113.0 1.0 copy-done.8
  114.0 0.6 collective-permute-done.23.rest_5_
  114.7 23.9 %all-to-all-done = bf16[64,8,2048]{2,1,0:T(8,128)(2,1)S(1)} async-done(((bf16[64,8,2048]{2,1,0:T(8,128)(2,1)}), bf16[64,8,2048]{2,1,0:T(8,128)(2,1)S(1)}, u32[]{:S(2)}, u32[]{:S(2)}) %all-to-all-start) | async-done | bytes 2097184 | tf_op jit(solution)/shard_map/all_to_all | solution.py:674
  138.5 6.7 %experts.1 = bf16[512,2048]{1,0:T(8,128)(2,1)} custom-call(bf16[512,2048]{1,0:T(8,128)(2,1)S(1)} %bitcast.10, bf16[2048,256]{1,0:T(8,128)(2,1)} %bitcast.16, bf16[2048,256]{1,0:T(8,128)(2,1)} %bitcast.19, bf16[256,2048]{1,0:T(8,128)(2,1)} %bitcast.21, bf16[2048,256]{1,0:T(8,128)(2,1)} %copy-done.7, bf16[2048,256]{1,0:T(8,128)(2,1)} %copy-done.8, ...), custom_call_target="tpu_custom_call" | custom-call | tf_op jit(solution)/shard_map/experts/pallas_call | solution.py:514
  145.3 6.0 %all-to-all-start.1 = ((bf16[64,8,2048]{2,1,0:T(8,128)(2,1)}), bf16[64,8,2048]{2,1,0:T(8,128)(2,1)S(1)}, u32[]{:S(2)}, u32[]{:S(2)}) async-start(bf16[64,8,2048]{2,1,0:T(8,128)(2,1)} %bitcast.14), calls=%async_computation.1 | async-start | bytes 4194304 | tf_op jit(solution)/shard_map/all_to_all | solution.py:678
  151.4 28.3 %all-to-all-done.1 = bf16[64,8,2048]{2,1,0:T(8,128)(2,1)S(1)} async-done(((bf16[64,8,2048]{2,1,0:T(8,128)(2,1)}), bf16[64,8,2048]{2,1,0:T(8,128)(2,1)S(1)}, u32[]{:S(2)}, u32[]{:S(2)}) %all-to-all-start.1) | async-done | bytes 2097184 | tf_op jit(solution)/shard_map/all_to_all | solution.py:678
  179.7 1.6 combine.1
  (64 shorter events, 1.5 us)
Async XLA Ops:
  0.0 38.1 %copy-start.1 = (bf16[256,512]{1,0:T(8,128)(2,1)S(1)}, bf16[256,512]{1,0:T(8,128)(2,1)}, u32[]{:S(2)}) copy-start(bf16[256,512]{1,0:T(8,128)(2,1)} %rest_0_.1) | copy-start | bytes 786436
  0.0 38.1 %copy-start.2 = (bf16[256,256]{1,0:T(8,128)(2,1)S(1)}, bf16[256,256]{1,0:T(8,128)(2,1)}, u32[]{:S(2)}) copy-start(bf16[256,256]{1,0:T(8,128)(2,1)} %rest_1_.1) | copy-start | bytes 393220
  2.3 19.2 %collective-permute-start = (bf16[160,256]{1,0:T(8,128)(2,1)S(1)}, bf16[160,256]{1,0:T(8,128)(2,1)S(1)}, u32[]{:S(2)}, u32[]{:S(2)}) collective-permute-start(bf16[160,256]{1,0:T(8,128)(2,1)S(1)} %fusion.12), channel_id=1, source_target_pairs={{64,1},{66,3},{68,5},{70,7},{72,9},{74,11},{76,13},{78,15},{80,17}... | collective-permute-start | bytes 245768 | tf_op jit(solution)/shard_map/ppermute | solution.py:630
  9.1 13.0 %collective-permute-start.1 = (bf16[160,256]{1,0:T(8,128)(2,1)S(1)}, bf16[160,256]{1,0:T(8,128)(2,1)S(1)}, u32[]{:S(2)}, u32[]{:S(2)}) collective-permute-start(bf16[160,256]{1,0:T(8,128)(2,1)S(1)} %fusion.12), channel_id=1, source_target_pairs={{96,0},{32,1},{98,2},{34,3},{100,4},{36,5},{102,6},{38,7},{104,8},... | collective-permute-start | bytes 245768 | tf_op jit(solution)/shard_map/ppermute | solution.py:630
  9.2 14.5 %collective-permute-start.2 = (bf16[160,256]{1,0:T(8,128)(2,1)S(1)}, bf16[160,256]{1,0:T(8,128)(2,1)S(1)}, u32[]{:S(2)}, u32[]{:S(2)}) collective-permute-start(bf16[160,256]{1,0:T(8,128)(2,1)S(1)} %fusion.12), channel_id=1, source_target_pairs={{24,0},{70,1},{26,2},{64,3},{28,4},{66,5},{30,6},{68,7},{0,8},{78,... | collective-permute-start | bytes 245768 | tf_op jit(solution)/shard_map/ppermute | solution.py:630
  10.3 16.3 %collective-permute-start.3 = (bf16[160,256]{1,0:T(8,128)(2,1)S(1)}, bf16[160,256]{1,0:T(8,128)(2,1)S(1)}, u32[]{:S(2)}, u32[]{:S(2)}) collective-permute-start(bf16[160,256]{1,0:T(8,128)(2,1)S(1)} %fusion.12), channel_id=1, source_target_pairs={{120,0},{38,1},{122,2},{32,3},{124,4},{34,5},{126,6},{36,7},{96,8}... | collective-permute-start | bytes 245768 | tf_op jit(solution)/shard_map/ppermute | solution.py:630
  11.7 15.0 %collective-permute-start.4 = (bf16[160,256]{1,0:T(8,128)(2,1)S(1)}, bf16[160,256]{1,0:T(8,128)(2,1)S(1)}, u32[]{:S(2)}, u32[]{:S(2)}) collective-permute-start(bf16[160,256]{1,0:T(8,128)(2,1)S(1)} %fusion.12), channel_id=1, source_target_pairs={{8,0},{66,1},{10,2},{68,3},{12,4},{70,5},{14,6},{64,7},{16,8},{74,... | collective-permute-start | bytes 245768 | tf_op jit(solution)/shard_map/ppermute | solution.py:630
  20.3 33.2 %copy-start.4 = (bf16[256,512]{1,0:T(8,128)(2,1)S(1)}, bf16[256,512]{1,0:T(8,128)(2,1)}, u32[]{:S(2)}) copy-start(bf16[256,512]{1,0:T(8,128)(2,1)} %rest_3_.1) | copy-start | bytes 786436
  21.5 5.1 %collective-permute-start.5 = (bf16[160,256]{1,0:T(8,128)(2,1)S(1)}, bf16[160,256]{1,0:T(8,128)(2,1)S(1)}, u32[]{:S(2)}, u32[]{:S(2)}) collective-permute-start(bf16[160,256]{1,0:T(8,128)(2,1)S(1)} %fusion.12), channel_id=1, source_target_pairs={{104,0},{34,1},{106,2},{36,3},{108,4},{38,5},{110,6},{32,7},{112,8... | collective-permute-start | bytes 245768 | tf_op jit(solution)/shard_map/ppermute | solution.py:630
  22.1 8.1 %collective-permute-start.6 = (bf16[160,256]{1,0:T(8,128)(2,1)S(1)}, bf16[160,256]{1,0:T(8,128)(2,1)S(1)}, u32[]{:S(2)}, u32[]{:S(2)}) collective-permute-start(bf16[160,256]{1,0:T(8,128)(2,1)S(1)} %fusion.12), channel_id=1, source_target_pairs={{16,0},{68,1},{18,2},{70,3},{20,4},{64,5},{22,6},{66,7},{24,8},{76... | collective-permute-start | bytes 245768 | tf_op jit(solution)/shard_map/ppermute | solution.py:630
  23.7 7.2 %collective-permute-start.7 = (bf16[160,256]{1,0:T(8,128)(2,1)S(1)}, bf16[160,256]{1,0:T(8,128)(2,1)S(1)}, u32[]{:S(2)}, u32[]{:S(2)}) collective-permute-start(bf16[160,256]{1,0:T(8,128)(2,1)S(1)} %fusion.12), channel_id=1, source_target_pairs={{112,0},{36,1},{114,2},{38,3},{116,4},{32,5},{118,6},{34,7},{120,8... | collective-permute-start | bytes 245768 | tf_op jit(solution)/shard_map/ppermute | solution.py:630
  30.9 11.3 %collective-permute-start.10 = (bf16[1280,256]{1,0:T(8,128)(2,1)S(1)}, bf16[1280,256]{1,0:T(8,128)(2,1)S(1)}, u32[]{:S(2)}, u32[]{:S(2)}) collective-permute-start(bf16[1280,256]{1,0:T(8,128)(2,1)S(1)} %constant_dynamic-update-slice_fusion.rest_6_), channel_id=1, source_target_pairs={{0,2},{1,9},{2,4},{3,11},{4,6},{5,13},{6,0},{7,15},{8,10},{9,17},{... | collective-permute-start | bytes 1966088 | tf_op jit(solution)/shard_map/ppermute | solution.py:638
  31.4 12.0 %collective-permute-start.11 = (bf16[1280,256]{1,0:T(8,128)(2,1)S(1)}, bf16[1280,256]{1,0:T(8,128)(2,1)S(1)}, u32[]{:S(2)}, u32[]{:S(2)}) collective-permute-start(bf16[1280,256]{1,0:T(8,128)(2,1)S(1)} %constant_dynamic-update-slice_fusion.rest_6_), channel_id=1, source_target_pairs={{0,6},{1,25},{2,0},{3,27},{4,2},{5,29},{6,4},{7,31},{8,14},{9,1},{... | collective-permute-start | bytes 1966088 | tf_op jit(solution)/shard_map/ppermute | solution.py:638
  33.6 19.9 %collective-permute-start.9 = (bf16[1280,256]{1,0:T(8,128)(2,1)S(1)}, bf16[1280,256]{1,0:T(8,128)(2,1)S(1)}, u32[]{:S(2)}, u32[]{:S(2)}) collective-permute-start(bf16[1280,256]{1,0:T(8,128)(2,1)S(1)} %constant_dynamic-update-slice_fusion.rest_6_), channel_id=1, source_target_pairs={{0,1},{1,0},{2,3},{3,2},{4,5},{5,4},{6,7},{7,6},{8,9},{9,8},{10,11... | collective-permute-start | bytes 1966088 | tf_op jit(solution)/shard_map/ppermute | solution.py:647
  38.1 14.1 %collective-permute-start.8 = (bf16[256,768]{1,0:T(8,128)(2,1)S(1)}, bf16[256,768]{1,0:T(8,128)(2,1)S(1)}, u32[]{:S(2)}, u32[]{:S(2)}) collective-permute-start(bf16[256,768]{1,0:T(8,128)(2,1)S(1)} %pad_maximum_fusion), channel_id=1, source_target_pairs={{0,120},{1,121},{2,122},{3,123},{4,124},{5,125},{6,126},{7,127},{8... | collective-permute-start | bytes 1179656 | tf_op jit(solution)/shard_map/ppermute | solution.py:607
  42.3 26.7 %collective-permute-start.14 = (bf16[640,256]{1,0:T(8,128)(2,1)S(1)}, bf16[640,256]{1,0:T(8,128)(2,1)S(1)}, u32[]{:S(2)}, u32[]{:S(2)}) collective-permute-start(bf16[640,256]{1,0:T(8,128)(2,1)S(1)} %slice.40), channel_id=1, source_target_pairs={{0,2},{1,9},{2,4},{3,11},{4,6},{5,13},{6,0},{7,15},{8,10},{9,17},{... | collective-permute-start | bytes 983048 | tf_op jit(solution)/shard_map/ppermute | solution.py:643
  43.4 25.7 %collective-permute-start.15 = (bf16[640,256]{1,0:T(8,128)(2,1)S(1)}, bf16[640,256]{1,0:T(8,128)(2,1)S(1)}, u32[]{:S(2)}, u32[]{:S(2)}) collective-permute-start(bf16[640,256]{1,0:T(8,128)(2,1)S(1)} %slice.41), channel_id=1, source_target_pairs={{0,6},{1,25},{2,0},{3,27},{4,2},{5,29},{6,4},{7,31},{8,14},{9,1},{... | collective-permute-start | bytes 983048 | tf_op jit(solution)/shard_map/ppermute | solution.py:643
  46.9 22.7 %collective-permute-start.12 = (bf16[1280,256]{1,0:T(8,128)(2,1)S(1)}, bf16[1280,256]{1,0:T(8,128)(2,1)S(1)}, u32[]{:S(2)}, u32[]{:S(2)}) collective-permute-start(bf16[1280,256]{1,0:T(8,128)(2,1)S(1)} %collective-permute-done.10.rest_5_), channel_id=1, source_target_pairs={{0,1},{1,0},{2,3},{3,2},{4,5},{5,4},{6,7},{7,6},{8,9},{9,8},{10,11... | collective-permute-start | bytes 1966088 | tf_op jit(solution)/shard_map/ppermute | solution.py:647
  52.2 17.4 %collective-permute-start.13 = (bf16[1280,256]{1,0:T(8,128)(2,1)S(1)}, bf16[1280,256]{1,0:T(8,128)(2,1)S(1)}, u32[]{:S(2)}, u32[]{:S(2)}) collective-permute-start(bf16[1280,256]{1,0:T(8,128)(2,1)S(1)} %collective-permute-done.11.rest_6_), channel_id=1, source_target_pairs={{0,1},{1,0},{2,3},{3,2},{4,5},{5,4},{6,7},{7,6},{8,9},{9,8},{10,11... | collective-permute-start | bytes 1966088 | tf_op jit(solution)/shard_map/ppermute | solution.py:647
  69.0 8.0 %collective-permute-start.16 = (bf16[640,256]{1,0:T(8,128)(2,1)S(1)}, bf16[640,256]{1,0:T(8,128)(2,1)S(1)}, u32[]{:S(2)}, u32[]{:S(2)}) collective-permute-start(bf16[640,256]{1,0:T(8,128)(2,1)S(1)} %collective-permute-done.14.rest_8_), channel_id=1, source_target_pairs={{0,1},{1,0},{2,3},{3,2},{4,5},{5,4},{6,7},{7,6},{8,9},{9,8},{10,11... | collective-permute-start | bytes 983048 | tf_op jit(solution)/shard_map/ppermute | solution.py:647
  69.1 7.9 %collective-permute-start.17 = (bf16[640,256]{1,0:T(8,128)(2,1)S(1)}, bf16[640,256]{1,0:T(8,128)(2,1)S(1)}, u32[]{:S(2)}, u32[]{:S(2)}) collective-permute-start(bf16[640,256]{1,0:T(8,128)(2,1)S(1)} %collective-permute-done.15.rest_9_), channel_id=1, source_target_pairs={{0,1},{1,0},{2,3},{3,2},{4,5},{5,4},{6,7},{7,6},{8,9},{9,8},{10,11... | collective-permute-start | bytes 983048 | tf_op jit(solution)/shard_map/ppermute | solution.py:647
  69.6 7.4 %copy-start.5 = (bf16[256,512]{1,0:T(8,128)(2,1)S(1)}, bf16[256,512]{1,0:T(8,128)(2,1)}, u32[]{:S(2)}) copy-start(bf16[256,512]{1,0:T(8,128)(2,1)} %rest_5_.1) | copy-start | bytes 786436
  77.0 22.7 %copy-start.3 = (f32[2048]{0:T(1024)S(1)}, f32[2048]{0:T(1024)}, u32[]{:S(2)}) copy-start(f32[2048]{0:T(1024)} %param.23) | copy-start | bytes 24580
  86.6 9.3 %collective-permute-start.18 = (bf16[128,640]{1,0:T(8,128)(2,1)}, bf16[128,640]{1,0:T(8,128)(2,1)S(1)}, u32[]{:S(2)}, u32[]{:S(2)}) collective-permute-start(bf16[128,640]{1,0:T(8,128)(2,1)} %get-tuple-element.46), channel_id=1, source_target_pairs={{0,120},{1,121},{2,122},{3,123},{4,124},{5,125},{6,126},{7,127},{8... | collective-permute-start | bytes 491528 | tf_op jit(solution)/shard_map/ppermute | solution.py:665
  88.1 7.9 %collective-permute-start.19 = (bf16[128,640]{1,0:T(8,128)(2,1)}, bf16[128,640]{1,0:T(8,128)(2,1)S(1)}, u32[]{:S(2)}, u32[]{:S(2)}) collective-permute-start(bf16[128,640]{1,0:T(8,128)(2,1)} %get-tuple-element.47), channel_id=1, source_target_pairs={{0,1},{1,0},{2,3},{3,2},{4,5},{5,4},{6,7},{7,6},{8,9},{9,8},{10,11... | collective-permute-start | bytes 491528 | tf_op jit(solution)/shard_map/ppermute | solution.py:667
  88.8 10.9 %collective-permute-start.20 = (bf16[128,640]{1,0:T(8,128)(2,1)S(1)}, bf16[128,640]{1,0:T(8,128)(2,1)S(1)}, u32[]{:S(2)}, u32[]{:S(2)}) collective-permute-start(bf16[128,640]{1,0:T(8,128)(2,1)S(1)} %get-tuple-element.48), channel_id=1, source_target_pairs={{0,121},{1,120},{2,123},{3,122},{4,125},{5,124},{6,127},{7,126},{8... | collective-permute-start | bytes 491528 | tf_op jit(solution)/shard_map/ppermute | solution.py:666
  103.5 5.3 %copy-start.6 = (bf16[1,2048,256]{2,1,0:T(8,128)(2,1)S(1)}, bf16[1,2048,256]{2,1,0:T(8,128)(2,1)}, u32[]{:S(2)}) copy-start(bf16[1,2048,256]{2,1,0:T(8,128)(2,1)} %param.26) | copy-start | bytes 3145732
  103.5 35.0 %all-to-all-start = ((bf16[64,8,2048]{2,1,0:T(8,128)(2,1)}), bf16[64,8,2048]{2,1,0:T(8,128)(2,1)S(1)}, u32[]{:S(2)}, u32[]{:S(2)}) async-start(bf16[64,8,2048]{2,1,0:T(8,128)(2,1)} %bitcast.15), calls=%async_computation | async-start | bytes 4194304 | tf_op jit(solution)/shard_map/all_to_all | solution.py:674
  108.8 2.7 %collective-permute-start.21 = (bf16[2048,256]{1,0:T(8,128)(2,1)S(1)}, bf16[2048,256]{1,0:T(8,128)(2,1)S(1)}, u32[]{:S(2)}, u32[]{:S(2)}) collective-permute-start(bf16[2048,256]{1,0:T(8,128)(2,1)S(1)} %bitcast.17), channel_id=1, source_target_pairs={{0,1},{1,0},{2,3},{3,2},{4,5},{5,4},{6,7},{7,6},{8,9},{9,8},{10,11... | collective-permute-start | bytes 3145736 | tf_op jit(solution)/shard_map/ppermute | solution.py:652
  109.0 4.1 %collective-permute-start.22 = (bf16[2048,256]{1,0:T(8,128)(2,1)}, bf16[2048,256]{1,0:T(8,128)(2,1)S(1)}, u32[]{:S(2)}, u32[]{:S(2)}) collective-permute-start(bf16[2048,256]{1,0:T(8,128)(2,1)} %bitcast.18), channel_id=1, source_target_pairs={{0,1},{1,0},{2,3},{3,2},{4,5},{5,4},{6,7},{7,6},{8,9},{9,8},{10,11... | collective-permute-start | bytes 3145736 | tf_op jit(solution)/shard_map/ppermute | solution.py:652
  109.4 5.3 %collective-permute-start.23 = (bf16[256,2048]{1,0:T(8,128)(2,1)}, bf16[256,2048]{1,0:T(8,128)(2,1)}, u32[]{:S(2)}, u32[]{:S(2)}) collective-permute-start(bf16[256,2048]{1,0:T(8,128)(2,1)} %bitcast.20), channel_id=1, source_target_pairs={{0,1},{1,0},{2,3},{3,2},{4,5},{5,4},{6,7},{7,6},{8,9},{9,8},{10,11... | collective-permute-start | bytes 3145736 | tf_op jit(solution)/shard_map/ppermute | solution.py:652
  111.5 1.5 copy-start.7
  113.0 1.0 copy-start.8
  145.2 6.1 %copy-start.9 = (f32[128,2]{0,1:T(2,128)S(1)}, f32[128,2]{0,1:T(2,128)}, u32[]{:S(2)}) copy-start(f32[128,2]{0,1:T(2,128)} %param.25) | copy-start | bytes 3076
  145.3 34.5 %copy-start = (bf16[128,2048]{1,0:T(8,128)(2,1)S(1)}, bf16[128,2048]{1,0:T(8,128)(2,1)}, u32[]{:S(2)}) copy-start(bf16[128,2048]{1,0:T(8,128)(2,1)} %get-tuple-element.53.hidden) | copy-start | bytes 1572868
  145.3 34.5 %all-to-all-start.1 = ((bf16[64,8,2048]{2,1,0:T(8,128)(2,1)}), bf16[64,8,2048]{2,1,0:T(8,128)(2,1)S(1)}, u32[]{:S(2)}, u32[]{:S(2)}) async-start(bf16[64,8,2048]{2,1,0:T(8,128)(2,1)} %bitcast.14), calls=%async_computation.1 | async-start | bytes 4194304 | tf_op jit(solution)/shard_map/all_to_all | solution.py:678

commit v7 on v6

--- a/solution.py
+++ b/solution.py
@@ -69,14 +69,12 @@
     return source[0] * PLANE + r, source[1]
 
 
-def line_pairs(k2, kz):
-    pairs = []
-    for s in range(N_SP):
-        for t in range(N_TP):
-            chip, core = shard_source(s, t, k2, kz)
-            if (chip, core) != (s, t):
-                pairs.append((chip * N_TP + core, s * N_TP + t))
-    return pairs
+def plane_pairs(table):
+    return [
+        ((from_z * PLANE + r) * N_TP + from_core, (z * PLANE + r) * N_TP + core)
+        for (z, core), (from_z, from_core) in table.items()
+        for r in range(PLANE)
+    ]
 
 
 def shard_first(s, t, k3, k2, kz):
@@ -288,35 +286,25 @@
         return
     core = field(0, 2)
     lane = lax.broadcasted_iota(jnp.int32, (ROWS, 128), 1)
-    for g in range(GROUPS):
+    targets = ((home_same, core), (home_cross, 1 - core), (away_same, 2 + core), (away_cross, 3 - core))
+    for target, g in targets:
         total = jnp.sum(l_ref[g], axis=1, keepdims=True)
         total = jnp.where(total > 0.0, total, 1.0)
         mean = jnp.concatenate([acc_ref[g, k] / total for k in range(2)], axis=1).astype(jnp.bfloat16)
         size = m_ref[g] * SCALE2 + jnp.log2(total)
         notes = jnp.zeros((ROWS, 128), jnp.bfloat16)
-        message = []
         for h in range(HEADS_HERE):
             cols = pl.ds(h * V_DIM, V_DIM)
             rows = slice(h * ROWS, (h + 1) * ROWS)
-            message.append(
-                jnp.dot(mean[rows], value_up_ref[:, cols], preferred_element_type=jnp.float32).astype(jnp.bfloat16)
-            )
+            target[:, cols] = jnp.dot(
+                mean[rows], value_up_ref[:, cols], preferred_element_type=jnp.float32
+            ).astype(jnp.bfloat16)
             left = size[rows]
             for n in range(3):
                 term = left.astype(jnp.bfloat16)
                 notes = jnp.where(lane == n * HEADS_HERE + h, term, notes)
                 left = left - term.astype(jnp.float32)
-        message = jnp.concatenate(message + [notes], axis=1)
-        same, cross = (home_same, home_cross) if g < 2 else (away_same, away_cross)
-
-        @pl.when(core == g % 2)
-        def _(same=same, message=message):
-            same[...] = message
-
-        @pl.when(core != g % 2)
-        def _(cross=cross, message=message):
-            cross[...] = message
-
+        target[:, pl.ds(HEADS_HERE * V_DIM, 128)] = notes
     for fetch in fetches:
         fetch.wait()
 
@@ -606,6 +594,10 @@
     queries = jnp.concatenate([query_nope, query_rope], axis=1)
     received = lax.ppermute(queries, AXES, mirror)
 
+    near = lax.ppermute(shard, AXES, plane_pairs(Z_FIRST))
+    far = lax.ppermute(shard, AXES, plane_pairs(Z_SECOND))
+    main = (tp_index == 0) == (sp_index < 2 * PLANE)
+    both = jnp.concatenate([jnp.where(main, shard, far), near], axis=0)
     flat = routes.reshape(-1)
     order = jnp.arange(flat.shape[0], dtype=jnp.int32)
     earlier = (flat[:, None] == flat[None, :]) & (order[None, :] < order[:, None])
@@ -623,12 +615,9 @@
     behind = jnp.arange(HEADS_HERE * QK_ROPE, dtype=jnp.int32) % QK_ROPE >= half_width
     cosine = jnp.cos(angles)
     sine = jnp.where(behind[None, :], jnp.sin(angles), -jnp.sin(angles))
-    main = (tp_index == 0) == (sp_index < 2 * PLANE)
-    got = []
-    for n in range(8):
-        k2, kz = divmod(n, 2)
-        piece = lax.ppermute(shard, AXES, line_pairs(k2, kz))
-        got.append(jnp.where(main, shard, piece) if n == 0 else piece)
+    got = [both]
+    for by in SHIFTS[1:]:
+        got.append(lax.ppermute(both, AXES, shift_pairs(0, by)))
     both = jnp.concatenate(got, axis=0)
     both, table, slots, slots_across, cosine, sine = lax.optimization_barrier(
         (both, table, slots, slots_across, cosine, sine)
@@ -646,11 +635,6 @@
     for group in own_parts:
         other_parts.append([lax.ppermute(part, "tp", swap) for part in group])
     pieces = (own_parts, other_parts)
-    own_weights = (w_gate[0], w_up[0], w_down[0])
-    other_weights = []
-    for w in own_weights:
-        other_weights.append(lax.ppermute(w, "tp", swap))
-
     state = ()
     for call in range(len(CALLS)):
         operands = (
@@ -674,6 +658,8 @@
     arrived = lax.all_to_all(
         outgoing.reshape(N_SP, CAP, width), "sp", split_axis=0, concat_axis=0, tiled=True
     ).reshape(N_SP * CAP, width)
+    own_weights = (w_gate[0], w_up[0], w_down[0])
+    other_weights = [lax.ppermute(w, "tp", swap) for w in own_weights]
     produced = experts(arrived, own_weights, other_weights)
     back = lax.all_to_all(
         produced.reshape(N_SP, CAP, width), "sp", split_axis=0, concat_axis=0, tiled=True

time: 183 us -> 175 us (0.956)
  starting transfers between devices: 52.6 us -> 45 us
    ppermute x11 -> x8, starting transfers between devices: 20.1 us -> 12 us  [the longest x1 6.87 us: local(): far = lax.ppermute(shard, AXES, plane_pairs(Z_SECOND))]
    ppermute x5, starting transfers between devices: 9.62 us -> 6 us  [local(): other_parts.append([lax.ppermute(part, 'tp', swap) for part in group])]
    ppermute x1, starting transfers between devices: 0.09 us -> 2.18 us  [local(): received = lax.ppermute(queries, AXES, mirror)]
    ppermute x1, starting transfers between devices: 1.42 us -> 3.33 us  [local(): mirror_same = lax.ppermute(away_same, AXES, mirror)]
    ppermute x11 -> x8, waiting for transfers between devices: 8.46 us -> 8.42 us  [the longest x3 4.19 us: local(): other_weights = [lax.ppermute(w, 'tp', swap) for w in own_weights]]
  transfers between devices with their start and end apart: 26 -> 23, of which waited for: 12 -> 14; matrix products, arithmetic and copies ran while one was open for 3% -> 3% of each run, Pallas kernels for 13% -> 13%
where the time goes in v7:
time: 175 us; the launch traced here: 173 us
  waiting for transfers between devices  75.3 us (43%)
  starting transfers between devices  45 us (26%)
  Pallas kernels  43.9 us (25%)
  other arithmetic  4.25 us (2%)
  local copies, waits for them, and re-layouts  4.07 us (2%)
    pallas_call x4, Pallas kernels, attention(): pl.pallas_call(functools.partial(attention_body, call, steps, offset, len...  31.7 us
    all_to_all x1, waiting for transfers between devices, local(): lax.all_to_all(produced.reshape(N_SP, CAP, width), 'sp', split_axis=0, co...  28.3 us
    all_to_all x1, waiting for transfers between devices, local(): lax.all_to_all(outgoing.reshape(N_SP, CAP, width), 'sp', split_axis=0, co...  23.9 us
    ppermute x1, starting transfers between devices, local(): far = lax.ppermute(shard, AXES, plane_pairs(Z_SECOND))  6.87 us
    pallas_call x1, Pallas kernels, experts(): pl.pallas_call(experts_body, out_shape=pltpu.HBM((count, width), jnp.bflo...  6.71 us
    all_to_all x1, starting transfers between devices, local(): lax.all_to_all(outgoing.reshape(N_SP, CAP, width), 'sp', split_axis=0, co...  6.58 us
    all_to_all x1, starting transfers between devices, local(): lax.all_to_all(produced.reshape(N_SP, CAP, width), 'sp', split_axis=0, co...  6.04 us
    ppermute x5, starting transfers between devices, local(): other_parts.append([lax.ppermute(part, 'tp', swap) for part in group])  6 us
  transfers between devices with their start and end apart: 23, of which 14 were waited for; matrix products, arithmetic and copies ran while one was open for 3% of the time, Pallas kernels for 13%

profile of v7, /device:TPU:1, one launch (start us, length us, event | category | flops | bytes accessed | tf_op | source)
XLA Modules:
  0.0 172.9 jit_solution(7733793909995946947)
XLA Ops:
  0.0 0.9 copy.42
  0.9 0.3 fusion.14
  1.3 0.9 fusion.12
  2.3 6.9 %collective-permute-start = (bf16[160,256]{1,0:T(8,128)(2,1)S(1)}, bf16[160,256]{1,0:T(8,128)(2,1)S(1)}, u32[]{:S(2)}, u32[]{:S(2)}) collective-permute-start(bf16[160,256]{1,0:T(8,128)(2,1)S(1)} %fusion.12), channel_id=1, source_target_pairs={{64,1},{66,3},{68,5},{70,7},{72,9},{74,11},{76,13},{78,15},{80,17}... | collective-permute-start | bytes 245768 | tf_op jit(solution)/shard_map/ppermute | solution.py:598
  9.4 1.9 %negate_select_fusion = (f32[512,256]{1,0:T(8,128)S(1)}, f32[512,256]{1,0:T(8,128)S(1)}) fusion(f32[256]{0:T(256)S(1)} %fusion.22, f32[512]{0:T(512)S(1)} %add_convert_fusion, pred[256]{0:T(512)(128)(4,1)S(1)} %fusion.23), kind=kLoop, calls=%fused_computation | loop fusion | flops 393216 | bytes 1051904 | tf_op jit(solution)/shard_map/jit(_where)/select_n | solution.py:617
  11.3 0.7 broadcast_multiply_fusion
  12.0 0.8 copy.44
  13.1 1.3 collective-permute-start.2
  14.4 0.2 convert_reduce_fusion
  14.8 0.7 dynamic-slice_reduce_fusion.table
  15.6 1.5 collective-permute-start.3
  17.1 1.5 collective-permute-start.4
  18.6 0.2 collective-permute-done.2
  18.9 1.2 collective-permute-done.3
  20.1 2.7 %collective-permute-done.4 = bf16[320,256]{1,0:T(8,128)(2,1)S(1)} collective-permute-done((bf16[320,256]{1,0:T(8,128)(2,1)S(1)}, bf16[320,256]{1,0:T(8,128)(2,1)S(1)}, u32[]{:S(2)}, u32[]{:S(2)}) %collective-permute-start.4) | collective-permute-done | bytes 163872 | tf_op jit(solution)/shard_map/ppermute | solution.py:620
  22.8 1.4 collective-permute-start.7
  24.2 1.8 %collective-permute-start.8 = (bf16[1280,256]{1,0:T(8,128)(2,1)S(1)}, bf16[1280,256]{1,0:T(8,128)(2,1)S(1)}, u32[]{:S(2)}, u32[]{:S(2)}) collective-permute-start(bf16[1280,256]{1,0:T(8,128)(2,1)S(1)} %constant_dynamic-update-slice_fusion.rest_6_), channel_id=1, source_target_pairs={{0,6},{1,25},{2,0},{3,27},{4,2},{5,29},{6,4},{7,31},{8,14},{9,1},{... | collective-permute-start | bytes 1966088 | tf_op jit(solution)/shard_map/ppermute | solution.py:627
  26.0 2.8 %collective-permute-start.6 = (bf16[1280,256]{1,0:T(8,128)(2,1)S(1)}, bf16[1280,256]{1,0:T(8,128)(2,1)S(1)}, u32[]{:S(2)}, u32[]{:S(2)}) collective-permute-start(bf16[1280,256]{1,0:T(8,128)(2,1)S(1)} %constant_dynamic-update-slice_fusion.rest_6_), channel_id=1, source_target_pairs={{0,1},{1,0},{2,3},{3,2},{4,5},{5,4},{6,7},{7,6},{8,9},{9,8},{10,11... | collective-permute-start | bytes 1966088 | tf_op jit(solution)/shard_map/ppermute | solution.py:636
  28.8 2.2 %collective-permute-start.5 = (bf16[256,768]{1,0:T(8,128)(2,1)S(1)}, bf16[256,768]{1,0:T(8,128)(2,1)S(1)}, u32[]{:S(2)}, u32[]{:S(2)}) collective-permute-start(bf16[256,768]{1,0:T(8,128)(2,1)S(1)} %pad_maximum_fusion), channel_id=1, source_target_pairs={{0,120},{1,121},{2,122},{3,123},{4,124},{5,125},{6,126},{7,127},{8... | collective-permute-start | bytes 1179656 | tf_op jit(solution)/shard_map/ppermute | solution.py:595
  31.0 3.5 %collective-permute-done.7.rest_5_ = bf16[1280,256]{1,0:T(8,128)(2,1)S(1)} collective-permute-done((bf16[1280,256]{1,0:T(8,128)(2,1)S(1)}, bf16[1280,256]{1,0:T(8,128)(2,1)S(1)}, u32[]{:S(2)}, u32[]{:S(2)}) %collective-permute-start.7) | collective-permute-done | bytes 655392 | tf_op jit(solution)/shard_map/ppermute | solution.py:627
  34.6 0.5 collective-permute-done.8.rest_6_
  35.1 3.5 %collective-permute-start.12 = (bf16[640,256]{1,0:T(8,128)(2,1)S(1)}, bf16[640,256]{1,0:T(8,128)(2,1)S(1)}, u32[]{:S(2)}, u32[]{:S(2)}) collective-permute-start(bf16[640,256]{1,0:T(8,128)(2,1)S(1)} %slice.41), channel_id=1, source_target_pairs={{0,6},{1,25},{2,0},{3,27},{4,2},{5,29},{6,4},{7,31},{8,14},{9,1},{... | collective-permute-start | bytes 983048 | tf_op jit(solution)/shard_map/ppermute | solution.py:632
  38.5 2.2 %collective-permute-start.10 = (bf16[1280,256]{1,0:T(8,128)(2,1)S(1)}, bf16[1280,256]{1,0:T(8,128)(2,1)S(1)}, u32[]{:S(2)}, u32[]{:S(2)}) collective-permute-start(bf16[1280,256]{1,0:T(8,128)(2,1)S(1)} %collective-permute-done.8.rest_6_), channel_id=1, source_target_pairs={{0,1},{1,0},{2,3},{3,2},{4,5},{5,4},{6,7},{7,6},{8,9},{9,8},{10,11... | collective-permute-start | bytes 1966088 | tf_op jit(solution)/shard_map/ppermute | solution.py:636
  40.8 3.0 %collective-permute-done.5.rest_2_ = bf16[256,768]{1,0:T(8,128)(2,1)S(1)} collective-permute-done((bf16[256,768]{1,0:T(8,128)(2,1)S(1)}, bf16[256,768]{1,0:T(8,128)(2,1)S(1)}, u32[]{:S(2)}, u32[]{:S(2)}) %collective-permute-start.5) | collective-permute-done | bytes 393248 | tf_op jit(solution)/shard_map/ppermute | solution.py:595
  43.8 0.4 collective-permute-start.9
  44.2 8.0 %shard_map.145 = (bf16[4,2,512,128]{3,2,1,0:T(8,128)(2,1)S(1)}, bf16[4,2,512,128]{3,2,1,0:T(8,128)(2,1)S(1)}, f32[4,512,128]{2,1,0:T(8,128)S(1)}, f32[4,512,128]{2,1,0:T(8,128)S(1)}, f32[4,2,512,128]{3,2,1,0:T(8,128)S(1)}) custom-call(s32[308]{0:T(512)S(1)} %dynamic-slice_reduce_fusion.table, bf16[256,512]{1,0:T(8,128)(2,1)S(1)} %copy-done.1, ...), custom_call_target="tpu_custom_call" | custom-call | flops 4026531840 | bytes 1048576 | tf_op jit(solution)/shard_map/pallas_call | solution.py:342
  52.3 7.3 %shard_map.146 = (f32[4,512,128]{2,1,0:T(8,128)S(1)}, f32[4,512,128]{2,1,0:T(8,128)S(1)}, f32[4,2,512,128]{3,2,1,0:T(8,128)S(1)}) custom-call(s32[308]{0:T(512)S(1)} %dynamic-slice_reduce_fusion.table, bf16[4,2,512,128]{3,2,1,0:T(8,128)(2,1)S(1)} %get-tuple-element.34.rest_0_, ...), custom_call_target="tpu_custom_call", output_to_operand_aliasing={{0}: (3, {}), {1}: (4, {}), {2}: (5, {})} | custom-call | flops 4026531840 | bytes 1048576 | tf_op jit(solution)/shard_map/pallas_call | solution.py:342
  59.6 0.2 collective-permute-start.13
  59.9 0.4 collective-permute-start.14
  60.2 7.4 %shard_map.147 = (f32[4,512,128]{2,1,0:T(8,128)S(1)}, f32[4,512,128]{2,1,0:T(8,128)S(1)}, f32[4,2,512,128]{3,2,1,0:T(8,128)S(1)}) custom-call(s32[308]{0:T(512)S(1)} %dynamic-slice_reduce_fusion.table, bf16[4,2,512,128]{3,2,1,0:T(8,128)(2,1)S(1)} %get-tuple-element.34.rest_0_, ...), custom_call_target="tpu_custom_call", output_to_operand_aliasing={{0}: (3, {}), {1}: (4, {}), {2}: (5, {})} | custom-call | flops 4026531840 | bytes 1048576 | tf_op jit(solution)/shard_map/pallas_call | solution.py:342
  67.6 9.0 %shard_map.148 = (bf16[128,640]{1,0:T(8,128)(2,1)S(1)}, bf16[128,640]{1,0:T(8,128)(2,1)}, bf16[128,640]{1,0:T(8,128)(2,1)}, bf16[128,640]{1,0:T(8,128)(2,1)S(1)}...) custom-call(s32[308]{0:T(512)S(1)} %dynamic-slice_reduce_fusion.tabl, ...), custom_call_target="tpu_custom_call", output_to_operand_aliasing={{6}: (3, {}), {7}: (4, {}), {8}: (5, {})} | custom-call | flops 4026531840 | bytes 1048576 | tf_op jit(solution)/shard_map/pallas_call | solution.py:342
  76.6 3.3 %collective-permute-start.15 = (bf16[128,640]{1,0:T(8,128)(2,1)}, bf16[128,640]{1,0:T(8,128)(2,1)S(1)}, u32[]{:S(2)}, u32[]{:S(2)}) collective-permute-start(bf16[128,640]{1,0:T(8,128)(2,1)} %get-tuple-element.46), channel_id=1, source_target_pairs={{0,120},{1,121},{2,122},{3,123},{4,124},{5,125},{6,126},{7,127},{8... | collective-permute-start | bytes 491528 | tf_op jit(solution)/shard_map/ppermute | solution.py:649
  79.9 0.7 collective-permute-start.16
  80.7 1.4 collective-permute-start.17
  82.1 3.9 %collective-permute-done.15.mirror_same = bf16[128,640]{1,0:T(8,128)(2,1)S(1)} collective-permute-done((bf16[128,640]{1,0:T(8,128)(2,1)}, bf16[128,640]{1,0:T(8,128)(2,1)S(1)}, u32[]{:S(2)}, u32[]{:S(2)}) %collective-permute-start.15) | collective-permute-done | bytes 163872 | tf_op jit(solution)/shard_map/ppermute | solution.py:649
  86.1 3.8 %collective-permute-done.17.mirror_cross = bf16[128,640]{1,0:T(8,128)(2,1)S(1)} collective-permute-done((bf16[128,640]{1,0:T(8,128)(2,1)S(1)}, bf16[128,640]{1,0:T(8,128)(2,1)S(1)}, u32[]{:S(2)}, u32[]{:S(2)}) %collective-permute-start.17) | collective-permute-done | bytes 163872 | tf_op jit(solution)/shard_map/ppermute | solution.py:650
  89.9 3.8 %project.1 = (bf16[128,2048]{1,0:T(8,128)(2,1)}, bf16[512,2048]{1,0:T(8,128)(2,1)}) custom-call(s32[1]{0:T(128)} %bitcast.core, bf16[128,640]{1,0:T(8,128)(2,1)S(1)} %get-tuple-element.45.local_part, bf16[128,640]{1,0:T(8,128)(2,1)S(1)} %collective-permute-done.15.mirror_same, bf16[128,640]{1,0:T(8,128)(2,1)S(1)} %collective-permute-done.16.swapped, ...), custom_call_target="tpu_custom_call" | custom-call | tf_op jit(solution)/shard_map/project/pallas_call | solution.py:441
  93.7 6.6 %all-to-all-start = ((bf16[64,8,2048]{2,1,0:T(8,128)(2,1)}), bf16[64,8,2048]{2,1,0:T(8,128)(2,1)S(1)}, u32[]{:S(2)}, u32[]{:S(2)}) async-start(bf16[64,8,2048]{2,1,0:T(8,128)(2,1)} %bitcast.15), calls=%async_computation | async-start | bytes 4194304 | tf_op jit(solution)/shard_map/all_to_all | solution.py:658
  100.5 0.4 collective-permute-start.19
  101.0 2.1 %collective-permute-done.18.rest_3_ = bf16[2048,256]{1,0:T(8,128)(2,1)S(1)} collective-permute-done((bf16[2048,256]{1,0:T(8,128)(2,1)S(1)}, bf16[2048,256]{1,0:T(8,128)(2,1)S(1)}, u32[]{:S(2)}, u32[]{:S(2)}) %collective-permute-start.18) | collective-permute-done | bytes 1048608 | tf_op jit(solution)/shard_map/ppermute | solution.py:662
  103.1 1.5 collective-permute-done.19.rest_4_
  104.6 1.0 copy-done.8
  105.6 0.6 collective-permute-done.20.rest_5_
  106.2 23.9 %all-to-all-done = bf16[64,8,2048]{2,1,0:T(8,128)(2,1)S(1)} async-done(((bf16[64,8,2048]{2,1,0:T(8,128)(2,1)}), bf16[64,8,2048]{2,1,0:T(8,128)(2,1)S(1)}, u32[]{:S(2)}, u32[]{:S(2)}) %all-to-all-start) | async-done | bytes 2097184 | tf_op jit(solution)/shard_map/all_to_all | solution.py:658
  130.1 6.7 %experts.1 = bf16[512,2048]{1,0:T(8,128)(2,1)} custom-call(bf16[512,2048]{1,0:T(8,128)(2,1)S(1)} %bitcast.10, bf16[2048,256]{1,0:T(8,128)(2,1)} %bitcast.16, bf16[2048,256]{1,0:T(8,128)(2,1)} %bitcast.19, bf16[256,2048]{1,0:T(8,128)(2,1)} %bitcast.21, bf16[2048,256]{1,0:T(8,128)(2,1)} %copy-done.7, bf16[2048,256]{1,0:T(8,128)(2,1)} %copy-done.8, ...), custom_call_target="tpu_custom_call" | custom-call | tf_op jit(solution)/shard_map/experts/pallas_call | solution.py:502
  136.8 6.0 %all-to-all-start.1 = ((bf16[64,8,2048]{2,1,0:T(8,128)(2,1)}), bf16[64,8,2048]{2,1,0:T(8,128)(2,1)S(1)}, u32[]{:S(2)}, u32[]{:S(2)}) async-start(bf16[64,8,2048]{2,1,0:T(8,128)(2,1)} %bitcast.14), calls=%async_computation.1 | async-start | bytes 4194304 | tf_op jit(solution)/shard_map/all_to_all | solution.py:664
  143.0 28.3 %all-to-all-done.1 = bf16[64,8,2048]{2,1,0:T(8,128)(2,1)S(1)} async-done(((bf16[64,8,2048]{2,1,0:T(8,128)(2,1)}), bf16[64,8,2048]{2,1,0:T(8,128)(2,1)S(1)}, u32[]{:S(2)}, u32[]{:S(2)}) %all-to-all-start.1) | async-done | bytes 2097184 | tf_op jit(solution)/shard_map/all_to_all | solution.py:664
  171.3 1.6 combine.1
  (56 shorter events, 1.5 us)
Async XLA Ops:
  0.0 28.8 %copy-start.1 = (bf16[256,512]{1,0:T(8,128)(2,1)S(1)}, bf16[256,512]{1,0:T(8,128)(2,1)}, u32[]{:S(2)}) copy-start(bf16[256,512]{1,0:T(8,128)(2,1)} %rest_0_.1) | copy-start | bytes 786436
  0.0 28.8 %copy-start.2 = (bf16[256,256]{1,0:T(8,128)(2,1)S(1)}, bf16[256,256]{1,0:T(8,128)(2,1)}, u32[]{:S(2)}) copy-start(bf16[256,256]{1,0:T(8,128)(2,1)} %rest_1_.1) | copy-start | bytes 393220
  2.3 10.7 %collective-permute-start = (bf16[160,256]{1,0:T(8,128)(2,1)S(1)}, bf16[160,256]{1,0:T(8,128)(2,1)S(1)}, u32[]{:S(2)}, u32[]{:S(2)}) collective-permute-start(bf16[160,256]{1,0:T(8,128)(2,1)S(1)} %fusion.12), channel_id=1, source_target_pairs={{64,1},{66,3},{68,5},{70,7},{72,9},{74,11},{76,13},{78,15},{80,17}... | collective-permute-start | bytes 245768 | tf_op jit(solution)/shard_map/ppermute | solution.py:598
  9.1 3.9 %collective-permute-start.1 = (bf16[160,256]{1,0:T(8,128)(2,1)S(1)}, bf16[160,256]{1,0:T(8,128)(2,1)S(1)}, u32[]{:S(2)}, u32[]{:S(2)}) collective-permute-start(bf16[160,256]{1,0:T(8,128)(2,1)S(1)} %fusion.12), channel_id=1, source_target_pairs={{96,0},{98,2},{100,4},{102,6},{104,8},{106,10},{108,12},{110,14},{... | collective-permute-start | bytes 245768 | tf_op jit(solution)/shard_map/ppermute | solution.py:597
  12.9 31.3 %copy-start.4 = (bf16[256,512]{1,0:T(8,128)(2,1)S(1)}, bf16[256,512]{1,0:T(8,128)(2,1)}, u32[]{:S(2)}) copy-start(bf16[256,512]{1,0:T(8,128)(2,1)} %rest_3_.1) | copy-start | bytes 786436
  13.1 5.7 %collective-permute-start.2 = (bf16[320,256]{1,0:T(8,128)(2,1)S(1)}, bf16[320,256]{1,0:T(8,128)(2,1)S(1)}, u32[]{:S(2)}, u32[]{:S(2)}) collective-permute-start(bf16[320,256]{1,0:T(8,128)(2,1)S(1)} %pad_maximum_fusion.1), channel_id=1, source_target_pairs={{0,8},{1,3},{2,10},{3,5},{4,12},{5,7},{6,14},{7,1},{8,16},{9,11},{... | collective-permute-start | bytes 491528 | tf_op jit(solution)/shard_map/ppermute | solution.py:620
  15.6 4.5 %collective-permute-start.3 = (bf16[320,256]{1,0:T(8,128)(2,1)S(1)}, bf16[320,256]{1,0:T(8,128)(2,1)S(1)}, u32[]{:S(2)}, u32[]{:S(2)}) collective-permute-start(bf16[320,256]{1,0:T(8,128)(2,1)S(1)} %pad_maximum_fusion.1), channel_id=1, source_target_pairs={{0,24},{1,7},{2,26},{3,1},{4,28},{5,3},{6,30},{7,5},{8,0},{9,15},{... | collective-permute-start | bytes 491528 | tf_op jit(solution)/shard_map/ppermute | solution.py:620
  17.1 5.7 %collective-permute-start.4 = (bf16[320,256]{1,0:T(8,128)(2,1)S(1)}, bf16[320,256]{1,0:T(8,128)(2,1)S(1)}, u32[]{:S(2)}, u32[]{:S(2)}) collective-permute-start(bf16[320,256]{1,0:T(8,128)(2,1)S(1)} %pad_maximum_fusion.1), channel_id=1, source_target_pairs={{0,16},{1,5},{2,18},{3,7},{4,20},{5,1},{6,22},{7,3},{8,24},{9,13},... | collective-permute-start | bytes 491528 | tf_op jit(solution)/shard_map/ppermute | solution.py:620
  22.8 11.7 %collective-permute-start.7 = (bf16[1280,256]{1,0:T(8,128)(2,1)S(1)}, bf16[1280,256]{1,0:T(8,128)(2,1)S(1)}, u32[]{:S(2)}, u32[]{:S(2)}) collective-permute-start(bf16[1280,256]{1,0:T(8,128)(2,1)S(1)} %constant_dynamic-update-slice_fusion.rest_6_), channel_id=1, source_target_pairs={{0,2},{1,9},{2,4},{3,11},{4,6},{5,13},{6,0},{7,15},{8,10},{9,17},{... | collective-permute-start | bytes 1966088 | tf_op jit(solution)/shard_map/ppermute | solution.py:627
  24.2 10.9 %collective-permute-start.8 = (bf16[1280,256]{1,0:T(8,128)(2,1)S(1)}, bf16[1280,256]{1,0:T(8,128)(2,1)S(1)}, u32[]{:S(2)}, u32[]{:S(2)}) collective-permute-start(bf16[1280,256]{1,0:T(8,128)(2,1)S(1)} %constant_dynamic-update-slice_fusion.rest_6_), channel_id=1, source_target_pairs={{0,6},{1,25},{2,0},{3,27},{4,2},{5,29},{6,4},{7,31},{8,14},{9,1},{... | collective-permute-start | bytes 1966088 | tf_op jit(solution)/shard_map/ppermute | solution.py:627
  26.0 18.2 %collective-permute-start.6 = (bf16[1280,256]{1,0:T(8,128)(2,1)S(1)}, bf16[1280,256]{1,0:T(8,128)(2,1)S(1)}, u32[]{:S(2)}, u32[]{:S(2)}) collective-permute-start(bf16[1280,256]{1,0:T(8,128)(2,1)S(1)} %constant_dynamic-update-slice_fusion.rest_6_), channel_id=1, source_target_pairs={{0,1},{1,0},{2,3},{3,2},{4,5},{5,4},{6,7},{7,6},{8,9},{9,8},{10,11... | collective-permute-start | bytes 1966088 | tf_op jit(solution)/shard_map/ppermute | solution.py:636
  28.8 15.0 %collective-permute-start.5 = (bf16[256,768]{1,0:T(8,128)(2,1)S(1)}, bf16[256,768]{1,0:T(8,128)(2,1)S(1)}, u32[]{:S(2)}, u32[]{:S(2)}) collective-permute-start(bf16[256,768]{1,0:T(8,128)(2,1)S(1)} %pad_maximum_fusion), channel_id=1, source_target_pairs={{0,120},{1,121},{2,122},{3,123},{4,124},{5,125},{6,126},{7,127},{8... | collective-permute-start | bytes 1179656 | tf_op jit(solution)/shard_map/ppermute | solution.py:595
  34.5 25.1 %collective-permute-start.11 = (bf16[640,256]{1,0:T(8,128)(2,1)S(1)}, bf16[640,256]{1,0:T(8,128)(2,1)S(1)}, u32[]{:S(2)}, u32[]{:S(2)}) collective-permute-start(bf16[640,256]{1,0:T(8,128)(2,1)S(1)} %slice.40), channel_id=1, source_target_pairs={{0,2},{1,9},{2,4},{3,11},{4,6},{5,13},{6,0},{7,15},{8,10},{9,17},{... | collective-permute-start | bytes 983048 | tf_op jit(solution)/shard_map/ppermute | solution.py:632
  35.1 24.8 %collective-permute-start.12 = (bf16[640,256]{1,0:T(8,128)(2,1)S(1)}, bf16[640,256]{1,0:T(8,128)(2,1)S(1)}, u32[]{:S(2)}, u32[]{:S(2)}) collective-permute-start(bf16[640,256]{1,0:T(8,128)(2,1)S(1)} %slice.41), channel_id=1, source_target_pairs={{0,6},{1,25},{2,0},{3,27},{4,2},{5,29},{6,4},{7,31},{8,14},{9,1},{... | collective-permute-start | bytes 983048 | tf_op jit(solution)/shard_map/ppermute | solution.py:632
  38.5 21.7 %collective-permute-start.10 = (bf16[1280,256]{1,0:T(8,128)(2,1)S(1)}, bf16[1280,256]{1,0:T(8,128)(2,1)S(1)}, u32[]{:S(2)}, u32[]{:S(2)}) collective-permute-start(bf16[1280,256]{1,0:T(8,128)(2,1)S(1)} %collective-permute-done.8.rest_6_), channel_id=1, source_target_pairs={{0,1},{1,0},{2,3},{3,2},{4,5},{5,4},{6,7},{7,6},{8,9},{9,8},{10,11... | collective-permute-start | bytes 1966088 | tf_op jit(solution)/shard_map/ppermute | solution.py:636
  43.8 16.4 %collective-permute-start.9 = (bf16[1280,256]{1,0:T(8,128)(2,1)S(1)}, bf16[1280,256]{1,0:T(8,128)(2,1)S(1)}, u32[]{:S(2)}, u32[]{:S(2)}) collective-permute-start(bf16[1280,256]{1,0:T(8,128)(2,1)S(1)} %collective-permute-done.7.rest_5_), channel_id=1, source_target_pairs={{0,1},{1,0},{2,3},{3,2},{4,5},{5,4},{6,7},{7,6},{8,9},{9,8},{10,11... | collective-permute-start | bytes 1966088 | tf_op jit(solution)/shard_map/ppermute | solution.py:636
  59.6 8.0 %collective-permute-start.13 = (bf16[640,256]{1,0:T(8,128)(2,1)S(1)}, bf16[640,256]{1,0:T(8,128)(2,1)S(1)}, u32[]{:S(2)}, u32[]{:S(2)}) collective-permute-start(bf16[640,256]{1,0:T(8,128)(2,1)S(1)} %collective-permute-done.11.rest_8_), channel_id=1, source_target_pairs={{0,1},{1,0},{2,3},{3,2},{4,5},{5,4},{6,7},{7,6},{8,9},{9,8},{10,11... | collective-permute-start | bytes 983048 | tf_op jit(solution)/shard_map/ppermute | solution.py:636
  59.9 7.8 %collective-permute-start.14 = (bf16[640,256]{1,0:T(8,128)(2,1)S(1)}, bf16[640,256]{1,0:T(8,128)(2,1)S(1)}, u32[]{:S(2)}, u32[]{:S(2)}) collective-permute-start(bf16[640,256]{1,0:T(8,128)(2,1)S(1)} %collective-permute-done.12.rest_9_), channel_id=1, source_target_pairs={{0,1},{1,0},{2,3},{3,2},{4,5},{5,4},{6,7},{7,6},{8,9},{9,8},{10,11... | collective-permute-start | bytes 983048 | tf_op jit(solution)/shard_map/ppermute | solution.py:636
  60.2 7.4 %copy-start.5 = (bf16[256,512]{1,0:T(8,128)(2,1)S(1)}, bf16[256,512]{1,0:T(8,128)(2,1)}, u32[]{:S(2)}) copy-start(bf16[256,512]{1,0:T(8,128)(2,1)} %rest_5_.1) | copy-start | bytes 786436
  67.6 22.2 %copy-start.3 = (f32[2048]{0:T(1024)S(1)}, f32[2048]{0:T(1024)}, u32[]{:S(2)}) copy-start(f32[2048]{0:T(1024)} %param.23) | copy-start | bytes 24580
  76.6 9.5 %collective-permute-start.15 = (bf16[128,640]{1,0:T(8,128)(2,1)}, bf16[128,640]{1,0:T(8,128)(2,1)S(1)}, u32[]{:S(2)}, u32[]{:S(2)}) collective-permute-start(bf16[128,640]{1,0:T(8,128)(2,1)} %get-tuple-element.46), channel_id=1, source_target_pairs={{0,120},{1,121},{2,122},{3,123},{4,124},{5,125},{6,126},{7,127},{8... | collective-permute-start | bytes 491528 | tf_op jit(solution)/shard_map/ppermute | solution.py:649
  79.9 6.1 %collective-permute-start.16 = (bf16[128,640]{1,0:T(8,128)(2,1)}, bf16[128,640]{1,0:T(8,128)(2,1)S(1)}, u32[]{:S(2)}, u32[]{:S(2)}) collective-permute-start(bf16[128,640]{1,0:T(8,128)(2,1)} %get-tuple-element.47), channel_id=1, source_target_pairs={{0,1},{1,0},{2,3},{3,2},{4,5},{5,4},{6,7},{7,6},{8,9},{9,8},{10,11... | collective-permute-start | bytes 491528 | tf_op jit(solution)/shard_map/ppermute | solution.py:651
  80.7 9.2 %collective-permute-start.17 = (bf16[128,640]{1,0:T(8,128)(2,1)S(1)}, bf16[128,640]{1,0:T(8,128)(2,1)S(1)}, u32[]{:S(2)}, u32[]{:S(2)}) collective-permute-start(bf16[128,640]{1,0:T(8,128)(2,1)S(1)} %get-tuple-element.48), channel_id=1, source_target_pairs={{0,121},{1,120},{2,123},{3,122},{4,125},{5,124},{6,127},{7,126},{8... | collective-permute-start | bytes 491528 | tf_op jit(solution)/shard_map/ppermute | solution.py:650
  93.7 6.6 %copy-start.6 = (bf16[1,2048,256]{2,1,0:T(8,128)(2,1)S(1)}, bf16[1,2048,256]{2,1,0:T(8,128)(2,1)}, u32[]{:S(2)}) copy-start(bf16[1,2048,256]{2,1,0:T(8,128)(2,1)} %param.26) | copy-start | bytes 3145732
  93.7 36.3 %all-to-all-start = ((bf16[64,8,2048]{2,1,0:T(8,128)(2,1)}), bf16[64,8,2048]{2,1,0:T(8,128)(2,1)S(1)}, u32[]{:S(2)}, u32[]{:S(2)}) async-start(bf16[64,8,2048]{2,1,0:T(8,128)(2,1)} %bitcast.15), calls=%async_computation | async-start | bytes 4194304 | tf_op jit(solution)/shard_map/all_to_all | solution.py:658
  100.3 2.7 %collective-permute-start.18 = (bf16[2048,256]{1,0:T(8,128)(2,1)S(1)}, bf16[2048,256]{1,0:T(8,128)(2,1)S(1)}, u32[]{:S(2)}, u32[]{:S(2)}) collective-permute-start(bf16[2048,256]{1,0:T(8,128)(2,1)S(1)} %bitcast.17), channel_id=1, source_target_pairs={{0,1},{1,0},{2,3},{3,2},{4,5},{5,4},{6,7},{7,6},{8,9},{9,8},{10,11... | collective-permute-start | bytes 3145736 | tf_op jit(solution)/shard_map/ppermute | solution.py:662
  100.5 4.1 %collective-permute-start.19 = (bf16[2048,256]{1,0:T(8,128)(2,1)}, bf16[2048,256]{1,0:T(8,128)(2,1)S(1)}, u32[]{:S(2)}, u32[]{:S(2)}) collective-permute-start(bf16[2048,256]{1,0:T(8,128)(2,1)} %bitcast.18), channel_id=1, source_target_pairs={{0,1},{1,0},{2,3},{3,2},{4,5},{5,4},{6,7},{7,6},{8,9},{9,8},{10,11... | collective-permute-start | bytes 3145736 | tf_op jit(solution)/shard_map/ppermute | solution.py:662
  100.9 5.3 %collective-permute-start.20 = (bf16[256,2048]{1,0:T(8,128)(2,1)}, bf16[256,2048]{1,0:T(8,128)(2,1)}, u32[]{:S(2)}, u32[]{:S(2)}) collective-permute-start(bf16[256,2048]{1,0:T(8,128)(2,1)} %bitcast.20), channel_id=1, source_target_pairs={{0,1},{1,0},{2,3},{3,2},{4,5},{5,4},{6,7},{7,6},{8,9},{9,8},{10,11... | collective-permute-start | bytes 3145736 | tf_op jit(solution)/shard_map/ppermute | solution.py:662
  103.1 1.5 copy-start.7
  104.6 1.0 copy-start.8
  136.8 6.1 %copy-start.9 = (f32[128,2]{0,1:T(2,128)S(1)}, f32[128,2]{0,1:T(2,128)}, u32[]{:S(2)}) copy-start(f32[128,2]{0,1:T(2,128)} %param.25) | copy-start | bytes 3076
  136.8 34.5 %copy-start = (bf16[128,2048]{1,0:T(8,128)(2,1)S(1)}, bf16[128,2048]{1,0:T(8,128)(2,1)}, u32[]{:S(2)}) copy-start(bf16[128,2048]{1,0:T(8,128)(2,1)} %get-tuple-element.53.hidden) | copy-start | bytes 1572868
  136.8 34.5 %all-to-all-start.1 = ((bf16[64,8,2048]{2,1,0:T(8,128)(2,1)}), bf16[64,8,2048]{2,1,0:T(8,128)(2,1)S(1)}, u32[]{:S(2)}, u32[]{:S(2)}) async-start(bf16[64,8,2048]{2,1,0:T(8,128)(2,1)} %bitcast.14), calls=%async_computation.1 | async-start | bytes 4194304 | tf_op jit(solution)/shard_map/all_to_all | solution.py:664

commit v8 on v7

--- a/solution.py
+++ b/solution.py
@@ -473,14 +473,18 @@
     stores = []
     for n in range(2):
         gate, up, down = weights[3 * n : 3 * n + 3]
-        loads[3 * n].wait()
-        loads[3 * n + 1].wait()
-        actives = []
-        for k in range(2):
-            x = rows[pl.ds(k * block, block), :]
-            gated = jnp.dot(x, gate[...], preferred_element_type=jnp.float32)
-            raised = jnp.dot(x, up[...], preferred_element_type=jnp.float32)
-            actives.append((gated / (1.0 + jnp.exp(-gated)) * raised).astype(jnp.bfloat16))
+        parts = []
+        for weight, load in ((gate, loads[3 * n]), (up, loads[3 * n + 1])):
+            load.wait()
+            parts.append(
+                [
+                    jnp.dot(rows[pl.ds(k * block, block), :], weight[...], preferred_element_type=jnp.float32)
+                    for k in range(2)
+                ]
+            )
+        actives = [
+            (gated / (1.0 + jnp.exp(-gated)) * raised).astype(jnp.bfloat16) for gated, raised in zip(*parts)
+        ]
         loads[3 * n + 2].wait()
         for k in range(2):
             at = pl.ds(k * block, block)

time: 175 us -> 175 us (level)
  no operation moved by 1% of the time
where the time goes in v8:
time: 175 us; the launch traced here: 173 us
  waiting for transfers between devices  75.3 us (43%)
  starting transfers between devices  45 us (26%)
  Pallas kernels  43.9 us (25%)
  other arithmetic  4.25 us (2%)
  local copies, waits for them, and re-layouts  4.07 us (2%)
    pallas_call x4, Pallas kernels, attention(): pl.pallas_call(functools.partial(attention_body, call, steps, offset, len...  31.7 us
    all_to_all x1, waiting for transfers between devices, local(): lax.all_to_all(produced.reshape(N_SP, CAP, width), 'sp', split_axis=0, co...  28.3 us
    all_to_all x1, waiting for transfers between devices, local(): lax.all_to_all(outgoing.reshape(N_SP, CAP, width), 'sp', split_axis=0, co...  23.9 us
    ppermute x1, starting transfers between devices, local(): far = lax.ppermute(shard, AXES, plane_pairs(Z_SECOND))  6.87 us
    pallas_call x1, Pallas kernels, experts(): pl.pallas_call(experts_body, out_shape=pltpu.HBM((count, width), jnp.bflo...  6.69 us
    all_to_all x1, starting transfers between devices, local(): lax.all_to_all(outgoing.reshape(N_SP, CAP, width), 'sp', split_axis=0, co...  6.58 us
    all_to_all x1, starting transfers between devices, local(): lax.all_to_all(produced.reshape(N_SP, CAP, width), 'sp', split_axis=0, co...  6.04 us
    ppermute x5, starting transfers between devices, local(): other_parts.append([lax.ppermute(part, 'tp', swap) for part in group])  6 us
  transfers between devices with their start and end apart: 23, of which 14 were waited for; matrix products, arithmetic and copies ran while one was open for 3% of the time, Pallas kernels for 13%

profile of v8, /device:TPU:1, one launch (start us, length us, event | category | flops | bytes accessed | tf_op | source)
XLA Modules:
  0.0 172.9 jit_solution(15698363516128496112)
XLA Ops:
  0.0 0.9 copy.42
  0.9 0.3 fusion.14
  1.3 0.9 fusion.12
  2.3 6.9 %collective-permute-start = (bf16[160,256]{1,0:T(8,128)(2,1)S(1)}, bf16[160,256]{1,0:T(8,128)(2,1)S(1)}, u32[]{:S(2)}, u32[]{:S(2)}) collective-permute-start(bf16[160,256]{1,0:T(8,128)(2,1)S(1)} %fusion.12), channel_id=1, source_target_pairs={{64,1},{66,3},{68,5},{70,7},{72,9},{74,11},{76,13},{78,15},{80,17}... | collective-permute-start | bytes 245768 | tf_op jit(solution)/shard_map/ppermute | solution.py:602
  9.4 1.9 %negate_select_fusion = (f32[512,256]{1,0:T(8,128)S(1)}, f32[512,256]{1,0:T(8,128)S(1)}) fusion(f32[256]{0:T(256)S(1)} %fusion.22, f32[512]{0:T(512)S(1)} %add_convert_fusion, pred[256]{0:T(512)(128)(4,1)S(1)} %fusion.23), kind=kLoop, calls=%fused_computation | loop fusion | flops 393216 | bytes 1051904 | tf_op jit(solution)/shard_map/jit(_where)/select_n | solution.py:621
  11.3 0.7 broadcast_multiply_fusion
  12.0 0.8 copy.44
  13.1 1.3 collective-permute-start.2
  14.4 0.2 convert_reduce_fusion
  14.8 0.7 dynamic-slice_reduce_fusion.table
  15.6 1.5 collective-permute-start.3
  17.1 1.5 collective-permute-start.4
  18.6 0.2 collective-permute-done.2
  18.9 1.2 collective-permute-done.3
  20.1 2.7 %collective-permute-done.4 = bf16[320,256]{1,0:T(8,128)(2,1)S(1)} collective-permute-done((bf16[320,256]{1,0:T(8,128)(2,1)S(1)}, bf16[320,256]{1,0:T(8,128)(2,1)S(1)}, u32[]{:S(2)}, u32[]{:S(2)}) %collective-permute-start.4) | collective-permute-done | bytes 163872 | tf_op jit(solution)/shard_map/ppermute | solution.py:624
  22.8 1.4 collective-permute-start.7
  24.2 1.8 %collective-permute-start.8 = (bf16[1280,256]{1,0:T(8,128)(2,1)S(1)}, bf16[1280,256]{1,0:T(8,128)(2,1)S(1)}, u32[]{:S(2)}, u32[]{:S(2)}) collective-permute-start(bf16[1280,256]{1,0:T(8,128)(2,1)S(1)} %constant_dynamic-update-slice_fusion.rest_6_), channel_id=1, source_target_pairs={{0,6},{1,25},{2,0},{3,27},{4,2},{5,29},{6,4},{7,31},{8,14},{9,1},{... | collective-permute-start | bytes 1966088 | tf_op jit(solution)/shard_map/ppermute | solution.py:631
  26.0 2.8 %collective-permute-start.6 = (bf16[1280,256]{1,0:T(8,128)(2,1)S(1)}, bf16[1280,256]{1,0:T(8,128)(2,1)S(1)}, u32[]{:S(2)}, u32[]{:S(2)}) collective-permute-start(bf16[1280,256]{1,0:T(8,128)(2,1)S(1)} %constant_dynamic-update-slice_fusion.rest_6_), channel_id=1, source_target_pairs={{0,1},{1,0},{2,3},{3,2},{4,5},{5,4},{6,7},{7,6},{8,9},{9,8},{10,11... | collective-permute-start | bytes 1966088 | tf_op jit(solution)/shard_map/ppermute | solution.py:640
  28.8 2.2 %collective-permute-start.5 = (bf16[256,768]{1,0:T(8,128)(2,1)S(1)}, bf16[256,768]{1,0:T(8,128)(2,1)S(1)}, u32[]{:S(2)}, u32[]{:S(2)}) collective-permute-start(bf16[256,768]{1,0:T(8,128)(2,1)S(1)} %pad_maximum_fusion), channel_id=1, source_target_pairs={{0,120},{1,121},{2,122},{3,123},{4,124},{5,125},{6,126},{7,127},{8... | collective-permute-start | bytes 1179656 | tf_op jit(solution)/shard_map/ppermute | solution.py:599
  31.0 3.5 %collective-permute-done.7.rest_5_ = bf16[1280,256]{1,0:T(8,128)(2,1)S(1)} collective-permute-done((bf16[1280,256]{1,0:T(8,128)(2,1)S(1)}, bf16[1280,256]{1,0:T(8,128)(2,1)S(1)}, u32[]{:S(2)}, u32[]{:S(2)}) %collective-permute-start.7) | collective-permute-done | bytes 655392 | tf_op jit(solution)/shard_map/ppermute | solution.py:631
  34.6 0.5 collective-permute-done.8.rest_6_
  35.1 3.5 %collective-permute-start.12 = (bf16[640,256]{1,0:T(8,128)(2,1)S(1)}, bf16[640,256]{1,0:T(8,128)(2,1)S(1)}, u32[]{:S(2)}, u32[]{:S(2)}) collective-permute-start(bf16[640,256]{1,0:T(8,128)(2,1)S(1)} %slice.41), channel_id=1, source_target_pairs={{0,6},{1,25},{2,0},{3,27},{4,2},{5,29},{6,4},{7,31},{8,14},{9,1},{... | collective-permute-start | bytes 983048 | tf_op jit(solution)/shard_map/ppermute | solution.py:636
  38.5 2.2 %collective-permute-start.10 = (bf16[1280,256]{1,0:T(8,128)(2,1)S(1)}, bf16[1280,256]{1,0:T(8,128)(2,1)S(1)}, u32[]{:S(2)}, u32[]{:S(2)}) collective-permute-start(bf16[1280,256]{1,0:T(8,128)(2,1)S(1)} %collective-permute-done.8.rest_6_), channel_id=1, source_target_pairs={{0,1},{1,0},{2,3},{3,2},{4,5},{5,4},{6,7},{7,6},{8,9},{9,8},{10,11... | collective-permute-start | bytes 1966088 | tf_op jit(solution)/shard_map/ppermute | solution.py:640
  40.8 3.0 %collective-permute-done.5.rest_2_ = bf16[256,768]{1,0:T(8,128)(2,1)S(1)} collective-permute-done((bf16[256,768]{1,0:T(8,128)(2,1)S(1)}, bf16[256,768]{1,0:T(8,128)(2,1)S(1)}, u32[]{:S(2)}, u32[]{:S(2)}) %collective-permute-start.5) | collective-permute-done | bytes 393248 | tf_op jit(solution)/shard_map/ppermute | solution.py:599
  43.8 0.4 collective-permute-start.9
  44.2 8.0 %shard_map.145 = (bf16[4,2,512,128]{3,2,1,0:T(8,128)(2,1)S(1)}, bf16[4,2,512,128]{3,2,1,0:T(8,128)(2,1)S(1)}, f32[4,512,128]{2,1,0:T(8,128)S(1)}, f32[4,512,128]{2,1,0:T(8,128)S(1)}, f32[4,2,512,128]{3,2,1,0:T(8,128)S(1)}) custom-call(s32[308]{0:T(512)S(1)} %dynamic-slice_reduce_fusion.table, bf16[256,512]{1,0:T(8,128)(2,1)S(1)} %copy-done.1, ...), custom_call_target="tpu_custom_call" | custom-call | flops 4026531840 | bytes 1048576 | tf_op jit(solution)/shard_map/pallas_call | solution.py:342
  52.3 7.3 %shard_map.146 = (f32[4,512,128]{2,1,0:T(8,128)S(1)}, f32[4,512,128]{2,1,0:T(8,128)S(1)}, f32[4,2,512,128]{3,2,1,0:T(8,128)S(1)}) custom-call(s32[308]{0:T(512)S(1)} %dynamic-slice_reduce_fusion.table, bf16[4,2,512,128]{3,2,1,0:T(8,128)(2,1)S(1)} %get-tuple-element.34.rest_0_, ...), custom_call_target="tpu_custom_call", output_to_operand_aliasing={{0}: (3, {}), {1}: (4, {}), {2}: (5, {})} | custom-call | flops 4026531840 | bytes 1048576 | tf_op jit(solution)/shard_map/pallas_call | solution.py:342
  59.6 0.2 collective-permute-start.13
  59.9 0.4 collective-permute-start.14
  60.2 7.4 %shard_map.147 = (f32[4,512,128]{2,1,0:T(8,128)S(1)}, f32[4,512,128]{2,1,0:T(8,128)S(1)}, f32[4,2,512,128]{3,2,1,0:T(8,128)S(1)}) custom-call(s32[308]{0:T(512)S(1)} %dynamic-slice_reduce_fusion.table, bf16[4,2,512,128]{3,2,1,0:T(8,128)(2,1)S(1)} %get-tuple-element.34.rest_0_, ...), custom_call_target="tpu_custom_call", output_to_operand_aliasing={{0}: (3, {}), {1}: (4, {}), {2}: (5, {})} | custom-call | flops 4026531840 | bytes 1048576 | tf_op jit(solution)/shard_map/pallas_call | solution.py:342
  67.6 9.0 %shard_map.148 = (bf16[128,640]{1,0:T(8,128)(2,1)S(1)}, bf16[128,640]{1,0:T(8,128)(2,1)}, bf16[128,640]{1,0:T(8,128)(2,1)}, bf16[128,640]{1,0:T(8,128)(2,1)S(1)}...) custom-call(s32[308]{0:T(512)S(1)} %dynamic-slice_reduce_fusion.tabl, ...), custom_call_target="tpu_custom_call", output_to_operand_aliasing={{6}: (3, {}), {7}: (4, {}), {8}: (5, {})} | custom-call | flops 4026531840 | bytes 1048576 | tf_op jit(solution)/shard_map/pallas_call | solution.py:342
  76.6 3.3 %collective-permute-start.15 = (bf16[128,640]{1,0:T(8,128)(2,1)}, bf16[128,640]{1,0:T(8,128)(2,1)S(1)}, u32[]{:S(2)}, u32[]{:S(2)}) collective-permute-start(bf16[128,640]{1,0:T(8,128)(2,1)} %get-tuple-element.46), channel_id=1, source_target_pairs={{0,120},{1,121},{2,122},{3,123},{4,124},{5,125},{6,126},{7,127},{8... | collective-permute-start | bytes 491528 | tf_op jit(solution)/shard_map/ppermute | solution.py:653
  79.9 0.7 collective-permute-start.16
  80.7 1.4 collective-permute-start.17
  82.1 3.9 %collective-permute-done.15.mirror_same = bf16[128,640]{1,0:T(8,128)(2,1)S(1)} collective-permute-done((bf16[128,640]{1,0:T(8,128)(2,1)}, bf16[128,640]{1,0:T(8,128)(2,1)S(1)}, u32[]{:S(2)}, u32[]{:S(2)}) %collective-permute-start.15) | collective-permute-done | bytes 163872 | tf_op jit(solution)/shard_map/ppermute | solution.py:653
  86.1 3.8 %collective-permute-done.17.mirror_cross = bf16[128,640]{1,0:T(8,128)(2,1)S(1)} collective-permute-done((bf16[128,640]{1,0:T(8,128)(2,1)S(1)}, bf16[128,640]{1,0:T(8,128)(2,1)S(1)}, u32[]{:S(2)}, u32[]{:S(2)}) %collective-permute-start.17) | collective-permute-done | bytes 163872 | tf_op jit(solution)/shard_map/ppermute | solution.py:654
  89.9 3.8 %project.1 = (bf16[128,2048]{1,0:T(8,128)(2,1)}, bf16[512,2048]{1,0:T(8,128)(2,1)}) custom-call(s32[1]{0:T(128)} %bitcast.core, bf16[128,640]{1,0:T(8,128)(2,1)S(1)} %get-tuple-element.45.local_part, bf16[128,640]{1,0:T(8,128)(2,1)S(1)} %collective-permute-done.15.mirror_same, bf16[128,640]{1,0:T(8,128)(2,1)S(1)} %collective-permute-done.16.swapped, ...), custom_call_target="tpu_custom_call" | custom-call | tf_op jit(solution)/shard_map/project/pallas_call | solution.py:441
  93.7 6.6 %all-to-all-start = ((bf16[64,8,2048]{2,1,0:T(8,128)(2,1)}), bf16[64,8,2048]{2,1,0:T(8,128)(2,1)S(1)}, u32[]{:S(2)}, u32[]{:S(2)}) async-start(bf16[64,8,2048]{2,1,0:T(8,128)(2,1)} %bitcast.15), calls=%async_computation | async-start | bytes 4194304 | tf_op jit(solution)/shard_map/all_to_all | solution.py:662
  100.5 0.4 collective-permute-start.19
  101.0 2.1 %collective-permute-done.18.rest_3_ = bf16[2048,256]{1,0:T(8,128)(2,1)S(1)} collective-permute-done((bf16[2048,256]{1,0:T(8,128)(2,1)S(1)}, bf16[2048,256]{1,0:T(8,128)(2,1)S(1)}, u32[]{:S(2)}, u32[]{:S(2)}) %collective-permute-start.18) | collective-permute-done | bytes 1048608 | tf_op jit(solution)/shard_map/ppermute | solution.py:666
  103.1 1.5 collective-permute-done.19.rest_4_
  104.6 1.0 copy-done.8
  105.6 0.6 collective-permute-done.20.rest_5_
  106.2 23.9 %all-to-all-done = bf16[64,8,2048]{2,1,0:T(8,128)(2,1)S(1)} async-done(((bf16[64,8,2048]{2,1,0:T(8,128)(2,1)}), bf16[64,8,2048]{2,1,0:T(8,128)(2,1)S(1)}, u32[]{:S(2)}, u32[]{:S(2)}) %all-to-all-start) | async-done | bytes 2097184 | tf_op jit(solution)/shard_map/all_to_all | solution.py:662
  130.1 6.7 %experts.1 = bf16[512,2048]{1,0:T(8,128)(2,1)} custom-call(bf16[512,2048]{1,0:T(8,128)(2,1)S(1)} %bitcast.10, bf16[2048,256]{1,0:T(8,128)(2,1)} %bitcast.16, bf16[2048,256]{1,0:T(8,128)(2,1)} %bitcast.19, bf16[256,2048]{1,0:T(8,128)(2,1)} %bitcast.21, bf16[2048,256]{1,0:T(8,128)(2,1)} %copy-done.7, bf16[2048,256]{1,0:T(8,128)(2,1)} %copy-done.8, ...), custom_call_target="tpu_custom_call" | custom-call | tf_op jit(solution)/shard_map/experts/pallas_call | solution.py:506
  136.8 6.0 %all-to-all-start.1 = ((bf16[64,8,2048]{2,1,0:T(8,128)(2,1)}), bf16[64,8,2048]{2,1,0:T(8,128)(2,1)S(1)}, u32[]{:S(2)}, u32[]{:S(2)}) async-start(bf16[64,8,2048]{2,1,0:T(8,128)(2,1)} %bitcast.14), calls=%async_computation.1 | async-start | bytes 4194304 | tf_op jit(solution)/shard_map/all_to_all | solution.py:668
  143.0 28.3 %all-to-all-done.1 = bf16[64,8,2048]{2,1,0:T(8,128)(2,1)S(1)} async-done(((bf16[64,8,2048]{2,1,0:T(8,128)(2,1)}), bf16[64,8,2048]{2,1,0:T(8,128)(2,1)S(1)}, u32[]{:S(2)}, u32[]{:S(2)}) %all-to-all-start.1) | async-done | bytes 2097184 | tf_op jit(solution)/shard_map/all_to_all | solution.py:668
  171.2 1.6 combine.1
  (56 shorter events, 1.5 us)
Async XLA Ops:
  0.0 28.8 %copy-start.1 = (bf16[256,512]{1,0:T(8,128)(2,1)S(1)}, bf16[256,512]{1,0:T(8,128)(2,1)}, u32[]{:S(2)}) copy-start(bf16[256,512]{1,0:T(8,128)(2,1)} %rest_0_.1) | copy-start | bytes 786436
  0.0 28.8 %copy-start.2 = (bf16[256,256]{1,0:T(8,128)(2,1)S(1)}, bf16[256,256]{1,0:T(8,128)(2,1)}, u32[]{:S(2)}) copy-start(bf16[256,256]{1,0:T(8,128)(2,1)} %rest_1_.1) | copy-start | bytes 393220
  2.3 10.7 %collective-permute-start = (bf16[160,256]{1,0:T(8,128)(2,1)S(1)}, bf16[160,256]{1,0:T(8,128)(2,1)S(1)}, u32[]{:S(2)}, u32[]{:S(2)}) collective-permute-start(bf16[160,256]{1,0:T(8,128)(2,1)S(1)} %fusion.12), channel_id=1, source_target_pairs={{64,1},{66,3},{68,5},{70,7},{72,9},{74,11},{76,13},{78,15},{80,17}... | collective-permute-start | bytes 245768 | tf_op jit(solution)/shard_map/ppermute | solution.py:602
  9.1 3.9 %collective-permute-start.1 = (bf16[160,256]{1,0:T(8,128)(2,1)S(1)}, bf16[160,256]{1,0:T(8,128)(2,1)S(1)}, u32[]{:S(2)}, u32[]{:S(2)}) collective-permute-start(bf16[160,256]{1,0:T(8,128)(2,1)S(1)} %fusion.12), channel_id=1, source_target_pairs={{96,0},{98,2},{100,4},{102,6},{104,8},{106,10},{108,12},{110,14},{... | collective-permute-start | bytes 245768 | tf_op jit(solution)/shard_map/ppermute | solution.py:601
  12.9 31.3 %copy-start.4 = (bf16[256,512]{1,0:T(8,128)(2,1)S(1)}, bf16[256,512]{1,0:T(8,128)(2,1)}, u32[]{:S(2)}) copy-start(bf16[256,512]{1,0:T(8,128)(2,1)} %rest_3_.1) | copy-start | bytes 786436
  13.1 5.7 %collective-permute-start.2 = (bf16[320,256]{1,0:T(8,128)(2,1)S(1)}, bf16[320,256]{1,0:T(8,128)(2,1)S(1)}, u32[]{:S(2)}, u32[]{:S(2)}) collective-permute-start(bf16[320,256]{1,0:T(8,128)(2,1)S(1)} %pad_maximum_fusion.1), channel_id=1, source_target_pairs={{0,8},{1,3},{2,10},{3,5},{4,12},{5,7},{6,14},{7,1},{8,16},{9,11},{... | collective-permute-start | bytes 491528 | tf_op jit(solution)/shard_map/ppermute | solution.py:624
  15.6 4.5 %collective-permute-start.3 = (bf16[320,256]{1,0:T(8,128)(2,1)S(1)}, bf16[320,256]{1,0:T(8,128)(2,1)S(1)}, u32[]{:S(2)}, u32[]{:S(2)}) collective-permute-start(bf16[320,256]{1,0:T(8,128)(2,1)S(1)} %pad_maximum_fusion.1), channel_id=1, source_target_pairs={{0,24},{1,7},{2,26},{3,1},{4,28},{5,3},{6,30},{7,5},{8,0},{9,15},{... | collective-permute-start | bytes 491528 | tf_op jit(solution)/shard_map/ppermute | solution.py:624
  17.1 5.7 %collective-permute-start.4 = (bf16[320,256]{1,0:T(8,128)(2,1)S(1)}, bf16[320,256]{1,0:T(8,128)(2,1)S(1)}, u32[]{:S(2)}, u32[]{:S(2)}) collective-permute-start(bf16[320,256]{1,0:T(8,128)(2,1)S(1)} %pad_maximum_fusion.1), channel_id=1, source_target_pairs={{0,16},{1,5},{2,18},{3,7},{4,20},{5,1},{6,22},{7,3},{8,24},{9,13},... | collective-permute-start | bytes 491528 | tf_op jit(solution)/shard_map/ppermute | solution.py:624
  22.8 11.7 %collective-permute-start.7 = (bf16[1280,256]{1,0:T(8,128)(2,1)S(1)}, bf16[1280,256]{1,0:T(8,128)(2,1)S(1)}, u32[]{:S(2)}, u32[]{:S(2)}) collective-permute-start(bf16[1280,256]{1,0:T(8,128)(2,1)S(1)} %constant_dynamic-update-slice_fusion.rest_6_), channel_id=1, source_target_pairs={{0,2},{1,9},{2,4},{3,11},{4,6},{5,13},{6,0},{7,15},{8,10},{9,17},{... | collective-permute-start | bytes 1966088 | tf_op jit(solution)/shard_map/ppermute | solution.py:631
  24.2 10.9 %collective-permute-start.8 = (bf16[1280,256]{1,0:T(8,128)(2,1)S(1)}, bf16[1280,256]{1,0:T(8,128)(2,1)S(1)}, u32[]{:S(2)}, u32[]{:S(2)}) collective-permute-start(bf16[1280,256]{1,0:T(8,128)(2,1)S(1)} %constant_dynamic-update-slice_fusion.rest_6_), channel_id=1, source_target_pairs={{0,6},{1,25},{2,0},{3,27},{4,2},{5,29},{6,4},{7,31},{8,14},{9,1},{... | collective-permute-start | bytes 1966088 | tf_op jit(solution)/shard_map/ppermute | solution.py:631
  26.0 18.2 %collective-permute-start.6 = (bf16[1280,256]{1,0:T(8,128)(2,1)S(1)}, bf16[1280,256]{1,0:T(8,128)(2,1)S(1)}, u32[]{:S(2)}, u32[]{:S(2)}) collective-permute-start(bf16[1280,256]{1,0:T(8,128)(2,1)S(1)} %constant_dynamic-update-slice_fusion.rest_6_), channel_id=1, source_target_pairs={{0,1},{1,0},{2,3},{3,2},{4,5},{5,4},{6,7},{7,6},{8,9},{9,8},{10,11... | collective-permute-start | bytes 1966088 | tf_op jit(solution)/shard_map/ppermute | solution.py:640
  28.8 15.0 %collective-permute-start.5 = (bf16[256,768]{1,0:T(8,128)(2,1)S(1)}, bf16[256,768]{1,0:T(8,128)(2,1)S(1)}, u32[]{:S(2)}, u32[]{:S(2)}) collective-permute-start(bf16[256,768]{1,0:T(8,128)(2,1)S(1)} %pad_maximum_fusion), channel_id=1, source_target_pairs={{0,120},{1,121},{2,122},{3,123},{4,124},{5,125},{6,126},{7,127},{8... | collective-permute-start | bytes 1179656 | tf_op jit(solution)/shard_map/ppermute | solution.py:599
  34.5 25.1 %collective-permute-start.11 = (bf16[640,256]{1,0:T(8,128)(2,1)S(1)}, bf16[640,256]{1,0:T(8,128)(2,1)S(1)}, u32[]{:S(2)}, u32[]{:S(2)}) collective-permute-start(bf16[640,256]{1,0:T(8,128)(2,1)S(1)} %slice.40), channel_id=1, source_target_pairs={{0,2},{1,9},{2,4},{3,11},{4,6},{5,13},{6,0},{7,15},{8,10},{9,17},{... | collective-permute-start | bytes 983048 | tf_op jit(solution)/shard_map/ppermute | solution.py:636
  35.1 24.8 %collective-permute-start.12 = (bf16[640,256]{1,0:T(8,128)(2,1)S(1)}, bf16[640,256]{1,0:T(8,128)(2,1)S(1)}, u32[]{:S(2)}, u32[]{:S(2)}) collective-permute-start(bf16[640,256]{1,0:T(8,128)(2,1)S(1)} %slice.41), channel_id=1, source_target_pairs={{0,6},{1,25},{2,0},{3,27},{4,2},{5,29},{6,4},{7,31},{8,14},{9,1},{... | collective-permute-start | bytes 983048 | tf_op jit(solution)/shard_map/ppermute | solution.py:636
  38.5 21.7 %collective-permute-start.10 = (bf16[1280,256]{1,0:T(8,128)(2,1)S(1)}, bf16[1280,256]{1,0:T(8,128)(2,1)S(1)}, u32[]{:S(2)}, u32[]{:S(2)}) collective-permute-start(bf16[1280,256]{1,0:T(8,128)(2,1)S(1)} %collective-permute-done.8.rest_6_), channel_id=1, source_target_pairs={{0,1},{1,0},{2,3},{3,2},{4,5},{5,4},{6,7},{7,6},{8,9},{9,8},{10,11... | collective-permute-start | bytes 1966088 | tf_op jit(solution)/shard_map/ppermute | solution.py:640
  43.8 16.4 %collective-permute-start.9 = (bf16[1280,256]{1,0:T(8,128)(2,1)S(1)}, bf16[1280,256]{1,0:T(8,128)(2,1)S(1)}, u32[]{:S(2)}, u32[]{:S(2)}) collective-permute-start(bf16[1280,256]{1,0:T(8,128)(2,1)S(1)} %collective-permute-done.7.rest_5_), channel_id=1, source_target_pairs={{0,1},{1,0},{2,3},{3,2},{4,5},{5,4},{6,7},{7,6},{8,9},{9,8},{10,11... | collective-permute-start | bytes 1966088 | tf_op jit(solution)/shard_map/ppermute | solution.py:640
  59.6 8.0 %collective-permute-start.13 = (bf16[640,256]{1,0:T(8,128)(2,1)S(1)}, bf16[640,256]{1,0:T(8,128)(2,1)S(1)}, u32[]{:S(2)}, u32[]{:S(2)}) collective-permute-start(bf16[640,256]{1,0:T(8,128)(2,1)S(1)} %collective-permute-done.11.rest_8_), channel_id=1, source_target_pairs={{0,1},{1,0},{2,3},{3,2},{4,5},{5,4},{6,7},{7,6},{8,9},{9,8},{10,11... | collective-permute-start | bytes 983048 | tf_op jit(solution)/shard_map/ppermute | solution.py:640
  59.9 7.8 %collective-permute-start.14 = (bf16[640,256]{1,0:T(8,128)(2,1)S(1)}, bf16[640,256]{1,0:T(8,128)(2,1)S(1)}, u32[]{:S(2)}, u32[]{:S(2)}) collective-permute-start(bf16[640,256]{1,0:T(8,128)(2,1)S(1)} %collective-permute-done.12.rest_9_), channel_id=1, source_target_pairs={{0,1},{1,0},{2,3},{3,2},{4,5},{5,4},{6,7},{7,6},{8,9},{9,8},{10,11... | collective-permute-start | bytes 983048 | tf_op jit(solution)/shard_map/ppermute | solution.py:640
  60.2 7.4 %copy-start.5 = (bf16[256,512]{1,0:T(8,128)(2,1)S(1)}, bf16[256,512]{1,0:T(8,128)(2,1)}, u32[]{:S(2)}) copy-start(bf16[256,512]{1,0:T(8,128)(2,1)} %rest_5_.1) | copy-start | bytes 786436
  67.6 22.2 %copy-start.3 = (f32[2048]{0:T(1024)S(1)}, f32[2048]{0:T(1024)}, u32[]{:S(2)}) copy-start(f32[2048]{0:T(1024)} %param.23) | copy-start | bytes 24580
  76.6 9.5 %collective-permute-start.15 = (bf16[128,640]{1,0:T(8,128)(2,1)}, bf16[128,640]{1,0:T(8,128)(2,1)S(1)}, u32[]{:S(2)}, u32[]{:S(2)}) collective-permute-start(bf16[128,640]{1,0:T(8,128)(2,1)} %get-tuple-element.46), channel_id=1, source_target_pairs={{0,120},{1,121},{2,122},{3,123},{4,124},{5,125},{6,126},{7,127},{8... | collective-permute-start | bytes 491528 | tf_op jit(solution)/shard_map/ppermute | solution.py:653
  79.9 6.1 %collective-permute-start.16 = (bf16[128,640]{1,0:T(8,128)(2,1)}, bf16[128,640]{1,0:T(8,128)(2,1)S(1)}, u32[]{:S(2)}, u32[]{:S(2)}) collective-permute-start(bf16[128,640]{1,0:T(8,128)(2,1)} %get-tuple-element.47), channel_id=1, source_target_pairs={{0,1},{1,0},{2,3},{3,2},{4,5},{5,4},{6,7},{7,6},{8,9},{9,8},{10,11... | collective-permute-start | bytes 491528 | tf_op jit(solution)/shard_map/ppermute | solution.py:655
  80.7 9.2 %collective-permute-start.17 = (bf16[128,640]{1,0:T(8,128)(2,1)S(1)}, bf16[128,640]{1,0:T(8,128)(2,1)S(1)}, u32[]{:S(2)}, u32[]{:S(2)}) collective-permute-start(bf16[128,640]{1,0:T(8,128)(2,1)S(1)} %get-tuple-element.48), channel_id=1, source_target_pairs={{0,121},{1,120},{2,123},{3,122},{4,125},{5,124},{6,127},{7,126},{8... | collective-permute-start | bytes 491528 | tf_op jit(solution)/shard_map/ppermute | solution.py:654
  93.7 6.6 %copy-start.6 = (bf16[1,2048,256]{2,1,0:T(8,128)(2,1)S(1)}, bf16[1,2048,256]{2,1,0:T(8,128)(2,1)}, u32[]{:S(2)}) copy-start(bf16[1,2048,256]{2,1,0:T(8,128)(2,1)} %param.26) | copy-start | bytes 3145732
  93.7 36.3 %all-to-all-start = ((bf16[64,8,2048]{2,1,0:T(8,128)(2,1)}), bf16[64,8,2048]{2,1,0:T(8,128)(2,1)S(1)}, u32[]{:S(2)}, u32[]{:S(2)}) async-start(bf16[64,8,2048]{2,1,0:T(8,128)(2,1)} %bitcast.15), calls=%async_computation | async-start | bytes 4194304 | tf_op jit(solution)/shard_map/all_to_all | solution.py:662
  100.3 2.7 %collective-permute-start.18 = (bf16[2048,256]{1,0:T(8,128)(2,1)S(1)}, bf16[2048,256]{1,0:T(8,128)(2,1)S(1)}, u32[]{:S(2)}, u32[]{:S(2)}) collective-permute-start(bf16[2048,256]{1,0:T(8,128)(2,1)S(1)} %bitcast.17), channel_id=1, source_target_pairs={{0,1},{1,0},{2,3},{3,2},{4,5},{5,4},{6,7},{7,6},{8,9},{9,8},{10,11... | collective-permute-start | bytes 3145736 | tf_op jit(solution)/shard_map/ppermute | solution.py:666
  100.5 4.1 %collective-permute-start.19 = (bf16[2048,256]{1,0:T(8,128)(2,1)}, bf16[2048,256]{1,0:T(8,128)(2,1)S(1)}, u32[]{:S(2)}, u32[]{:S(2)}) collective-permute-start(bf16[2048,256]{1,0:T(8,128)(2,1)} %bitcast.18), channel_id=1, source_target_pairs={{0,1},{1,0},{2,3},{3,2},{4,5},{5,4},{6,7},{7,6},{8,9},{9,8},{10,11... | collective-permute-start | bytes 3145736 | tf_op jit(solution)/shard_map/ppermute | solution.py:666
  100.9 5.3 %collective-permute-start.20 = (bf16[256,2048]{1,0:T(8,128)(2,1)}, bf16[256,2048]{1,0:T(8,128)(2,1)}, u32[]{:S(2)}, u32[]{:S(2)}) collective-permute-start(bf16[256,2048]{1,0:T(8,128)(2,1)} %bitcast.20), channel_id=1, source_target_pairs={{0,1},{1,0},{2,3},{3,2},{4,5},{5,4},{6,7},{7,6},{8,9},{9,8},{10,11... | collective-permute-start | bytes 3145736 | tf_op jit(solution)/shard_map/ppermute | solution.py:666
  103.1 1.5 copy-start.7
  104.6 1.0 copy-start.8
  136.8 6.1 %copy-start.9 = (f32[128,2]{0,1:T(2,128)S(1)}, f32[128,2]{0,1:T(2,128)}, u32[]{:S(2)}) copy-start(f32[128,2]{0,1:T(2,128)} %param.25) | copy-start | bytes 3076
  136.8 34.5 %copy-start = (bf16[128,2048]{1,0:T(8,128)(2,1)S(1)}, bf16[128,2048]{1,0:T(8,128)(2,1)}, u32[]{:S(2)}) copy-start(bf16[128,2048]{1,0:T(8,128)(2,1)} %get-tuple-element.53.hidden) | copy-start | bytes 1572868
  136.8 34.5 %all-to-all-start.1 = ((bf16[64,8,2048]{2,1,0:T(8,128)(2,1)}), bf16[64,8,2048]{2,1,0:T(8,128)(2,1)S(1)}, u32[]{:S(2)}, u32[]{:S(2)}) async-start(bf16[64,8,2048]{2,1,0:T(8,128)(2,1)} %bitcast.14), calls=%async_computation.1 | async-start | bytes 4194304 | tf_op jit(solution)/shard_map/all_to_all | solution.py:668

commit v9 on v8

--- a/solution.py
+++ b/solution.py
@@ -290,7 +290,8 @@
     for target, g in targets:
         total = jnp.sum(l_ref[g], axis=1, keepdims=True)
         total = jnp.where(total > 0.0, total, 1.0)
-        mean = jnp.concatenate([acc_ref[g, k] / total for k in range(2)], axis=1).astype(jnp.bfloat16)
+        inverse = 1.0 / total
+        mean = jnp.concatenate([acc_ref[g, k] * inverse for k in range(2)], axis=1).astype(jnp.bfloat16)
         size = m_ref[g] * SCALE2 + jnp.log2(total)
         notes = jnp.zeros((ROWS, 128), jnp.bfloat16)
         for h in range(HEADS_HERE):
@@ -384,8 +385,11 @@
         most = jnp.maximum(sizes[0], sizes[1])
         first, second = (jnp.exp2(size - most) for size in sizes)
         cols = slice(h * V_DIM, (h + 1) * V_DIM)
-        value = first * one[:, cols].astype(jnp.float32) + second * two[:, cols].astype(jnp.float32)
-        outs.append((value / (first + second)).astype(jnp.bfloat16))
+        inverse = 1.0 / (first + second)
+        value = (first * inverse) * one[:, cols].astype(jnp.float32) + (second * inverse) * two[:, cols].astype(
+            jnp.float32
+        )
+        outs.append(value.astype(jnp.bfloat16))
     return jnp.concatenate(outs, axis=1)
 
 
@@ -527,10 +531,9 @@
     )
     high = pick.astype(jnp.bfloat16)
     low = (pick - high.astype(jnp.float32)).astype(jnp.bfloat16)
-    rows = back[...]
-    mixed = jnp.dot(high, rows, preferred_element_type=jnp.float32) + jnp.dot(
-        low, rows, preferred_element_type=jnp.float32
-    )
+    both = jnp.dot(jnp.concatenate([high, low], axis=0), back[...], preferred_element_type=jnp.float32)
+    count = hidden.shape[0]
+    mixed = both[:count] + both[count:]
     out_ref[...] = (hidden[...].astype(jnp.float32) + mixed).astype(jnp.bfloat16)
 
 

time: 175 us -> 175 us (level)
  no operation moved by 1% of the time
where the time goes in v9:
time: 175 us; the launch traced here: 173 us
  waiting for transfers between devices  75.3 us (43%)
  starting transfers between devices  45 us (26%)
  Pallas kernels  44.4 us (25%)
  other arithmetic  4.25 us (2%)
  local copies, waits for them, and re-layouts  4.07 us (2%)
    pallas_call x4, Pallas kernels, attention(): pl.pallas_call(functools.partial(attention_body, call, steps, offset, len...  31.7 us
    all_to_all x1, waiting for transfers between devices, local(): lax.all_to_all(produced.reshape(N_SP, CAP, width), 'sp', split_axis=0, co...  28.3 us
    all_to_all x1, waiting for transfers between devices, local(): lax.all_to_all(outgoing.reshape(N_SP, CAP, width), 'sp', split_axis=0, co...  23.9 us
    ppermute x1, starting transfers between devices, local(): far = lax.ppermute(shard, AXES, plane_pairs(Z_SECOND))  6.87 us
    pallas_call x1, Pallas kernels, experts(): pl.pallas_call(experts_body, out_shape=pltpu.HBM((count, width), jnp.bflo...  6.69 us
    all_to_all x1, starting transfers between devices, local(): lax.all_to_all(outgoing.reshape(N_SP, CAP, width), 'sp', split_axis=0, co...  6.57 us
    all_to_all x1, starting transfers between devices, local(): lax.all_to_all(produced.reshape(N_SP, CAP, width), 'sp', split_axis=0, co...  6.03 us
    ppermute x5, starting transfers between devices, local(): other_parts.append([lax.ppermute(part, 'tp', swap) for part in group])  6 us
  transfers between devices with their start and end apart: 23, of which 14 were waited for; matrix products, arithmetic and copies ran while one was open for 3% of the time, Pallas kernels for 13%

profile of v9, /device:TPU:1, one launch (start us, length us, event | category | flops | bytes accessed | tf_op | source)
XLA Modules:
  0.0 173.4 jit_solution(1887610312407820664)
XLA Ops:
  0.0 0.9 copy.42
  0.9 0.3 fusion.14
  1.3 0.9 fusion.12
  2.3 6.9 %collective-permute-start = (bf16[160,256]{1,0:T(8,128)(2,1)S(1)}, bf16[160,256]{1,0:T(8,128)(2,1)S(1)}, u32[]{:S(2)}, u32[]{:S(2)}) collective-permute-start(bf16[160,256]{1,0:T(8,128)(2,1)S(1)} %fusion.12), channel_id=1, source_target_pairs={{64,1},{66,3},{68,5},{70,7},{72,9},{74,11},{76,13},{78,15},{80,17}... | collective-permute-start | bytes 245768 | tf_op jit(solution)/shard_map/ppermute | solution.py:605
  9.4 1.9 %negate_select_fusion = (f32[512,256]{1,0:T(8,128)S(1)}, f32[512,256]{1,0:T(8,128)S(1)}) fusion(f32[256]{0:T(256)S(1)} %fusion.22, f32[512]{0:T(512)S(1)} %add_convert_fusion, pred[256]{0:T(512)(128)(4,1)S(1)} %fusion.23), kind=kLoop, calls=%fused_computation | loop fusion | flops 393216 | bytes 1051904 | tf_op jit(solution)/shard_map/jit(_where)/select_n | solution.py:624
  11.3 0.7 broadcast_multiply_fusion
  12.0 0.8 copy.44
  13.1 1.3 collective-permute-start.2
  14.4 0.2 convert_reduce_fusion
  14.8 0.7 dynamic-slice_reduce_fusion.table
  15.6 1.5 collective-permute-start.3
  17.1 1.5 collective-permute-start.4
  18.6 0.2 collective-permute-done.2
  18.9 1.2 collective-permute-done.3
  20.1 2.7 %collective-permute-done.4 = bf16[320,256]{1,0:T(8,128)(2,1)S(1)} collective-permute-done((bf16[320,256]{1,0:T(8,128)(2,1)S(1)}, bf16[320,256]{1,0:T(8,128)(2,1)S(1)}, u32[]{:S(2)}, u32[]{:S(2)}) %collective-permute-start.4) | collective-permute-done | bytes 163872 | tf_op jit(solution)/shard_map/ppermute | solution.py:627
  22.8 1.4 collective-permute-start.7
  24.2 1.8 %collective-permute-start.8 = (bf16[1280,256]{1,0:T(8,128)(2,1)S(1)}, bf16[1280,256]{1,0:T(8,128)(2,1)S(1)}, u32[]{:S(2)}, u32[]{:S(2)}) collective-permute-start(bf16[1280,256]{1,0:T(8,128)(2,1)S(1)} %constant_dynamic-update-slice_fusion.rest_6_), channel_id=1, source_target_pairs={{0,6},{1,25},{2,0},{3,27},{4,2},{5,29},{6,4},{7,31},{8,14},{9,1},{... | collective-permute-start | bytes 1966088 | tf_op jit(solution)/shard_map/ppermute | solution.py:634
  26.0 2.8 %collective-permute-start.6 = (bf16[1280,256]{1,0:T(8,128)(2,1)S(1)}, bf16[1280,256]{1,0:T(8,128)(2,1)S(1)}, u32[]{:S(2)}, u32[]{:S(2)}) collective-permute-start(bf16[1280,256]{1,0:T(8,128)(2,1)S(1)} %constant_dynamic-update-slice_fusion.rest_6_), channel_id=1, source_target_pairs={{0,1},{1,0},{2,3},{3,2},{4,5},{5,4},{6,7},{7,6},{8,9},{9,8},{10,11... | collective-permute-start | bytes 1966088 | tf_op jit(solution)/shard_map/ppermute | solution.py:643
  28.8 2.2 %collective-permute-start.5 = (bf16[256,768]{1,0:T(8,128)(2,1)S(1)}, bf16[256,768]{1,0:T(8,128)(2,1)S(1)}, u32[]{:S(2)}, u32[]{:S(2)}) collective-permute-start(bf16[256,768]{1,0:T(8,128)(2,1)S(1)} %pad_maximum_fusion), channel_id=1, source_target_pairs={{0,120},{1,121},{2,122},{3,123},{4,124},{5,125},{6,126},{7,127},{8... | collective-permute-start | bytes 1179656 | tf_op jit(solution)/shard_map/ppermute | solution.py:602
  31.0 3.5 %collective-permute-done.7.rest_5_ = bf16[1280,256]{1,0:T(8,128)(2,1)S(1)} collective-permute-done((bf16[1280,256]{1,0:T(8,128)(2,1)S(1)}, bf16[1280,256]{1,0:T(8,128)(2,1)S(1)}, u32[]{:S(2)}, u32[]{:S(2)}) %collective-permute-start.7) | collective-permute-done | bytes 655392 | tf_op jit(solution)/shard_map/ppermute | solution.py:634
  34.6 0.5 collective-permute-done.8.rest_6_
  35.1 3.5 %collective-permute-start.12 = (bf16[640,256]{1,0:T(8,128)(2,1)S(1)}, bf16[640,256]{1,0:T(8,128)(2,1)S(1)}, u32[]{:S(2)}, u32[]{:S(2)}) collective-permute-start(bf16[640,256]{1,0:T(8,128)(2,1)S(1)} %slice.41), channel_id=1, source_target_pairs={{0,6},{1,25},{2,0},{3,27},{4,2},{5,29},{6,4},{7,31},{8,14},{9,1},{... | collective-permute-start | bytes 983048 | tf_op jit(solution)/shard_map/ppermute | solution.py:639
  38.5 2.2 %collective-permute-start.10 = (bf16[1280,256]{1,0:T(8,128)(2,1)S(1)}, bf16[1280,256]{1,0:T(8,128)(2,1)S(1)}, u32[]{:S(2)}, u32[]{:S(2)}) collective-permute-start(bf16[1280,256]{1,0:T(8,128)(2,1)S(1)} %collective-permute-done.8.rest_6_), channel_id=1, source_target_pairs={{0,1},{1,0},{2,3},{3,2},{4,5},{5,4},{6,7},{7,6},{8,9},{9,8},{10,11... | collective-permute-start | bytes 1966088 | tf_op jit(solution)/shard_map/ppermute | solution.py:643
  40.8 3.0 %collective-permute-done.5.rest_2_ = bf16[256,768]{1,0:T(8,128)(2,1)S(1)} collective-permute-done((bf16[256,768]{1,0:T(8,128)(2,1)S(1)}, bf16[256,768]{1,0:T(8,128)(2,1)S(1)}, u32[]{:S(2)}, u32[]{:S(2)}) %collective-permute-start.5) | collective-permute-done | bytes 393248 | tf_op jit(solution)/shard_map/ppermute | solution.py:602
  43.8 0.4 collective-permute-start.9
  44.2 8.0 %shard_map.145 = (bf16[4,2,512,128]{3,2,1,0:T(8,128)(2,1)S(1)}, bf16[4,2,512,128]{3,2,1,0:T(8,128)(2,1)S(1)}, f32[4,512,128]{2,1,0:T(8,128)S(1)}, f32[4,512,128]{2,1,0:T(8,128)S(1)}, f32[4,2,512,128]{3,2,1,0:T(8,128)S(1)}) custom-call(s32[308]{0:T(512)S(1)} %dynamic-slice_reduce_fusion.table, bf16[256,512]{1,0:T(8,128)(2,1)S(1)} %copy-done.1, ...), custom_call_target="tpu_custom_call" | custom-call | flops 4026531840 | bytes 1048576 | tf_op jit(solution)/shard_map/pallas_call | solution.py:343
  52.3 7.3 %shard_map.146 = (f32[4,512,128]{2,1,0:T(8,128)S(1)}, f32[4,512,128]{2,1,0:T(8,128)S(1)}, f32[4,2,512,128]{3,2,1,0:T(8,128)S(1)}) custom-call(s32[308]{0:T(512)S(1)} %dynamic-slice_reduce_fusion.table, bf16[4,2,512,128]{3,2,1,0:T(8,128)(2,1)S(1)} %get-tuple-element.34.rest_0_, ...), custom_call_target="tpu_custom_call", output_to_operand_aliasing={{0}: (3, {}), {1}: (4, {}), {2}: (5, {})} | custom-call | flops 4026531840 | bytes 1048576 | tf_op jit(solution)/shard_map/pallas_call | solution.py:343
  59.6 0.2 collective-permute-start.13
  59.9 0.4 collective-permute-start.14
  60.2 7.4 %shard_map.147 = (f32[4,512,128]{2,1,0:T(8,128)S(1)}, f32[4,512,128]{2,1,0:T(8,128)S(1)}, f32[4,2,512,128]{3,2,1,0:T(8,128)S(1)}) custom-call(s32[308]{0:T(512)S(1)} %dynamic-slice_reduce_fusion.table, bf16[4,2,512,128]{3,2,1,0:T(8,128)(2,1)S(1)} %get-tuple-element.34.rest_0_, ...), custom_call_target="tpu_custom_call", output_to_operand_aliasing={{0}: (3, {}), {1}: (4, {}), {2}: (5, {})} | custom-call | flops 4026531840 | bytes 1048576 | tf_op jit(solution)/shard_map/pallas_call | solution.py:343
  67.6 9.0 %shard_map.148 = (bf16[128,640]{1,0:T(8,128)(2,1)S(1)}, bf16[128,640]{1,0:T(8,128)(2,1)}, bf16[128,640]{1,0:T(8,128)(2,1)}, bf16[128,640]{1,0:T(8,128)(2,1)S(1)}...) custom-call(s32[308]{0:T(512)S(1)} %dynamic-slice_reduce_fusion.tabl, ...), custom_call_target="tpu_custom_call", output_to_operand_aliasing={{6}: (3, {}), {7}: (4, {}), {8}: (5, {})} | custom-call | flops 4026531840 | bytes 1048576 | tf_op jit(solution)/shard_map/pallas_call | solution.py:343
  76.6 3.3 %collective-permute-start.15 = (bf16[128,640]{1,0:T(8,128)(2,1)}, bf16[128,640]{1,0:T(8,128)(2,1)S(1)}, u32[]{:S(2)}, u32[]{:S(2)}) collective-permute-start(bf16[128,640]{1,0:T(8,128)(2,1)} %get-tuple-element.46), channel_id=1, source_target_pairs={{0,120},{1,121},{2,122},{3,123},{4,124},{5,125},{6,126},{7,127},{8... | collective-permute-start | bytes 491528 | tf_op jit(solution)/shard_map/ppermute | solution.py:656
  79.9 0.7 collective-permute-start.16
  80.7 1.4 collective-permute-start.17
  82.1 3.9 %collective-permute-done.15.mirror_same = bf16[128,640]{1,0:T(8,128)(2,1)S(1)} collective-permute-done((bf16[128,640]{1,0:T(8,128)(2,1)}, bf16[128,640]{1,0:T(8,128)(2,1)S(1)}, u32[]{:S(2)}, u32[]{:S(2)}) %collective-permute-start.15) | collective-permute-done | bytes 163872 | tf_op jit(solution)/shard_map/ppermute | solution.py:656
  86.1 3.8 %collective-permute-done.17.mirror_cross = bf16[128,640]{1,0:T(8,128)(2,1)S(1)} collective-permute-done((bf16[128,640]{1,0:T(8,128)(2,1)S(1)}, bf16[128,640]{1,0:T(8,128)(2,1)S(1)}, u32[]{:S(2)}, u32[]{:S(2)}) %collective-permute-start.17) | collective-permute-done | bytes 163872 | tf_op jit(solution)/shard_map/ppermute | solution.py:657
  89.9 4.4 %project.1 = (bf16[128,2048]{1,0:T(8,128)(2,1)}, bf16[512,2048]{1,0:T(8,128)(2,1)}) custom-call(s32[1]{0:T(128)} %bitcast.core, bf16[128,640]{1,0:T(8,128)(2,1)S(1)} %get-tuple-element.45.local_part, bf16[128,640]{1,0:T(8,128)(2,1)S(1)} %collective-permute-done.15.mirror_same, bf16[128,640]{1,0:T(8,128)(2,1)S(1)} %collective-permute-done.16.swapped, ...), custom_call_target="tpu_custom_call" | custom-call | tf_op jit(solution)/shard_map/project/pallas_call | solution.py:445
  94.3 6.6 %all-to-all-start = ((bf16[64,8,2048]{2,1,0:T(8,128)(2,1)}), bf16[64,8,2048]{2,1,0:T(8,128)(2,1)S(1)}, u32[]{:S(2)}, u32[]{:S(2)}) async-start(bf16[64,8,2048]{2,1,0:T(8,128)(2,1)} %bitcast.15), calls=%async_computation | async-start | bytes 4194304 | tf_op jit(solution)/shard_map/all_to_all | solution.py:665
  101.1 0.4 collective-permute-start.19
  101.6 2.1 %collective-permute-done.18.rest_3_ = bf16[2048,256]{1,0:T(8,128)(2,1)S(1)} collective-permute-done((bf16[2048,256]{1,0:T(8,128)(2,1)S(1)}, bf16[2048,256]{1,0:T(8,128)(2,1)S(1)}, u32[]{:S(2)}, u32[]{:S(2)}) %collective-permute-start.18) | collective-permute-done | bytes 1048608 | tf_op jit(solution)/shard_map/ppermute | solution.py:669
  103.6 1.5 collective-permute-done.19.rest_4_
  105.1 1.0 copy-done.8
  106.1 0.6 collective-permute-done.20.rest_5_
  106.8 23.9 %all-to-all-done = bf16[64,8,2048]{2,1,0:T(8,128)(2,1)S(1)} async-done(((bf16[64,8,2048]{2,1,0:T(8,128)(2,1)}), bf16[64,8,2048]{2,1,0:T(8,128)(2,1)S(1)}, u32[]{:S(2)}, u32[]{:S(2)}) %all-to-all-start) | async-done | bytes 2097184 | tf_op jit(solution)/shard_map/all_to_all | solution.py:665
  130.6 6.7 %experts.1 = bf16[512,2048]{1,0:T(8,128)(2,1)} custom-call(bf16[512,2048]{1,0:T(8,128)(2,1)S(1)} %bitcast.10, bf16[2048,256]{1,0:T(8,128)(2,1)} %bitcast.16, bf16[2048,256]{1,0:T(8,128)(2,1)} %bitcast.19, bf16[256,2048]{1,0:T(8,128)(2,1)} %bitcast.21, bf16[2048,256]{1,0:T(8,128)(2,1)} %copy-done.7, bf16[2048,256]{1,0:T(8,128)(2,1)} %copy-done.8, ...), custom_call_target="tpu_custom_call" | custom-call | tf_op jit(solution)/shard_map/experts/pallas_call | solution.py:510
  137.4 6.0 %all-to-all-start.1 = ((bf16[64,8,2048]{2,1,0:T(8,128)(2,1)}), bf16[64,8,2048]{2,1,0:T(8,128)(2,1)S(1)}, u32[]{:S(2)}, u32[]{:S(2)}) async-start(bf16[64,8,2048]{2,1,0:T(8,128)(2,1)} %bitcast.14), calls=%async_computation.1 | async-start | bytes 4194304 | tf_op jit(solution)/shard_map/all_to_all | solution.py:671
  143.5 28.3 %all-to-all-done.1 = bf16[64,8,2048]{2,1,0:T(8,128)(2,1)S(1)} async-done(((bf16[64,8,2048]{2,1,0:T(8,128)(2,1)}), bf16[64,8,2048]{2,1,0:T(8,128)(2,1)S(1)}, u32[]{:S(2)}, u32[]{:S(2)}) %all-to-all-start.1) | async-done | bytes 2097184 | tf_op jit(solution)/shard_map/all_to_all | solution.py:671
  171.8 1.6 combine.1
  (56 shorter events, 1.5 us)
Async XLA Ops:
  0.0 28.8 %copy-start.1 = (bf16[256,512]{1,0:T(8,128)(2,1)S(1)}, bf16[256,512]{1,0:T(8,128)(2,1)}, u32[]{:S(2)}) copy-start(bf16[256,512]{1,0:T(8,128)(2,1)} %rest_0_.1) | copy-start | bytes 786436
  0.0 28.8 %copy-start.2 = (bf16[256,256]{1,0:T(8,128)(2,1)S(1)}, bf16[256,256]{1,0:T(8,128)(2,1)}, u32[]{:S(2)}) copy-start(bf16[256,256]{1,0:T(8,128)(2,1)} %rest_1_.1) | copy-start | bytes 393220
  2.3 10.7 %collective-permute-start = (bf16[160,256]{1,0:T(8,128)(2,1)S(1)}, bf16[160,256]{1,0:T(8,128)(2,1)S(1)}, u32[]{:S(2)}, u32[]{:S(2)}) collective-permute-start(bf16[160,256]{1,0:T(8,128)(2,1)S(1)} %fusion.12), channel_id=1, source_target_pairs={{64,1},{66,3},{68,5},{70,7},{72,9},{74,11},{76,13},{78,15},{80,17}... | collective-permute-start | bytes 245768 | tf_op jit(solution)/shard_map/ppermute | solution.py:605
  9.1 3.9 %collective-permute-start.1 = (bf16[160,256]{1,0:T(8,128)(2,1)S(1)}, bf16[160,256]{1,0:T(8,128)(2,1)S(1)}, u32[]{:S(2)}, u32[]{:S(2)}) collective-permute-start(bf16[160,256]{1,0:T(8,128)(2,1)S(1)} %fusion.12), channel_id=1, source_target_pairs={{96,0},{98,2},{100,4},{102,6},{104,8},{106,10},{108,12},{110,14},{... | collective-permute-start | bytes 245768 | tf_op jit(solution)/shard_map/ppermute | solution.py:604
  12.9 31.3 %copy-start.4 = (bf16[256,512]{1,0:T(8,128)(2,1)S(1)}, bf16[256,512]{1,0:T(8,128)(2,1)}, u32[]{:S(2)}) copy-start(bf16[256,512]{1,0:T(8,128)(2,1)} %rest_3_.1) | copy-start | bytes 786436
  13.1 5.7 %collective-permute-start.2 = (bf16[320,256]{1,0:T(8,128)(2,1)S(1)}, bf16[320,256]{1,0:T(8,128)(2,1)S(1)}, u32[]{:S(2)}, u32[]{:S(2)}) collective-permute-start(bf16[320,256]{1,0:T(8,128)(2,1)S(1)} %pad_maximum_fusion.1), channel_id=1, source_target_pairs={{0,8},{1,3},{2,10},{3,5},{4,12},{5,7},{6,14},{7,1},{8,16},{9,11},{... | collective-permute-start | bytes 491528 | tf_op jit(solution)/shard_map/ppermute | solution.py:627
  15.6 4.5 %collective-permute-start.3 = (bf16[320,256]{1,0:T(8,128)(2,1)S(1)}, bf16[320,256]{1,0:T(8,128)(2,1)S(1)}, u32[]{:S(2)}, u32[]{:S(2)}) collective-permute-start(bf16[320,256]{1,0:T(8,128)(2,1)S(1)} %pad_maximum_fusion.1), channel_id=1, source_target_pairs={{0,24},{1,7},{2,26},{3,1},{4,28},{5,3},{6,30},{7,5},{8,0},{9,15},{... | collective-permute-start | bytes 491528 | tf_op jit(solution)/shard_map/ppermute | solution.py:627
  17.1 5.7 %collective-permute-start.4 = (bf16[320,256]{1,0:T(8,128)(2,1)S(1)}, bf16[320,256]{1,0:T(8,128)(2,1)S(1)}, u32[]{:S(2)}, u32[]{:S(2)}) collective-permute-start(bf16[320,256]{1,0:T(8,128)(2,1)S(1)} %pad_maximum_fusion.1), channel_id=1, source_target_pairs={{0,16},{1,5},{2,18},{3,7},{4,20},{5,1},{6,22},{7,3},{8,24},{9,13},... | collective-permute-start | bytes 491528 | tf_op jit(solution)/shard_map/ppermute | solution.py:627
  22.8 11.7 %collective-permute-start.7 = (bf16[1280,256]{1,0:T(8,128)(2,1)S(1)}, bf16[1280,256]{1,0:T(8,128)(2,1)S(1)}, u32[]{:S(2)}, u32[]{:S(2)}) collective-permute-start(bf16[1280,256]{1,0:T(8,128)(2,1)S(1)} %constant_dynamic-update-slice_fusion.rest_6_), channel_id=1, source_target_pairs={{0,2},{1,9},{2,4},{3,11},{4,6},{5,13},{6,0},{7,15},{8,10},{9,17},{... | collective-permute-start | bytes 1966088 | tf_op jit(solution)/shard_map/ppermute | solution.py:634
  24.2 10.9 %collective-permute-start.8 = (bf16[1280,256]{1,0:T(8,128)(2,1)S(1)}, bf16[1280,256]{1,0:T(8,128)(2,1)S(1)}, u32[]{:S(2)}, u32[]{:S(2)}) collective-permute-start(bf16[1280,256]{1,0:T(8,128)(2,1)S(1)} %constant_dynamic-update-slice_fusion.rest_6_), channel_id=1, source_target_pairs={{0,6},{1,25},{2,0},{3,27},{4,2},{5,29},{6,4},{7,31},{8,14},{9,1},{... | collective-permute-start | bytes 1966088 | tf_op jit(solution)/shard_map/ppermute | solution.py:634
  26.0 18.2 %collective-permute-start.6 = (bf16[1280,256]{1,0:T(8,128)(2,1)S(1)}, bf16[1280,256]{1,0:T(8,128)(2,1)S(1)}, u32[]{:S(2)}, u32[]{:S(2)}) collective-permute-start(bf16[1280,256]{1,0:T(8,128)(2,1)S(1)} %constant_dynamic-update-slice_fusion.rest_6_), channel_id=1, source_target_pairs={{0,1},{1,0},{2,3},{3,2},{4,5},{5,4},{6,7},{7,6},{8,9},{9,8},{10,11... | collective-permute-start | bytes 1966088 | tf_op jit(solution)/shard_map/ppermute | solution.py:643
  28.8 15.0 %collective-permute-start.5 = (bf16[256,768]{1,0:T(8,128)(2,1)S(1)}, bf16[256,768]{1,0:T(8,128)(2,1)S(1)}, u32[]{:S(2)}, u32[]{:S(2)}) collective-permute-start(bf16[256,768]{1,0:T(8,128)(2,1)S(1)} %pad_maximum_fusion), channel_id=1, source_target_pairs={{0,120},{1,121},{2,122},{3,123},{4,124},{5,125},{6,126},{7,127},{8... | collective-permute-start | bytes 1179656 | tf_op jit(solution)/shard_map/ppermute | solution.py:602
  34.5 25.1 %collective-permute-start.11 = (bf16[640,256]{1,0:T(8,128)(2,1)S(1)}, bf16[640,256]{1,0:T(8,128)(2,1)S(1)}, u32[]{:S(2)}, u32[]{:S(2)}) collective-permute-start(bf16[640,256]{1,0:T(8,128)(2,1)S(1)} %slice.40), channel_id=1, source_target_pairs={{0,2},{1,9},{2,4},{3,11},{4,6},{5,13},{6,0},{7,15},{8,10},{9,17},{... | collective-permute-start | bytes 983048 | tf_op jit(solution)/shard_map/ppermute | solution.py:639
  35.1 24.8 %collective-permute-start.12 = (bf16[640,256]{1,0:T(8,128)(2,1)S(1)}, bf16[640,256]{1,0:T(8,128)(2,1)S(1)}, u32[]{:S(2)}, u32[]{:S(2)}) collective-permute-start(bf16[640,256]{1,0:T(8,128)(2,1)S(1)} %slice.41), channel_id=1, source_target_pairs={{0,6},{1,25},{2,0},{3,27},{4,2},{5,29},{6,4},{7,31},{8,14},{9,1},{... | collective-permute-start | bytes 983048 | tf_op jit(solution)/shard_map/ppermute | solution.py:639
  38.5 21.7 %collective-permute-start.10 = (bf16[1280,256]{1,0:T(8,128)(2,1)S(1)}, bf16[1280,256]{1,0:T(8,128)(2,1)S(1)}, u32[]{:S(2)}, u32[]{:S(2)}) collective-permute-start(bf16[1280,256]{1,0:T(8,128)(2,1)S(1)} %collective-permute-done.8.rest_6_), channel_id=1, source_target_pairs={{0,1},{1,0},{2,3},{3,2},{4,5},{5,4},{6,7},{7,6},{8,9},{9,8},{10,11... | collective-permute-start | bytes 1966088 | tf_op jit(solution)/shard_map/ppermute | solution.py:643
  43.8 16.4 %collective-permute-start.9 = (bf16[1280,256]{1,0:T(8,128)(2,1)S(1)}, bf16[1280,256]{1,0:T(8,128)(2,1)S(1)}, u32[]{:S(2)}, u32[]{:S(2)}) collective-permute-start(bf16[1280,256]{1,0:T(8,128)(2,1)S(1)} %collective-permute-done.7.rest_5_), channel_id=1, source_target_pairs={{0,1},{1,0},{2,3},{3,2},{4,5},{5,4},{6,7},{7,6},{8,9},{9,8},{10,11... | collective-permute-start | bytes 1966088 | tf_op jit(solution)/shard_map/ppermute | solution.py:643
  59.6 8.0 %collective-permute-start.13 = (bf16[640,256]{1,0:T(8,128)(2,1)S(1)}, bf16[640,256]{1,0:T(8,128)(2,1)S(1)}, u32[]{:S(2)}, u32[]{:S(2)}) collective-permute-start(bf16[640,256]{1,0:T(8,128)(2,1)S(1)} %collective-permute-done.11.rest_8_), channel_id=1, source_target_pairs={{0,1},{1,0},{2,3},{3,2},{4,5},{5,4},{6,7},{7,6},{8,9},{9,8},{10,11... | collective-permute-start | bytes 983048 | tf_op jit(solution)/shard_map/ppermute | solution.py:643
  59.9 7.8 %collective-permute-start.14 = (bf16[640,256]{1,0:T(8,128)(2,1)S(1)}, bf16[640,256]{1,0:T(8,128)(2,1)S(1)}, u32[]{:S(2)}, u32[]{:S(2)}) collective-permute-start(bf16[640,256]{1,0:T(8,128)(2,1)S(1)} %collective-permute-done.12.rest_9_), channel_id=1, source_target_pairs={{0,1},{1,0},{2,3},{3,2},{4,5},{5,4},{6,7},{7,6},{8,9},{9,8},{10,11... | collective-permute-start | bytes 983048 | tf_op jit(solution)/shard_map/ppermute | solution.py:643
  60.2 7.4 %copy-start.5 = (bf16[256,512]{1,0:T(8,128)(2,1)S(1)}, bf16[256,512]{1,0:T(8,128)(2,1)}, u32[]{:S(2)}) copy-start(bf16[256,512]{1,0:T(8,128)(2,1)} %rest_5_.1) | copy-start | bytes 786436
  67.6 22.2 %copy-start.3 = (f32[2048]{0:T(1024)S(1)}, f32[2048]{0:T(1024)}, u32[]{:S(2)}) copy-start(f32[2048]{0:T(1024)} %param.23) | copy-start | bytes 24580
  76.6 9.5 %collective-permute-start.15 = (bf16[128,640]{1,0:T(8,128)(2,1)}, bf16[128,640]{1,0:T(8,128)(2,1)S(1)}, u32[]{:S(2)}, u32[]{:S(2)}) collective-permute-start(bf16[128,640]{1,0:T(8,128)(2,1)} %get-tuple-element.46), channel_id=1, source_target_pairs={{0,120},{1,121},{2,122},{3,123},{4,124},{5,125},{6,126},{7,127},{8... | collective-permute-start | bytes 491528 | tf_op jit(solution)/shard_map/ppermute | solution.py:656
  79.9 6.1 %collective-permute-start.16 = (bf16[128,640]{1,0:T(8,128)(2,1)}, bf16[128,640]{1,0:T(8,128)(2,1)S(1)}, u32[]{:S(2)}, u32[]{:S(2)}) collective-permute-start(bf16[128,640]{1,0:T(8,128)(2,1)} %get-tuple-element.47), channel_id=1, source_target_pairs={{0,1},{1,0},{2,3},{3,2},{4,5},{5,4},{6,7},{7,6},{8,9},{9,8},{10,11... | collective-permute-start | bytes 491528 | tf_op jit(solution)/shard_map/ppermute | solution.py:658
  80.7 9.2 %collective-permute-start.17 = (bf16[128,640]{1,0:T(8,128)(2,1)S(1)}, bf16[128,640]{1,0:T(8,128)(2,1)S(1)}, u32[]{:S(2)}, u32[]{:S(2)}) collective-permute-start(bf16[128,640]{1,0:T(8,128)(2,1)S(1)} %get-tuple-element.48), channel_id=1, source_target_pairs={{0,121},{1,120},{2,123},{3,122},{4,125},{5,124},{6,127},{7,126},{8... | collective-permute-start | bytes 491528 | tf_op jit(solution)/shard_map/ppermute | solution.py:657
  94.3 6.6 %copy-start.6 = (bf16[1,2048,256]{2,1,0:T(8,128)(2,1)S(1)}, bf16[1,2048,256]{2,1,0:T(8,128)(2,1)}, u32[]{:S(2)}) copy-start(bf16[1,2048,256]{2,1,0:T(8,128)(2,1)} %param.26) | copy-start | bytes 3145732
  94.3 36.3 %all-to-all-start = ((bf16[64,8,2048]{2,1,0:T(8,128)(2,1)}), bf16[64,8,2048]{2,1,0:T(8,128)(2,1)S(1)}, u32[]{:S(2)}, u32[]{:S(2)}) async-start(bf16[64,8,2048]{2,1,0:T(8,128)(2,1)} %bitcast.15), calls=%async_computation | async-start | bytes 4194304 | tf_op jit(solution)/shard_map/all_to_all | solution.py:665
  100.9 2.7 %collective-permute-start.18 = (bf16[2048,256]{1,0:T(8,128)(2,1)S(1)}, bf16[2048,256]{1,0:T(8,128)(2,1)S(1)}, u32[]{:S(2)}, u32[]{:S(2)}) collective-permute-start(bf16[2048,256]{1,0:T(8,128)(2,1)S(1)} %bitcast.17), channel_id=1, source_target_pairs={{0,1},{1,0},{2,3},{3,2},{4,5},{5,4},{6,7},{7,6},{8,9},{9,8},{10,11... | collective-permute-start | bytes 3145736 | tf_op jit(solution)/shard_map/ppermute | solution.py:669
  101.1 4.1 %collective-permute-start.19 = (bf16[2048,256]{1,0:T(8,128)(2,1)}, bf16[2048,256]{1,0:T(8,128)(2,1)S(1)}, u32[]{:S(2)}, u32[]{:S(2)}) collective-permute-start(bf16[2048,256]{1,0:T(8,128)(2,1)} %bitcast.18), channel_id=1, source_target_pairs={{0,1},{1,0},{2,3},{3,2},{4,5},{5,4},{6,7},{7,6},{8,9},{9,8},{10,11... | collective-permute-start | bytes 3145736 | tf_op jit(solution)/shard_map/ppermute | solution.py:669
  101.5 5.3 %collective-permute-start.20 = (bf16[256,2048]{1,0:T(8,128)(2,1)}, bf16[256,2048]{1,0:T(8,128)(2,1)}, u32[]{:S(2)}, u32[]{:S(2)}) collective-permute-start(bf16[256,2048]{1,0:T(8,128)(2,1)} %bitcast.20), channel_id=1, source_target_pairs={{0,1},{1,0},{2,3},{3,2},{4,5},{5,4},{6,7},{7,6},{8,9},{9,8},{10,11... | collective-permute-start | bytes 3145736 | tf_op jit(solution)/shard_map/ppermute | solution.py:669
  103.6 1.5 copy-start.7
  105.1 1.0 copy-start.8
  137.3 6.1 %copy-start.9 = (f32[128,2]{0,1:T(2,128)S(1)}, f32[128,2]{0,1:T(2,128)}, u32[]{:S(2)}) copy-start(f32[128,2]{0,1:T(2,128)} %param.25) | copy-start | bytes 3076
  137.3 34.5 %copy-start = (bf16[128,2048]{1,0:T(8,128)(2,1)S(1)}, bf16[128,2048]{1,0:T(8,128)(2,1)}, u32[]{:S(2)}) copy-start(bf16[128,2048]{1,0:T(8,128)(2,1)} %get-tuple-element.53.hidden) | copy-start | bytes 1572868
  137.4 34.4 %all-to-all-start.1 = ((bf16[64,8,2048]{2,1,0:T(8,128)(2,1)}), bf16[64,8,2048]{2,1,0:T(8,128)(2,1)S(1)}, u32[]{:S(2)}, u32[]{:S(2)}) async-start(bf16[64,8,2048]{2,1,0:T(8,128)(2,1)} %bitcast.14), calls=%async_computation.1 | async-start | bytes 4194304 | tf_op jit(solution)/shard_map/all_to_all | solution.py:671

commit v10 on v9

--- a/solution.py
+++ b/solution.py
@@ -385,11 +385,8 @@
         most = jnp.maximum(sizes[0], sizes[1])
         first, second = (jnp.exp2(size - most) for size in sizes)
         cols = slice(h * V_DIM, (h + 1) * V_DIM)
-        inverse = 1.0 / (first + second)
-        value = (first * inverse) * one[:, cols].astype(jnp.float32) + (second * inverse) * two[:, cols].astype(
-            jnp.float32
-        )
-        outs.append(value.astype(jnp.bfloat16))
+        value = first * one[:, cols].astype(jnp.float32) + second * two[:, cols].astype(jnp.float32)
+        outs.append((value / (first + second)).astype(jnp.bfloat16))
     return jnp.concatenate(outs, axis=1)
 
 
@@ -462,13 +459,32 @@
     )(core, *messages, gain, slots, in_vmem(residual), in_vmem(out_early), in_hbm(out_proj))
 
 
-def experts_body(rows, *rest):
-    sources = rest[:6]
-    out_hbm = rest[6]
-    weights = rest[7:13]
-    first, out, sems, out_sems = rest[13:]
-    loads = []
-    for n in range(6):
+def stage_body(source, after, target, sem):
+    load = pltpu.make_async_copy(source, target, sem)
+    load.start()
+    load.wait()
+
+
+def stage(x, after):
+    hbm = pl.BlockSpec(memory_space=pltpu.HBM)
+    return pl.pallas_call(
+        stage_body,
+        out_shape=pltpu.VMEM(x.shape, x.dtype),
+        in_specs=[hbm, hbm],
+        out_specs=pl.BlockSpec(memory_space=pltpu.VMEM),
+        scratch_shapes=[pltpu.SemaphoreType.DMA],
+        compiler_params=pltpu.CompilerParams(vmem_limit_bytes=2**20),
+        name="stage",
+    )(in_hbm(x), in_hbm(after))
+
+
+def experts_body(rows, ready, *rest):
+    sources = (None, *rest[:5])
+    out_hbm = rest[5]
+    weights = (ready, *rest[6:11])
+    first, out, sems, out_sems = rest[11:]
+    loads = [None]
+    for n in range(1, 6):
         load = pltpu.make_async_copy(sources[n], weights[n], sems.at[n])
         load.start()
         loads.append(load)
@@ -479,7 +495,8 @@
         gate, up, down = weights[3 * n : 3 * n + 3]
         parts = []
         for weight, load in ((gate, loads[3 * n]), (up, loads[3 * n + 1])):
-            load.wait()
+            if load is not None:
+                load.wait()
             parts.append(
                 [
                     jnp.dot(rows[pl.ds(k * block, block), :], weight[...], preferred_element_type=jnp.float32)
@@ -510,9 +527,9 @@
     return pl.pallas_call(
         experts_body,
         out_shape=pltpu.HBM((count, width), jnp.bfloat16),
-        in_specs=[pl.BlockSpec(memory_space=pltpu.VMEM)] + [hbm] * 6,
+        in_specs=[pl.BlockSpec(memory_space=pltpu.VMEM)] * 2 + [hbm] * 5,
         out_specs=hbm,
-        scratch_shapes=[pltpu.VMEM(w.shape, w.dtype) for w in (*own, *other)]
+        scratch_shapes=[pltpu.VMEM(w.shape, w.dtype) for w in (*own[1:], *other)]
         + [
             pltpu.VMEM((count, width), jnp.bfloat16),
             pltpu.VMEM((count, width), jnp.bfloat16),
@@ -521,7 +538,7 @@
         ],
         compiler_params=pltpu.CompilerParams(vmem_limit_bytes=28 * 2**20),
         name="experts",
-    )(rows, *[in_hbm(w) for w in (*own, *other)])
+    )(rows, in_vmem(own[0]), *[in_hbm(w) for w in (*own[1:], *other)])
 
 
 def combine_body(back, hidden, slots, weights, out_ref):
@@ -667,7 +684,8 @@
     ).reshape(N_SP * CAP, width)
     own_weights = (w_gate[0], w_up[0], w_down[0])
     other_weights = [lax.ppermute(w, "tp", swap) for w in own_weights]
-    produced = experts(arrived, own_weights, other_weights)
+    own_ready = (stage(own_weights[0], outgoing), *own_weights[1:])
+    produced = experts(arrived, own_ready, other_weights)
     back = lax.all_to_all(
         produced.reshape(N_SP, CAP, width), "sp", split_axis=0, concat_axis=0, tiled=True
     ).reshape(N_SP * CAP, width)

time: 175 us -> 176 us (level)
  waiting for transfers between devices: 75.3 us -> 71.2 us
  local copies, waits for them, and re-layouts: 4.07 us -> 6.67 us
    ppermute x3, waiting for transfers between devices: 4.1 us -> 2.15 us  [local(): got.append(lax.ppermute(both, AXES, shift_pairs(0, by)))]
    unnamed x26 -> x24, local copies, waits for them, and re-layouts: 2.84 us -> 4.78 us
  transfers between devices with their start and end apart: 23 -> 23, of which waited for: 14 -> 12; matrix products, arithmetic and copies ran while one was open for 3% -> 4% of each run, Pallas kernels for 13% -> 14%
where the time goes in v10:
time: 176 us; the launch traced here: 174 us
  waiting for transfers between devices  71.2 us (40%)
  starting transfers between devices  46.3 us (26%)
  Pallas kernels  44.7 us (25%)
  local copies, waits for them, and re-layouts  6.67 us (4%)
  other arithmetic  4.87 us (3%)
    pallas_call x4, Pallas kernels, attention(): pl.pallas_call(functools.partial(attention_body, call, steps, offset, len...  32 us
    all_to_all x1, waiting for transfers between devices, local(): lax.all_to_all(produced.reshape(N_SP, CAP, width), 'sp', split_axis=0, co...  28.3 us
    all_to_all x1, waiting for transfers between devices, local(): lax.all_to_all(outgoing.reshape(N_SP, CAP, width), 'sp', split_axis=0, co...  23.7 us
    ppermute x5, starting transfers between devices, local(): other_parts.append([lax.ppermute(part, 'tp', swap) for part in group])  7.15 us
    all_to_all x1, starting transfers between devices, local(): lax.all_to_all(outgoing.reshape(N_SP, CAP, width), 'sp', split_axis=0, co...  7.02 us
    ppermute x1, starting transfers between devices, local(): far = lax.ppermute(shard, AXES, plane_pairs(Z_SECOND))  6.87 us
    all_to_all x1, starting transfers between devices, local(): lax.all_to_all(produced.reshape(N_SP, CAP, width), 'sp', split_axis=0, co...  6.05 us
    pallas_call x1, Pallas kernels, experts(): pl.pallas_call(experts_body, out_shape=pltpu.HBM((count, width), jnp.bflo...  5.99 us
  transfers between devices with their start and end apart: 23, of which 12 were waited for; matrix products, arithmetic and copies ran while one was open for 4% of the time, Pallas kernels for 14%

profile of v10, /device:TPU:1, one launch (start us, length us, event | category | flops | bytes accessed | tf_op | source)
XLA Modules:
  0.0 174.1 jit_solution(6788221432484665731)
XLA Ops:
  0.0 0.9 copy.42
  1.3 0.9 fusion.12
  2.3 6.9 %collective-permute-start = (bf16[160,256]{1,0:T(8,128)(2,1)S(1)}, bf16[160,256]{1,0:T(8,128)(2,1)S(1)}, u32[]{:S(2)}, u32[]{:S(2)}) collective-permute-start(bf16[160,256]{1,0:T(8,128)(2,1)S(1)} %fusion.12), channel_id=1, source_target_pairs={{64,1},{66,3},{68,5},{70,7},{72,9},{74,11},{76,13},{78,15},{80,17}... | collective-permute-start | bytes 245768 | tf_op jit(solution)/shard_map/ppermute | solution.py:622
  9.4 1.9 %negate_select_fusion = (f32[512,256]{1,0:T(8,128)S(1)}, f32[512,256]{1,0:T(8,128)S(1)}) fusion(f32[256]{0:T(256)S(1)} %fusion.22, f32[512]{0:T(512)S(1)} %add_convert_fusion, pred[256]{0:T(512)(128)(4,1)S(1)} %fusion.23), kind=kLoop, calls=%fused_computation | loop fusion | flops 393216 | bytes 1051904 | tf_op jit(solution)/shard_map/jit(_where)/select_n | solution.py:641
  11.3 0.7 broadcast_multiply_fusion
  12.0 0.8 copy.44
  12.9 0.7 constant_dynamic-update-slice_fusion.4
  13.6 1.3 collective-permute-start.2
  15.3 0.7 dynamic-slice_reduce_fusion.table
  16.1 1.5 collective-permute-start.3
  17.6 1.5 collective-permute-start.4
  19.1 0.6 constant_dynamic-update-slice_fusion.3
  19.8 0.7 constant_dynamic-update-slice_fusion.2
  20.6 0.7 constant_dynamic-update-slice_fusion.1
  21.3 2.0 %collective-permute-done.4 = bf16[320,256]{1,0:T(8,128)(2,1)S(1)} collective-permute-done((bf16[320,256]{1,0:T(8,128)(2,1)S(1)}, bf16[320,256]{1,0:T(8,128)(2,1)S(1)}, u32[]{:S(2)}, u32[]{:S(2)}) %collective-permute-start.4) | collective-permute-done | bytes 163872 | tf_op jit(solution)/shard_map/ppermute | solution.py:644
  23.3 0.7 constant_dynamic-update-slice_fusion.rest_6_
  23.9 1.3 collective-permute-start.7
  25.2 1.7 collective-permute-start.8
  27.0 3.0 %collective-permute-start.6 = (bf16[1280,256]{1,0:T(8,128)(2,1)}, bf16[1280,256]{1,0:T(8,128)(2,1)S(1)}, u32[]{:S(2)}, u32[]{:S(2)}) collective-permute-start(bf16[1280,256]{1,0:T(8,128)(2,1)} %constant_dynamic-update-slice_fusion.rest_6_), channel_id=1, source_target_pairs={{0,1},{1,0},{2,3},{3,2},{4,5},{5,4},{6,7},{7,6},{8,9},{9,8},{10,11... | collective-permute-start | bytes 1966088 | tf_op jit(solution)/shard_map/ppermute | solution.py:660
  30.0 2.2 %collective-permute-start.5 = (bf16[256,768]{1,0:T(8,128)(2,1)S(1)}, bf16[256,768]{1,0:T(8,128)(2,1)S(1)}, u32[]{:S(2)}, u32[]{:S(2)}) collective-permute-start(bf16[256,768]{1,0:T(8,128)(2,1)S(1)} %pad_maximum_fusion), channel_id=1, source_target_pairs={{0,120},{1,121},{2,122},{3,123},{4,124},{5,125},{6,126},{7,127},{8... | collective-permute-start | bytes 1179656 | tf_op jit(solution)/shard_map/ppermute | solution.py:619
  32.2 3.7 %collective-permute-done.7.rest_5_ = bf16[1280,256]{1,0:T(8,128)(2,1)S(1)} collective-permute-done((bf16[1280,256]{1,0:T(8,128)(2,1)}, bf16[1280,256]{1,0:T(8,128)(2,1)S(1)}, u32[]{:S(2)}, u32[]{:S(2)}) %collective-permute-start.7) | collective-permute-done | bytes 655392 | tf_op jit(solution)/shard_map/ppermute | solution.py:651
  36.4 3.4 %collective-permute-start.12 = (bf16[640,256]{1,0:T(8,128)(2,1)S(1)}, bf16[640,256]{1,0:T(8,128)(2,1)S(1)}, u32[]{:S(2)}, u32[]{:S(2)}) collective-permute-start(bf16[640,256]{1,0:T(8,128)(2,1)S(1)} %slice.41), channel_id=1, source_target_pairs={{0,6},{1,25},{2,0},{3,27},{4,2},{5,29},{6,4},{7,31},{8,14},{9,1},{... | collective-permute-start | bytes 983048 | tf_op jit(solution)/shard_map/ppermute | solution.py:656
  39.8 2.4 %collective-permute-start.10 = (bf16[1280,256]{1,0:T(8,128)(2,1)S(1)}, bf16[1280,256]{1,0:T(8,128)(2,1)S(1)}, u32[]{:S(2)}, u32[]{:S(2)}) collective-permute-start(bf16[1280,256]{1,0:T(8,128)(2,1)S(1)} %collective-permute-done.8.rest_6_), channel_id=1, source_target_pairs={{0,1},{1,0},{2,3},{3,2},{4,5},{5,4},{6,7},{7,6},{8,9},{9,8},{10,11... | collective-permute-start | bytes 1966088 | tf_op jit(solution)/shard_map/ppermute | solution.py:660
  42.2 2.1 %collective-permute-done.5.rest_2_ = bf16[256,768]{1,0:T(8,128)(2,1)S(1)} collective-permute-done((bf16[256,768]{1,0:T(8,128)(2,1)S(1)}, bf16[256,768]{1,0:T(8,128)(2,1)S(1)}, u32[]{:S(2)}, u32[]{:S(2)}) %collective-permute-start.5) | collective-permute-done | bytes 393248 | tf_op jit(solution)/shard_map/ppermute | solution.py:619
  44.2 1.2 collective-permute-start.9
  45.4 8.5 %shard_map.145 = (bf16[4,2,512,128]{3,2,1,0:T(8,128)(2,1)S(1)}, bf16[4,2,512,128]{3,2,1,0:T(8,128)(2,1)S(1)}, f32[4,512,128]{2,1,0:T(8,128)S(1)}, f32[4,512,128]{2,1,0:T(8,128)S(1)}, f32[4,2,512,128]{3,2,1,0:T(8,128)S(1)}) custom-call(s32[308]{0:T(512)S(1)} %dynamic-slice_reduce_fusion.table, bf16[256,512]{1,0:T(8,128)(2,1)S(1)} %copy-done.1, ...), custom_call_target="tpu_custom_call" | custom-call | flops 4026531840 | bytes 1048576 | tf_op jit(solution)/shard_map/pallas_call | solution.py:343
  53.9 7.3 %shard_map.146 = (f32[4,512,128]{2,1,0:T(8,128)S(1)}, f32[4,512,128]{2,1,0:T(8,128)S(1)}, f32[4,2,512,128]{3,2,1,0:T(8,128)S(1)}) custom-call(s32[308]{0:T(512)S(1)} %dynamic-slice_reduce_fusion.table, bf16[4,2,512,128]{3,2,1,0:T(8,128)(2,1)S(1)} %get-tuple-element.34.rest_0_, ...), custom_call_target="tpu_custom_call", output_to_operand_aliasing={{0}: (3, {}), {1}: (4, {}), {2}: (5, {})} | custom-call | flops 4026531840 | bytes 1048576 | tf_op jit(solution)/shard_map/pallas_call | solution.py:343
  61.4 0.5 collective-permute-start.14
  61.8 7.3 %shard_map.147 = (f32[4,512,128]{2,1,0:T(8,128)S(1)}, f32[4,512,128]{2,1,0:T(8,128)S(1)}, f32[4,2,512,128]{3,2,1,0:T(8,128)S(1)}) custom-call(s32[308]{0:T(512)S(1)} %dynamic-slice_reduce_fusion.table, bf16[4,2,512,128]{3,2,1,0:T(8,128)(2,1)S(1)} %get-tuple-element.34.rest_0_, ...), custom_call_target="tpu_custom_call", output_to_operand_aliasing={{0}: (3, {}), {1}: (4, {}), {2}: (5, {})} | custom-call | flops 4026531840 | bytes 1048576 | tf_op jit(solution)/shard_map/pallas_call | solution.py:343
  69.2 8.9 %shard_map.148 = (bf16[128,640]{1,0:T(8,128)(2,1)S(1)}, bf16[128,640]{1,0:T(8,128)(2,1)}, bf16[128,640]{1,0:T(8,128)(2,1)}, bf16[128,640]{1,0:T(8,128)(2,1)S(1)}...) custom-call(s32[308]{0:T(512)S(1)} %dynamic-slice_reduce_fusion.tabl, ...), custom_call_target="tpu_custom_call", output_to_operand_aliasing={{6}: (3, {}), {7}: (4, {}), {8}: (5, {})} | custom-call | flops 4026531840 | bytes 1048576 | tf_op jit(solution)/shard_map/pallas_call | solution.py:343
  78.1 3.4 %collective-permute-start.15 = (bf16[128,640]{1,0:T(8,128)(2,1)}, bf16[128,640]{1,0:T(8,128)(2,1)S(1)}, u32[]{:S(2)}, u32[]{:S(2)}) collective-permute-start(bf16[128,640]{1,0:T(8,128)(2,1)} %get-tuple-element.46), channel_id=1, source_target_pairs={{0,120},{1,121},{2,122},{3,123},{4,124},{5,125},{6,126},{7,127},{8... | collective-permute-start | bytes 491528 | tf_op jit(solution)/shard_map/ppermute | solution.py:673
  81.5 0.7 collective-permute-start.16
  82.2 1.4 collective-permute-start.17
  83.7 4.0 %collective-permute-done.15.mirror_same = bf16[128,640]{1,0:T(8,128)(2,1)S(1)} collective-permute-done((bf16[128,640]{1,0:T(8,128)(2,1)}, bf16[128,640]{1,0:T(8,128)(2,1)S(1)}, u32[]{:S(2)}, u32[]{:S(2)}) %collective-permute-start.15) | collective-permute-done | bytes 163872 | tf_op jit(solution)/shard_map/ppermute | solution.py:673
  87.6 3.8 %collective-permute-done.17.mirror_cross = bf16[128,640]{1,0:T(8,128)(2,1)S(1)} collective-permute-done((bf16[128,640]{1,0:T(8,128)(2,1)S(1)}, bf16[128,640]{1,0:T(8,128)(2,1)S(1)}, u32[]{:S(2)}, u32[]{:S(2)}) %collective-permute-start.17) | collective-permute-done | bytes 163872 | tf_op jit(solution)/shard_map/ppermute | solution.py:674
  91.4 3.8 %project.1 = (bf16[128,2048]{1,0:T(8,128)(2,1)}, bf16[512,2048]{1,0:T(8,128)(2,1)}) custom-call(s32[1]{0:T(128)} %bitcast.core, bf16[128,640]{1,0:T(8,128)(2,1)S(1)} %get-tuple-element.45.local_part, bf16[128,640]{1,0:T(8,128)(2,1)S(1)} %collective-permute-done.15.mirror_same, bf16[128,640]{1,0:T(8,128)(2,1)S(1)} %collective-permute-done.16.swapped, ...), custom_call_target="tpu_custom_call" | custom-call | tf_op jit(solution)/shard_map/project/pallas_call | solution.py:442
  95.2 7.0 %all-to-all-start = ((bf16[64,8,2048]{2,1,0:T(8,128)(2,1)}), bf16[64,8,2048]{2,1,0:T(8,128)(2,1)S(1)}, u32[]{:S(2)}, u32[]{:S(2)}) async-start(bf16[64,8,2048]{2,1,0:T(8,128)(2,1)} %bitcast.15), calls=%async_computation | async-start | bytes 4194304 | tf_op jit(solution)/shard_map/all_to_all | solution.py:682
  102.4 0.4 collective-permute-start.19
  102.9 1.2 stage.1.ready
  104.2 1.0 collective-permute-done.18.rest_2_
  105.2 1.5 collective-permute-done.19.rest_3_
  106.7 1.0 copy-done.7
  107.7 0.6 collective-permute-done.20.rest_4_
  108.3 23.7 %all-to-all-done = bf16[64,8,2048]{2,1,0:T(8,128)(2,1)S(1)} async-done(((bf16[64,8,2048]{2,1,0:T(8,128)(2,1)}), bf16[64,8,2048]{2,1,0:T(8,128)(2,1)S(1)}, u32[]{:S(2)}, u32[]{:S(2)}) %all-to-all-start) | async-done | bytes 2097184 | tf_op jit(solution)/shard_map/all_to_all | solution.py:682
  132.0 6.0 %experts.1 = bf16[512,2048]{1,0:T(8,128)(2,1)} custom-call(bf16[512,2048]{1,0:T(8,128)(2,1)S(1)} %bitcast.10, bf16[2048,256]{1,0:T(8,128)(2,1)S(1)} %stage.1.ready, bf16[2048,256]{1,0:T(8,128)(2,1)} %bitcast.6.rest_0_, bf16[256,2048]{1,0:T(8,128)(2,1)} %bitcast.7.rest_1_, bf16[2048,256]{1,0:T(8,128)(2,1)} %copy-done.6, bf16[2048,256]{1,0:T(8,128)(2,1)} %copy-done.7, ...), custom_call_target="tpu_custom_call" | custom-call | tf_op jit(solution)/shard_map/experts/pallas_call | solution.py:527
  138.0 6.0 %all-to-all-start.1 = ((bf16[64,8,2048]{2,1,0:T(8,128)(2,1)}), bf16[64,8,2048]{2,1,0:T(8,128)(2,1)S(1)}, u32[]{:S(2)}, u32[]{:S(2)}) async-start(bf16[64,8,2048]{2,1,0:T(8,128)(2,1)} %bitcast.14), calls=%async_computation.1 | async-start | bytes 4194304 | tf_op jit(solution)/shard_map/all_to_all | solution.py:689
  144.2 28.3 %all-to-all-done.1 = bf16[64,8,2048]{2,1,0:T(8,128)(2,1)S(1)} async-done(((bf16[64,8,2048]{2,1,0:T(8,128)(2,1)}), bf16[64,8,2048]{2,1,0:T(8,128)(2,1)S(1)}, u32[]{:S(2)}, u32[]{:S(2)}) %all-to-all-start.1) | async-done | bytes 2097184 | tf_op jit(solution)/shard_map/all_to_all | solution.py:689
  172.5 1.6 combine.1
  (55 shorter events, 2.5 us)
Async XLA Ops:
  0.0 30.0 %copy-start.1 = (bf16[256,512]{1,0:T(8,128)(2,1)S(1)}, bf16[256,512]{1,0:T(8,128)(2,1)}, u32[]{:S(2)}) copy-start(bf16[256,512]{1,0:T(8,128)(2,1)} %rest_0_.1) | copy-start | bytes 786436
  0.0 30.0 %copy-start.2 = (bf16[256,256]{1,0:T(8,128)(2,1)S(1)}, bf16[256,256]{1,0:T(8,128)(2,1)}, u32[]{:S(2)}) copy-start(bf16[256,256]{1,0:T(8,128)(2,1)} %rest_1_.1) | copy-start | bytes 393220
  2.3 10.7 %collective-permute-start = (bf16[160,256]{1,0:T(8,128)(2,1)S(1)}, bf16[160,256]{1,0:T(8,128)(2,1)S(1)}, u32[]{:S(2)}, u32[]{:S(2)}) collective-permute-start(bf16[160,256]{1,0:T(8,128)(2,1)S(1)} %fusion.12), channel_id=1, source_target_pairs={{64,1},{66,3},{68,5},{70,7},{72,9},{74,11},{76,13},{78,15},{80,17}... | collective-permute-start | bytes 245768 | tf_op jit(solution)/shard_map/ppermute | solution.py:622
  9.1 4.4 %collective-permute-start.1 = (bf16[160,256]{1,0:T(8,128)(2,1)S(1)}, bf16[160,256]{1,0:T(8,128)(2,1)S(1)}, u32[]{:S(2)}, u32[]{:S(2)}) collective-permute-start(bf16[160,256]{1,0:T(8,128)(2,1)S(1)} %fusion.12), channel_id=1, source_target_pairs={{96,0},{98,2},{100,4},{102,6},{104,8},{106,10},{108,12},{110,14},{... | collective-permute-start | bytes 245768 | tf_op jit(solution)/shard_map/ppermute | solution.py:621
  12.9 32.5 %copy-start.4 = (bf16[256,512]{1,0:T(8,128)(2,1)S(1)}, bf16[256,512]{1,0:T(8,128)(2,1)}, u32[]{:S(2)}) copy-start(bf16[256,512]{1,0:T(8,128)(2,1)} %rest_3_.1) | copy-start | bytes 786436
  13.6 6.2 %collective-permute-start.2 = (bf16[320,256]{1,0:T(8,128)(2,1)S(1)}, bf16[320,256]{1,0:T(8,128)(2,1)S(1)}, u32[]{:S(2)}, u32[]{:S(2)}) collective-permute-start(bf16[320,256]{1,0:T(8,128)(2,1)S(1)} %pad_maximum_fusion.1), channel_id=1, source_target_pairs={{0,8},{1,3},{2,10},{3,5},{4,12},{5,7},{6,14},{7,1},{8,16},{9,11},{... | collective-permute-start | bytes 491528 | tf_op jit(solution)/shard_map/ppermute | solution.py:644
  16.1 4.5 %collective-permute-start.3 = (bf16[320,256]{1,0:T(8,128)(2,1)S(1)}, bf16[320,256]{1,0:T(8,128)(2,1)S(1)}, u32[]{:S(2)}, u32[]{:S(2)}) collective-permute-start(bf16[320,256]{1,0:T(8,128)(2,1)S(1)} %pad_maximum_fusion.1), channel_id=1, source_target_pairs={{0,24},{1,7},{2,26},{3,1},{4,28},{5,3},{6,30},{7,5},{8,0},{9,15},{... | collective-permute-start | bytes 491528 | tf_op jit(solution)/shard_map/ppermute | solution.py:644
  17.6 5.7 %collective-permute-start.4 = (bf16[320,256]{1,0:T(8,128)(2,1)S(1)}, bf16[320,256]{1,0:T(8,128)(2,1)S(1)}, u32[]{:S(2)}, u32[]{:S(2)}) collective-permute-start(bf16[320,256]{1,0:T(8,128)(2,1)S(1)} %pad_maximum_fusion.1), channel_id=1, source_target_pairs={{0,16},{1,5},{2,18},{3,7},{4,20},{5,1},{6,22},{7,3},{8,24},{9,13},... | collective-permute-start | bytes 491528 | tf_op jit(solution)/shard_map/ppermute | solution.py:644
  23.9 11.9 %collective-permute-start.7 = (bf16[1280,256]{1,0:T(8,128)(2,1)}, bf16[1280,256]{1,0:T(8,128)(2,1)S(1)}, u32[]{:S(2)}, u32[]{:S(2)}) collective-permute-start(bf16[1280,256]{1,0:T(8,128)(2,1)} %constant_dynamic-update-slice_fusion.rest_6_), channel_id=1, source_target_pairs={{0,2},{1,9},{2,4},{3,11},{4,6},{5,13},{6,0},{7,15},{8,10},{9,17},{... | collective-permute-start | bytes 1966088 | tf_op jit(solution)/shard_map/ppermute | solution.py:651
  25.2 11.1 %collective-permute-start.8 = (bf16[1280,256]{1,0:T(8,128)(2,1)}, bf16[1280,256]{1,0:T(8,128)(2,1)S(1)}, u32[]{:S(2)}, u32[]{:S(2)}) collective-permute-start(bf16[1280,256]{1,0:T(8,128)(2,1)} %constant_dynamic-update-slice_fusion.rest_6_), channel_id=1, source_target_pairs={{0,6},{1,25},{2,0},{3,27},{4,2},{5,29},{6,4},{7,31},{8,14},{9,1},{... | collective-permute-start | bytes 1966088 | tf_op jit(solution)/shard_map/ppermute | solution.py:651
  27.0 18.4 %collective-permute-start.6 = (bf16[1280,256]{1,0:T(8,128)(2,1)}, bf16[1280,256]{1,0:T(8,128)(2,1)S(1)}, u32[]{:S(2)}, u32[]{:S(2)}) collective-permute-start(bf16[1280,256]{1,0:T(8,128)(2,1)} %constant_dynamic-update-slice_fusion.rest_6_), channel_id=1, source_target_pairs={{0,1},{1,0},{2,3},{3,2},{4,5},{5,4},{6,7},{7,6},{8,9},{9,8},{10,11... | collective-permute-start | bytes 1966088 | tf_op jit(solution)/shard_map/ppermute | solution.py:660
  30.0 14.2 %collective-permute-start.5 = (bf16[256,768]{1,0:T(8,128)(2,1)S(1)}, bf16[256,768]{1,0:T(8,128)(2,1)S(1)}, u32[]{:S(2)}, u32[]{:S(2)}) collective-permute-start(bf16[256,768]{1,0:T(8,128)(2,1)S(1)} %pad_maximum_fusion), channel_id=1, source_target_pairs={{0,120},{1,121},{2,122},{3,123},{4,124},{5,125},{6,126},{7,127},{8... | collective-permute-start | bytes 1179656 | tf_op jit(solution)/shard_map/ppermute | solution.py:619
  35.9 25.4 %collective-permute-start.11 = (bf16[640,256]{1,0:T(8,128)(2,1)S(1)}, bf16[640,256]{1,0:T(8,128)(2,1)S(1)}, u32[]{:S(2)}, u32[]{:S(2)}) collective-permute-start(bf16[640,256]{1,0:T(8,128)(2,1)S(1)} %slice.40), channel_id=1, source_target_pairs={{0,2},{1,9},{2,4},{3,11},{4,6},{5,13},{6,0},{7,15},{8,10},{9,17},{... | collective-permute-start | bytes 983048 | tf_op jit(solution)/shard_map/ppermute | solution.py:656
  36.4 25.0 %collective-permute-start.12 = (bf16[640,256]{1,0:T(8,128)(2,1)S(1)}, bf16[640,256]{1,0:T(8,128)(2,1)S(1)}, u32[]{:S(2)}, u32[]{:S(2)}) collective-permute-start(bf16[640,256]{1,0:T(8,128)(2,1)S(1)} %slice.41), channel_id=1, source_target_pairs={{0,6},{1,25},{2,0},{3,27},{4,2},{5,29},{6,4},{7,31},{8,14},{9,1},{... | collective-permute-start | bytes 983048 | tf_op jit(solution)/shard_map/ppermute | solution.py:656
  39.8 22.1 %collective-permute-start.10 = (bf16[1280,256]{1,0:T(8,128)(2,1)S(1)}, bf16[1280,256]{1,0:T(8,128)(2,1)S(1)}, u32[]{:S(2)}, u32[]{:S(2)}) collective-permute-start(bf16[1280,256]{1,0:T(8,128)(2,1)S(1)} %collective-permute-done.8.rest_6_), channel_id=1, source_target_pairs={{0,1},{1,0},{2,3},{3,2},{4,5},{5,4},{6,7},{7,6},{8,9},{9,8},{10,11... | collective-permute-start | bytes 1966088 | tf_op jit(solution)/shard_map/ppermute | solution.py:660
  44.2 17.6 %collective-permute-start.9 = (bf16[1280,256]{1,0:T(8,128)(2,1)S(1)}, bf16[1280,256]{1,0:T(8,128)(2,1)S(1)}, u32[]{:S(2)}, u32[]{:S(2)}) collective-permute-start(bf16[1280,256]{1,0:T(8,128)(2,1)S(1)} %collective-permute-done.7.rest_5_), channel_id=1, source_target_pairs={{0,1},{1,0},{2,3},{3,2},{4,5},{5,4},{6,7},{7,6},{8,9},{9,8},{10,11... | collective-permute-start | bytes 1966088 | tf_op jit(solution)/shard_map/ppermute | solution.py:660
  61.2 7.9 %collective-permute-start.13 = (bf16[640,256]{1,0:T(8,128)(2,1)S(1)}, bf16[640,256]{1,0:T(8,128)(2,1)S(1)}, u32[]{:S(2)}, u32[]{:S(2)}) collective-permute-start(bf16[640,256]{1,0:T(8,128)(2,1)S(1)} %collective-permute-done.11.rest_8_), channel_id=1, source_target_pairs={{0,1},{1,0},{2,3},{3,2},{4,5},{5,4},{6,7},{7,6},{8,9},{9,8},{10,11... | collective-permute-start | bytes 983048 | tf_op jit(solution)/shard_map/ppermute | solution.py:660
  61.4 7.8 %collective-permute-start.14 = (bf16[640,256]{1,0:T(8,128)(2,1)S(1)}, bf16[640,256]{1,0:T(8,128)(2,1)S(1)}, u32[]{:S(2)}, u32[]{:S(2)}) collective-permute-start(bf16[640,256]{1,0:T(8,128)(2,1)S(1)} %collective-permute-done.12.rest_9_), channel_id=1, source_target_pairs={{0,1},{1,0},{2,3},{3,2},{4,5},{5,4},{6,7},{7,6},{8,9},{9,8},{10,11... | collective-permute-start | bytes 983048 | tf_op jit(solution)/shard_map/ppermute | solution.py:660
  61.8 7.3 %copy-start.5 = (bf16[256,512]{1,0:T(8,128)(2,1)S(1)}, bf16[256,512]{1,0:T(8,128)(2,1)}, u32[]{:S(2)}) copy-start(bf16[256,512]{1,0:T(8,128)(2,1)} %rest_5_.1) | copy-start | bytes 786436
  69.2 22.2 %copy-start.3 = (f32[2048]{0:T(1024)S(1)}, f32[2048]{0:T(1024)}, u32[]{:S(2)}) copy-start(f32[2048]{0:T(1024)} %param.23) | copy-start | bytes 24580
  78.1 9.5 %collective-permute-start.15 = (bf16[128,640]{1,0:T(8,128)(2,1)}, bf16[128,640]{1,0:T(8,128)(2,1)S(1)}, u32[]{:S(2)}, u32[]{:S(2)}) collective-permute-start(bf16[128,640]{1,0:T(8,128)(2,1)} %get-tuple-element.46), channel_id=1, source_target_pairs={{0,120},{1,121},{2,122},{3,123},{4,124},{5,125},{6,126},{7,127},{8... | collective-permute-start | bytes 491528 | tf_op jit(solution)/shard_map/ppermute | solution.py:673
  81.5 6.1 %collective-permute-start.16 = (bf16[128,640]{1,0:T(8,128)(2,1)}, bf16[128,640]{1,0:T(8,128)(2,1)S(1)}, u32[]{:S(2)}, u32[]{:S(2)}) collective-permute-start(bf16[128,640]{1,0:T(8,128)(2,1)} %get-tuple-element.47), channel_id=1, source_target_pairs={{0,1},{1,0},{2,3},{3,2},{4,5},{5,4},{6,7},{7,6},{8,9},{9,8},{10,11... | collective-permute-start | bytes 491528 | tf_op jit(solution)/shard_map/ppermute | solution.py:675
  82.2 9.2 %collective-permute-start.17 = (bf16[128,640]{1,0:T(8,128)(2,1)S(1)}, bf16[128,640]{1,0:T(8,128)(2,1)S(1)}, u32[]{:S(2)}, u32[]{:S(2)}) collective-permute-start(bf16[128,640]{1,0:T(8,128)(2,1)S(1)} %get-tuple-element.48), channel_id=1, source_target_pairs={{0,121},{1,120},{2,123},{3,122},{4,125},{5,124},{6,127},{7,126},{8... | collective-permute-start | bytes 491528 | tf_op jit(solution)/shard_map/ppermute | solution.py:674
  95.2 36.8 %all-to-all-start = ((bf16[64,8,2048]{2,1,0:T(8,128)(2,1)}), bf16[64,8,2048]{2,1,0:T(8,128)(2,1)S(1)}, u32[]{:S(2)}, u32[]{:S(2)}) async-start(bf16[64,8,2048]{2,1,0:T(8,128)(2,1)} %bitcast.15), calls=%async_computation | async-start | bytes 4194304 | tf_op jit(solution)/shard_map/all_to_all | solution.py:682
  102.3 3.0 %collective-permute-start.18 = (bf16[2048,256]{1,0:T(8,128)(2,1)}, bf16[2048,256]{1,0:T(8,128)(2,1)S(1)}, u32[]{:S(2)}, u32[]{:S(2)}) collective-permute-start(bf16[2048,256]{1,0:T(8,128)(2,1)} %bitcast.5.source), channel_id=1, source_target_pairs={{0,1},{1,0},{2,3},{3,2},{4,5},{5,4},{6,7},{7,6},{8,9},{9,8},{10,11... | collective-permute-start | bytes 3145736 | tf_op jit(solution)/shard_map/ppermute | solution.py:686
  102.4 4.3 %collective-permute-start.19 = (bf16[2048,256]{1,0:T(8,128)(2,1)}, bf16[2048,256]{1,0:T(8,128)(2,1)S(1)}, u32[]{:S(2)}, u32[]{:S(2)}) collective-permute-start(bf16[2048,256]{1,0:T(8,128)(2,1)} %bitcast.6.rest_0_), channel_id=1, source_target_pairs={{0,1},{1,0},{2,3},{3,2},{4,5},{5,4},{6,7},{7,6},{8,9},{9,8},{10,11... | collective-permute-start | bytes 3145736 | tf_op jit(solution)/shard_map/ppermute | solution.py:686
  102.8 5.5 %collective-permute-start.20 = (bf16[256,2048]{1,0:T(8,128)(2,1)}, bf16[256,2048]{1,0:T(8,128)(2,1)}, u32[]{:S(2)}, u32[]{:S(2)}) collective-permute-start(bf16[256,2048]{1,0:T(8,128)(2,1)} %bitcast.7.rest_1_), channel_id=1, source_target_pairs={{0,1},{1,0},{2,3},{3,2},{4,5},{5,4},{6,7},{7,6},{8,9},{9,8},{10,11... | collective-permute-start | bytes 3145736 | tf_op jit(solution)/shard_map/ppermute | solution.py:686
  105.2 1.5 copy-start.6
  106.7 1.0 copy-start.7
  138.0 6.1 %copy-start.8 = (f32[128,2]{0,1:T(2,128)S(1)}, f32[128,2]{0,1:T(2,128)}, u32[]{:S(2)}) copy-start(f32[128,2]{0,1:T(2,128)} %param.25) | copy-start | bytes 3076
  138.0 34.5 %copy-start = (bf16[128,2048]{1,0:T(8,128)(2,1)S(1)}, bf16[128,2048]{1,0:T(8,128)(2,1)}, u32[]{:S(2)}) copy-start(bf16[128,2048]{1,0:T(8,128)(2,1)} %get-tuple-element.53.hidden) | copy-start | bytes 1572868
  138.0 34.5 %all-to-all-start.1 = ((bf16[64,8,2048]{2,1,0:T(8,128)(2,1)}), bf16[64,8,2048]{2,1,0:T(8,128)(2,1)S(1)}, u32[]{:S(2)}, u32[]{:S(2)}) async-start(bf16[64,8,2048]{2,1,0:T(8,128)(2,1)} %bitcast.14), calls=%async_computation.1 | async-start | bytes 4194304 | tf_op jit(solution)/shard_map/all_to_all | solution.py:689
